TPU v7x, 128 devices: a whole 4x4x4 slice. The times are simulated.
128 devices in a mesh: sp: 16 (over z, y), dp: 8 (over x, core).
Axes of the slice: x: 4, y: 4, z: 4, core: 2. Of those that a mesh axis runs over, the one named last changes fastest.
Arguments:
- query: bfloat16 [8, 3072, 3072], P('dp', 'sp'), may hold values from -18 to 18
- latent: bfloat16 [8, 3072, 1024], P('dp', 'sp'), may hold values from -6 to 6
- rope_key: bfloat16 [8, 3072, 32], P('dp', 'sp'), may hold values from -5 to 5
- latent_norm_gain: float32 [1024], replicated, may hold values from 0.1 to 1.9
- key_up_matrix: bfloat16 [2048, 1024], P('dp'), may hold values from -0.1875 to 0.1875
- value_up_matrix: bfloat16 [2048, 1024], P('dp'), may hold values from -0.1875 to 0.1875
- out_grad: bfloat16 [8, 3072, 2048], P('dp', 'sp'), may hold values from -6 to 6
Outputs:
- query_grad: bfloat16 [8, 3072, 3072], P('dp', 'sp')
- latent_grad: float32 [8, 3072, 1024], P('dp', 'sp')
- rope_key_grad: float32 [8, 3072, 32], P('dp', 'sp')
- key_weight_grad: float32 [2048, 1024], P('dp')
- value_weight_grad: float32 [2048, 1024], P('dp')
- gain_grad: float32 [1024], replicated
All inputs are finite; a program needn't handle non-finite values.
Results may differ from a plain program's by a relative error of at most 0.011.
Values may be sent and summed in bfloat16 or wider, within the bound.
No kernel may reach another device: no remote copies, remote signals or barrier semaphores. Data moves between devices by JAX's collectives and lax.ppermute only.
A program may use at most 256 MiB of HBM per device.

v0:
```python
import functools

import jax
import jax.numpy as jnp
from jax import lax
from jax.sharding import Mesh
from jax.sharding import PartitionSpec as P

ATTENTION_HEADS = 32
PLAIN_HEAD_WIDTH = 64
ROPE = 32
VALUE_HEAD_WIDTH = 64
SPAN = 64
DP = ("dp_0", "dp_1")
SP = ("sp_0", "sp_1")
SP_DP = ("sp_0", "sp_1", "dp_0", "dp_1")


eps = 1e-06
rope_base = 10000.0


def from_everyone(value, axis):
    size = lax.axis_size(axis)
    return lax.all_to_all(
        jnp.broadcast_to(value[None], (size, *value.shape)), axis, 0, 0, tiled=True
    )


def in_order(blocks, dim):
    blocks = jnp.moveaxis(blocks, 0, dim)
    shape = blocks.shape
    return blocks.reshape(*shape[:dim], shape[dim] * shape[dim + 1], *shape[dim + 2 :])


def gather_directly(value, axis, dim):
    blocks = from_everyone(value, axis)
    return in_order(blocks, dim)


def split_up(value, dim, size):
    shape = value.shape
    blocks = value.reshape(*shape[:dim], size, shape[dim] // size, *shape[dim + 1 :])
    return jnp.moveaxis(blocks, dim, 0)


def sent_and_summed(value, axis, dim):
    blocks = split_up(value, dim, lax.axis_size(axis))
    arrived = lax.all_to_all(blocks, axis, split_axis=0, concat_axis=0, tiled=True)
    return arrived.sum(axis=0)


def edges_of(length, count):
    unit = 8 if length >= 8 * count else 1
    return [length // unit * k // count * unit for k in range(1, count)]


def all_blocks(value, axes, turns):
    blocks = value[None]
    for k in turns:
        blocks = lax.all_gather(blocks, axes[k], axis=0, tiled=True)
    carried = [lax.axis_size(axes[k]) for k in reversed(turns)]
    blocks = blocks.reshape(*carried, *value.shape)
    turned = sorted(range(len(turns)), key=lambda place: turns[len(turns) - 1 - place])
    return blocks.transpose(*turned, *range(len(turns), blocks.ndim)).reshape(-1, *value.shape)


def gather_all_axes(value, axes, dim):
    numbers = list(range(len(axes)))[::-1]
    widest = value.shape.index(max(value.shape[:-1] or value.shape))
    edges = [0, *edges_of(value.shape[widest], len(axes)), value.shape[widest]]
    finished = []
    for k, (start, end) in enumerate(zip(edges, edges[1:])):
        if end > start:
            section = lax.slice_in_dim(value, start, end, axis=widest)
            finished.append(all_blocks(section, axes, numbers[k:] + numbers[:k]))
    return in_order(jnp.concatenate(finished, axis=widest + 1), dim)


def by_axis(value, axes):
    return functools.reduce(lax.psum, axes, value)


def rotate(values, cosine, sine):
    half = values.shape[-1] // 2
    first = values[..., :half]
    second = values[..., half:]
    return jnp.concatenate(
        [first * cosine - second * sine, second * cosine + first * sine], axis=-1
    )


def angles(length, width):
    inverse = 1.0 / rope_base ** (jnp.arange(0, width, 2, dtype=jnp.float32) / width)
    turned = jnp.arange(length, dtype=jnp.float32)[:, None] * inverse[None, :]
    return (jnp.cos(turned), jnp.sin(turned))


def attend_backward(arrived, rope_full):
    f32 = jnp.float32
    bf16 = jnp.bfloat16
    length = arrived.shape[0]
    local_heads = arrived.shape[1]
    width = PLAIN_HEAD_WIDTH + ROPE
    scale = width ** (-0.5)
    block = 512
    cosine, sine = angles(length, ROPE)
    neg = jnp.finfo(f32).min
    q_nope = arrived[:, :, :PLAIN_HEAD_WIDTH]
    q_rope = rotate(
        arrived[:, :, PLAIN_HEAD_WIDTH:width].astype(f32), cosine[:, None, :], sine[:, None, :]
    ).astype(bf16)
    key_nope = arrived[:, :, width : width + PLAIN_HEAD_WIDTH]
    values = arrived[:, :, width + PLAIN_HEAD_WIDTH : width + PLAIN_HEAD_WIDTH + VALUE_HEAD_WIDTH]
    d_out = arrived[:, :, width + PLAIN_HEAD_WIDTH + VALUE_HEAD_WIDTH :]
    k_rope = rotate(rope_full.astype(f32), cosine, sine).astype(bf16)
    dk_nope = jnp.zeros((length, local_heads, PLAIN_HEAD_WIDTH), f32)
    dk_rope = jnp.zeros((length, ROPE), f32)
    d_vals = jnp.zeros((length, local_heads, VALUE_HEAD_WIDTH), f32)
    dq_parts = []
    for begin in range(0, length, block):
        end = begin + block
        qn = q_nope[begin:end]
        qr = q_rope[begin:end]
        go = d_out[begin:end]
        scores = jnp.einsum("qhd,khd->hqk", qn, key_nope[:end], preferred_element_type=f32)
        scores = (
            scores + jnp.einsum("qhd,kd->hqk", qr, k_rope[:end], preferred_element_type=f32)
        ) * scale
        q_seg = jnp.arange(begin, end) // SPAN
        k_seg = jnp.arange(end) // SPAN
        allowed = k_seg[None, :] <= q_seg[:, None]
        scores = jnp.where(allowed[None], scores, neg)
        probs = jax.nn.softmax(scores, axis=-1)
        d_probs = jnp.einsum("qhd,khd->hqk", go, values[:end], preferred_element_type=f32)
        d_scores = probs * (d_probs - jnp.sum(probs * d_probs, axis=-1, keepdims=True))
        ds_b = d_scores.astype(bf16)
        p_b = probs.astype(bf16)
        dq_n = jnp.einsum("hqk,khd->qhd", ds_b, key_nope[:end], preferred_element_type=f32) * scale
        dq_r = jnp.einsum("hqk,kd->qhd", ds_b, k_rope[:end], preferred_element_type=f32) * scale
        dq_r = rotate(dq_r, cosine[begin:end, None, :], -sine[begin:end, None, :])
        dq_parts.append(jnp.concatenate([dq_n, dq_r], axis=-1).astype(bf16))
        dk_nope = dk_nope.at[:end].add(
            jnp.einsum("hqk,qhd->khd", ds_b, qn, preferred_element_type=f32) * scale
        )
        dk_rope = dk_rope.at[:end].add(
            jnp.einsum("hqk,qhd->kd", ds_b, qr, preferred_element_type=f32) * scale
        )
        d_vals = d_vals.at[:end].add(
            jnp.einsum("hqk,qhd->khd", p_b, go, preferred_element_type=f32)
        )
    query_part = jnp.concatenate(dq_parts, axis=0)
    grads = jnp.concatenate([query_part, dk_nope.astype(bf16), d_vals.astype(bf16)], axis=-1)
    return (grads, rotate(dk_rope, cosine, -sine))


def local(query, latent, rope_key, latent_norm_gain, key_up_matrix, value_up_matrix, out_grad):
    f32 = jnp.float32
    bf16 = jnp.bfloat16
    tokens = latent.shape[1]
    width = PLAIN_HEAD_WIDTH + ROPE
    head_cols = ATTENTION_HEADS * PLAIN_HEAD_WIDTH
    lat = latent[0].astype(f32)
    inv_rms = lax.rsqrt(jnp.mean(lat * lat, axis=-1, keepdims=True) + eps)
    normed = lat * inv_rms
    nlat = (normed * latent_norm_gain).astype(bf16)
    stacked = jnp.stack([key_up_matrix, value_up_matrix])
    whole = lax.all_gather(stacked, DP, axis=1, tiled=True)
    kv_tok = jnp.einsum("tc,gnc->tgn", nlat, whole, preferred_element_type=f32).astype(bf16)
    heads_query = query[0].reshape(tokens, ATTENTION_HEADS, width)
    key_nope = kv_tok[:, 0].reshape(tokens, ATTENTION_HEADS, PLAIN_HEAD_WIDTH)
    values = kv_tok[:, 1].reshape(tokens, ATTENTION_HEADS, VALUE_HEAD_WIDTH)
    d_out = out_grad[0].reshape(tokens, ATTENTION_HEADS, VALUE_HEAD_WIDTH)
    packed = jnp.concatenate([heads_query, key_nope, values, d_out], axis=2)
    arrived = lax.all_to_all(packed, SP, split_axis=1, concat_axis=0, tiled=True)
    rope_full = gather_directly(rope_key[0], SP, 0)
    grads_heads, rope_full_grad = attend_backward(arrived, rope_full)
    returned = lax.all_to_all(grads_heads, SP, split_axis=0, concat_axis=1, tiled=True)
    rope_grad = sent_and_summed(rope_full_grad, SP, 0)
    query_grad = returned[:, :, :width].reshape(tokens, ATTENTION_HEADS * width)
    key_cols = returned[:, :, width : width + PLAIN_HEAD_WIDTH].reshape(tokens, head_cols)
    value_cols = returned[:, :, width + PLAIN_HEAD_WIDTH :].reshape(tokens, head_cols)
    dkv = jnp.stack([key_cols, value_cols], axis=1)
    d_nlat = jnp.einsum("tgn,gnc->tc", dkv, whole, preferred_element_type=f32)
    latents_all = gather_all_axes(nlat[None], DP, 0)
    columns = lax.all_to_all(dkv[None], DP, split_axis=3, concat_axis=0, tiled=True)
    partial_value = jnp.einsum("stgr,stc->grc", columns, latents_all, preferred_element_type=f32)
    weight_grads = lax.psum(partial_value, SP)
    gain_grad = by_axis(jnp.sum(d_nlat * normed, axis=0), SP_DP)
    scaled = d_nlat * latent_norm_gain
    latent_grad = inv_rms * (scaled - normed * jnp.mean(scaled * normed, axis=-1, keepdims=True))
    return (
        query_grad[None],
        latent_grad[None],
        rope_grad[None],
        weight_grads[0],
        weight_grads[1],
        gain_grad,
    )


def solution(mesh):
    split = Mesh(mesh.devices.reshape(4, 4, 4, 2), ("sp_0", "sp_1", "dp_0", "dp_1"))
    in_specs = (
        P(DP, SP, None),
        P(DP, SP, None),
        P(DP, SP, None),
        P(),
        P(DP, None),
        P(DP, None),
        P(DP, SP, None),
    )
    out_specs = (P(DP, SP, None), P(DP, SP, None), P(DP, SP, None), P(DP, None), P(DP, None), P())
    return jax.shard_map(local, mesh=split, in_specs=in_specs, out_specs=out_specs, check_vma=False)
```

profile of v0, /device:TPU:0, one launch (start us, length us, event | category | flops | bytes accessed | tf_op | source)
XLA Modules:
  0.0 623.8 jit_solution(4799579515403184759)
XLA Ops:
  11.1 14.5 %all-gather.2 = bf16[4,96,1024]{2,1,0:T(8,128)(2,1)} all-gather(bf16[1,96,1024]{2,1,0:T(8,128)(2,1)S(1)} %get-tuple-element.261), channel_id=4, replica_groups=mesh['sp_0'=4,'sp_1'=4,'dp_0'=4,'dp_1'=2] {'dp_0'}, dimensions={0}, use_global_device_ids=true | all-gather | bytes 983040 | tf_op jit(solution)/shard_map/all_gather | solution.py:61
  26.4 8.6 %all-to-all-start.1 = ((bf16[16,192,32]{1,2,0:T(8,128)(2,1)}), bf16[16,192,32]{1,2,0:T(8,128)(2,1)S(1)}, u32[]{:S(2)}, u32[]{:S(2)}) async-start(bf16[16,192,32]{1,2,0:T(8,128)(2,1)} %broadcast_in_dim.80), calls=%async_computation.1 | async-start | bytes 524288 | tf_op jit(solution)/shard_map/all_to_all | solution.py:25
  40.2 3.9 reshape_squeeze.12
  45.3 17.1 %all-gather.8.cloned.1.call-done = bf16[2,2048,1024]{2,1,0:T(8,128)(2,1)} async-done(((bf16[2,256,1024]{2,1,0:T(8,128)(2,1)}), bf16[2,2048,1024]{2,1,0:T(8,128)(2,1)}) %all-gather.8.cloned.1.call-update) | async-done | bytes 8388624 | tf_op jit(solution)/shard_map/all_gather | solution.py:168
  62.4 6.2 convolution_convert_fusion
  75.6 3.1 copy.81
  78.7 5.6 pad_maximum_fusion
  84.4 4.0 copy.83
  88.3 7.2 %all-to-all-start = ((bf16[192,32,288]{2,0,1:T(8,128)(2,1)}), bf16[192,32,288]{2,0,1:T(8,128)(2,1)}, u32[]{:S(2)}, u32[]{:S(2)}) async-start(bf16[192,32,288]{2,0,1:T(8,128)(2,1)} %copy.83), calls=%async_computation | async-start | bytes 9437184 | tf_op jit(solution)/shard_map/all_to_all | solution.py:175
  105.9 61.1 %all-to-all-done = bf16[192,32,288]{2,0,1:T(8,128)(2,1)} async-done(((bf16[192,32,288]{2,0,1:T(8,128)(2,1)}), bf16[192,32,288]{2,0,1:T(8,128)(2,1)}, u32[]{:S(2)}, u32[]{:S(2)}) %all-to-all-start) | async-done | bytes 3538976 | tf_op jit(solution)/shard_map/all_to_all | solution.py:175
  167.0 8.3 %copy.84 = bf16[16,192,2,288]{1,0,3,2:T(8,128)(2,1)} copy(bf16[16,192,2,288]{3,1,2,0:T(8,128)(2,1)} %bitcast.8) | data formatting | bytes 7077888 | tf_op jit(solution)/shard_map/all_to_all | solution.py:175
  175.3 7.2 %all_to_all.48 = bf16[3072,2,288]{0,2,1:T(8,128)(2,1)S(1)} reshape(bf16[16,192,2,288]{1,0,3,2:T(8,128)(2,1)} %copy.84) | data formatting | bytes 7077888 | tf_op jit(solution)/shard_map/all_to_all | solution.py:175
  188.7 3.7 convolution_bitcast_fusion.5
  220.1 5.3 fusion.11
  225.4 7.3 %fusion.297 = (f32[2,512]{1,0:T(2,128)S(1)}, f32[2,512,2048]{2,1,0:T(8,128)S(1)}) fusion(f32[2,512,2048]{2,1,0:T(8,128)} %fusion.11), kind=kOutput, calls=%fused_computation.433 | output fusion | flops 4196351 | bytes 16781312 | tf_op jit(solution)/shard_map/sub | solution.py:134
  232.7 4.1 multiply_reduce_fusion.2
  236.9 4.6 multiply_convert_fusion.2
  247.1 4.3 fusion.9
  251.4 6.3 %fusion.298 = (f32[2,512]{1,0:T(2,128)S(1)}, f32[2,512,2560]{2,1,0:T(8,128)}) fusion(f32[2,512,2560]{2,1,0:T(8,128)S(1)} %fusion.9), kind=kOutput, calls=%fused_computation.434 | output fusion | flops 5245439 | bytes 20975616 | tf_op jit(solution)/shard_map/sub | solution.py:134
  258.5 6.1 multiply_reduce_fusion.1
  270.0 3.4 fusion.120
  273.5 3.1 fusion.147
  276.7 6.1 fusion.7
  282.7 14.9 %fusion.299 = (f32[2,512]{1,0:T(2,128)S(1)}, f32[2,512,3072]{2,1,0:T(8,128)}) fusion(f32[2,512,3072]{2,1,0:T(8,128)} %fusion.7), kind=kOutput, calls=%fused_computation.435 | output fusion | flops 6294527 | bytes 25169920 | tf_op jit(solution)/shard_map/sub | solution.py:134
  297.6 11.8 %multiply_reduce_fusion = (f32[2,512]{1,0:T(2,128)S(1)}, f32[2,512,3072]{2,1,0:T(8,128)}) fusion(f32[2,512,3072]{2,1,0:T(8,128)} %get-tuple-element.301, f32[2,512]{1,0:T(2,128)S(1)} %get-tuple-element.300, bf16[3072,2,288]{0,2,1:T(8,128)(2,1)} %copy-done.6), kind=kOutput, calls=%fused_computation.10 | convolution fusion | flops 412089344 | bytes 26091520 | tf_op jit(solution)/shard_map/qhd,khd->hqk/dot_general | solution.py:135
  309.5 7.4 %multiply_convert_fusion = bf16[2,512,3072]{2,1,0:T(8,128)(2,1)S(1)} fusion(f32[2,512,3072]{2,1,0:T(8,128)} %get-tuple-element.313, f32[2,512]{1,0:T(2,128)S(1)} %get-tuple-element.312, f32[2,512,3072]{2,1,0:T(8,128)S(1)} %bitcast.325, f32[2,512]{1,0:T(2,128)S(1)} %get-tuple-element.300), kind=kLoop, calls=%fused_computation.9 | loop fusion | flops 12582912 | bytes 31465472 | tf_op jit(solution)/shard_map/convert_element_type | solution.py:137
  316.9 3.8 fusion.111
  320.7 2.6 fusion.114
  325.9 6.4 %fusion.99 = f32[3072,2,64]{0,2,1:T(8,128)} fusion(f32[3072,2,64]{0,2,1:T(8,128)} %scatter-add.59, f32[512,2,64]{0,2,1:T(8,128)} %convolution_bitcast_fusion.5, bf16[3072,2,288]{0,2,1:T(8,128)(2,1)} %copy-done.6, f32[2,512]{1,0:T(2,128)S(1)} %get-tuple-element.292, f32[2,512,1024]{2,1,0:T(8,128)} %copy-done.19), kind=kOutput, calls=%fused_computation.121 | convolution fusion | flops 137496576 | bytes 9310208 | tf_op jit(solution)/shard_map/hqk,qhd->khd/dot_general | solution.py:150
  332.3 2.9 fusion.103
  335.3 8.0 %fusion.77 = f32[3072,2,64]{0,2,1:T(8,128)} fusion(f32[3072,2,64]{0,2,1:T(8,128)} %fusion.99, bf16[3072,2,288]{0,2,1:T(8,128)(2,1)} %copy-done.6, f32[2,512]{1,0:T(2,128)S(1)} %get-tuple-element.294, f32[2,512,1536]{2,1,0:T(8,128)} %copy-done.16), kind=kOutput, calls=%fused_computation.91 | convolution fusion | flops 206244352 | bytes 14290944 | tf_op jit(solution)/shard_map/hqk,qhd->khd/dot_general | solution.py:150
  343.3 2.8 fusion.58
  346.1 9.4 %fusion.65 = f32[3072,2,64]{0,2,1:T(8,128)} fusion(f32[3072,2,64]{0,2,1:T(8,128)} %fusion.77, bf16[3072,2,288]{0,2,1:T(8,128)(2,1)} %copy-done.6, f32[2,512]{1,0:T(2,128)S(1)} %get-tuple-element.296, f32[2,512,2048]{2,1,0:T(8,128)} %fusion.11), kind=kOutput, calls=%fused_computation.84 | convolution fusion | flops 274992128 | bytes 19009536 | tf_op jit(solution)/shard_map/hqk,qhd->khd/dot_general | solution.py:150
  355.5 4.4 fusion.70
  359.9 11.3 %fusion.31 = f32[3072,2,64]{0,2,1:T(8,128)} fusion(f32[3072,2,64]{0,2,1:T(8,128)} %fusion.65, bf16[3072,2,288]{0,2,1:T(8,128)(2,1)} %copy-done.6, f32[2,512]{1,0:T(2,128)S(1)} %get-tuple-element.298, f32[2,512,2560]{2,1,0:T(8,128)} %copy-done.3), kind=kOutput, calls=%fused_computation.52 | convolution fusion | flops 343739904 | bytes 23728128 | tf_op jit(solution)/shard_map/hqk,qhd->khd/dot_general | solution.py:150
  371.2 5.1 fusion.24
  376.3 12.7 %fusion.42 = bf16[3072,2,64]{0,2,1:T(8,128)(2,1)} fusion(f32[3072,2,64]{0,2,1:T(8,128)} %fusion.31, bf16[3072,2,288]{0,2,1:T(8,128)(2,1)} %copy-done.6, f32[2,512]{1,0:T(2,128)S(1)} %copy-done.72, f32[2,512,3072]{2,1,0:T(8,128)} %fusion.7), kind=kOutput, calls=%fused_computation.58 | convolution fusion | flops 412880896 | bytes 27660288 | tf_op jit(solution)/shard_map/hqk,qhd->khd/dot_general | solution.py:150
  389.2 4.7 fusion.45
  396.7 8.6 %copy.95 = bf16[3072,2,224]{2,1,0:T(2,128)(2,1)} copy(bf16[3072,2,224]{0,2,1:T(8,128)(2,1)} %pad_maximum_fusion.1) | data formatting | bytes 5505024 | tf_op jit(solution)/shard_map/concatenate | solution.py:153
  405.3 5.1 all-to-all-start.2
  410.5 4.2 copy.123
  414.7 3.7 reshape.969
  418.4 3.6 copy.124
  424.4 31.9 %all-to-all-done.2 = bf16[3072,2,224]{2,1,0:T(2,128)(2,1)} async-done(((bf16[3072,2,224]{2,1,0:T(2,128)(2,1)}), bf16[3072,2,224]{2,1,0:T(2,128)(2,1)}, u32[]{:S(2)}, u32[]{:S(2)}) %all-to-all-start.2) | async-done | bytes 2752544 | tf_op jit(solution)/shard_map/all_to_all | solution.py:178
  460.5 2.7 fusion.290
  463.2 2.6 copy.99
  468.0 2.6 copy.100
  472.8 2.7 fusion.128
  475.5 6.1 copy.105
  481.6 4.4 all-to-all-start.4
  488.4 3.9 fusion.85
  492.3 4.3 fusion.50
  498.8 14.3 %all-to-all-done.4 = bf16[1,192,2,2048]{1,2,0,3:T(2,128)(2,1)} async-done(((bf16[1,192,2,2048]{1,2,0,3:T(2,128)(2,1)}), bf16[1,192,2,2048]{1,2,0,3:T(2,128)(2,1)}, u32[]{:S(2)}, u32[]{:S(2)}) %all-to-all-start.4) | async-done | bytes 1572896 | tf_op jit(solution)/shard_map/all_to_all | solution.py:186
  513.1 3.9 copy.120
  517.0 4.6 fusion.90
  524.9 19.4 %all_to_all.64 = f32[16,192,32]{1,2,0:T(8,128)} all-to-all(f32[16,192,32]{1,2,0:T(8,128)S(1)} %copy.104), channel_id=1, replica_groups=mesh['sp_0'=4,'sp_1'=4,'dp_0'=4,'dp_1'=2] {'sp_0','sp_1'}, dimensions={0} | all-to-all | bytes 786432 | tf_op jit(solution)/shard_map/all_to_all | solution.py:49
  547.3 3.0 broadcast_in_dim_reshape.3
  550.3 5.3 fusion.140
  555.6 8.8 %psum.36 = f32[1024]{0:T(1024)S(1)} all-reduce(f32[1024]{0:T(1024)S(1)} %get-tuple-element.246), channel_id=1, replica_groups=mesh['sp_0'=4,'sp_1'=4,'dp_0'=4,'dp_1'=2] {'sp_0'}, use_global_device_ids=true, to_apply=%region_23.24 | all-reduce | flops 1024 | bytes 8192 | tf_op jit(solution)/shard_map/psum | solution.py:81
  564.4 8.7 %psum.37 = f32[1024]{0:T(1024)S(1)} all-reduce(f32[1024]{0:T(1024)S(1)} %psum.36), channel_id=1, replica_groups=mesh['sp_0'=4,'sp_1'=4,'dp_0'=4,'dp_1'=2] {'sp_1'}, use_global_device_ids=true, to_apply=%region_24.25 | all-reduce | flops 1024 | bytes 8192 | tf_op jit(solution)/shard_map/psum | solution.py:81
  573.2 9.4 %psum.38 = f32[1024]{0:T(1024)S(1)} all-reduce(f32[1024]{0:T(1024)S(1)} %psum.37), channel_id=1, replica_groups=mesh['sp_0'=4,'sp_1'=4,'dp_0'=4,'dp_1'=2] {'dp_0'}, use_global_device_ids=true, to_apply=%region_25.26 | all-reduce | flops 1024 | bytes 8192 | tf_op jit(solution)/shard_map/psum | solution.py:81
  582.6 3.0 psum.39
  586.8 27.2 %all-reduce.5.cloned.1.call-done = f32[2,256,1024]{2,1,0:T(8,128)} async-done(((f32[2,256,1024]{2,1,0:T(8,128)}), f32[2,256,1024]{2,1,0:T(8,128)}) %all-reduce.5.cloned.1.call-update) | async-done | bytes 2097168 | tf_op jit(solution)/shard_map/psum | solution.py:188
  614.0 3.1 slice_bitcast_fusion
  (282 shorter events, 102.1 us)
Async XLA Ops:
  7.2 18.4 %copy-start.73 = (bf16[1,192,32]{1,2,0:T(8,128)(2,1)S(1)}, bf16[1,192,32]{1,2,0:T(8,128)(2,1)}, u32[]{:S(2)}) copy-start(bf16[1,192,32]{1,2,0:T(8,128)(2,1)} %param.51) | copy-start | bytes 36868
  7.2 55.2 %all-gather.8.cloned.1.call-start = ((), (), s32[]{:S(2)}) async-start(), calls=%async_computation.5 | async-start | bytes 9437184 | tf_op jit(solution)/shard_map/all_gather | solution.py:168
  9.6 28.7 %copy-start.41 = (bf16[1,192,2048]{2,1,0:T(8,128)(2,1)S(1)}, bf16[1,192,2048]{2,1,0:T(8,128)(2,1)}, u32[]{:S(2)}) copy-start(bf16[1,192,2048]{2,1,0:T(8,128)(2,1)} %param.55) | copy-start | bytes 2359300
  9.6 400.9 %all-gather.12.cloned.1.call-start = ((), (), s32[]{:S(2)}) async-start(), calls=%async_computation.8 | async-start | bytes 2359296 | tf_op jit(solution)/shard_map/all_gather | solution.py:61
  10.9 51.5 %copy-start.74 = (f32[192]{0:T(256)}, f32[192]{0:T(256)S(1)}, u32[]{:S(2)}) copy-start(f32[192]{0:T(256)S(1)} %add_rsqrt_fusion) | copy-start | bytes 2308
  26.4 62.0 %all-to-all-start.1 = ((bf16[16,192,32]{1,2,0:T(8,128)(2,1)}), bf16[16,192,32]{1,2,0:T(8,128)(2,1)S(1)}, u32[]{:S(2)}, u32[]{:S(2)}) async-start(bf16[16,192,32]{1,2,0:T(8,128)(2,1)} %broadcast_in_dim.80), calls=%async_computation.1 | async-start | bytes 524288 | tf_op jit(solution)/shard_map/all_to_all | solution.py:25
  35.0 383.5 %all-gather.10.cloned.1.call-start = ((), (), s32[]{:S(2)}) async-start(), calls=%async_computation.7 | async-start | bytes 1966080 | tf_op jit(solution)/shard_map/all_gather | solution.py:61
  88.3 78.7 %all-to-all-start = ((bf16[192,32,288]{2,0,1:T(8,128)(2,1)}), bf16[192,32,288]{2,0,1:T(8,128)(2,1)}, u32[]{:S(2)}, u32[]{:S(2)}) async-start(bf16[192,32,288]{2,0,1:T(8,128)(2,1)} %copy.83), calls=%async_computation | async-start | bytes 9437184 | tf_op jit(solution)/shard_map/all_to_all | solution.py:175
  95.6 8.9 %copy-start.76 = (f32[16]{0:T(128)}, f32[16]{0:T(128)S(1)}, u32[]{:S(2)}) copy-start(f32[16]{0:T(128)S(1)} %negate_power_fusion) | copy-start | bytes 196
  182.5 30.2 %copy-start.6 = (bf16[3072,2,288]{0,2,1:T(8,128)(2,1)}, bf16[3072,2,288]{0,2,1:T(8,128)(2,1)S(1)}, u32[]{:S(2)}) copy-start(bf16[3072,2,288]{0,2,1:T(8,128)(2,1)S(1)} %all_to_all.48) | copy-start | bytes 10616836
  195.5 3.9 copy-start.14
  204.6 3.8 copy-start.4
  241.5 4.1 copy-start.2
  251.4 7.1 %copy-start.3 = (f32[2,512,2560]{2,1,0:T(8,128)}, f32[2,512,2560]{2,1,0:T(8,128)S(1)}, u32[]{:S(2)}) copy-start(f32[2,512,2560]{2,1,0:T(8,128)S(1)} %fusion.9) | copy-start | bytes 31457284
  258.5 6.1 slice-start.5
  258.5 6.7 %slice-start.6 = ((s8[10485760]{0:T(1024)(128)(4,1)}), s8[4194304]{0:T(1024)(128)(4,1)S(1)}, s32[]{:S(2)}) async-start(s8[10485760]{0:T(1024)(128)(4,1)} %bitcast.326), calls=%async_computation.15 | async-start | bytes 8388608
  258.5 7.3 %slice-start.7 = ((s8[10485760]{0:T(1024)(128)(4,1)}), s8[2097152]{0:T(1024)(128)(4,1)S(1)}, s32[]{:S(2)}) async-start(s8[10485760]{0:T(1024)(128)(4,1)} %bitcast.326), calls=%async_computation.16 | async-start | bytes 4194304
  267.7 5.8 copy-start.1
  297.6 11.8 %copy-start.71 = (f32[2,512]{1,0:T(2,128)}, f32[2,512]{1,0:T(2,128)S(1)}, u32[]{:S(2)}) copy-start(f32[2,512]{1,0:T(2,128)S(1)} %get-tuple-element.300) | copy-start | bytes 12292
  297.6 11.8 %slice-start.2 = ((s8[12582912]{0:T(1024)(128)(4,1)}), s8[4194304]{0:T(1024)(128)(4,1)S(1)}, s32[]{:S(2)}) async-start(s8[12582912]{0:T(1024)(128)(4,1)} %bitcast.324), calls=%async_computation.11 | async-start | bytes 8388608
  297.6 11.8 %slice-start.3 = ((s8[12582912]{0:T(1024)(128)(4,1)}), s8[4194304]{0:T(1024)(128)(4,1)S(1)}, s32[]{:S(2)}) async-start(s8[12582912]{0:T(1024)(128)(4,1)} %bitcast.324), calls=%async_computation.12 | async-start | bytes 8388608
  297.6 11.8 %slice-start.4 = ((s8[12582912]{0:T(1024)(128)(4,1)}), s8[4194304]{0:T(1024)(128)(4,1)S(1)}, s32[]{:S(2)}) async-start(s8[12582912]{0:T(1024)(128)(4,1)} %bitcast.324), calls=%async_computation.13 | async-start | bytes 8388608
  320.7 3.9 copy-start.33
  371.2 5.1 copy-start.72
  389.0 4.9 copy-start.54
  389.0 4.9 copy-start.67
  389.0 4.9 copy-start.68
  389.0 5.0 copy-start.47
  389.0 5.0 copy-start.50
  389.0 5.0 copy-start.65
  389.0 5.0 copy-start.66
  389.0 5.0 copy-start.55
  389.0 5.0 copy-start.63
  389.0 5.0 copy-start.64
  389.0 5.1 copy-start.51
  389.0 5.1 copy-start.61
  389.1 5.1 copy-start.62
  389.1 5.1 copy-start.52
  389.1 5.1 copy-start.59
  389.1 5.1 copy-start.60
  389.1 5.1 copy-start.53
  389.1 5.1 copy-start.57
  389.1 5.1 copy-start.58
  389.1 5.1 copy-start.45
  389.1 5.2 copy-start.46
  389.1 5.2 copy-start.48
  389.2 5.2 copy-start.49
  405.3 50.9 %all-to-all-start.2 = ((bf16[3072,2,224]{2,1,0:T(2,128)(2,1)}), bf16[3072,2,224]{2,1,0:T(2,128)(2,1)}, u32[]{:S(2)}, u32[]{:S(2)}) async-start(bf16[3072,2,224]{2,1,0:T(2,128)(2,1)} %copy.95), calls=%async_computation.2 | async-start | bytes 6291456 | tf_op jit(solution)/shard_map/all_to_all | solution.py:178
  414.7 7.3 %copy-start.10 = (bf16[3072,2,16]{0,2,1:T(8,128)(2,1)S(1)}, bf16[3072,2,16]{0,2,1:T(8,128)(2,1)}, u32[]{:S(2)}) copy-start(bf16[3072,2,16]{0,2,1:T(8,128)(2,1)} %copy-done.8) | copy-start | bytes 589828
  414.7 7.3 %copy-start.13 = (bf16[3072,2,16]{0,2,1:T(8,128)(2,1)S(1)}, bf16[3072,2,16]{0,2,1:T(8,128)(2,1)}, u32[]{:S(2)}) copy-start(bf16[3072,2,16]{0,2,1:T(8,128)(2,1)} %copy-done.11) | copy-start | bytes 589828
  418.4 4.8 copy-start.5
  481.6 31.5 %all-to-all-start.4 = ((bf16[1,192,2,2048]{1,2,0,3:T(2,128)(2,1)}), bf16[1,192,2,2048]{1,2,0,3:T(2,128)(2,1)}, u32[]{:S(2)}, u32[]{:S(2)}) async-start(bf16[1,192,2,2048]{1,2,0,3:T(2,128)(2,1)} %copy.105), calls=%async_computation.4 | async-start | bytes 4194304 | tf_op jit(solution)/shard_map/all_to_all | solution.py:186
  485.9 128.1 %all-reduce.5.cloned.1.call-start = ((), (), s32[]{:S(2)}) async-start(), calls=%async_computation.6 | async-start | bytes 4194304 | tf_op jit(solution)/shard_map/psum | solution.py:188
  486.0 10.6 %slice-start = ((s8[6291456]{0:T(1024)(128)(4,1)}), s8[4194304]{0:T(1024)(128)(4,1)S(1)}, s32[]{:S(2)}) async-start(s8[6291456]{0:T(1024)(128)(4,1)} %bitcast.322), calls=%async_computation.9 | async-start | bytes 8388608
  488.4 8.2 %slice-start.1 = ((s8[6291456]{0:T(1024)(128)(4,1)}), s8[2097152]{0:T(1024)(128)(4,1)S(1)}, s32[]{:S(2)}) async-start(s8[6291456]{0:T(1024)(128)(4,1)} %bitcast.322), calls=%async_computation.10 | async-start | bytes 4194304
  492.3 4.3 copy-start.44
  498.8 18.2 %copy-start.39 = (bf16[8,1,96,1024]{3,0,2,1:T(8,128)(2,1)S(1)}, bf16[8,1,96,1024]{3,0,2,1:T(8,128)(2,1)}, u32[]{:S(2)}) copy-start(bf16[8,1,96,1024]{3,0,2,1:T(8,128)(2,1)} %reshape.969) | copy-start | bytes 4718596
  517.0 4.6 copy-start.77
  521.6 24.4 %copy-start.18 = (bf16[192,16,2,224]{3,0,2,1:T(8,128)(2,1)S(1)}, bf16[192,16,2,224]{3,0,2,1:T(8,128)(2,1)}, u32[]{:S(2)}) copy-start(bf16[192,16,2,224]{3,0,2,1:T(8,128)(2,1)} %copy-done.17) | copy-start | bytes 8257540
  546.2 4.0 copy-start.29
  546.2 4.0 copy-start.30
  546.3 4.0 copy-start.31
  546.3 4.0 copy-start.70
  546.3 4.0 copy-start.75
  (30 other events, 63.0 us)
Sparse Core Ops, SparseCore 0:
  10.3 52.0 all-gather.7
  64.1 12.6 all-gather.11
  78.4 27.7 all-gather.9
  521.7 92.2 all-reduce.4
where the time goes:
time: 634 us; the launch traced here: 624 us
  matrix products  182 us (29%)
  waiting for transfers between devices  152 us (24%)
  local copies, waits for them, and re-layouts  105 us (17%)
  other arithmetic  78.7 us (12%)
  blocking collectives  66.1 us (10%)
  starting transfers between devices  25.5 us (4%)
  between operations  15.3 us (2%)
    all_to_all x1, waiting for transfers between devices, local(): lax.all_to_all(packed, SP, split_axis=1, concat_axis=0, tiled=True)  61.1 us
    dot_general x6, matrix products, attend_backward(): jnp.einsum('hqk,qhd->khd', p_b, go, preferred_element_type=f32)  51.5 us
    sub x6, other arithmetic, attend_backward(): probs = jax.nn.softmax(scores, axis=-1)  32.6 us
    all_to_all x1, waiting for transfers between devices, local(): lax.all_to_all(grads_heads, SP, split_axis=0, concat_axis=1, tiled=True)  31.9 us
    psum x4, blocking collectives, by_axis(): return functools.reduce(lax.psum, axes, value)  30 us
    psum x1, waiting for transfers between devices, local(): weight_grads = lax.psum(partial_value, SP)  27.2 us
    dot_general x6, matrix products, attend_backward(): jnp.einsum('qhd,khd->hqk', go, values[:end], preferred_element_type=f32)  27.1 us
    dot_general x6, matrix products, attend_backward(): jnp.einsum('hqk,qhd->khd', ds_b, qn, preferred_element_type=f32) * scale  21.1 us
  transfers between devices with their start and end apart: 8, of which 5 were waited for; matrix products, arithmetic and copies ran while one was open for 50% of the time, Pallas kernels for 0%

commit v1 on v0

v1 whole, which is shorter than its diff:
```python
import functools

import jax
import jax.numpy as jnp
import numpy as np
from jax import lax
from jax.experimental import pallas as pl
from jax.experimental.pallas import tpu as pltpu
from jax.sharding import Mesh
from jax.sharding import PartitionSpec as P

ATTENTION_HEADS = 32
PLAIN = 64
ROPE = 32
HALF = ROPE // 2
WIDTH = PLAIN + ROPE
LATENT = 1024
SPAN = 64
LENGTH = 3072
DP = ("dp_0", "dp_1")
SP = ("sp_0", "sp_1")
ALL = SP + DP
NSP = 16
NDP = 8
TOKENS = LENGTH // NSP
BLOCK = 512
SCALE = WIDTH**-0.5
LOG2E = 1.4426950408889634

eps = 1e-06
rope_base = 10000.0
f32 = jnp.float32
bf16 = jnp.bfloat16


def angles(positions):
    inverse = 1.0 / rope_base ** (jnp.arange(0, ROPE, 2, dtype=f32) / ROPE)
    turned = positions.astype(f32)[:, None] * inverse[None, :]
    return jnp.cos(turned), jnp.sin(turned)


def lanes_of(shape):
    return lax.broadcasted_iota(jnp.int32, shape, 1)


def pack_body(q_ref, g_ref, kr_ref, cos_ref, sin_ref, out_ref):
    lane = lanes_of((TOKENS, 128))
    cosine = cos_ref[...]
    sine = sin_ref[...]

    def turn(x):
        inside = (lane % ROPE) < HALF
        swapped = jnp.where(inside, pltpu.roll(x, 128 - HALF, 1), pltpu.roll(x, HALF, 1))
        return x * cosine + swapped * sine

    key = turn(kr_ref[...])
    key = pltpu.roll(key, ROPE, 1)

    def emit(slot, qn0, qr0, qn1, qr1, grads):
        first = jnp.where(lane < PLAIN, qn0, pltpu.roll(grads, PLAIN, 1))
        second = jnp.where(lane < PLAIN, qn1, grads)
        third = turn(jnp.where(lane < ROPE, qr0, jnp.where(lane >= 96, qr1, 0.0)))
        third = jnp.where((lane >= ROPE) & (lane < 2 * ROPE), key, third)
        out_ref[slot, :, 0:128] = first.astype(bf16)
        out_ref[slot, :, 128:256] = second.astype(bf16)
        out_ref[slot, :, 256:384] = third.astype(bf16)

    for pair in range(NSP // 2):
        a0, a1, a2 = [
            q_ref[:, 384 * pair + 128 * k : 384 * pair + 128 * (k + 1)].astype(f32) for k in range(3)
        ]
        g0 = g_ref[:, 256 * pair : 256 * pair + 128].astype(f32)
        g1 = g_ref[:, 256 * pair + 128 : 256 * pair + 256].astype(f32)
        qn1 = jnp.where(lane < ROPE, pltpu.roll(a0, ROPE, 1), pltpu.roll(a1, ROPE, 1))
        emit(2 * pair, a0, pltpu.roll(a0, 64, 1), qn1, pltpu.roll(a1, 64, 1), g0)
        emit(2 * pair + 1, pltpu.roll(a1, 64, 1), a2, pltpu.roll(a2, 96, 1), a2, g1)


def pack(query, grads, key, cosine, sine):
    return pl.pallas_call(
        pack_body,
        out_shape=jax.ShapeDtypeStruct((NSP, TOKENS, 384), bf16),
        cost_estimate=pl.CostEstimate(flops=2_000_000_000, bytes_accessed=5_000_000, transcendentals=0),
        name="pack",
    )(query, grads, key, cosine, sine)


def attend_body(head, qd_ref, kv_ref, cos_ref, sin_ref, out_ref, p_buf, dp_buf, m_buf, kt_buf, acc, dq_acc):
    blocks = LENGTH // BLOCK
    lane = lanes_of((BLOCK, 128))
    factor = SCALE * LOG2E
    tile = 128 * head
    low = 0 if head == 0 else 96

    def prepare(j, carry):
        rows = pl.ds(pl.multiple_of(j * BLOCK, BLOCK), BLOCK)
        kt = kv_ref[rows, :].astype(f32).T
        rt = qd_ref[rows, 256:384].astype(f32).T
        kt_buf[:, rows] = jnp.concatenate([kt[0:PLAIN], rt[ROPE : 2 * ROPE]], axis=0).astype(bf16)
        acc[rows, :] = jnp.zeros((BLOCK, 256), f32)
        return carry

    lax.fori_loop(0, blocks, prepare, 0)
    key_seg = lax.broadcasted_iota(jnp.int32, (BLOCK, BLOCK), 0) // SPAN
    query_seg = lax.broadcasted_iota(jnp.int32, (BLOCK, BLOCK), 1) // SPAN
    allowed = key_seg <= query_seg

    def one_block(i, carry):
        rows = pl.ds(pl.multiple_of(i * BLOCK, BLOCK), BLOCK)
        qd = qd_ref[rows, tile : tile + 128].astype(f32)
        rt = qd_ref[rows, 256:384].astype(f32)
        qdt = qd.T
        rtt = rt.T
        none = jnp.zeros((32, BLOCK), f32)
        left = jnp.concatenate(
            [qdt[0:PLAIN], none, none, none, rtt[low : low + ROPE], none, none], axis=0
        ).astype(bf16)
        left_d = jnp.concatenate([none, none, qdt[PLAIN:128]], axis=0).astype(bf16)
        right = jnp.concatenate(
            [jnp.where(lane < PLAIN, qd, 0.0), jnp.where((lane >= low) & (lane < low + ROPE), rt, 0.0)], axis=1
        ).astype(bf16)
        right_d = jnp.where(lane < PLAIN, 0.0, qd).astype(bf16)

        def gather_stats(j, stats, masked):
            top, total, inner = stats
            keys = pl.ds(pl.multiple_of(j * BLOCK, BLOCK), BLOCK)
            kv = kv_ref[keys, :]
            both = jnp.concatenate([kv, qd_ref[keys, 256:384]], axis=1)
            scores = jnp.dot(both, left, preferred_element_type=f32) * factor
            if masked:
                scores = jnp.where(allowed, scores, -jnp.inf)
            d_probs = jnp.dot(kv, left_d, preferred_element_type=f32)
            new_top = jnp.maximum(top, jnp.max(scores, axis=0, keepdims=True))
            probs = jnp.exp2(scores - new_top)
            shrink = jnp.exp2(top - new_top)
            total = total * shrink + jnp.sum(probs, axis=0, keepdims=True)
            inner = inner * shrink + jnp.sum(probs * d_probs, axis=0, keepdims=True)
            p_buf[keys, :] = probs
            dp_buf[keys, :] = d_probs
            m_buf[j] = jnp.broadcast_to(new_top, (8, BLOCK))
            return new_top, total, inner

        start = (
            jnp.full((1, BLOCK), jnp.finfo(f32).min, f32),
            jnp.zeros((1, BLOCK), f32),
            jnp.zeros((1, BLOCK), f32),
        )
        stats = lax.fori_loop(0, i, functools.partial(gather_stats, masked=False), start)
        top, total, inner = gather_stats(i, stats, True)
        inverse = 1.0 / total
        inner = inner * inverse
        dq_acc[...] = jnp.zeros((WIDTH, BLOCK), f32)

        def gradients(j, carry):
            keys = pl.ds(pl.multiple_of(j * BLOCK, BLOCK), BLOCK)
            grow = jnp.exp2(m_buf[j][0:1] - top) * inverse
            probs = p_buf[keys, :] * grow
            ds = (probs * (dp_buf[keys, :] - inner)).astype(bf16)
            pb = probs.astype(bf16)
            dq_acc[...] += jnp.dot(kt_buf[:, keys], ds, preferred_element_type=f32)
            acc[keys, :] += jnp.dot(ds, right, preferred_element_type=f32)
            acc[keys, 0:128] += jnp.dot(pb, right_d, preferred_element_type=f32)
            return carry

        lax.fori_loop(0, i + 1, gradients, 0)
        dq = dq_acc[...] * SCALE
        cosine = cos_ref[:, rows]
        sine = sin_ref[:, rows]
        first, second = dq[PLAIN : PLAIN + HALF], dq[PLAIN + HALF : WIDTH]
        pieces = [dq[0:PLAIN], first * cosine + second * sine, second * cosine - first * sine]
        pieces = [none] + pieces if head == 0 else pieces + [none]
        out_ref[rows, 128:256] = jnp.concatenate(pieces, axis=0).T.astype(bf16)
        return carry

    lax.fori_loop(0, blocks, one_block, 0)

    def finish(j, carry):
        rows = pl.ds(pl.multiple_of(j * BLOCK, BLOCK), BLOCK)
        plain = acc[rows, 0:128]
        out_ref[rows, 0:128] = jnp.where(lane < PLAIN, plain * SCALE, plain).astype(bf16)
        turned = acc[rows, 128:256] * SCALE
        kept = out_ref[rows, 128:256].astype(f32)
        mine = (lane >= low) & (lane < low + ROPE)
        out_ref[rows, 128:256] = jnp.where(mine, turned, kept).astype(bf16)
        return carry

    lax.fori_loop(0, blocks, finish, 0)


def attend(head, arrived, kv, cosine, sine):
    return pl.pallas_call(
        functools.partial(attend_body, head),
        grid=(1,),
        in_specs=[
            pl.BlockSpec((LENGTH, 384), lambda g: (0, 0)),
            pl.BlockSpec((LENGTH, 128), lambda g: (0, head)),
            pl.BlockSpec((HALF, LENGTH), lambda g: (0, 0)),
            pl.BlockSpec((HALF, LENGTH), lambda g: (0, 0)),
        ],
        out_specs=pl.BlockSpec((LENGTH, 256), lambda g: (0, 0)),
        out_shape=jax.ShapeDtypeStruct((LENGTH, 256), bf16),
        scratch_shapes=[
            pltpu.VMEM((LENGTH, BLOCK), f32),
            pltpu.VMEM((LENGTH, BLOCK), f32),
            pltpu.VMEM((LENGTH // BLOCK, 8, BLOCK), f32),
            pltpu.VMEM((WIDTH, LENGTH), bf16),
            pltpu.VMEM((LENGTH, 256), f32),
            pltpu.VMEM((WIDTH, BLOCK), f32),
        ],
        compiler_params=pltpu.CompilerParams(vmem_limit_bytes=48 * 1024 * 1024),
        cost_estimate=pl.CostEstimate(
            flops=12_000_000_000, bytes_accessed=6_000_000, transcendentals=5_000_000
        ),
        name=f"attend{head}",
    )(arrived, kv, cosine, sine)


def finish_body(r0_ref, r1_ref, w_ref, lat_ref, gain_ref, cos_ref, sin_ref, dq_ref, dlat_ref, drope_ref, acc, rope):
    step = pl.program_id(0)
    lane = lanes_of((TOKENS, 128))

    @pl.when(step == 0)
    def _():
        acc[...] = jnp.zeros_like(acc)
        rope[...] = jnp.zeros_like(rope)

    tiles = []
    for half in range(2):
        r0 = r0_ref[half]
        r1 = r1_ref[half]
        both = jnp.concatenate([r0[:, 0:128], r1[:, 0:128]], axis=1)
        acc[...] += jnp.dot(both, w_ref[half], preferred_element_type=f32)
        t0 = r0[:, 128:256].astype(f32)
        t1 = r1[:, 128:256].astype(f32)
        rope[...] += jnp.where(lane < ROPE, t0, jnp.where(lane >= 96, t1, 0.0))
        tiles.append((t0, t1))
    (x0, x1), (y0, y1) = tiles
    dq_ref[:, 0:128] = jnp.where(lane < 96, pltpu.roll(x0, 96, 1), pltpu.roll(x1, 96, 1)).astype(bf16)
    dq_ref[:, 128:256] = jnp.where(lane < 64, pltpu.roll(x1, 96, 1), pltpu.roll(y0, 32, 1)).astype(bf16)
    dq_ref[:, 256:384] = jnp.where(lane < 32, pltpu.roll(y0, 32, 1), pltpu.roll(y1, 32, 1)).astype(bf16)

    @pl.when(step == NSP // 2 - 1)
    def _():
        lat = lat_ref[...].astype(f32)
        inv_rms = lax.rsqrt(jnp.mean(lat * lat, axis=-1, keepdims=True) + eps)
        normed = lat * inv_rms
        scaled = acc[...] * gain_ref[...]
        dlat_ref[...] = inv_rms * (scaled - normed * jnp.mean(scaled * normed, axis=-1, keepdims=True))
        x = rope[...]
        x = x + pltpu.roll(x, 32, 1)
        swapped = jnp.where(lane < HALF, pltpu.roll(x, 128 - HALF, 1), pltpu.roll(x, HALF, 1))
        drope_ref[...] = (x * cos_ref[...] - swapped * sin_ref[...])[:, 0:ROPE]


def finish(r0, r1, weights, latent, gain, cosine, sine):
    half = NSP // 2
    return pl.pallas_call(
        finish_body,
        grid=(half,),
        in_specs=[
            pl.BlockSpec((2, TOKENS, 256), lambda g: (g, 0, 0)),
            pl.BlockSpec((2, TOKENS, 256), lambda g: (g, 0, 0)),
            pl.BlockSpec((2, 256, LATENT), lambda g: (g, 0, 0)),
            pl.BlockSpec((TOKENS, LATENT), lambda g: (0, 0)),
            pl.BlockSpec((1, LATENT), lambda g: (0, 0)),
            pl.BlockSpec((TOKENS, 128), lambda g: (0, 0)),
            pl.BlockSpec((TOKENS, 128), lambda g: (0, 0)),
        ],
        out_specs=[
            pl.BlockSpec((TOKENS, 384), lambda g: (0, g)),
            pl.BlockSpec((TOKENS, LATENT), lambda g: (0, 0)),
            pl.BlockSpec((TOKENS, ROPE), lambda g: (0, 0)),
        ],
        out_shape=[
            jax.ShapeDtypeStruct((TOKENS, ATTENTION_HEADS * WIDTH), bf16),
            jax.ShapeDtypeStruct((TOKENS, LATENT), f32),
            jax.ShapeDtypeStruct((TOKENS, ROPE), f32),
        ],
        scratch_shapes=[pltpu.VMEM((TOKENS, LATENT), f32), pltpu.VMEM((TOKENS, 128), f32)],
        cost_estimate=pl.CostEstimate(flops=2_000_000_000, bytes_accessed=14_000_000, transcendentals=0),
        name="finish",
    )(r0, r1, weights, latent, gain, cosine, sine)


def to_heads():
    return [(NDP * a + d, NDP * (2 * d + a // 8) + a % 8) for a in range(NSP) for d in range(NDP)]


def to_rows():
    return [(b, a) for a, b in to_heads()]


def everyone(value, axes, size):
    return lax.all_to_all(jnp.broadcast_to(value[None], (size, *value.shape)), axes, 0, 0, tiled=True)


def local(query, latent, rope_key, gain, key_up, value_up, out_grad):
    place = lax.axis_index(SP)
    gain_row = gain[None, :]
    lat = latent[0].astype(f32)
    inv_rms = lax.rsqrt(jnp.mean(lat * lat, axis=-1, keepdims=True) + eps)
    nlat = (lat * inv_rms * gain_row).astype(bf16)
    nlat_all = lax.all_gather(nlat, SP, axis=0, tiled=True)

    rows = jnp.stack([key_up.reshape(4, 64, LATENT), value_up.reshape(4, 64, LATENT)], axis=1)
    rows = rows.reshape(512, LATENT)
    mine = lax.dynamic_slice_in_dim(rows, (place // 8) * 256, 256, axis=0)
    own = lax.ppermute(mine, ALL, to_heads())
    whole = lax.all_gather(rows, DP, axis=0, tiled=True)

    positions = place * TOKENS + jnp.arange(TOKENS)
    cosine, sine = angles(positions)
    cos_lanes = jnp.tile(cosine, (1, 8))
    sin_lanes = jnp.tile(jnp.concatenate([-sine, sine], axis=1), (1, 4))
    key = jnp.pad(rope_key[0].astype(f32), ((0, 0), (0, 96)))
    packed = pack(query[0], out_grad[0], key, cos_lanes, sin_lanes)
    arrived = lax.all_to_all(packed, SP, 0, 0, tiled=True).reshape(LENGTH, 384)

    kv = lax.dot_general(nlat_all, own, (((1,), (1,)), ((), ())), preferred_element_type=f32).astype(bf16)
    cos_all, sin_all = angles(jnp.arange(LENGTH))
    cos_all, sin_all = cos_all.T, sin_all.T
    g0 = attend(0, arrived, kv, cos_all, sin_all)
    r0 = lax.all_to_all(g0.reshape(NSP, TOKENS, 256), SP, 0, 0, tiled=True)
    g1 = attend(1, arrived, kv, cos_all, sin_all)
    r1 = lax.all_to_all(g1.reshape(NSP, TOKENS, 256), SP, 0, 0, tiled=True)

    parts = [
        lax.dot_general(g[:, 0:128], nlat_all, (((0,), (0,)), ((), ())), preferred_element_type=f32)
        for g in (g0, g1)
    ]
    part = jnp.concatenate(parts, axis=0)
    gain_part = jnp.sum(part * own.astype(f32), axis=0) / gain
    gain_part = everyone(gain_part.reshape(8, 128), DP, NDP).sum(axis=0)
    gain_grad = everyone(gain_part, SP, NSP).sum(axis=0).reshape(LATENT)

    pieces = part.astype(bf16).reshape(2, 2, 4, 16, LATENT).transpose(0, 2, 1, 3, 4).reshape(NDP, 32, LATENT)
    pieces = lax.all_to_all(pieces, DP, 0, 0, tiled=True)
    piece = pieces.astype(f32).sum(axis=0).astype(bf16)
    piece = lax.ppermute(piece, ALL, to_rows())
    grads = everyone(piece, SP, NSP).reshape(NSP, 2, 16, LATENT)
    key_grad = grads[:, 0].reshape(256, LATENT).astype(f32)
    value_grad = grads[:, 1].reshape(256, LATENT).astype(f32)

    dq, dlat, drope = finish(
        r0, r1, whole.reshape(NSP, 256, LATENT), latent[0], gain_row, cos_lanes, sin_lanes
    )
    return dq[None], dlat[None], drope[None], key_grad, value_grad, gain_grad


def solution(mesh):
    split = Mesh(mesh.devices.reshape(4, 4, 4, 2), ("sp_0", "sp_1", "dp_0", "dp_1"))
    in_specs = (
        P(DP, SP, None),
        P(DP, SP, None),
        P(DP, SP, None),
        P(),
        P(DP, None),
        P(DP, None),
        P(DP, SP, None),
    )
    out_specs = (P(DP, SP, None), P(DP, SP, None), P(DP, SP, None), P(DP, None), P(DP, None), P())
    return jax.shard_map(local, mesh=split, in_specs=in_specs, out_specs=out_specs, check_vma=False)
```

time: 634 us -> 331 us (0.52); the launches traced: 624 us -> 330 us
  matrix products: 182 us -> 10.2 us
  local copies, waits for them, and re-layouts: 105 us -> 7.87 us
  Pallas kernels: 0 us -> 70.1 us
  other arithmetic: 78.7 us -> 9.52 us
  blocking collectives: 66.1 us -> 46.2 us
    dot_general x51 -> x3, matrix products: 182 us -> 10.2 us  [the longest x1 5.82 us: local(): lax.dot_general(nlat_all, own, (((1,), (1,)), ((), ())), preferred_elemen...]
    all_gather x3 -> x2, waiting for transfers between devices: 17.2 us -> 98.2 us  [the longest x1 98.2 us: local(): nlat_all = lax.all_gather(nlat, SP, axis=0, tiled=True)]
    pallas_call x0 -> x4, Pallas kernels: none -> 70.1 us  [the longest x2 55.6 us: attend(): pl.pallas_call(functools.partial(attend_body, head), grid=(1,), in_specs=...]
    all_to_all x4, waiting for transfers between devices: 107 us -> 50.3 us  [the longest x1 23.6 us: local(): r1 = lax.all_to_all(g1.reshape(NSP, TOKENS, 256), SP, 0, 0, tiled=True)]
    sub x7 -> x0, other arithmetic: 33.5 us -> none  [the longest x6 32.6 us: attend_backward(): probs = jax.nn.softmax(scores, axis=-1)]
    psum x4 -> x0, blocking collectives: 30 us -> none  [by_axis(): return functools.reduce(lax.psum, axes, value)]
    psum x1 -> x0, waiting for transfers between devices: 27.2 us -> none  [local(): weight_grads = lax.psum(partial_value, SP)]
    all_to_all x1 -> x3, blocking collectives: 19.4 us -> 46.2 us  [the longest x2 33.4 us: everyone(): lax.all_to_all(jnp.broadcast_to(value[None], (size, *value.shape)), axes,...]
  transfers between devices with their start and end apart: 8 -> 8, of which waited for: 5 -> 4; matrix products, arithmetic and copies ran while one was open for 50% -> 6% of each run, Pallas kernels for 0% -> 18%
where the time goes in v1:
time: 331 us; the launch traced here: 330 us
  waiting for transfers between devices  149 us (45%)
  Pallas kernels  70.1 us (21%)
  blocking collectives  46.2 us (14%)
  starting transfers between devices  23.1 us (7%)
  between operations  14.3 us (4%)
  matrix products  10.2 us (3%)
  other arithmetic  9.52 us (3%)
  local copies, waits for them, and re-layouts  7.87 us (2%)
    all_gather x1, waiting for transfers between devices, local(): nlat_all = lax.all_gather(nlat, SP, axis=0, tiled=True)  98.2 us
    pallas_call x2, Pallas kernels, attend(): pl.pallas_call(functools.partial(attend_body, head), grid=(1,), in_specs=...  55.6 us
    all_to_all x2, blocking collectives, everyone(): lax.all_to_all(jnp.broadcast_to(value[None], (size, *value.shape)), axes,...  33.4 us
    all_to_all x1, waiting for transfers between devices, local(): r1 = lax.all_to_all(g1.reshape(NSP, TOKENS, 256), SP, 0, 0, tiled=True)  23.6 us
    all_to_all x1, waiting for transfers between devices, local(): r0 = lax.all_to_all(g0.reshape(NSP, TOKENS, 256), SP, 0, 0, tiled=True)  19.2 us
    all_to_all x1, blocking collectives, local(): pieces = lax.all_to_all(pieces, DP, 0, 0, tiled=True)  12.8 us
    pallas_call x1, Pallas kernels, finish(): pl.pallas_call(finish_body, grid=(half,), in_specs=[pl.BlockSpec((2, TOKE...  9.75 us
    all_to_all x1, starting transfers between devices, local(): arrived = lax.all_to_all(packed, SP, 0, 0, tiled=True).reshape(LENGTH, 384)  8.29 us
  transfers between devices with their start and end apart: 8, of which 4 were waited for; matrix products, arithmetic and copies ran while one was open for 6% of the time, Pallas kernels for 18%

profile of v1, /device:TPU:0, one launch (start us, length us, event | category | flops | bytes accessed | tf_op | source)
XLA Modules:
  0.0 329.7 jit_solution(15151686694083296039)
XLA Ops:
  7.2 0.0 all-gather.3.cloned.1.call-start
  7.2 1.2 fusion.1
  8.4 1.9 fusion.3
  10.3 0.0 copy-start.8
  10.3 0.0 all-gather.3.cloned.1.call-update
  10.3 0.0 all-gather.5.cloned.1.call-start
  10.4 2.3 pad_maximum_fusion
  12.6 0.0 all-gather.5.cloned.1.call-update
  12.7 0.1 fusion.8
  12.9 0.7 copy.28.sin_ref
  13.6 0.7 copy.27.cos_ref
  14.4 0.0 copy-done.8
  14.4 0.1 copy.26
  14.5 0.7 pad_convert_fusion.kr_ref
  15.1 4.7 %pack.1 = bf16[16,192,384]{2,1,0:T(8,128)(2,1)} custom-call(bf16[192,3072]{1,0:T(8,128)(2,1)} %bitcast.58, bf16[192,2048]{1,0:T(8,128)(2,1)} %bitcast.60, f32[192,128]{1,0:T(8,128)} %pad_convert_fusion.kr_ref, f32[192,128]{1,0:T(8,128)} %copy.27.cos_ref, f32[192,128]{1,0:T(8,128)} %copy.28.sin_ref), custom_call_target="tpu_custom_call" | custom-call | flops 2000000000 | bytes 5000000 | tf_op jit(solution)/shard_map/pack/pallas_call | solution.py:80
  19.9 0.0 copy-start.2
  19.9 8.3 %all-to-all-start = ((bf16[16,192,384]{2,1,0:T(8,128)(2,1)}), bf16[16,192,384]{2,1,0:T(8,128)(2,1)S(1)}, u32[]{:S(2)}, u32[]{:S(2)}) async-start(bf16[16,192,384]{2,1,0:T(8,128)(2,1)} %pack.1), calls=%async_computation | async-start | bytes 4718592 | tf_op jit(solution)/shard_map/all_to_all | solution.py:317
  28.2 0.0 copy-done.2
  28.2 0.7 collective-permute-start
  29.0 0.8 multiply_sine_fusion
  29.7 0.0 collective-permute-done
  29.7 0.0 copy-start.5
  29.7 98.2 %all-gather.3.cloned.1.call-done = bf16[3072,1024]{1,0:T(8,128)(2,1)} async-done(((bf16[192,1024]{1,0:T(8,128)(2,1)}), bf16[3072,1024]{1,0:T(8,128)(2,1)}) %all-gather.3.cloned.1.call-update) | async-done | bytes 6291472 | tf_op jit(solution)/shard_map/all_gather | solution.py:303
  127.9 5.8 %convolution_convert_fusion.kv_ref = bf16[3072,256]{1,0:T(8,128)(2,1)} fusion(bf16[3072,1024]{1,0:T(8,128)(2,1)} %all-gather.3.cloned.1.call-done, bf16[256,1024]{1,0:T(8,128)(2,1)S(1)} %collective-permute-done), kind=kOutput, calls=%fused_computation | convolution fusion | flops 1611399168 | bytes 8388608 | tf_op jit(solution)/shard_map/dot_general | solution.py:319
  133.8 0.0 copy-done.5
  133.8 0.0 all-to-all-done
  133.8 0.0 copy-start
  133.8 1.4 copy-done
  135.2 0.0 copy-start.1
  135.2 27.9 %attend1.1 = bf16[3072,256]{1,0:T(8,128)(2,1)} custom-call(bf16[3072,384]{1,0:T(8,128)(2,1)S(1)} %bitcast.41, bf16[3072,256]{1,0:T(8,128)(2,1)S(1)} %copy-done, f32[16,3072]{1,0:T(8,128)S(1)} %get-tuple-element.33.cos_ref, f32[16,3072]{1,0:T(8,128)S(1)} %get-tuple-element.32.sin_ref), custom_call_target="tpu_custom_call" | custom-call | flops 12000000000 | bytes 6000000 | tf_op jit(solution)/shard_map/attend1/pallas_call | solution.py:191
  163.1 0.0 copy-done.1
  163.1 2.1 fusion.4
  165.2 27.7 %attend0.1 = bf16[3072,256]{1,0:T(8,128)(2,1)} custom-call(bf16[3072,384]{1,0:T(8,128)(2,1)S(1)} %bitcast.42, bf16[3072,256]{1,0:T(8,128)(2,1)S(1)} %copy-done, f32[16,3072]{1,0:T(8,128)S(1)} %get-tuple-element.33.cos_ref, f32[16,3072]{1,0:T(8,128)S(1)} %get-tuple-element.32.sin_ref), custom_call_target="tpu_custom_call" | custom-call | flops 12000000000 | bytes 6000000 | tf_op jit(solution)/shard_map/attend0/pallas_call | solution.py:191
  192.9 0.0 copy-start.6
  192.9 0.0 copy-start.7
  192.9 2.2 fusion.6
  195.1 0.0 copy-done.6
  195.2 0.2 multiply_reduce_fusion
  195.3 0.0 copy-done.7
  195.3 11.2 %all_to_all.35 = f32[8,8,128]{2,1,0:T(8,128)S(1)} all-to-all(f32[8,8,128]{2,1,0:T(8,128)S(1)} %broadcast_in_dim.42), channel_id=1, replica_groups=mesh['sp_0'=4,'sp_1'=4,'dp_0'=4,'dp_1'=2] {'dp_0','dp_1'}, dimensions={0} | all-to-all | bytes 65536 | tf_op jit(solution)/shard_map/all_to_all | solution.py:294
  206.6 0.6 broadcast_in_dim.43
  207.2 6.0 %all-to-all-start.6 = ((f32[16,8,128]{2,1,0:T(8,128)}), f32[16,8,128]{2,1,0:T(8,128)S(1)}, u32[]{:S(2)}, u32[]{:S(2)}) async-start(f32[16,8,128]{2,1,0:T(8,128)} %broadcast_in_dim.43), calls=%async_computation.6 | async-start | bytes 131072 | tf_op jit(solution)/shard_map/all_to_all | solution.py:294
  213.2 0.1 fusion
  213.3 7.5 %all-to-all-done.6 = f32[16,8,128]{2,1,0:T(8,128)S(1)} async-done(((f32[16,8,128]{2,1,0:T(8,128)}), f32[16,8,128]{2,1,0:T(8,128)S(1)}, u32[]{:S(2)}, u32[]{:S(2)}) %all-to-all-start.6) | async-done | bytes 65568 | tf_op jit(solution)/shard_map/all_to_all | solution.py:294
  220.9 12.8 %all_to_all.36 = bf16[8,32,1024]{2,1,0:T(8,128)(2,1)S(1)} all-to-all(bf16[8,32,1024]{2,1,0:T(8,128)(2,1)S(1)} %bitcast.49), channel_id=1, replica_groups=mesh['sp_0'=4,'sp_1'=4,'dp_0'=4,'dp_1'=2] {'dp_0','dp_1'}, dimensions={0} | all-to-all | bytes 1048576 | tf_op jit(solution)/shard_map/all_to_all | solution.py:337
  233.6 3.7 %all-to-all-start.2 = ((bf16[16,192,256]{2,1,0:T(8,128)(2,1)}), bf16[16,192,256]{2,1,0:T(8,128)(2,1)S(1)}, u32[]{:S(2)}, u32[]{:S(2)}) async-start(bf16[16,192,256]{2,1,0:T(8,128)(2,1)} %bitcast.13), calls=%async_computation.2 | async-start | bytes 3145728 | tf_op jit(solution)/shard_map/all_to_all | solution.py:325
  237.3 0.1 reduce_sum.49
  237.4 0.7 collective-permute-start.1
  238.1 0.0 collective-permute-done.1
  238.1 23.6 %all-to-all-done.2.r1_ref = bf16[16,192,256]{2,1,0:T(8,128)(2,1)S(1)} async-done(((bf16[16,192,256]{2,1,0:T(8,128)(2,1)}), bf16[16,192,256]{2,1,0:T(8,128)(2,1)S(1)}, u32[]{:S(2)}, u32[]{:S(2)}) %all-to-all-start.2) | async-done | bytes 1572896 | tf_op jit(solution)/shard_map/all_to_all | solution.py:325
  261.7 0.0 copy-start.3
  261.7 0.1 broadcast_in_dim.40
  261.8 22.2 %all_to_all.37 = bf16[16,32,1024]{2,1,0:T(8,128)(2,1)} all-to-all(bf16[16,32,1024]{2,1,0:T(8,128)(2,1)S(1)} %broadcast_in_dim.40), channel_id=1, replica_groups=mesh['sp_0'=4,'sp_1'=4,'dp_0'=4,'dp_1'=2] {'sp_0','sp_1'}, dimensions={0} | all-to-all | bytes 2097152 | tf_op jit(solution)/shard_map/all_to_all | solution.py:294
  284.0 0.0 copy-done.3
  284.0 3.7 %all-to-all-start.1 = ((bf16[16,192,256]{2,1,0:T(8,128)(2,1)}), bf16[16,192,256]{2,1,0:T(8,128)(2,1)S(1)}, u32[]{:S(2)}, u32[]{:S(2)}) async-start(bf16[16,192,256]{2,1,0:T(8,128)(2,1)} %bitcast.12), calls=%async_computation.1 | async-start | bytes 3145728 | tf_op jit(solution)/shard_map/all_to_all | solution.py:323
  287.7 0.6 reduce_sum.52
  288.3 1.3 fusion.9
  289.6 1.6 bitcast_convert_fusion
  291.3 19.2 %all-to-all-done.1.r0_ref = bf16[16,192,256]{2,1,0:T(8,128)(2,1)S(1)} async-done(((bf16[16,192,256]{2,1,0:T(8,128)(2,1)}), bf16[16,192,256]{2,1,0:T(8,128)(2,1)S(1)}, u32[]{:S(2)}, u32[]{:S(2)}) %all-to-all-start.1) | async-done | bytes 1572896 | tf_op jit(solution)/shard_map/all_to_all | solution.py:323
  310.4 0.0 copy-start.4
  310.4 0.0 all-gather.5.cloned.1.call-done
  310.4 1.1 copy-done.4
  311.6 9.8 %finish.1 = (bf16[192,3072]{1,0:T(8,128)(2,1)}, f32[192,1024]{1,0:T(8,128)}, f32[192,32]{1,0:T(8,128)}) custom-call(bf16[16,192,256]{2,1,0:T(8,128)(2,1)} %copy-done.4, bf16[16,192,256]{2,1,0:T(8,128)(2,1)} %copy-done.3, bf16[16,256,1024]{2,1,0:T(8,128)(2,1)} %bitcast.43, bf16[192,1024]{1,0:T(8,128)(2,1)} %bitcast.47, f32[1,1024]{1,0:T(1,128)} %bitcast.56, ...), custom_call_target="tpu_custom_call" | custom-call | flops 2000000000 | bytes 14000000 | tf_op jit(solution)/shard_map/finish/pallas_call | solution.py:257
  321.3 1.6 copy.34
  (12 shorter events, 0.2 us)
Async XLA Ops:
  7.2 120.8 %all-gather.3.cloned.1.call-start = ((), (), s32[]{:S(2)}) async-start(), calls=%async_computation.7 | async-start | bytes 6684672 | tf_op jit(solution)/shard_map/all_gather | solution.py:303
  10.3 4.1 %copy-start.8 = (bf16[1,192,32]{1,2,0:T(8,128)(2,1)S(1)}, bf16[1,192,32]{1,2,0:T(8,128)(2,1)}, u32[]{:S(2)}) copy-start(bf16[1,192,32]{1,2,0:T(8,128)(2,1)} %param.9) | copy-start | bytes 36868
  10.3 300.1 %all-gather.5.cloned.1.call-start = ((), (), s32[]{:S(2)}) async-start(), calls=%async_computation.8 | async-start | bytes 9437184 | tf_op jit(solution)/shard_map/all_gather | solution.py:309
  19.9 8.3 %copy-start.2 = (bf16[4,2,64,1024]{3,2,1,0:T(8,128)(2,1)S(1)}, bf16[4,2,64,1024]{3,2,1,0:T(8,128)(2,1)}, u32[]{:S(2)}) copy-start(bf16[4,2,64,1024]{3,2,1,0:T(8,128)(2,1)} %pad_maximum_fusion) | copy-start | bytes 3145732
  19.9 113.9 %all-to-all-start = ((bf16[16,192,384]{2,1,0:T(8,128)(2,1)}), bf16[16,192,384]{2,1,0:T(8,128)(2,1)S(1)}, u32[]{:S(2)}, u32[]{:S(2)}) async-start(bf16[16,192,384]{2,1,0:T(8,128)(2,1)} %pack.1), calls=%async_computation | async-start | bytes 4718592 | tf_op jit(solution)/shard_map/all_to_all | solution.py:317
  28.2 1.5 collective-permute-start
  29.7 104.0 %copy-start.5 = (bf16[256,1024]{1,0:T(8,128)(2,1)}, bf16[256,1024]{1,0:T(8,128)(2,1)S(1)}, u32[]{:S(2)}) copy-start(bf16[256,1024]{1,0:T(8,128)(2,1)S(1)} %collective-permute-done) | copy-start | bytes 1572868
  133.8 1.4 copy-start
  135.2 27.9 %copy-start.1 = (bf16[3072,1024]{1,0:T(8,128)(2,1)S(1)}, bf16[3072,1024]{1,0:T(8,128)(2,1)}, u32[]{:S(2)}) copy-start(bf16[3072,1024]{1,0:T(8,128)(2,1)} %all-gather.3.cloned.1.call-done) | copy-start | bytes 18874372
  192.9 2.2 copy-start.6
  192.9 2.4 copy-start.7
  207.2 13.7 %all-to-all-start.6 = ((f32[16,8,128]{2,1,0:T(8,128)}), f32[16,8,128]{2,1,0:T(8,128)S(1)}, u32[]{:S(2)}, u32[]{:S(2)}) async-start(f32[16,8,128]{2,1,0:T(8,128)} %broadcast_in_dim.43), calls=%async_computation.6 | async-start | bytes 131072 | tf_op jit(solution)/shard_map/all_to_all | solution.py:294
  233.6 28.1 %all-to-all-start.2 = ((bf16[16,192,256]{2,1,0:T(8,128)(2,1)}), bf16[16,192,256]{2,1,0:T(8,128)(2,1)S(1)}, u32[]{:S(2)}, u32[]{:S(2)}) async-start(bf16[16,192,256]{2,1,0:T(8,128)(2,1)} %bitcast.13), calls=%async_computation.2 | async-start | bytes 3145728 | tf_op jit(solution)/shard_map/all_to_all | solution.py:325
  237.4 0.7 collective-permute-start.1
  261.7 22.3 %copy-start.3 = (bf16[16,192,256]{2,1,0:T(8,128)(2,1)}, bf16[16,192,256]{2,1,0:T(8,128)(2,1)S(1)}, u32[]{:S(2)}) copy-start(bf16[16,192,256]{2,1,0:T(8,128)(2,1)S(1)} %all-to-all-done.2.r1_ref) | copy-start | bytes 4718596
  284.0 26.4 %all-to-all-start.1 = ((bf16[16,192,256]{2,1,0:T(8,128)(2,1)}), bf16[16,192,256]{2,1,0:T(8,128)(2,1)S(1)}, u32[]{:S(2)}, u32[]{:S(2)}) async-start(bf16[16,192,256]{2,1,0:T(8,128)(2,1)} %bitcast.12), calls=%async_computation.1 | async-start | bytes 3145728 | tf_op jit(solution)/shard_map/all_to_all | solution.py:323
  310.4 1.2 copy-start.4
Sparse Core Ops, SparseCore 0:
  10.7 117.2 all-gather.2
  130.2 51.5 all-gather.4

commit v2 on v1

--- a/solution.py
+++ b/solution.py
@@ -2,7 +2,6 @@
 
 import jax
 import jax.numpy as jnp
-import numpy as np
 from jax import lax
 from jax.experimental import pallas as pl
 from jax.experimental.pallas import tpu as pltpu
@@ -43,7 +42,7 @@
     return lax.broadcasted_iota(jnp.int32, shape, 1)
 
 
-def pack_body(q_ref, g_ref, kr_ref, cos_ref, sin_ref, out_ref):
+def pack_body(q_ref, g_ref, kr_ref, cos_ref, sin_ref, out_ref, other_ref):
     lane = lanes_of((TOKENS, 128))
     cosine = cos_ref[...]
     sine = sin_ref[...]
@@ -62,8 +61,8 @@
         third = turn(jnp.where(lane < ROPE, qr0, jnp.where(lane >= 96, qr1, 0.0)))
         third = jnp.where((lane >= ROPE) & (lane < 2 * ROPE), key, third)
         out_ref[slot, :, 0:128] = first.astype(bf16)
-        out_ref[slot, :, 128:256] = second.astype(bf16)
-        out_ref[slot, :, 256:384] = third.astype(bf16)
+        out_ref[slot, :, 128:256] = third.astype(bf16)
+        other_ref[slot] = second.astype(bf16)
 
     for pair in range(NSP // 2):
         a0, a1, a2 = [
@@ -79,23 +78,25 @@
 def pack(query, grads, key, cosine, sine):
     return pl.pallas_call(
         pack_body,
-        out_shape=jax.ShapeDtypeStruct((NSP, TOKENS, 384), bf16),
+        out_shape=[
+            jax.ShapeDtypeStruct((NSP, TOKENS, 256), bf16),
+            jax.ShapeDtypeStruct((NSP, TOKENS, 128), bf16),
+        ],
         cost_estimate=pl.CostEstimate(flops=2_000_000_000, bytes_accessed=5_000_000, transcendentals=0),
         name="pack",
     )(query, grads, key, cosine, sine)
 
 
-def attend_body(head, qd_ref, kv_ref, cos_ref, sin_ref, out_ref, p_buf, dp_buf, m_buf, kt_buf, acc, dq_acc):
+def attend_body(head, qd_ref, rt_ref, kv_ref, cos_ref, sin_ref, out_ref, p_buf, dp_buf, m_buf, kt_buf, acc, dq_acc):
     blocks = LENGTH // BLOCK
     lane = lanes_of((BLOCK, 128))
     factor = SCALE * LOG2E
-    tile = 128 * head
     low = 0 if head == 0 else 96
 
     def prepare(j, carry):
         rows = pl.ds(pl.multiple_of(j * BLOCK, BLOCK), BLOCK)
         kt = kv_ref[rows, :].astype(f32).T
-        rt = qd_ref[rows, 256:384].astype(f32).T
+        rt = rt_ref[rows, :].astype(f32).T
         kt_buf[:, rows] = jnp.concatenate([kt[0:PLAIN], rt[ROPE : 2 * ROPE]], axis=0).astype(bf16)
         acc[rows, :] = jnp.zeros((BLOCK, 256), f32)
         return carry
@@ -107,8 +108,8 @@
 
     def one_block(i, carry):
         rows = pl.ds(pl.multiple_of(i * BLOCK, BLOCK), BLOCK)
-        qd = qd_ref[rows, tile : tile + 128].astype(f32)
-        rt = qd_ref[rows, 256:384].astype(f32)
+        qd = qd_ref[rows, :].astype(f32)
+        rt = rt_ref[rows, :].astype(f32)
         qdt = qd.T
         rtt = rt.T
         none = jnp.zeros((32, BLOCK), f32)
@@ -125,7 +126,7 @@
             top, total, inner = stats
             keys = pl.ds(pl.multiple_of(j * BLOCK, BLOCK), BLOCK)
             kv = kv_ref[keys, :]
-            both = jnp.concatenate([kv, qd_ref[keys, 256:384]], axis=1)
+            both = jnp.concatenate([kv, rt_ref[keys, :]], axis=1)
             scores = jnp.dot(both, left, preferred_element_type=f32) * factor
             if masked:
                 scores = jnp.where(allowed, scores, -jnp.inf)
@@ -187,12 +188,13 @@
     lax.fori_loop(0, blocks, finish, 0)
 
 
-def attend(head, arrived, kv, cosine, sine):
+def attend(head, arrived, turned, kv, cosine, sine):
     return pl.pallas_call(
         functools.partial(attend_body, head),
         grid=(1,),
         in_specs=[
-            pl.BlockSpec((LENGTH, 384), lambda g: (0, 0)),
+            pl.BlockSpec((LENGTH, 128), lambda g: (0, 0)),
+            pl.BlockSpec((LENGTH, 128), lambda g: (0, 1)),
             pl.BlockSpec((LENGTH, 128), lambda g: (0, head)),
             pl.BlockSpec((HALF, LENGTH), lambda g: (0, 0)),
             pl.BlockSpec((HALF, LENGTH), lambda g: (0, 0)),
@@ -211,8 +213,7 @@
         cost_estimate=pl.CostEstimate(
             flops=12_000_000_000, bytes_accessed=6_000_000, transcendentals=5_000_000
         ),
-        name=f"attend{head}",
-    )(arrived, kv, cosine, sine)
+    )(arrived, turned, kv, cosine, sine)
 
 
 def finish_body(r0_ref, r1_ref, w_ref, lat_ref, gain_ref, cos_ref, sin_ref, dq_ref, dlat_ref, drope_ref, acc, rope):
@@ -294,7 +295,37 @@
     return lax.all_to_all(jnp.broadcast_to(value[None], (size, *value.shape)), axes, 0, 0, tiled=True)
 
 
-def local(query, latent, rope_key, gain, key_up, value_up, out_grad):
+def shifted(value, axis, k):
+    return lax.ppermute(value, axis, [(i, (i + k) % 4) for i in range(4)])
+
+
+SWAP = [(0, 1), (1, 0)]
+
+
+def sum_everywhere(value):
+    value = value + lax.ppermute(value, "dp_1", SWAP)
+    for axis in ("dp_0", "sp_1", "sp_0"):
+        others = [shifted(value, axis, k) for k in (1, 2, 3)]
+        value = (value + others[1]) + (others[0] + others[2])
+    return value
+
+
+def reduce_over_rows(pieces):
+    across, core = lax.axis_index("dp_0"), lax.axis_index("dp_1")
+    pairs = pieces.reshape(4, 2, *pieces.shape[1:])
+    kept = lax.dynamic_index_in_dim(pairs, core, 1, keepdims=False)
+    given = lax.dynamic_index_in_dim(pairs, 1 - core, 1, keepdims=False)
+    given = lax.ppermute(given, "dp_1", SWAP)
+    kept = kept.astype(f32) + given.astype(f32)
+    total = lax.dynamic_index_in_dim(kept, across, 0, keepdims=False)
+    kept = kept.astype(bf16)
+    for k in (1, 2, 3):
+        sent = lax.dynamic_index_in_dim(kept, (across + k) & 3, 0, keepdims=False)
+        total = total + shifted(sent, "dp_0", k).astype(f32)
+    return total.astype(bf16)
+
+
+def program(query, latent, rope_key, gain, key_up, value_up, out_grad):
     place = lax.axis_index(SP)
     gain_row = gain[None, :]
     lat = latent[0].astype(f32)
@@ -313,15 +344,18 @@
     cos_lanes = jnp.tile(cosine, (1, 8))
     sin_lanes = jnp.tile(jnp.concatenate([-sine, sine], axis=1), (1, 4))
     key = jnp.pad(rope_key[0].astype(f32), ((0, 0), (0, 96)))
-    packed = pack(query[0], out_grad[0], key, cos_lanes, sin_lanes)
-    arrived = lax.all_to_all(packed, SP, 0, 0, tiled=True).reshape(LENGTH, 384)
-
+    first, second = pack(query[0], out_grad[0], key, cos_lanes, sin_lanes)
+    first = lax.all_to_all(first, SP, 0, 0, tiled=True).reshape(LENGTH, 256)
     kv = lax.dot_general(nlat_all, own, (((1,), (1,)), ((), ())), preferred_element_type=f32).astype(bf16)
+    second, kv = lax.optimization_barrier((second, kv))
+    second = lax.all_to_all(second, SP, 0, 0, tiled=True).reshape(LENGTH, 128)
     cos_all, sin_all = angles(jnp.arange(LENGTH))
     cos_all, sin_all = cos_all.T, sin_all.T
-    g0 = attend(0, arrived, kv, cos_all, sin_all)
+    g0 = attend(0, first, first, kv, cos_all, sin_all)
+    kv, g0 = lax.optimization_barrier((kv, g0))
     r0 = lax.all_to_all(g0.reshape(NSP, TOKENS, 256), SP, 0, 0, tiled=True)
-    g1 = attend(1, arrived, kv, cos_all, sin_all)
+    g1 = attend(1, second, first, kv, cos_all, sin_all)
+    r0, g1 = lax.optimization_barrier((r0, g1))
     r1 = lax.all_to_all(g1.reshape(NSP, TOKENS, 256), SP, 0, 0, tiled=True)
 
     parts = [
@@ -329,14 +363,12 @@
         for g in (g0, g1)
     ]
     part = jnp.concatenate(parts, axis=0)
+    pieces = part.astype(bf16).reshape(2, 2, 4, 16, LATENT).transpose(0, 2, 1, 3, 4).reshape(NDP, 32, LATENT)
+    piece = reduce_over_rows(pieces)
     gain_part = jnp.sum(part * own.astype(f32), axis=0) / gain
-    gain_part = everyone(gain_part.reshape(8, 128), DP, NDP).sum(axis=0)
-    gain_grad = everyone(gain_part, SP, NSP).sum(axis=0).reshape(LATENT)
-
-    pieces = part.astype(bf16).reshape(2, 2, 4, 16, LATENT).transpose(0, 2, 1, 3, 4).reshape(NDP, 32, LATENT)
-    pieces = lax.all_to_all(pieces, DP, 0, 0, tiled=True)
-    piece = pieces.astype(f32).sum(axis=0).astype(bf16)
+    gain_grad = sum_everywhere(gain_part.reshape(8, 128)).reshape(LATENT)
     piece = lax.ppermute(piece, ALL, to_rows())
+    r1, piece = lax.optimization_barrier((r1, piece))
     grads = everyone(piece, SP, NSP).reshape(NSP, 2, 16, LATENT)
     key_grad = grads[:, 0].reshape(256, LATENT).astype(f32)
     value_grad = grads[:, 1].reshape(256, LATENT).astype(f32)
@@ -359,4 +391,4 @@
         P(DP, SP, None),
     )
     out_specs = (P(DP, SP, None), P(DP, SP, None), P(DP, SP, None), P(DP, None), P(DP, None), P())
-    return jax.shard_map(local, mesh=split, in_specs=in_specs, out_specs=out_specs, check_vma=False)
+    return jax.shard_map(program, mesh=split, in_specs=in_specs, out_specs=out_specs, check_vma=False)

time: 331 us -> 289 us (0.87)
  blocking collectives: 46.2 us -> 0 us
  starting transfers between devices: 23.1 us -> 69.3 us
  waiting for transfers between devices: 149 us -> 104 us
  matrix products: 10.2 us -> 14.1 us
    all_to_all x3 -> x0, blocking collectives: 46.2 us -> none  [the longest x2 33.4 us: everyone(): lax.all_to_all(jnp.broadcast_to(value[None], (size, *value.shape)), axes,...]
    all_to_all x3 -> x4, waiting for transfers between devices: 42.7 us -> 3.23 us  [the longest x1 3.22 us: program(): r1 = lax.all_to_all(g1.reshape(NSP, TOKENS, 256), SP, 0, 0, tiled=True)]
    ppermute x2 -> x16, starting transfers between devices: 1.36 us -> 28.4 us  [the longest x12 23.7 us: shifted(): return lax.ppermute(value, axis, [(i, (i + k) % 4) for i in range(4)])]
    all_to_all x3 -> x4, starting transfers between devices: 15.7 us -> 29.3 us  [the longest x1 8.29 us: program(): first = lax.all_to_all(first, SP, 0, 0, tiled=True).reshape(LENGTH, 256)]
    ppermute x2 -> x16, waiting for transfers between devices: 0.01 us -> 9.59 us  [the longest x12 7.84 us: shifted(): return lax.ppermute(value, axis, [(i, (i + k) % 4) for i in range(4)])]
    all_to_all x1, waiting for transfers between devices: 7.54 us -> 0.01 us  [everyone(): lax.all_to_all(jnp.broadcast_to(value[None], (size, *value.shape)), axes,...]
    all_gather x2, waiting for transfers between devices: 98.2 us -> 91.4 us  [the longest x1 91.4 us: program(): nlat_all = lax.all_gather(nlat, SP, axis=0, tiled=True)]
    all_to_all x1, starting transfers between devices: 5.99 us -> 11.6 us  [everyone(): lax.all_to_all(jnp.broadcast_to(value[None], (size, *value.shape)), axes,...]
  transfers between devices with their start and end apart: 8 -> 23, of which waited for: 4 -> 11; matrix products, arithmetic and copies ran while one was open for 6% -> 8% of each run, Pallas kernels for 18% -> 24%
where the time goes in v2:
time: 289 us; the launch traced here: 288 us
  waiting for transfers between devices  104 us (36%)
  Pallas kernels  70.4 us (24%)
  starting transfers between devices  69.3 us (24%)
  between operations  14.4 us (5%)
  matrix products  14.1 us (5%)
  other arithmetic  8.41 us (3%)
  local copies, waits for them, and re-layouts  7.29 us (3%)
    all_gather x1, waiting for transfers between devices, program(): nlat_all = lax.all_gather(nlat, SP, axis=0, tiled=True)  91.4 us
    pallas_call x2, Pallas kernels, attend(): pl.pallas_call(functools.partial(attend_body, head), grid=(1,), in_specs=...  55.9 us
    ppermute x12, starting transfers between devices, shifted(): return lax.ppermute(value, axis, [(i, (i + k) % 4) for i in range(4)])  23.7 us
    all_to_all x1, starting transfers between devices, everyone(): lax.all_to_all(jnp.broadcast_to(value[None], (size, *value.shape)), axes,...  11.6 us
    pallas_call x1, Pallas kernels, finish(): pl.pallas_call(finish_body, grid=(half,), in_specs=[pl.BlockSpec((2, TOKE...  9.78 us
    all_to_all x1, starting transfers between devices, program(): first = lax.all_to_all(first, SP, 0, 0, tiled=True).reshape(LENGTH, 256)  8.29 us
    dot_general x2, matrix products, program(): lax.dot_general(g[:, 0:128], nlat_all, (((0,), (0,)), ((), ())), preferre...  8.28 us
    ppermute x12, waiting for transfers between devices, shifted(): return lax.ppermute(value, axis, [(i, (i + k) % 4) for i in range(4)])  7.84 us
  transfers between devices with their start and end apart: 23, of which 11 were waited for; matrix products, arithmetic and copies ran while one was open for 8% of the time, Pallas kernels for 24%

profile of v2, /device:TPU:0, one launch (start us, length us, event | category | flops | bytes accessed | tf_op | source)
XLA Modules:
  0.0 288.1 jit_solution(7451526084590432982)
XLA Ops:
  7.2 0.0 all-gather.3.cloned.1.call-start
  7.2 1.2 fusion.1
  8.5 1.9 fusion.3
  10.4 0.0 all-gather.3.cloned.1.call-update
  10.4 0.0 all-gather.5.cloned.1.call-start
  10.5 0.0 copy-start.9
  10.5 1.1 pad_maximum_fusion
  11.6 0.0 all-gather.5.cloned.1.call-update
  11.6 0.1 fusion.11
  11.8 0.7 copy.19.sin_ref
  12.6 0.7 copy.18.cos_ref
  13.3 0.1 copy.17
  13.4 0.7 pad_convert_fusion.kr_ref
  14.1 4.7 %pack.1 = (bf16[16,192,256]{2,1,0:T(8,128)(2,1)}, bf16[16,192,128]{2,1,0:T(8,128)(2,1)}) custom-call(bf16[192,3072]{1,0:T(8,128)(2,1)} %bitcast.84, bf16[192,2048]{1,0:T(8,128)(2,1)} %bitcast.86, f32[192,128]{1,0:T(8,128)} %pad_convert_fusion.kr_ref, f32[192,128]{1,0:T(8,128)} %copy.18.cos_ref, f32[192,128]{1,0:T(8,128)} %copy.19.sin_ref), custom_call_target="tpu_custom_call" | custom-call | flops 2000000000 | bytes 5000000 | tf_op jit(solution)/shard_map/pack/pallas_call | solution.py:79
  18.8 8.3 %all-to-all-start = ((bf16[16,192,256]{2,1,0:T(8,128)(2,1)}), bf16[16,192,256]{2,1,0:T(8,128)(2,1)S(1)}, u32[]{:S(2)}, u32[]{:S(2)}) async-start(bf16[16,192,256]{2,1,0:T(8,128)(2,1)} %get-tuple-element.21), calls=%async_computation | async-start | bytes 3145728 | tf_op jit(solution)/shard_map/all_to_all | solution.py:348
  27.1 0.7 collective-permute-start
  27.9 0.8 multiply_sine_fusion
  28.6 0.0 copy-start.4
  28.6 91.4 %all-gather.3.cloned.1.call-done = bf16[3072,1024]{1,0:T(8,128)(2,1)} async-done(((bf16[192,1024]{1,0:T(8,128)(2,1)}), bf16[3072,1024]{1,0:T(8,128)(2,1)}) %all-gather.3.cloned.1.call-update) | async-done | bytes 6291472 | tf_op jit(solution)/shard_map/all_gather | solution.py:334
  120.0 5.8 %convolution_convert_fusion.kv_ref = bf16[3072,256]{1,0:T(8,128)(2,1)} fusion(bf16[3072,1024]{1,0:T(8,128)(2,1)} %all-gather.3.cloned.1.call-done, bf16[256,1024]{1,0:T(8,128)(2,1)S(1)} %collective-permute-done), kind=kOutput, calls=%fused_computation | convolution fusion | flops 1611399168 | bytes 8388608 | tf_op jit(solution)/shard_map/dot_general | solution.py:349
  125.8 6.6 %all-to-all-start.2 = ((bf16[16,192,128]{2,1,0:T(8,128)(2,1)}), bf16[16,192,128]{2,1,0:T(8,128)(2,1)S(1)}, u32[]{:S(2)}, u32[]{:S(2)}) async-start(bf16[16,192,128]{2,1,0:T(8,128)(2,1)} %get-tuple-element.23), calls=%async_computation.2 | async-start | bytes 1572864 | tf_op jit(solution)/shard_map/all_to_all | solution.py:351
  132.4 1.5 copy-done
  134.0 27.9 %shard_map.118 = bf16[3072,256]{1,0:T(8,128)(2,1)} custom-call(bf16[3072,256]{1,0:T(8,128)(2,1)S(1)} %bitcast.65, bf16[3072,256]{1,0:T(8,128)(2,1)S(1)} %bitcast.66, bf16[3072,256]{1,0:T(8,128)(2,1)S(1)} %copy-done, f32[16,3072]{1,0:T(8,128)S(1)} %get-tuple-element.52.cos_ref, f32[16,3072]{1,0:T(8,128)S(1)} %get-tuple-element.51.sin_ref), custom_call_target="tpu_custom_call" | custom-call | flops 12000000000 | bytes 6000000 | tf_op jit(solution)/shard_map/pallas_call | solution.py:192
  161.9 7.3 %all-to-all-start.1 = ((bf16[16,192,256]{2,1,0:T(8,128)(2,1)}), bf16[16,192,256]{2,1,0:T(8,128)(2,1)}, u32[]{:S(2)}, u32[]{:S(2)}) async-start(bf16[16,192,256]{2,1,0:T(8,128)(2,1)} %bitcast.12), calls=%async_computation.1 | async-start | bytes 3145728 | tf_op jit(solution)/shard_map/all_to_all | solution.py:356
  169.2 4.2 %fusion.6 = f32[128,1024]{1,0:T(8,128)S(1)} fusion(bf16[3072,1024]{1,0:T(8,128)(2,1)} %all-gather.3.cloned.1.call-done, bf16[3072,256]{1,0:T(8,128)(2,1)} %shard_map.118), kind=kOutput, calls=%fused_computation.12 | convolution fusion | flops 805306368 | bytes 7602176 | tf_op jit(solution)/shard_map/dot_general | solution.py:362
  173.5 28.0 %shard_map.119 = bf16[3072,256]{1,0:T(8,128)(2,1)} custom-call(bf16[3072,128]{1,0:T(8,128)(2,1)S(1)} %bitcast.68, bf16[3072,256]{1,0:T(8,128)(2,1)S(1)} %bitcast.67, bf16[3072,256]{1,0:T(8,128)(2,1)S(1)} %copy-done.1, f32[16,3072]{1,0:T(8,128)S(1)} %get-tuple-element.52.cos_ref, f32[16,3072]{1,0:T(8,128)S(1)} %get-tuple-element.51.sin_ref), custom_call_target="tpu_custom_call" | custom-call | flops 12000000000 | bytes 6000000 | tf_op jit(solution)/shard_map/pallas_call | solution.py:192
  201.5 7.2 %all-to-all-start.3 = ((bf16[16,192,256]{2,1,0:T(8,128)(2,1)}), bf16[16,192,256]{2,1,0:T(8,128)(2,1)S(1)}, u32[]{:S(2)}, u32[]{:S(2)}) async-start(bf16[16,192,256]{2,1,0:T(8,128)(2,1)} %bitcast.14), calls=%async_computation.3 | async-start | bytes 3145728 | tf_op jit(solution)/shard_map/all_to_all | solution.py:359
  208.6 4.0 %fusion.4 = f32[128,1024]{1,0:T(8,128)S(1)} fusion(bf16[3072,1024]{1,0:T(8,128)(2,1)} %all-gather.3.cloned.1.call-done, bf16[3072,256]{1,0:T(8,128)(2,1)} %shard_map.119), kind=kOutput, calls=%fused_computation.10 | convolution fusion | flops 805306368 | bytes 7602176 | tf_op jit(solution)/shard_map/dot_general | solution.py:362
  212.7 0.1 fusion
  212.8 0.7 dynamic-slice_bitcast_fusion
  213.6 1.7 collective-permute-done.1
  215.3 0.1 fusion.12
  215.4 1.0 collective-permute-start.2
  216.4 3.3 %collective-permute-start.3 = (bf16[32,1024]{1,0:T(8,128)(2,1)S(1)}, bf16[32,1024]{1,0:T(8,128)(2,1)S(1)}, u32[]{:S(2)}, u32[]{:S(2)}) collective-permute-start(bf16[32,1024]{1,0:T(8,128)(2,1)S(1)} %get-tuple-element.50), channel_id=1, source_target_pairs={{0,4},{2,6},{4,0},{6,2},{1,5},{3,7},{5,1},{7,3},{8,12},{10,14},{12... | collective-permute-start | bytes 196616 | tf_op jit(solution)/shard_map/ppermute | solution.py:299
  219.7 2.1 collective-permute-start.4
  221.8 0.2 multiply_reduce_fusion
  222.0 1.3 collective-permute-done.3
  223.2 0.8 collective-permute-done.4
  224.0 0.7 collective-permute-start.5
  224.7 3.4 %collective-permute-start.6 = (f32[8,128]{1,0:T(8,128)S(1)}, f32[8,128]{1,0:T(8,128)S(1)}, u32[]{:S(2)}, u32[]{:S(2)}) collective-permute-start(f32[8,128]{1,0:T(8,128)S(1)} %divide_bitcast_fusion), channel_id=1, source_target_pairs={{0,1},{1,0},{2,3},{3,2},{4,5},{5,4},{6,7},{7,6},{8,9},{9,8},{10,11... | collective-permute-start | bytes 12296 | tf_op jit(solution)/shard_map/ppermute | solution.py:306
  228.1 3.2 %all-to-all-done.3.r1_ref = bf16[16,192,256]{2,1,0:T(8,128)(2,1)S(1)} async-done(((bf16[16,192,256]{2,1,0:T(8,128)(2,1)}), bf16[16,192,256]{2,1,0:T(8,128)(2,1)S(1)}, u32[]{:S(2)}, u32[]{:S(2)}) %all-to-all-start.3) | async-done | bytes 1572896 | tf_op jit(solution)/shard_map/all_to_all | solution.py:359
  231.3 1.2 broadcast_in_dim.27
  232.5 0.3 copy-done.3
  232.9 11.6 %all-to-all-start.4 = ((bf16[16,32,1024]{2,1,0:T(8,128)(2,1)}), bf16[16,32,1024]{2,1,0:T(8,128)(2,1)S(1)}, u32[]{:S(2)}, u32[]{:S(2)}) async-start(bf16[16,32,1024]{2,1,0:T(8,128)(2,1)} %broadcast_in_dim.27), calls=%async_computation.4 | async-start | bytes 2097152 | tf_op jit(solution)/shard_map/all_to_all | solution.py:295
  244.5 1.1 collective-permute-start.7
  245.6 2.3 collective-permute-start.8
  247.8 1.0 collective-permute-start.9
  248.8 0.9 collective-permute-done.7
  249.7 0.7 collective-permute-done.8
  250.4 1.1 collective-permute-done.9
  251.4 3.4 %collective-permute-start.10 = (f32[8,128]{1,0:T(8,128)S(1)}, f32[8,128]{1,0:T(8,128)S(1)}, u32[]{:S(2)}, u32[]{:S(2)}) collective-permute-start(f32[8,128]{1,0:T(8,128)S(1)} %add_add_fusion.1), channel_id=1, source_target_pairs={{0,16},{8,24},{16,0},{24,8},{1,17},{9,25},{17,1},{25,9},{2,18},{10... | collective-permute-start | bytes 12296 | tf_op jit(solution)/shard_map/ppermute | solution.py:299
  254.9 0.6 collective-permute-start.11
  255.4 2.7 collective-permute-start.12
  258.1 0.1 collective-permute-done.10
  258.3 1.4 collective-permute-done.11
  259.7 3.1 %collective-permute-start.13 = (f32[8,128]{1,0:T(8,128)S(1)}, f32[8,128]{1,0:T(8,128)S(1)}, u32[]{:S(2)}, u32[]{:S(2)}) collective-permute-start(f32[8,128]{1,0:T(8,128)S(1)} %add_add_fusion), channel_id=1, source_target_pairs={{0,64},{32,96},{64,0},{96,32},{1,65},{33,97},{65,1},{97,33},{2,66}... | collective-permute-start | bytes 12296 | tf_op jit(solution)/shard_map/ppermute | solution.py:299
  262.8 0.6 collective-permute-start.14
  263.3 2.7 collective-permute-start.15
  266.0 1.6 collective-permute-done.14
  267.6 0.6 add_bitcast_fusion
  268.2 9.8 %finish.1 = (bf16[192,3072]{1,0:T(8,128)(2,1)}, f32[192,1024]{1,0:T(8,128)}, f32[192,32]{1,0:T(8,128)}) custom-call(bf16[16,192,256]{2,1,0:T(8,128)(2,1)} %all-to-all-done.1.r0_ref, bf16[16,192,256]{2,1,0:T(8,128)(2,1)} %copy-done.3, bf16[16,256,1024]{2,1,0:T(8,128)(2,1)} %bitcast.69, bf16[192,1024]{1,0:T(8,128)(2,1)} %bitcast.73, f32[1,1024]{1,0:T(1,128)} %bitcast.83, ...), custom_call_target="tpu_custom_call" | custom-call | flops 2000000000 | bytes 14000000 | tf_op jit(solution)/shard_map/finish/pallas_call | solution.py:258
  278.0 1.6 copy.25
  279.5 0.1 fusion.13
  279.7 1.6 bitcast_convert_fusion
  (44 shorter events, 0.3 us)
Async XLA Ops:
  7.2 3.3 %copy-start.7 = (bf16[256,1024]{1,0:T(8,128)(2,1)S(1)}, bf16[256,1024]{1,0:T(8,128)(2,1)}, u32[]{:S(2)}) copy-start(bf16[256,1024]{1,0:T(8,128)(2,1)} %param.11) | copy-start | bytes 1572868
  7.2 3.3 %copy-start.6 = (bf16[256,1024]{1,0:T(8,128)(2,1)S(1)}, bf16[256,1024]{1,0:T(8,128)(2,1)}, u32[]{:S(2)}) copy-start(bf16[256,1024]{1,0:T(8,128)(2,1)} %param.12) | copy-start | bytes 1572868
  7.2 112.9 %all-gather.3.cloned.1.call-start = ((), (), s32[]{:S(2)}) async-start(), calls=%async_computation.5 | async-start | bytes 6684672 | tf_op jit(solution)/shard_map/all_gather | solution.py:334
  10.4 257.8 %all-gather.5.cloned.1.call-start = ((), (), s32[]{:S(2)}) async-start(), calls=%async_computation.6 | async-start | bytes 9437184 | tf_op jit(solution)/shard_map/all_gather | solution.py:340
  10.5 2.8 copy-start.9
  18.8 8.3 %copy-start.2 = (bf16[4,2,64,1024]{3,2,1,0:T(8,128)(2,1)S(1)}, bf16[4,2,64,1024]{3,2,1,0:T(8,128)(2,1)}, u32[]{:S(2)}) copy-start(bf16[4,2,64,1024]{3,2,1,0:T(8,128)(2,1)} %pad_maximum_fusion) | copy-start | bytes 3145732
  18.8 107.1 %all-to-all-start = ((bf16[16,192,256]{2,1,0:T(8,128)(2,1)}), bf16[16,192,256]{2,1,0:T(8,128)(2,1)S(1)}, u32[]{:S(2)}, u32[]{:S(2)}) async-start(bf16[16,192,256]{2,1,0:T(8,128)(2,1)} %get-tuple-element.21), calls=%async_computation | async-start | bytes 3145728 | tf_op jit(solution)/shard_map/all_to_all | solution.py:348
  27.1 1.5 collective-permute-start
  28.6 97.2 %copy-start.4 = (bf16[256,1024]{1,0:T(8,128)(2,1)}, bf16[256,1024]{1,0:T(8,128)(2,1)S(1)}, u32[]{:S(2)}) copy-start(bf16[256,1024]{1,0:T(8,128)(2,1)S(1)} %collective-permute-done) | copy-start | bytes 1572868
  125.8 36.1 %all-to-all-start.2 = ((bf16[16,192,128]{2,1,0:T(8,128)(2,1)}), bf16[16,192,128]{2,1,0:T(8,128)(2,1)S(1)}, u32[]{:S(2)}, u32[]{:S(2)}) async-start(bf16[16,192,128]{2,1,0:T(8,128)(2,1)} %get-tuple-element.23), calls=%async_computation.2 | async-start | bytes 1572864 | tf_op jit(solution)/shard_map/all_to_all | solution.py:351
  132.4 1.6 copy-start
  161.9 39.5 %all-to-all-start.1 = ((bf16[16,192,256]{2,1,0:T(8,128)(2,1)}), bf16[16,192,256]{2,1,0:T(8,128)(2,1)}, u32[]{:S(2)}, u32[]{:S(2)}) async-start(bf16[16,192,256]{2,1,0:T(8,128)(2,1)} %bitcast.12), calls=%async_computation.1 | async-start | bytes 3145728 | tf_op jit(solution)/shard_map/all_to_all | solution.py:356
  169.2 4.3 %copy-start.1 = (bf16[3072,256]{1,0:T(8,128)(2,1)S(1)}, bf16[3072,256]{1,0:T(8,128)(2,1)}, u32[]{:S(2)}) copy-start(bf16[3072,256]{1,0:T(8,128)(2,1)} %convolution_convert_fusion.kv_ref) | copy-start | bytes 4718596
  201.5 29.8 %all-to-all-start.3 = ((bf16[16,192,256]{2,1,0:T(8,128)(2,1)}), bf16[16,192,256]{2,1,0:T(8,128)(2,1)S(1)}, u32[]{:S(2)}, u32[]{:S(2)}) async-start(bf16[16,192,256]{2,1,0:T(8,128)(2,1)} %bitcast.14), calls=%async_computation.3 | async-start | bytes 3145728 | tf_op jit(solution)/shard_map/all_to_all | solution.py:359
  213.5 1.7 collective-permute-start.1
  213.6 8.3 %copy-start.5 = (bf16[256,1024]{1,0:T(8,128)(2,1)S(1)}, bf16[256,1024]{1,0:T(8,128)(2,1)}, u32[]{:S(2)}) copy-start(bf16[256,1024]{1,0:T(8,128)(2,1)} %copy-done.4) | copy-start | bytes 1572868
  213.6 11.2 %copy-start.8 = (f32[1024]{0:T(1024)S(1)}, f32[1024]{0:T(1024)}, u32[]{:S(2)}) copy-start(f32[1024]{0:T(1024)} %param.10) | copy-start | bytes 12292
  215.4 6.6 %collective-permute-start.2 = (bf16[32,1024]{1,0:T(8,128)(2,1)S(1)}, bf16[32,1024]{1,0:T(8,128)(2,1)S(1)}, u32[]{:S(2)}, u32[]{:S(2)}) collective-permute-start(bf16[32,1024]{1,0:T(8,128)(2,1)S(1)} %get-tuple-element.48), channel_id=1, source_target_pairs={{0,2},{2,4},{4,6},{6,0},{1,3},{3,5},{5,7},{7,1},{8,10},{10,12},{12... | collective-permute-start | bytes 196616 | tf_op jit(solution)/shard_map/ppermute | solution.py:299
  216.4 6.9 %collective-permute-start.3 = (bf16[32,1024]{1,0:T(8,128)(2,1)S(1)}, bf16[32,1024]{1,0:T(8,128)(2,1)S(1)}, u32[]{:S(2)}, u32[]{:S(2)}) collective-permute-start(bf16[32,1024]{1,0:T(8,128)(2,1)S(1)} %get-tuple-element.50), channel_id=1, source_target_pairs={{0,4},{2,6},{4,0},{6,2},{1,5},{3,7},{5,1},{7,3},{8,12},{10,14},{12... | collective-permute-start | bytes 196616 | tf_op jit(solution)/shard_map/ppermute | solution.py:299
  219.7 4.3 %collective-permute-start.4 = (bf16[32,1024]{1,0:T(8,128)(2,1)S(1)}, bf16[32,1024]{1,0:T(8,128)(2,1)S(1)}, u32[]{:S(2)}, u32[]{:S(2)}) collective-permute-start(bf16[32,1024]{1,0:T(8,128)(2,1)S(1)} %get-tuple-element.49), channel_id=1, source_target_pairs={{0,6},{2,0},{4,2},{6,4},{1,7},{3,1},{5,3},{7,5},{8,14},{10,8},{12,... | collective-permute-start | bytes 196616 | tf_op jit(solution)/shard_map/ppermute | solution.py:299
  224.0 4.1 %collective-permute-start.5 = (bf16[32,1024]{1,0:T(8,128)(2,1)S(1)}, bf16[32,1024]{1,0:T(8,128)(2,1)S(1)}, u32[]{:S(2)}, u32[]{:S(2)}) collective-permute-start(bf16[32,1024]{1,0:T(8,128)(2,1)S(1)} %fusion.10), channel_id=1, source_target_pairs={{0,0},{16,1},{32,2},{48,3},{64,4},{80,5},{96,6},{112,7},{1,8},{17,... | collective-permute-start | bytes 196616 | tf_op jit(solution)/shard_map/ppermute | solution.py:370
  224.7 19.7 %collective-permute-start.6 = (f32[8,128]{1,0:T(8,128)S(1)}, f32[8,128]{1,0:T(8,128)S(1)}, u32[]{:S(2)}, u32[]{:S(2)}) collective-permute-start(f32[8,128]{1,0:T(8,128)S(1)} %divide_bitcast_fusion), channel_id=1, source_target_pairs={{0,1},{1,0},{2,3},{3,2},{4,5},{5,4},{6,7},{7,6},{8,9},{9,8},{10,11... | collective-permute-start | bytes 12296 | tf_op jit(solution)/shard_map/ppermute | solution.py:306
  231.3 1.6 copy-start.3
  232.9 46.7 %all-to-all-start.4 = ((bf16[16,32,1024]{2,1,0:T(8,128)(2,1)}), bf16[16,32,1024]{2,1,0:T(8,128)(2,1)S(1)}, u32[]{:S(2)}, u32[]{:S(2)}) async-start(bf16[16,32,1024]{2,1,0:T(8,128)(2,1)} %broadcast_in_dim.27), calls=%async_computation.4 | async-start | bytes 2097152 | tf_op jit(solution)/shard_map/all_to_all | solution.py:295
  244.5 5.2 %collective-permute-start.7 = (f32[8,128]{1,0:T(8,128)S(1)}, f32[8,128]{1,0:T(8,128)S(1)}, u32[]{:S(2)}, u32[]{:S(2)}) collective-permute-start(f32[8,128]{1,0:T(8,128)S(1)} %fusion.18), channel_id=1, source_target_pairs={{0,4},{2,6},{4,0},{6,2},{1,5},{3,7},{5,1},{7,3},{8,12},{10,14},{12... | collective-permute-start | bytes 12296 | tf_op jit(solution)/shard_map/ppermute | solution.py:299
  245.6 4.8 %collective-permute-start.8 = (f32[8,128]{1,0:T(8,128)S(1)}, f32[8,128]{1,0:T(8,128)S(1)}, u32[]{:S(2)}, u32[]{:S(2)}) collective-permute-start(f32[8,128]{1,0:T(8,128)S(1)} %fusion.18), channel_id=1, source_target_pairs={{0,2},{2,4},{4,6},{6,0},{1,3},{3,5},{5,7},{7,1},{8,10},{10,12},{12... | collective-permute-start | bytes 12296 | tf_op jit(solution)/shard_map/ppermute | solution.py:299
  247.8 3.6 %collective-permute-start.9 = (f32[8,128]{1,0:T(8,128)S(1)}, f32[8,128]{1,0:T(8,128)S(1)}, u32[]{:S(2)}, u32[]{:S(2)}) collective-permute-start(f32[8,128]{1,0:T(8,128)S(1)} %fusion.18), channel_id=1, source_target_pairs={{0,6},{2,0},{4,2},{6,4},{1,7},{3,1},{5,3},{7,5},{8,14},{10,8},{12,... | collective-permute-start | bytes 12296 | tf_op jit(solution)/shard_map/ppermute | solution.py:299
  251.4 6.8 %collective-permute-start.10 = (f32[8,128]{1,0:T(8,128)S(1)}, f32[8,128]{1,0:T(8,128)S(1)}, u32[]{:S(2)}, u32[]{:S(2)}) collective-permute-start(f32[8,128]{1,0:T(8,128)S(1)} %add_add_fusion.1), channel_id=1, source_target_pairs={{0,16},{8,24},{16,0},{24,8},{1,17},{9,25},{17,1},{25,9},{2,18},{10... | collective-permute-start | bytes 12296 | tf_op jit(solution)/shard_map/ppermute | solution.py:299
  254.9 4.8 %collective-permute-start.11 = (f32[8,128]{1,0:T(8,128)S(1)}, f32[8,128]{1,0:T(8,128)S(1)}, u32[]{:S(2)}, u32[]{:S(2)}) collective-permute-start(f32[8,128]{1,0:T(8,128)S(1)} %add_add_fusion.1), channel_id=1, source_target_pairs={{0,8},{8,16},{16,24},{24,0},{1,9},{9,17},{17,25},{25,1},{2,10},{10... | collective-permute-start | bytes 12296 | tf_op jit(solution)/shard_map/ppermute | solution.py:299
  255.4 4.3 %collective-permute-start.12 = (f32[8,128]{1,0:T(8,128)S(1)}, f32[8,128]{1,0:T(8,128)S(1)}, u32[]{:S(2)}, u32[]{:S(2)}) collective-permute-start(f32[8,128]{1,0:T(8,128)S(1)} %add_add_fusion.1), channel_id=1, source_target_pairs={{0,24},{8,0},{16,8},{24,16},{1,25},{9,1},{17,9},{25,17},{2,26},{10... | collective-permute-start | bytes 12296 | tf_op jit(solution)/shard_map/ppermute | solution.py:299
  259.7 6.3 %collective-permute-start.13 = (f32[8,128]{1,0:T(8,128)S(1)}, f32[8,128]{1,0:T(8,128)S(1)}, u32[]{:S(2)}, u32[]{:S(2)}) collective-permute-start(f32[8,128]{1,0:T(8,128)S(1)} %add_add_fusion), channel_id=1, source_target_pairs={{0,64},{32,96},{64,0},{96,32},{1,65},{33,97},{65,1},{97,33},{2,66}... | collective-permute-start | bytes 12296 | tf_op jit(solution)/shard_map/ppermute | solution.py:299
  262.8 4.8 %collective-permute-start.14 = (f32[8,128]{1,0:T(8,128)S(1)}, f32[8,128]{1,0:T(8,128)S(1)}, u32[]{:S(2)}, u32[]{:S(2)}) collective-permute-start(f32[8,128]{1,0:T(8,128)S(1)} %add_add_fusion), channel_id=1, source_target_pairs={{0,32},{32,64},{64,96},{96,0},{1,33},{33,65},{65,97},{97,1},{2,34}... | collective-permute-start | bytes 12296 | tf_op jit(solution)/shard_map/ppermute | solution.py:299
  263.3 4.3 %collective-permute-start.15 = (f32[8,128]{1,0:T(8,128)S(1)}, f32[8,128]{1,0:T(8,128)S(1)}, u32[]{:S(2)}, u32[]{:S(2)}) collective-permute-start(f32[8,128]{1,0:T(8,128)S(1)} %add_add_fusion), channel_id=1, source_target_pairs={{0,96},{32,0},{64,32},{96,64},{1,97},{33,1},{65,33},{97,65},{2,98}... | collective-permute-start | bytes 12296 | tf_op jit(solution)/shard_map/ppermute | solution.py:299
Sparse Core Ops, SparseCore 0:
  10.7 109.2 all-gather.2
  122.3 51.1 all-gather.4

commit v3 on v2

--- a/solution.py
+++ b/solution.py
@@ -302,27 +302,28 @@
 SWAP = [(0, 1), (1, 0)]
 
 
-def sum_everywhere(value):
-    value = value + lax.ppermute(value, "dp_1", SWAP)
-    for axis in ("dp_0", "sp_1", "sp_0"):
-        others = [shifted(value, axis, k) for k in (1, 2, 3)]
-        value = (value + others[1]) + (others[0] + others[2])
-    return value
-
-
-def reduce_over_rows(pieces):
+def sum_of_four(value, axis):
+    others = [shifted(value, axis, k) for k in (1, 2, 3)]
+    return (value + others[1]) + (others[0] + others[2])
+
+
+def reduce_over_rows(pieces, small):
     across, core = lax.axis_index("dp_0"), lax.axis_index("dp_1")
     pairs = pieces.reshape(4, 2, *pieces.shape[1:])
     kept = lax.dynamic_index_in_dim(pairs, core, 1, keepdims=False)
     given = lax.dynamic_index_in_dim(pairs, 1 - core, 1, keepdims=False)
+    given, small = lax.optimization_barrier((given, small))
     given = lax.ppermute(given, "dp_1", SWAP)
+    small = small + lax.ppermute(small, "dp_1", SWAP)
     kept = kept.astype(f32) + given.astype(f32)
     total = lax.dynamic_index_in_dim(kept, across, 0, keepdims=False)
     kept = kept.astype(bf16)
+    kept, small = lax.optimization_barrier((kept, small))
     for k in (1, 2, 3):
         sent = lax.dynamic_index_in_dim(kept, (across + k) & 3, 0, keepdims=False)
         total = total + shifted(sent, "dp_0", k).astype(f32)
-    return total.astype(bf16)
+    small = sum_of_four(small, "dp_0")
+    return lax.optimization_barrier((total.astype(bf16), small))
 
 
 def program(query, latent, rope_key, gain, key_up, value_up, out_grad):
@@ -331,12 +332,11 @@
     lat = latent[0].astype(f32)
     inv_rms = lax.rsqrt(jnp.mean(lat * lat, axis=-1, keepdims=True) + eps)
     nlat = (lat * inv_rms * gain_row).astype(bf16)
-    nlat_all = lax.all_gather(nlat, SP, axis=0, tiled=True)
-
     rows = jnp.stack([key_up.reshape(4, 64, LATENT), value_up.reshape(4, 64, LATENT)], axis=1)
     rows = rows.reshape(512, LATENT)
     mine = lax.dynamic_slice_in_dim(rows, (place // 8) * 256, 256, axis=0)
     own = lax.ppermute(mine, ALL, to_heads())
+    nlat_all = lax.all_gather(nlat, SP, axis=0, tiled=True)
     whole = lax.all_gather(rows, DP, axis=0, tiled=True)
 
     positions = place * TOKENS + jnp.arange(TOKENS)
@@ -345,6 +345,7 @@
     sin_lanes = jnp.tile(jnp.concatenate([-sine, sine], axis=1), (1, 4))
     key = jnp.pad(rope_key[0].astype(f32), ((0, 0), (0, 96)))
     first, second = pack(query[0], out_grad[0], key, cos_lanes, sin_lanes)
+    first, nlat_all, own = lax.optimization_barrier((first, nlat_all, own))
     first = lax.all_to_all(first, SP, 0, 0, tiled=True).reshape(LENGTH, 256)
     kv = lax.dot_general(nlat_all, own, (((1,), (1,)), ((), ())), preferred_element_type=f32).astype(bf16)
     second, kv = lax.optimization_barrier((second, kv))
@@ -364,10 +365,12 @@
     ]
     part = jnp.concatenate(parts, axis=0)
     pieces = part.astype(bf16).reshape(2, 2, 4, 16, LATENT).transpose(0, 2, 1, 3, 4).reshape(NDP, 32, LATENT)
-    piece = reduce_over_rows(pieces)
-    gain_part = jnp.sum(part * own.astype(f32), axis=0) / gain
-    gain_grad = sum_everywhere(gain_part.reshape(8, 128)).reshape(LATENT)
+    gain_part = (jnp.sum(part * own.astype(f32), axis=0) / gain).reshape(8, 128)
+    piece, gain_part = reduce_over_rows(pieces, gain_part)
     piece = lax.ppermute(piece, ALL, to_rows())
+    gain_part = sum_of_four(gain_part, "sp_1")
+    piece, gain_part = lax.optimization_barrier((piece, gain_part))
+    gain_grad = sum_of_four(gain_part, "sp_0").reshape(LATENT)
     r1, piece = lax.optimization_barrier((r1, piece))
     grads = everyone(piece, SP, NSP).reshape(NSP, 2, 16, LATENT)
     key_grad = grads[:, 0].reshape(256, LATENT).astype(f32)

time: 289 us -> 295 us (1.021)
  waiting for transfers between devices: 104 us -> 116 us
  starting transfers between devices: 69.3 us -> 62 us
    all_to_all x1, waiting for transfers between devices: 0.01 us -> 17.7 us  [program(): first = lax.all_to_all(first, SP, 0, 0, tiled=True).reshape(LENGTH, 256)]
    all_gather x1, waiting for transfers between devices: 91.4 us -> 87 us  [program(): nlat_all = lax.all_gather(nlat, SP, axis=0, tiled=True)]
    all_to_all x1, waiting for transfers between devices: 3.22 us -> 0.01 us  [program(): r1 = lax.all_to_all(g1.reshape(NSP, TOKENS, 256), SP, 0, 0, tiled=True)]
    all_to_all x1, starting transfers between devices: 8.29 us -> 5.29 us  [program(): first = lax.all_to_all(first, SP, 0, 0, tiled=True).reshape(LENGTH, 256)]
    all_to_all x1, starting transfers between devices: 6.57 us -> 3.62 us  [program(): second = lax.all_to_all(second, SP, 0, 0, tiled=True).reshape(LENGTH, 128)]
  transfers between devices with their start and end apart: 23 -> 23, of which waited for: 11 -> 9; matrix products, arithmetic and copies ran while one was open for 8% -> 8% of each run, Pallas kernels for 24% -> 24%
where the time goes in v3:
time: 295 us; the launch traced here: 293 us
  waiting for transfers between devices  116 us (39%)
  Pallas kernels  70.4 us (24%)
  starting transfers between devices  62 us (21%)
  between operations  14.4 us (5%)
  matrix products  14 us (5%)
  other arithmetic  8.41 us (3%)
  local copies, waits for them, and re-layouts  8.01 us (3%)
    all_gather x1, waiting for transfers between devices, program(): nlat_all = lax.all_gather(nlat, SP, axis=0, tiled=True)  87 us
    pallas_call x2, Pallas kernels, attend(): pl.pallas_call(functools.partial(attend_body, head), grid=(1,), in_specs=...  55.9 us
    ppermute x12, starting transfers between devices, shifted(): return lax.ppermute(value, axis, [(i, (i + k) % 4) for i in range(4)])  22.9 us
    all_to_all x1, waiting for transfers between devices, program(): first = lax.all_to_all(first, SP, 0, 0, tiled=True).reshape(LENGTH, 256)  17.7 us
    all_to_all x1, starting transfers between devices, everyone(): lax.all_to_all(jnp.broadcast_to(value[None], (size, *value.shape)), axes,...  13.8 us
    ppermute x12, waiting for transfers between devices, shifted(): return lax.ppermute(value, axis, [(i, (i + k) % 4) for i in range(4)])  10.2 us
    pallas_call x1, Pallas kernels, finish(): pl.pallas_call(finish_body, grid=(half,), in_specs=[pl.BlockSpec((2, TOKE...  9.79 us
    dot_general x2, matrix products, program(): lax.dot_general(g[:, 0:128], nlat_all, (((0,), (0,)), ((), ())), preferre...  8.24 us
  transfers between devices with their start and end apart: 23, of which 9 were waited for; matrix products, arithmetic and copies ran while one was open for 8% of the time, Pallas kernels for 24%

profile of v3, /device:TPU:0, one launch (start us, length us, event | category | flops | bytes accessed | tf_op | source)
XLA Modules:
  0.0 293.3 jit_solution(13127206020632564659)
XLA Ops:
  7.2 0.0 all-gather.3.cloned.1.call-start
  7.2 1.2 fusion.1
  8.5 1.9 fusion.3
  10.4 0.0 all-gather.3.cloned.1.call-update
  10.4 0.0 all-gather.5.cloned.1.call-start
  10.5 1.1 pad_maximum_fusion
  11.6 0.0 all-gather.5.cloned.1.call-update
  11.6 1.1 constant_dynamic-slice_fusion
  12.7 0.7 collective-permute-start
  13.4 0.1 fusion.11
  13.6 0.7 copy.19.sin_ref
  14.3 0.7 copy.18.cos_ref
  15.1 0.1 copy.17
  15.2 0.7 pad_convert_fusion.kr_ref
  15.9 4.7 %pack.1 = (bf16[16,192,256]{2,1,0:T(8,128)(2,1)}, bf16[16,192,128]{2,1,0:T(8,128)(2,1)}) custom-call(bf16[192,3072]{1,0:T(8,128)(2,1)} %bitcast.82, bf16[192,2048]{1,0:T(8,128)(2,1)} %bitcast.84, f32[192,128]{1,0:T(8,128)} %pad_convert_fusion.kr_ref, f32[192,128]{1,0:T(8,128)} %copy.18.cos_ref, f32[192,128]{1,0:T(8,128)} %copy.19.sin_ref), custom_call_target="tpu_custom_call" | custom-call | flops 2000000000 | bytes 5000000 | tf_op jit(solution)/shard_map/pack/pallas_call | solution.py:79
  20.5 87.0 %all-gather.3.cloned.1.call-done = bf16[3072,1024]{1,0:T(8,128)(2,1)} async-done(((bf16[192,1024]{1,0:T(8,128)(2,1)}), bf16[3072,1024]{1,0:T(8,128)(2,1)}) %all-gather.3.cloned.1.call-update) | async-done | bytes 6291472 | tf_op jit(solution)/shard_map/all_gather | solution.py:339
  107.6 5.3 %all-to-all-start = ((bf16[16,192,256]{2,1,0:T(8,128)(2,1)}), bf16[16,192,256]{2,1,0:T(8,128)(2,1)S(1)}, u32[]{:S(2)}, u32[]{:S(2)}) async-start(bf16[16,192,256]{2,1,0:T(8,128)(2,1)} %get-tuple-element.35), calls=%async_computation | async-start | bytes 3145728 | tf_op jit(solution)/shard_map/all_to_all | solution.py:349
  112.9 0.8 multiply_sine_fusion
  113.7 0.0 copy-done.3
  113.7 5.8 %convolution_convert_fusion.kv_ref = bf16[3072,256]{1,0:T(8,128)(2,1)} fusion(bf16[3072,1024]{1,0:T(8,128)(2,1)} %all-gather.3.cloned.1.call-done, bf16[256,1024]{1,0:T(8,128)(2,1)S(1)} %collective-permute-done), kind=kOutput, calls=%fused_computation | convolution fusion | flops 1611399168 | bytes 8388608 | tf_op jit(solution)/shard_map/dot_general | solution.py:350
  119.5 17.7 %all-to-all-done = bf16[16,192,256]{2,1,0:T(8,128)(2,1)S(1)} async-done(((bf16[16,192,256]{2,1,0:T(8,128)(2,1)}), bf16[16,192,256]{2,1,0:T(8,128)(2,1)S(1)}, u32[]{:S(2)}, u32[]{:S(2)}) %all-to-all-start) | async-done | bytes 1572896 | tf_op jit(solution)/shard_map/all_to_all | solution.py:349
  137.1 3.6 %all-to-all-start.2 = ((bf16[16,192,128]{2,1,0:T(8,128)(2,1)}), bf16[16,192,128]{2,1,0:T(8,128)(2,1)S(1)}, u32[]{:S(2)}, u32[]{:S(2)}) async-start(bf16[16,192,128]{2,1,0:T(8,128)(2,1)} %get-tuple-element.37), calls=%async_computation.2 | async-start | bytes 1572864 | tf_op jit(solution)/shard_map/all_to_all | solution.py:352
  140.8 1.5 copy-done
  142.2 27.9 %shard_map.118 = bf16[3072,256]{1,0:T(8,128)(2,1)} custom-call(bf16[3072,256]{1,0:T(8,128)(2,1)S(1)} %bitcast.63, bf16[3072,256]{1,0:T(8,128)(2,1)S(1)} %bitcast.64, bf16[3072,256]{1,0:T(8,128)(2,1)S(1)} %copy-done, f32[16,3072]{1,0:T(8,128)S(1)} %get-tuple-element.74.cos_ref, f32[16,3072]{1,0:T(8,128)S(1)} %get-tuple-element.73.sin_ref), custom_call_target="tpu_custom_call" | custom-call | flops 12000000000 | bytes 6000000 | tf_op jit(solution)/shard_map/pallas_call | solution.py:192
  170.2 7.2 %all-to-all-start.1 = ((bf16[16,192,256]{2,1,0:T(8,128)(2,1)}), bf16[16,192,256]{2,1,0:T(8,128)(2,1)}, u32[]{:S(2)}, u32[]{:S(2)}) async-start(bf16[16,192,256]{2,1,0:T(8,128)(2,1)} %bitcast.12), calls=%async_computation.1 | async-start | bytes 3145728 | tf_op jit(solution)/shard_map/all_to_all | solution.py:357
  177.4 4.1 %fusion.6 = f32[128,1024]{1,0:T(8,128)S(1)} fusion(bf16[3072,1024]{1,0:T(8,128)(2,1)} %all-gather.3.cloned.1.call-done, bf16[3072,256]{1,0:T(8,128)(2,1)} %shard_map.118), kind=kOutput, calls=%fused_computation.12 | convolution fusion | flops 805306368 | bytes 7602176 | tf_op jit(solution)/shard_map/dot_general | solution.py:363
  181.6 28.0 %shard_map.119 = bf16[3072,256]{1,0:T(8,128)(2,1)} custom-call(bf16[3072,128]{1,0:T(8,128)(2,1)S(1)} %bitcast.66, bf16[3072,256]{1,0:T(8,128)(2,1)S(1)} %bitcast.65, bf16[3072,256]{1,0:T(8,128)(2,1)S(1)} %copy-done.1, f32[16,3072]{1,0:T(8,128)S(1)} %get-tuple-element.74.cos_ref, f32[16,3072]{1,0:T(8,128)S(1)} %get-tuple-element.73.sin_ref), custom_call_target="tpu_custom_call" | custom-call | flops 12000000000 | bytes 6000000 | tf_op jit(solution)/shard_map/pallas_call | solution.py:192
  209.6 7.2 %all-to-all-start.3 = ((bf16[16,192,256]{2,1,0:T(8,128)(2,1)}), bf16[16,192,256]{2,1,0:T(8,128)(2,1)S(1)}, u32[]{:S(2)}, u32[]{:S(2)}) async-start(bf16[16,192,256]{2,1,0:T(8,128)(2,1)} %bitcast.14), calls=%async_computation.3 | async-start | bytes 3145728 | tf_op jit(solution)/shard_map/all_to_all | solution.py:360
  216.8 0.0 copy-start.4
  216.8 4.1 %fusion.4 = f32[128,1024]{1,0:T(8,128)S(1)} fusion(bf16[3072,1024]{1,0:T(8,128)(2,1)} %all-gather.3.cloned.1.call-done, bf16[3072,256]{1,0:T(8,128)(2,1)} %shard_map.119), kind=kOutput, calls=%fused_computation.10 | convolution fusion | flops 805306368 | bytes 7602176 | tf_op jit(solution)/shard_map/dot_general | solution.py:363
  220.9 0.2 multiply_reduce_fusion
  221.1 0.5 copy-done.7
  221.6 0.1 fusion
  221.8 0.1 collective-permute-start.1
  221.9 0.5 collective-permute-start.2
  222.4 1.0 collective-permute-done.2
  223.4 0.1 fusion.12
  223.5 3.0 %collective-permute-start.6 = (f32[8,128]{1,0:T(8,128)S(1)}, f32[8,128]{1,0:T(8,128)S(1)}, u32[]{:S(2)}, u32[]{:S(2)}) collective-permute-start(f32[8,128]{1,0:T(8,128)S(1)} %add.113), channel_id=1, source_target_pairs={{0,4},{2,6},{4,0},{6,2},{1,5},{3,7},{5,1},{7,3},{8,12},{10,14},{12... | collective-permute-start | bytes 12296 | tf_op jit(solution)/shard_map/ppermute | solution.py:299
  226.5 0.5 collective-permute-start.7
  227.0 2.7 collective-permute-start.8
  229.7 0.1 collective-permute-start.3
  229.8 1.5 collective-permute-start.4
  231.3 1.8 collective-permute-start.5
  233.0 2.9 collective-permute-done.3
  236.0 0.9 collective-permute-done.5
  236.9 3.5 %collective-permute-start.10 = (f32[8,128]{1,0:T(8,128)S(1)}, f32[8,128]{1,0:T(8,128)S(1)}, u32[]{:S(2)}, u32[]{:S(2)}) collective-permute-start(f32[8,128]{1,0:T(8,128)S(1)} %add_add_fusion.1), channel_id=1, source_target_pairs={{0,16},{8,24},{16,0},{24,8},{1,17},{9,25},{17,1},{25,9},{2,18},{10... | collective-permute-start | bytes 12296 | tf_op jit(solution)/shard_map/ppermute | solution.py:299
  240.3 0.6 collective-permute-start.11
  240.9 2.7 collective-permute-start.12
  243.6 0.7 collective-permute-start.9
  244.3 0.9 collective-permute-done.11
  245.2 1.2 broadcast_in_dim.27
  246.4 0.3 copy-done.2
  246.7 13.8 %all-to-all-start.4 = ((bf16[16,32,1024]{2,1,0:T(8,128)(2,1)}), bf16[16,32,1024]{2,1,0:T(8,128)(2,1)S(1)}, u32[]{:S(2)}, u32[]{:S(2)}) async-start(bf16[16,32,1024]{2,1,0:T(8,128)(2,1)} %broadcast_in_dim.27), calls=%async_computation.4 | async-start | bytes 2097152 | tf_op jit(solution)/shard_map/all_to_all | solution.py:295
  260.5 3.4 %collective-permute-start.13 = (f32[8,128]{1,0:T(8,128)S(1)}, f32[8,128]{1,0:T(8,128)S(1)}, u32[]{:S(2)}, u32[]{:S(2)}) collective-permute-start(f32[8,128]{1,0:T(8,128)S(1)} %add_add_fusion), channel_id=1, source_target_pairs={{0,64},{32,96},{64,0},{96,32},{1,65},{33,97},{65,1},{97,33},{2,66}... | collective-permute-start | bytes 12296 | tf_op jit(solution)/shard_map/ppermute | solution.py:299
  264.0 0.6 collective-permute-start.14
  264.5 2.7 collective-permute-start.15
  267.2 3.1 %collective-permute-done.13 = f32[8,128]{1,0:T(8,128)S(1)} collective-permute-done((f32[8,128]{1,0:T(8,128)S(1)}, f32[8,128]{1,0:T(8,128)S(1)}, u32[]{:S(2)}, u32[]{:S(2)}) %collective-permute-start.13) | collective-permute-done | bytes 4128 | tf_op jit(solution)/shard_map/ppermute | solution.py:299
  270.3 1.6 collective-permute-done.14
  271.9 0.8 collective-permute-done.15
  272.7 0.6 add_bitcast_fusion
  273.3 9.8 %finish.1 = (bf16[192,3072]{1,0:T(8,128)(2,1)}, f32[192,1024]{1,0:T(8,128)}, f32[192,32]{1,0:T(8,128)}) custom-call(bf16[16,192,256]{2,1,0:T(8,128)(2,1)} %all-to-all-done.1.r0_ref, bf16[16,192,256]{2,1,0:T(8,128)(2,1)} %copy-done.2, bf16[16,256,1024]{2,1,0:T(8,128)(2,1)} %bitcast.67, bf16[192,1024]{1,0:T(8,128)(2,1)} %bitcast.71, f32[1,1024]{1,0:T(1,128)} %bitcast.81, ...), custom_call_target="tpu_custom_call" | custom-call | flops 2000000000 | bytes 14000000 | tf_op jit(solution)/shard_map/finish/pallas_call | solution.py:258
  283.1 1.6 copy.25
  284.7 0.1 fusion.13
  284.8 1.6 bitcast_convert_fusion
  (42 shorter events, 0.3 us)
Async XLA Ops:
  7.2 3.3 %copy-start.6 = (bf16[256,1024]{1,0:T(8,128)(2,1)S(1)}, bf16[256,1024]{1,0:T(8,128)(2,1)}, u32[]{:S(2)}) copy-start(bf16[256,1024]{1,0:T(8,128)(2,1)} %param.11) | copy-start | bytes 1572868
  7.2 3.3 %copy-start.5 = (bf16[256,1024]{1,0:T(8,128)(2,1)S(1)}, bf16[256,1024]{1,0:T(8,128)(2,1)}, u32[]{:S(2)}) copy-start(bf16[256,1024]{1,0:T(8,128)(2,1)} %param.12) | copy-start | bytes 1572868
  7.2 100.4 %all-gather.3.cloned.1.call-start = ((), (), s32[]{:S(2)}) async-start(), calls=%async_computation.5 | async-start | bytes 6684672 | tf_op jit(solution)/shard_map/all_gather | solution.py:339
  10.4 262.9 %all-gather.5.cloned.1.call-start = ((), (), s32[]{:S(2)}) async-start(), calls=%async_computation.6 | async-start | bytes 9437184 | tf_op jit(solution)/shard_map/all_gather | solution.py:340
  11.6 3.5 %copy-start.8 = (bf16[1,192,32]{1,2,0:T(8,128)(2,1)S(1)}, bf16[1,192,32]{1,2,0:T(8,128)(2,1)}, u32[]{:S(2)}) copy-start(bf16[1,192,32]{1,2,0:T(8,128)(2,1)} %param.9) | copy-start | bytes 36868
  12.7 7.9 %collective-permute-start = (bf16[256,1024]{1,0:T(8,128)(2,1)S(1)}, bf16[256,1024]{1,0:T(8,128)(2,1)S(1)}, u32[]{:S(2)}, u32[]{:S(2)}) collective-permute-start(bf16[256,1024]{1,0:T(8,128)(2,1)S(1)} %constant_dynamic-slice_fusion), channel_id=1, source_target_pairs={{0,0},{1,16},{2,32},{3,48},{4,64},{5,80},{6,96},{7,112},{8,1},{9,1... | collective-permute-start | bytes 1572872 | tf_op jit(solution)/shard_map/ppermute | solution.py:338
  20.5 93.1 %copy-start.3 = (bf16[256,1024]{1,0:T(8,128)(2,1)}, bf16[256,1024]{1,0:T(8,128)(2,1)S(1)}, u32[]{:S(2)}) copy-start(bf16[256,1024]{1,0:T(8,128)(2,1)S(1)} %collective-permute-done) | copy-start | bytes 1572868
  107.6 29.6 %all-to-all-start = ((bf16[16,192,256]{2,1,0:T(8,128)(2,1)}), bf16[16,192,256]{2,1,0:T(8,128)(2,1)S(1)}, u32[]{:S(2)}, u32[]{:S(2)}) async-start(bf16[16,192,256]{2,1,0:T(8,128)(2,1)} %get-tuple-element.35), calls=%async_computation | async-start | bytes 3145728 | tf_op jit(solution)/shard_map/all_to_all | solution.py:349
  137.1 33.0 %all-to-all-start.2 = ((bf16[16,192,128]{2,1,0:T(8,128)(2,1)}), bf16[16,192,128]{2,1,0:T(8,128)(2,1)S(1)}, u32[]{:S(2)}, u32[]{:S(2)}) async-start(bf16[16,192,128]{2,1,0:T(8,128)(2,1)} %get-tuple-element.37), calls=%async_computation.2 | async-start | bytes 1572864 | tf_op jit(solution)/shard_map/all_to_all | solution.py:352
  140.8 1.5 copy-start
  170.2 39.4 %all-to-all-start.1 = ((bf16[16,192,256]{2,1,0:T(8,128)(2,1)}), bf16[16,192,256]{2,1,0:T(8,128)(2,1)}, u32[]{:S(2)}, u32[]{:S(2)}) async-start(bf16[16,192,256]{2,1,0:T(8,128)(2,1)} %bitcast.12), calls=%async_computation.1 | async-start | bytes 3145728 | tf_op jit(solution)/shard_map/all_to_all | solution.py:357
  177.4 4.2 %copy-start.1 = (bf16[3072,256]{1,0:T(8,128)(2,1)S(1)}, bf16[3072,256]{1,0:T(8,128)(2,1)}, u32[]{:S(2)}) copy-start(bf16[3072,256]{1,0:T(8,128)(2,1)} %convolution_convert_fusion.kv_ref) | copy-start | bytes 4718596
  209.6 35.6 %all-to-all-start.3 = ((bf16[16,192,256]{2,1,0:T(8,128)(2,1)}), bf16[16,192,256]{2,1,0:T(8,128)(2,1)S(1)}, u32[]{:S(2)}, u32[]{:S(2)}) async-start(bf16[16,192,256]{2,1,0:T(8,128)(2,1)} %bitcast.14), calls=%async_computation.3 | async-start | bytes 3145728 | tf_op jit(solution)/shard_map/all_to_all | solution.py:360
  216.8 4.1 %copy-start.4 = (bf16[256,1024]{1,0:T(8,128)(2,1)S(1)}, bf16[256,1024]{1,0:T(8,128)(2,1)}, u32[]{:S(2)}) copy-start(bf16[256,1024]{1,0:T(8,128)(2,1)} %copy-done.3) | copy-start | bytes 1572868
  220.9 0.7 copy-start.7
  221.8 1.6 collective-permute-start.1
  221.9 1.5 collective-permute-start.2
  223.5 7.8 %collective-permute-start.6 = (f32[8,128]{1,0:T(8,128)S(1)}, f32[8,128]{1,0:T(8,128)S(1)}, u32[]{:S(2)}, u32[]{:S(2)}) collective-permute-start(f32[8,128]{1,0:T(8,128)S(1)} %add.113), channel_id=1, source_target_pairs={{0,4},{2,6},{4,0},{6,2},{1,5},{3,7},{5,1},{7,3},{8,12},{10,14},{12... | collective-permute-start | bytes 12296 | tf_op jit(solution)/shard_map/ppermute | solution.py:299
  226.5 6.6 %collective-permute-start.7 = (f32[8,128]{1,0:T(8,128)S(1)}, f32[8,128]{1,0:T(8,128)S(1)}, u32[]{:S(2)}, u32[]{:S(2)}) collective-permute-start(f32[8,128]{1,0:T(8,128)S(1)} %add.113), channel_id=1, source_target_pairs={{0,2},{2,4},{4,6},{6,0},{1,3},{3,5},{5,7},{7,1},{8,10},{10,12},{12... | collective-permute-start | bytes 12296 | tf_op jit(solution)/shard_map/ppermute | solution.py:299
  227.0 6.0 %collective-permute-start.8 = (f32[8,128]{1,0:T(8,128)S(1)}, f32[8,128]{1,0:T(8,128)S(1)}, u32[]{:S(2)}, u32[]{:S(2)}) collective-permute-start(f32[8,128]{1,0:T(8,128)S(1)} %add.113), channel_id=1, source_target_pairs={{0,6},{2,0},{4,2},{6,4},{1,7},{3,1},{5,3},{7,5},{8,14},{10,8},{12,... | collective-permute-start | bytes 12296 | tf_op jit(solution)/shard_map/ppermute | solution.py:299
  229.7 6.2 %collective-permute-start.3 = (bf16[32,1024]{1,0:T(8,128)(2,1)S(1)}, bf16[32,1024]{1,0:T(8,128)(2,1)S(1)}, u32[]{:S(2)}, u32[]{:S(2)}) collective-permute-start(bf16[32,1024]{1,0:T(8,128)(2,1)S(1)} %get-tuple-element.70), channel_id=1, source_target_pairs={{0,2},{2,4},{4,6},{6,0},{1,3},{3,5},{5,7},{7,1},{8,10},{10,12},{12... | collective-permute-start | bytes 196616 | tf_op jit(solution)/shard_map/ppermute | solution.py:299
  229.8 6.2 %collective-permute-start.4 = (bf16[32,1024]{1,0:T(8,128)(2,1)S(1)}, bf16[32,1024]{1,0:T(8,128)(2,1)S(1)}, u32[]{:S(2)}, u32[]{:S(2)}) collective-permute-start(bf16[32,1024]{1,0:T(8,128)(2,1)S(1)} %get-tuple-element.72), channel_id=1, source_target_pairs={{0,4},{2,6},{4,0},{6,2},{1,5},{3,7},{5,1},{7,3},{8,12},{10,14},{12... | collective-permute-start | bytes 196616 | tf_op jit(solution)/shard_map/ppermute | solution.py:299
  231.3 5.6 %collective-permute-start.5 = (bf16[32,1024]{1,0:T(8,128)(2,1)S(1)}, bf16[32,1024]{1,0:T(8,128)(2,1)S(1)}, u32[]{:S(2)}, u32[]{:S(2)}) collective-permute-start(bf16[32,1024]{1,0:T(8,128)(2,1)S(1)} %get-tuple-element.71), channel_id=1, source_target_pairs={{0,6},{2,0},{4,2},{6,4},{1,7},{3,1},{5,3},{7,5},{8,14},{10,8},{12,... | collective-permute-start | bytes 196616 | tf_op jit(solution)/shard_map/ppermute | solution.py:299
  236.9 7.4 %collective-permute-start.10 = (f32[8,128]{1,0:T(8,128)S(1)}, f32[8,128]{1,0:T(8,128)S(1)}, u32[]{:S(2)}, u32[]{:S(2)}) collective-permute-start(f32[8,128]{1,0:T(8,128)S(1)} %add_add_fusion.1), channel_id=1, source_target_pairs={{0,16},{8,24},{16,0},{24,8},{1,17},{9,25},{17,1},{25,9},{2,18},{10... | collective-permute-start | bytes 12296 | tf_op jit(solution)/shard_map/ppermute | solution.py:299
  240.3 4.8 %collective-permute-start.11 = (f32[8,128]{1,0:T(8,128)S(1)}, f32[8,128]{1,0:T(8,128)S(1)}, u32[]{:S(2)}, u32[]{:S(2)}) collective-permute-start(f32[8,128]{1,0:T(8,128)S(1)} %add_add_fusion.1), channel_id=1, source_target_pairs={{0,8},{8,16},{16,24},{24,0},{1,9},{9,17},{17,25},{25,1},{2,10},{10... | collective-permute-start | bytes 12296 | tf_op jit(solution)/shard_map/ppermute | solution.py:299
  240.9 4.2 %collective-permute-start.12 = (f32[8,128]{1,0:T(8,128)S(1)}, f32[8,128]{1,0:T(8,128)S(1)}, u32[]{:S(2)}, u32[]{:S(2)}) collective-permute-start(f32[8,128]{1,0:T(8,128)S(1)} %add_add_fusion.1), channel_id=1, source_target_pairs={{0,24},{8,0},{16,8},{24,16},{1,25},{9,1},{17,9},{25,17},{2,26},{10... | collective-permute-start | bytes 12296 | tf_op jit(solution)/shard_map/ppermute | solution.py:299
  243.6 1.6 collective-permute-start.9
  245.2 1.6 copy-start.2
  246.7 37.9 %all-to-all-start.4 = ((bf16[16,32,1024]{2,1,0:T(8,128)(2,1)}), bf16[16,32,1024]{2,1,0:T(8,128)(2,1)S(1)}, u32[]{:S(2)}, u32[]{:S(2)}) async-start(bf16[16,32,1024]{2,1,0:T(8,128)(2,1)} %broadcast_in_dim.27), calls=%async_computation.4 | async-start | bytes 2097152 | tf_op jit(solution)/shard_map/all_to_all | solution.py:295
  260.5 9.8 %collective-permute-start.13 = (f32[8,128]{1,0:T(8,128)S(1)}, f32[8,128]{1,0:T(8,128)S(1)}, u32[]{:S(2)}, u32[]{:S(2)}) collective-permute-start(f32[8,128]{1,0:T(8,128)S(1)} %add_add_fusion), channel_id=1, source_target_pairs={{0,64},{32,96},{64,0},{96,32},{1,65},{33,97},{65,1},{97,33},{2,66}... | collective-permute-start | bytes 12296 | tf_op jit(solution)/shard_map/ppermute | solution.py:299
  264.0 7.9 %collective-permute-start.14 = (f32[8,128]{1,0:T(8,128)S(1)}, f32[8,128]{1,0:T(8,128)S(1)}, u32[]{:S(2)}, u32[]{:S(2)}) collective-permute-start(f32[8,128]{1,0:T(8,128)S(1)} %add_add_fusion), channel_id=1, source_target_pairs={{0,32},{32,64},{64,96},{96,0},{1,33},{33,65},{65,97},{97,1},{2,34}... | collective-permute-start | bytes 12296 | tf_op jit(solution)/shard_map/ppermute | solution.py:299
  264.5 8.2 %collective-permute-start.15 = (f32[8,128]{1,0:T(8,128)S(1)}, f32[8,128]{1,0:T(8,128)S(1)}, u32[]{:S(2)}, u32[]{:S(2)}) collective-permute-start(f32[8,128]{1,0:T(8,128)S(1)} %add_add_fusion), channel_id=1, source_target_pairs={{0,96},{32,0},{64,32},{96,64},{1,97},{33,1},{65,33},{97,65},{2,98}... | collective-permute-start | bytes 12296 | tf_op jit(solution)/shard_map/ppermute | solution.py:299
Sparse Core Ops, SparseCore 0:
  10.7 96.8 all-gather.2
  109.9 49.1 all-gather.4

commit v4 on v3

--- a/solution.py
+++ b/solution.py
@@ -216,71 +216,90 @@
     )(arrived, turned, kv, cosine, sine)
 
 
-def finish_body(r0_ref, r1_ref, w_ref, lat_ref, gain_ref, cos_ref, sin_ref, dq_ref, dlat_ref, drope_ref, acc, rope):
-    step = pl.program_id(0)
+def project_body(order_ref, nlat_ref, *refs):
+    weights, rest = refs[:NDP], refs[NDP:]
+    nlat = nlat_ref[...]
+    if len(rest) == 2:
+        rest[1][:, :, 0:128] = rest[0][...]
+    out_ref = rest[-1]
+    base = out_ref.shape[2] - 128
+    for step in range(NDP):
+        made = lax.dot_general(nlat, weights[step][...], (((1,), (1,)), ((), ())), preferred_element_type=f32)
+        slot = 2 * order_ref[step]
+        out_ref[slot, :, base : base + 128] = made[:, 0:128].astype(bf16)
+        out_ref[slot + 1, :, base : base + 128] = made[:, 128:256].astype(bf16)
+
+
+def project(order, nlat, weights, extra):
+    extras = [] if extra is None else [extra]
+    memory = pl.BlockSpec(memory_space=pltpu.VMEM)
+    return pl.pallas_call(
+        project_body,
+        in_specs=[pl.BlockSpec(memory_space=pltpu.SMEM)] + [memory] * (1 + NDP + len(extras)),
+        out_specs=memory,
+        out_shape=jax.ShapeDtypeStruct((NSP, TOKENS, 128 * (1 + len(extras))), bf16),
+        cost_estimate=pl.CostEstimate(flops=2_000_000_000, bytes_accessed=6_000_000, transcendentals=0),
+        name="project",
+    )(order, nlat, *weights, *extras)
+
+
+def finish_body(order_ref, r0_ref, r1_ref, lat_ref, gain_ref, cos_ref, sin_ref, *refs):
+    evens, odds = refs[:NDP], refs[NDP : 2 * NDP]
+    dq_ref, dlat_ref, drope_ref, acc = refs[2 * NDP :]
     lane = lanes_of((TOKENS, 128))
-
-    @pl.when(step == 0)
-    def _():
-        acc[...] = jnp.zeros_like(acc)
-        rope[...] = jnp.zeros_like(rope)
-
-    tiles = []
-    for half in range(2):
-        r0 = r0_ref[half]
-        r1 = r1_ref[half]
-        both = jnp.concatenate([r0[:, 0:128], r1[:, 0:128]], axis=1)
-        acc[...] += jnp.dot(both, w_ref[half], preferred_element_type=f32)
-        t0 = r0[:, 128:256].astype(f32)
-        t1 = r1[:, 128:256].astype(f32)
-        rope[...] += jnp.where(lane < ROPE, t0, jnp.where(lane >= 96, t1, 0.0))
-        tiles.append((t0, t1))
-    (x0, x1), (y0, y1) = tiles
-    dq_ref[:, 0:128] = jnp.where(lane < 96, pltpu.roll(x0, 96, 1), pltpu.roll(x1, 96, 1)).astype(bf16)
-    dq_ref[:, 128:256] = jnp.where(lane < 64, pltpu.roll(x1, 96, 1), pltpu.roll(y0, 32, 1)).astype(bf16)
-    dq_ref[:, 256:384] = jnp.where(lane < 32, pltpu.roll(y0, 32, 1), pltpu.roll(y1, 32, 1)).astype(bf16)
-
-    @pl.when(step == NSP // 2 - 1)
-    def _():
-        lat = lat_ref[...].astype(f32)
-        inv_rms = lax.rsqrt(jnp.mean(lat * lat, axis=-1, keepdims=True) + eps)
-        normed = lat * inv_rms
-        scaled = acc[...] * gain_ref[...]
-        dlat_ref[...] = inv_rms * (scaled - normed * jnp.mean(scaled * normed, axis=-1, keepdims=True))
-        x = rope[...]
-        x = x + pltpu.roll(x, 32, 1)
-        swapped = jnp.where(lane < HALF, pltpu.roll(x, 128 - HALF, 1), pltpu.roll(x, HALF, 1))
-        drope_ref[...] = (x * cos_ref[...] - swapped * sin_ref[...])[:, 0:ROPE]
-
-
-def finish(r0, r1, weights, latent, gain, cosine, sine):
-    half = NSP // 2
+    rope = jnp.zeros((TOKENS, 128), f32)
+    for step in range(NDP):
+        slot = 2 * order_ref[step]
+        tiles = []
+        for half in range(2):
+            r0 = r0_ref[slot + half]
+            r1 = r1_ref[slot + half]
+            rows = slice(128 * half, 128 * half + 128)
+            both = jnp.concatenate([r0[:, 0:128], r1[:, 0:128]], axis=1)
+            weights = jnp.concatenate([evens[step][rows, :], odds[step][rows, :]], axis=0)
+            added = jnp.dot(both, weights, preferred_element_type=f32)
+            if step == 0 and half == 0:
+                acc[...] = added
+            else:
+                acc[...] += added
+            t0 = r0[:, 128:256].astype(f32)
+            t1 = r1[:, 128:256].astype(f32)
+            rope = rope + jnp.where(lane < ROPE, t0, jnp.where(lane >= 96, t1, 0.0))
+            tiles.append((t0, t1))
+        (x0, x1), (y0, y1) = tiles
+        dq = [
+            jnp.where(lane < 96, pltpu.roll(x0, 96, 1), pltpu.roll(x1, 96, 1)),
+            jnp.where(lane < 64, pltpu.roll(x1, 96, 1), pltpu.roll(y0, 32, 1)),
+            jnp.where(lane < 32, pltpu.roll(y0, 32, 1), pltpu.roll(y1, 32, 1)),
+        ]
+        start = pl.multiple_of(384 * order_ref[step], 128)
+        dq_ref[:, pl.ds(start, 384)] = jnp.concatenate(dq, axis=1).astype(bf16)
+
+    lat = lat_ref[...].astype(f32)
+    inv_rms = lax.rsqrt(jnp.mean(lat * lat, axis=-1, keepdims=True) + eps)
+    normed = lat * inv_rms
+    scaled = acc[...] * gain_ref[...]
+    dlat_ref[...] = inv_rms * (scaled - normed * jnp.mean(scaled * normed, axis=-1, keepdims=True))
+    x = rope + pltpu.roll(rope, 32, 1)
+    swapped = jnp.where(lane < HALF, pltpu.roll(x, 128 - HALF, 1), pltpu.roll(x, HALF, 1))
+    drope_ref[...] = (x * cos_ref[...] - swapped * sin_ref[...])[:, 0:ROPE]
+
+
+def finish(order, r0, r1, latent, gain, cosine, sine, evens, odds):
+    memory = pl.BlockSpec(memory_space=pltpu.VMEM)
     return pl.pallas_call(
         finish_body,
-        grid=(half,),
-        in_specs=[
-            pl.BlockSpec((2, TOKENS, 256), lambda g: (g, 0, 0)),
-            pl.BlockSpec((2, TOKENS, 256), lambda g: (g, 0, 0)),
-            pl.BlockSpec((2, 256, LATENT), lambda g: (g, 0, 0)),
-            pl.BlockSpec((TOKENS, LATENT), lambda g: (0, 0)),
-            pl.BlockSpec((1, LATENT), lambda g: (0, 0)),
-            pl.BlockSpec((TOKENS, 128), lambda g: (0, 0)),
-            pl.BlockSpec((TOKENS, 128), lambda g: (0, 0)),
-        ],
-        out_specs=[
-            pl.BlockSpec((TOKENS, 384), lambda g: (0, g)),
-            pl.BlockSpec((TOKENS, LATENT), lambda g: (0, 0)),
-            pl.BlockSpec((TOKENS, ROPE), lambda g: (0, 0)),
-        ],
+        in_specs=[pl.BlockSpec(memory_space=pltpu.SMEM)] + [memory] * (6 + 2 * NDP),
+        out_specs=[memory] * 3,
         out_shape=[
             jax.ShapeDtypeStruct((TOKENS, ATTENTION_HEADS * WIDTH), bf16),
             jax.ShapeDtypeStruct((TOKENS, LATENT), f32),
             jax.ShapeDtypeStruct((TOKENS, ROPE), f32),
         ],
-        scratch_shapes=[pltpu.VMEM((TOKENS, LATENT), f32), pltpu.VMEM((TOKENS, 128), f32)],
+        scratch_shapes=[pltpu.VMEM((TOKENS, LATENT), f32)],
         cost_estimate=pl.CostEstimate(flops=2_000_000_000, bytes_accessed=14_000_000, transcendentals=0),
         name="finish",
-    )(r0, r1, weights, latent, gain, cosine, sine)
+    )(order, r0, r1, latent, gain, cosine, sine, *evens, *odds)
 
 
 def to_heads():
@@ -300,6 +319,11 @@
 
 
 SWAP = [(0, 1), (1, 0)]
+
+
+def all_shards(rows):
+    near = [rows] + [shifted(rows, "dp_0", k) for k in (1, 3, 2)]
+    return near + [lax.ppermute(piece, "dp_1", SWAP) for piece in near]
 
 
 def sum_of_four(value, axis):
@@ -334,10 +358,15 @@
     nlat = (lat * inv_rms * gain_row).astype(bf16)
     rows = jnp.stack([key_up.reshape(4, 64, LATENT), value_up.reshape(4, 64, LATENT)], axis=1)
     rows = rows.reshape(512, LATENT)
+    across, core = lax.axis_index("dp_0"), lax.axis_index("dp_1")
+    shards = ((across + jnp.array([0, -1, 1, 2], jnp.int32)) & 3) * 2
+    order = jnp.concatenate([shards + core, shards + 1 - core])
+    by_head = rows.reshape(2, 2, 128, LATENT)
+    evens = all_shards(by_head[:, 0].reshape(256, LATENT))
+    odds = all_shards(by_head[:, 1].reshape(256, LATENT))
+    nlat_all = lax.all_gather(nlat, SP, axis=0, tiled=True)
     mine = lax.dynamic_slice_in_dim(rows, (place // 8) * 256, 256, axis=0)
     own = lax.ppermute(mine, ALL, to_heads())
-    nlat_all = lax.all_gather(nlat, SP, axis=0, tiled=True)
-    whole = lax.all_gather(rows, DP, axis=0, tiled=True)
 
     positions = place * TOKENS + jnp.arange(TOKENS)
     cosine, sine = angles(positions)
@@ -345,17 +374,17 @@
     sin_lanes = jnp.tile(jnp.concatenate([-sine, sine], axis=1), (1, 4))
     key = jnp.pad(rope_key[0].astype(f32), ((0, 0), (0, 96)))
     first, second = pack(query[0], out_grad[0], key, cos_lanes, sin_lanes)
-    first, nlat_all, own = lax.optimization_barrier((first, nlat_all, own))
     first = lax.all_to_all(first, SP, 0, 0, tiled=True).reshape(LENGTH, 256)
-    kv = lax.dot_general(nlat_all, own, (((1,), (1,)), ((), ())), preferred_element_type=f32).astype(bf16)
-    second, kv = lax.optimization_barrier((second, kv))
-    second = lax.all_to_all(second, SP, 0, 0, tiled=True).reshape(LENGTH, 128)
+    kv0 = project(order, nlat, evens, None)
+    kv0 = lax.all_to_all(kv0, SP, 0, 0, tiled=True).reshape(LENGTH, 128)
+    second = project(order, nlat, odds, second)
+    second = lax.all_to_all(second, SP, 0, 0, tiled=True).reshape(LENGTH, 256)
     cos_all, sin_all = angles(jnp.arange(LENGTH))
     cos_all, sin_all = cos_all.T, sin_all.T
-    g0 = attend(0, first, first, kv, cos_all, sin_all)
-    kv, g0 = lax.optimization_barrier((kv, g0))
+    g0 = attend(0, first, first, kv0, cos_all, sin_all)
+    second, g0 = lax.optimization_barrier((second, g0))
     r0 = lax.all_to_all(g0.reshape(NSP, TOKENS, 256), SP, 0, 0, tiled=True)
-    g1 = attend(1, second, first, kv, cos_all, sin_all)
+    g1 = attend(1, second, first, second, cos_all, sin_all)
     r0, g1 = lax.optimization_barrier((r0, g1))
     r1 = lax.all_to_all(g1.reshape(NSP, TOKENS, 256), SP, 0, 0, tiled=True)
 
@@ -376,9 +405,7 @@
     key_grad = grads[:, 0].reshape(256, LATENT).astype(f32)
     value_grad = grads[:, 1].reshape(256, LATENT).astype(f32)
 
-    dq, dlat, drope = finish(
-        r0, r1, whole.reshape(NSP, 256, LATENT), latent[0], gain_row, cos_lanes, sin_lanes
-    )
+    dq, dlat, drope = finish(order, r0, r1, latent[0], gain_row, cos_lanes, sin_lanes, evens, odds)
     return dq[None], dlat[None], drope[None], key_grad, value_grad, gain_grad
 
 

time: 295 us -> 271 us (0.919)
  waiting for transfers between devices: 116 us -> 56.9 us
  starting transfers between devices: 62 us -> 95.1 us
  Pallas kernels: 70.4 us -> 78.6 us
  matrix products: 14 us -> 6.36 us
    all_gather x1, waiting for transfers between devices: 87 us -> 0.02 us  [program(): nlat_all = lax.all_gather(nlat, SP, axis=0, tiled=True)]
    ppermute x12 -> x18, waiting for transfers between devices: 10.2 us -> 34.4 us  [shifted(): return lax.ppermute(value, axis, [(i, (i + k) % 4) for i in range(4)])]
    all_to_all x1, waiting for transfers between devices: 17.7 us -> 0.01 us  [program(): first = lax.all_to_all(first, SP, 0, 0, tiled=True).reshape(LENGTH, 256)]
    all_to_all x1, waiting for transfers between devices: 0.01 us -> 14 us  [program(): r0 = lax.all_to_all(g0.reshape(NSP, TOKENS, 256), SP, 0, 0, tiled=True)]
    ppermute x12 -> x18, starting transfers between devices: 22.9 us -> 33.9 us  [shifted(): return lax.ppermute(value, axis, [(i, (i + k) % 4) for i in range(4)])]
    pallas_call x1 -> x3, Pallas kernels: 9.79 us -> 17.9 us  [the longest x2 10.1 us: project(): pl.pallas_call(project_body, in_specs=[pl.BlockSpec(memory_space=pltpu.SM...]
    all_to_all x1 -> x2, starting transfers between devices: 3.62 us -> 10.8 us  [the longest x1 6.87 us: program(): kv0 = lax.all_to_all(kv0, SP, 0, 0, tiled=True).reshape(LENGTH, 128)]
    all_to_all x1, starting transfers between devices: 7.18 us -> 13.1 us  [program(): r1 = lax.all_to_all(g1.reshape(NSP, TOKENS, 256), SP, 0, 0, tiled=True)]
  transfers between devices with their start and end apart: 23 -> 37, of which waited for: 9 -> 9; matrix products, arithmetic and copies ran while one was open for 8% -> 6% of each run, Pallas kernels for 24% -> 29%
where the time goes in v4:
time: 271 us; the launch traced here: 270 us
  starting transfers between devices  95.1 us (35%)
  Pallas kernels  78.6 us (29%)
  waiting for transfers between devices  56.9 us (21%)
  between operations  14.5 us (5%)
  local copies, waits for them, and re-layouts  9.45 us (3%)
  other arithmetic  9.08 us (3%)
  matrix products  6.36 us (2%)
    pallas_call x2, Pallas kernels, attend(): pl.pallas_call(functools.partial(attend_body, head), grid=(1,), in_specs=...  56 us
    ppermute x18, waiting for transfers between devices, shifted(): return lax.ppermute(value, axis, [(i, (i + k) % 4) for i in range(4)])  34.4 us
    ppermute x18, starting transfers between devices, shifted(): return lax.ppermute(value, axis, [(i, (i + k) % 4) for i in range(4)])  33.9 us
    all_to_all x1, waiting for transfers between devices, program(): r0 = lax.all_to_all(g0.reshape(NSP, TOKENS, 256), SP, 0, 0, tiled=True)  14 us
    all_to_all x1, starting transfers between devices, everyone(): lax.all_to_all(jnp.broadcast_to(value[None], (size, *value.shape)), axes,...  13.8 us
    all_to_all x1, starting transfers between devices, program(): r1 = lax.all_to_all(g1.reshape(NSP, TOKENS, 256), SP, 0, 0, tiled=True)  13.1 us
    pallas_call x2, Pallas kernels, project(): pl.pallas_call(project_body, in_specs=[pl.BlockSpec(memory_space=pltpu.SM...  10.1 us
    all_to_all x1, starting transfers between devices, program(): first = lax.all_to_all(first, SP, 0, 0, tiled=True).reshape(LENGTH, 256)  8.18 us
  transfers between devices with their start and end apart: 37, of which 9 were waited for; matrix products, arithmetic and copies ran while one was open for 6% of the time, Pallas kernels for 29%

profile of v4, /device:TPU:0, one launch (start us, length us, event | category | flops | bytes accessed | tf_op | source)
XLA Modules:
  0.0 269.9 jit_solution(15427067819955446810)
XLA Ops:
  7.2 1.2 fusion.1
  8.5 1.9 fusion.3.nlat_ref
  10.7 1.7 collective-permute-start.7
  12.4 0.1 fusion.11
  12.5 0.7 copy.20.sin_ref
  13.3 0.7 copy.19.cos_ref
  14.0 0.1 copy.18
  14.1 0.7 pad_convert_fusion.kr_ref
  14.8 4.8 %pack.1 = (bf16[16,192,256]{2,1,0:T(8,128)(2,1)}, bf16[16,192,128]{2,1,0:T(8,128)(2,1)}) custom-call(bf16[192,3072]{1,0:T(8,128)(2,1)} %bitcast.92, bf16[192,2048]{1,0:T(8,128)(2,1)} %bitcast.94, f32[192,128]{1,0:T(8,128)} %pad_convert_fusion.kr_ref, f32[192,128]{1,0:T(8,128)} %copy.19.cos_ref, f32[192,128]{1,0:T(8,128)} %copy.20.sin_ref), custom_call_target="tpu_custom_call" | custom-call | flops 2000000000 | bytes 5000000 | tf_op jit(solution)/shard_map/pack/pallas_call | solution.py:79
  19.6 8.2 %all-to-all-start.1 = ((bf16[16,192,256]{2,1,0:T(8,128)(2,1)}), bf16[16,192,256]{2,1,0:T(8,128)(2,1)S(1)}, u32[]{:S(2)}, u32[]{:S(2)}) async-start(bf16[16,192,256]{2,1,0:T(8,128)(2,1)} %get-tuple-element.26), calls=%async_computation.1 | async-start | bytes 3145728 | tf_op jit(solution)/shard_map/all_to_all | solution.py:377
  27.8 1.8 collective-permute-start.8
  29.6 1.8 collective-permute-start.9
  31.4 0.5 collective-permute-start.11
  31.9 19.6 %collective-permute-done.8.refs_2_ = bf16[256,1024]{1,0:T(8,128)(2,1)} collective-permute-done((bf16[256,1024]{1,0:T(8,128)(2,1)S(1)}, bf16[256,1024]{1,0:T(8,128)(2,1)}, u32[]{:S(2)}, u32[]{:S(2)}) %collective-permute-start.8) | collective-permute-done | bytes 524320 | tf_op jit(solution)/shard_map/ppermute | solution.py:318
  51.5 0.5 collective-permute-start.13
  52.0 2.4 collective-permute-start
  54.4 1.3 collective-permute-start.1
  55.8 1.5 collective-permute-start.2
  57.3 0.6 pad_add_fusion.order_ref
  57.9 4.7 %project.3 = bf16[16,192,128]{2,1,0:T(8,128)(2,1)} custom-call(s32[8]{0:T(128)} %pad_add_fusion.order_ref, bf16[192,1024]{1,0:T(8,128)(2,1)} %fusion.3.nlat_ref, bf16[256,1024]{1,0:T(8,128)(2,1)} %bitcast.77, bf16[256,1024]{1,0:T(8,128)(2,1)} %copy-done.7, bf16[256,1024]{1,0:T(8,128)(2,1)} %collective-permute-done.8.refs_2_, ...), custom_call_target="tpu_custom_call" | custom-call | flops 2000000000 | bytes 6000000 | tf_op jit(solution)/shard_map/project/pallas_call | solution.py:236
  62.6 6.9 %all-to-all-start.2 = ((bf16[16,192,128]{2,1,0:T(8,128)(2,1)}), bf16[16,192,128]{2,1,0:T(8,128)(2,1)S(1)}, u32[]{:S(2)}, u32[]{:S(2)}) async-start(bf16[16,192,128]{2,1,0:T(8,128)(2,1)} %project.3), calls=%async_computation.2 | async-start | bytes 1572864 | tf_op jit(solution)/shard_map/all_to_all | solution.py:379
  69.6 0.5 collective-permute-start.4
  70.2 10.2 %collective-permute-done.2.refs_3_.refs_11_ = bf16[256,1024]{1,0:T(8,128)(2,1)} collective-permute-done((bf16[256,1024]{1,0:T(8,128)(2,1)S(1)}, bf16[256,1024]{1,0:T(8,128)(2,1)}, u32[]{:S(2)}, u32[]{:S(2)}) %collective-permute-start.2) | collective-permute-done | bytes 524320 | tf_op jit(solution)/shard_map/ppermute | solution.py:318
  80.4 2.2 collective-permute-done.6.refs_7_.refs_15_
  82.6 5.4 %project.2 = bf16[16,192,256]{2,1,0:T(8,128)(2,1)} custom-call(s32[8]{0:T(128)} %pad_add_fusion.order_ref, bf16[192,1024]{1,0:T(8,128)(2,1)} %fusion.3.nlat_ref, bf16[256,1024]{1,0:T(8,128)(2,1)} %bitcast.83, bf16[256,1024]{1,0:T(8,128)(2,1)} %collective-permute-done.refs_1_.refs_9_, bf16[256,1024]{1,0:T(8,128)(2,1)} %collective-permute-done.1.refs_2_.refs_10_, ...), custom_call_target="tpu_custom_call" | custom-call | flops 2000000000 | bytes 6000000 | tf_op jit(solution)/shard_map/project/pallas_call | solution.py:236
  88.0 5.1 %all-to-all-done.2 = bf16[16,192,128]{2,1,0:T(8,128)(2,1)S(1)} async-done(((bf16[16,192,128]{2,1,0:T(8,128)(2,1)}), bf16[16,192,128]{2,1,0:T(8,128)(2,1)S(1)}, u32[]{:S(2)}, u32[]{:S(2)}) %all-to-all-start.2) | async-done | bytes 786464 | tf_op jit(solution)/shard_map/all_to_all | solution.py:379
  93.1 0.9 copy-done
  93.9 3.9 %all-to-all-start = ((bf16[16,192,256]{2,1,0:T(8,128)(2,1)}), bf16[16,192,256]{2,1,0:T(8,128)(2,1)S(1)}, u32[]{:S(2)}, u32[]{:S(2)}) async-start(bf16[16,192,256]{2,1,0:T(8,128)(2,1)} %project.2), calls=%async_computation | async-start | bytes 3145728 | tf_op jit(solution)/shard_map/all_to_all | solution.py:381
  97.8 0.8 multiply_sine_fusion
  98.6 1.1 copy-done.1
  99.7 27.9 %shard_map.127 = bf16[3072,256]{1,0:T(8,128)(2,1)} custom-call(bf16[3072,256]{1,0:T(8,128)(2,1)S(1)} %bitcast.60, bf16[3072,256]{1,0:T(8,128)(2,1)S(1)} %bitcast.61, bf16[3072,128]{1,0:T(8,128)(2,1)S(1)} %bitcast.65, f32[16,3072]{1,0:T(8,128)S(1)} %get-tuple-element.66.cos_ref, f32[16,3072]{1,0:T(8,128)S(1)} %get-tuple-element.65.sin_ref), custom_call_target="tpu_custom_call" | custom-call | flops 12000000000 | bytes 6000000 | tf_op jit(solution)/shard_map/pallas_call | solution.py:192
  127.6 7.0 %all-to-all-start.3 = ((bf16[16,192,256]{2,1,0:T(8,128)(2,1)}), bf16[16,192,256]{2,1,0:T(8,128)(2,1)}, u32[]{:S(2)}, u32[]{:S(2)}) async-start(bf16[16,192,256]{2,1,0:T(8,128)(2,1)} %bitcast.14), calls=%async_computation.3 | async-start | bytes 3145728 | tf_op jit(solution)/shard_map/all_to_all | solution.py:386
  134.6 1.9 constant_dynamic-slice_fusion
  136.5 5.3 %collective-permute-start.14 = (bf16[256,1024]{1,0:T(8,128)(2,1)}, bf16[256,1024]{1,0:T(8,128)(2,1)}, u32[]{:S(2)}, u32[]{:S(2)}) collective-permute-start(bf16[256,1024]{1,0:T(8,128)(2,1)} %constant_dynamic-slice_fusion), channel_id=1, source_target_pairs={{0,0},{1,16},{2,32},{3,48},{4,64},{5,80},{6,96},{7,112},{8,1},{9,1... | collective-permute-start | bytes 1572872 | tf_op jit(solution)/shard_map/ppermute | solution.py:369
  141.9 28.1 %shard_map.128 = bf16[3072,256]{1,0:T(8,128)(2,1)} custom-call(bf16[3072,256]{1,0:T(8,128)(2,1)S(1)} %bitcast.63, bf16[3072,256]{1,0:T(8,128)(2,1)S(1)} %bitcast.62, bf16[3072,256]{1,0:T(8,128)(2,1)S(1)} %bitcast.64, f32[16,3072]{1,0:T(8,128)S(1)} %get-tuple-element.66.cos_ref, f32[16,3072]{1,0:T(8,128)S(1)} %get-tuple-element.65.sin_ref), custom_call_target="tpu_custom_call" | custom-call | flops 12000000000 | bytes 6000000 | tf_op jit(solution)/shard_map/pallas_call | solution.py:192
  169.9 14.0 %all-to-all-done.3.r0_ref = bf16[16,192,256]{2,1,0:T(8,128)(2,1)} async-done(((bf16[16,192,256]{2,1,0:T(8,128)(2,1)}), bf16[16,192,256]{2,1,0:T(8,128)(2,1)}, u32[]{:S(2)}, u32[]{:S(2)}) %all-to-all-start.3) | async-done | bytes 1572896 | tf_op jit(solution)/shard_map/all_to_all | solution.py:386
  184.0 13.1 %all-to-all-start.4 = ((bf16[16,192,256]{2,1,0:T(8,128)(2,1)}), bf16[16,192,256]{2,1,0:T(8,128)(2,1)S(1)}, u32[]{:S(2)}, u32[]{:S(2)}) async-start(bf16[16,192,256]{2,1,0:T(8,128)(2,1)} %bitcast.15), calls=%async_computation.4 | async-start | bytes 3145728 | tf_op jit(solution)/shard_map/all_to_all | solution.py:389
  197.1 4.2 %fusion.4 = f32[128,1024]{1,0:T(8,128)S(1)} fusion(bf16[3072,1024]{1,0:T(8,128)(2,1)} %all-gather.2.cloned.1.call-done, bf16[3072,256]{1,0:T(8,128)(2,1)} %shard_map.128), kind=kOutput, calls=%fused_computation.9 | convolution fusion | flops 805306368 | bytes 7602176 | tf_op jit(solution)/shard_map/dot_general | solution.py:392
  201.3 0.6 copy-done.2
  201.9 2.2 fusion.6
  204.1 1.2 multiply_reduce_fusion
  205.6 0.5 collective-permute-start.16
  206.1 1.0 collective-permute-done.16
  207.2 3.4 %collective-permute-start.20 = (f32[8,128]{1,0:T(8,128)S(1)}, f32[8,128]{1,0:T(8,128)S(1)}, u32[]{:S(2)}, u32[]{:S(2)}) collective-permute-start(f32[8,128]{1,0:T(8,128)S(1)} %add.133), channel_id=1, source_target_pairs={{0,4},{2,6},{4,0},{6,2},{1,5},{3,7},{5,1},{7,3},{8,12},{10,14},{12... | collective-permute-start | bytes 12296 | tf_op jit(solution)/shard_map/ppermute | solution.py:318
  210.6 3.2 %collective-permute-start.22 = (f32[8,128]{1,0:T(8,128)S(1)}, f32[8,128]{1,0:T(8,128)S(1)}, u32[]{:S(2)}, u32[]{:S(2)}) collective-permute-start(f32[8,128]{1,0:T(8,128)S(1)} %add.133), channel_id=1, source_target_pairs={{0,6},{2,0},{4,2},{6,4},{1,7},{3,1},{5,3},{7,5},{8,14},{10,8},{12,... | collective-permute-start | bytes 12296 | tf_op jit(solution)/shard_map/ppermute | solution.py:318
  214.0 1.5 collective-permute-start.18
  215.4 1.8 collective-permute-start.19
  217.2 2.9 %collective-permute-done.17 = bf16[32,1024]{1,0:T(8,128)(2,1)S(1)} collective-permute-done((bf16[32,1024]{1,0:T(8,128)(2,1)S(1)}, bf16[32,1024]{1,0:T(8,128)(2,1)S(1)}, u32[]{:S(2)}, u32[]{:S(2)}) %collective-permute-start.17) | collective-permute-done | bytes 65568 | tf_op jit(solution)/shard_map/ppermute | solution.py:318
  220.1 0.9 collective-permute-done.19
  221.0 3.5 %collective-permute-start.24 = (f32[8,128]{1,0:T(8,128)S(1)}, f32[8,128]{1,0:T(8,128)S(1)}, u32[]{:S(2)}, u32[]{:S(2)}) collective-permute-start(f32[8,128]{1,0:T(8,128)S(1)} %add_add_fusion.1), channel_id=1, source_target_pairs={{0,16},{8,24},{16,0},{24,8},{1,17},{9,25},{17,1},{25,9},{2,18},{10... | collective-permute-start | bytes 12296 | tf_op jit(solution)/shard_map/ppermute | solution.py:318
  224.5 0.6 collective-permute-start.25
  225.1 2.7 collective-permute-start.26
  227.7 0.7 collective-permute-start.23
  228.4 0.9 collective-permute-done.25
  229.4 1.2 broadcast_in_dim.27
  230.6 0.3 copy-done.4
  230.9 13.8 %all-to-all-start.5 = ((bf16[16,32,1024]{2,1,0:T(8,128)(2,1)}), bf16[16,32,1024]{2,1,0:T(8,128)(2,1)S(1)}, u32[]{:S(2)}, u32[]{:S(2)}) async-start(bf16[16,32,1024]{2,1,0:T(8,128)(2,1)} %broadcast_in_dim.27), calls=%async_computation.5 | async-start | bytes 2097152 | tf_op jit(solution)/shard_map/all_to_all | solution.py:314
  244.6 3.4 %collective-permute-start.27 = (f32[8,128]{1,0:T(8,128)S(1)}, f32[8,128]{1,0:T(8,128)S(1)}, u32[]{:S(2)}, u32[]{:S(2)}) collective-permute-start(f32[8,128]{1,0:T(8,128)S(1)} %add_add_fusion), channel_id=1, source_target_pairs={{0,64},{32,96},{64,0},{96,32},{1,65},{33,97},{65,1},{97,33},{2,66}... | collective-permute-start | bytes 12296 | tf_op jit(solution)/shard_map/ppermute | solution.py:318
  248.1 0.6 collective-permute-start.28
  248.7 2.7 collective-permute-start.29
  251.3 7.8 %finish.1 = (bf16[192,3072]{1,0:T(8,128)(2,1)}, f32[192,1024]{1,0:T(8,128)}, f32[192,32]{1,0:T(8,128)}) custom-call(s32[8]{0:T(128)} %pad_add_fusion.order_ref, bf16[16,192,256]{2,1,0:T(8,128)(2,1)} %all-to-all-done.3.r0_ref, bf16[16,192,256]{2,1,0:T(8,128)(2,1)} %copy-done.4, bf16[192,1024]{1,0:T(8,128)(2,1)} %bitcast.69, f32[1,1024]{1,0:T(1,128)} %bitcast.91, ...), custom_call_target="tpu_custom_call" | custom-call | flops 2000000000 | bytes 14000000 | tf_op jit(solution)/shard_map/finish/pallas_call | solution.py:290
  259.2 1.6 copy.24
  260.8 0.6 add_bitcast_fusion
  261.4 1.6 bitcast_convert_fusion
  (83 shorter events, 1.1 us)
Async XLA Ops:
  7.2 3.3 %copy-start.10 = (bf16[256,1024]{1,0:T(8,128)(2,1)S(1)}, bf16[256,1024]{1,0:T(8,128)(2,1)}, u32[]{:S(2)}) copy-start(bf16[256,1024]{1,0:T(8,128)(2,1)} %param.12) | copy-start | bytes 1572868
  7.2 3.3 %copy-start.9 = (bf16[256,1024]{1,0:T(8,128)(2,1)S(1)}, bf16[256,1024]{1,0:T(8,128)(2,1)}, u32[]{:S(2)}) copy-start(bf16[256,1024]{1,0:T(8,128)(2,1)} %param.13) | copy-start | bytes 1572868
  7.2 189.9 %all-gather.2.cloned.1.call-start = ((), (), s32[]{:S(2)}) async-start(), calls=%async_computation.6 | async-start | bytes 6684672 | tf_op jit(solution)/shard_map/all_gather | solution.py:367
  10.5 4.2 %copy-start.3 = (bf16[4,2,64,1024]{3,2,1,0:T(8,128)(2,1)}, bf16[4,2,64,1024]{3,2,1,0:T(8,128)(2,1)S(1)}, u32[]{:S(2)}) copy-start(bf16[4,2,64,1024]{3,2,1,0:T(8,128)(2,1)S(1)} %pad_maximum_fusion) | copy-start | bytes 3145732
  10.6 3.5 %copy-start.12 = (bf16[1,192,32]{1,2,0:T(8,128)(2,1)S(1)}, bf16[1,192,32]{1,2,0:T(8,128)(2,1)}, u32[]{:S(2)}) copy-start(bf16[1,192,32]{1,2,0:T(8,128)(2,1)} %param.10) | copy-start | bytes 36868
  10.7 20.7 %copy-start.5 = (bf16[2,1,128,1024]{3,2,1,0:T(8,128)(2,1)}, bf16[2,1,128,1024]{3,2,1,0:T(8,128)(2,1)S(1)}, u32[]{:S(2)}) copy-start(bf16[2,1,128,1024]{3,2,1,0:T(8,128)(2,1)S(1)} %get-tuple-element.60) | copy-start | bytes 1572868
  10.7 58.8 %copy-start.6 = (bf16[2,1,128,1024]{3,2,1,0:T(8,128)(2,1)}, bf16[2,1,128,1024]{3,2,1,0:T(8,128)(2,1)S(1)}, u32[]{:S(2)}) copy-start(bf16[2,1,128,1024]{3,2,1,0:T(8,128)(2,1)S(1)} %get-tuple-element.61) | copy-start | bytes 1572868
  10.7 20.7 %collective-permute-start.7 = (bf16[256,1024]{1,0:T(8,128)(2,1)S(1)}, bf16[256,1024]{1,0:T(8,128)(2,1)S(1)}, u32[]{:S(2)}, u32[]{:S(2)}) collective-permute-start(bf16[256,1024]{1,0:T(8,128)(2,1)S(1)} %bitcast.73), channel_id=1, source_target_pairs={{0,2},{2,4},{4,6},{6,0},{1,3},{3,5},{5,7},{7,1},{8,10},{10,12},{12... | collective-permute-start | bytes 1572872 | tf_op jit(solution)/shard_map/ppermute | solution.py:318
  19.6 37.7 %copy-start.13 = (s32[4]{0:T(128)S(1)}, s32[4]{0:T(128)}, u32[]{:S(2)}) copy-start(s32[4]{0:T(128)} %constant.86.clone) | copy-start | bytes 52
  19.6 43.0 %all-to-all-start.1 = ((bf16[16,192,256]{2,1,0:T(8,128)(2,1)}), bf16[16,192,256]{2,1,0:T(8,128)(2,1)S(1)}, u32[]{:S(2)}, u32[]{:S(2)}) async-start(bf16[16,192,256]{2,1,0:T(8,128)(2,1)} %get-tuple-element.26), calls=%async_computation.1 | async-start | bytes 3145728 | tf_op jit(solution)/shard_map/all_to_all | solution.py:377
  27.8 23.7 %collective-permute-start.8 = (bf16[256,1024]{1,0:T(8,128)(2,1)S(1)}, bf16[256,1024]{1,0:T(8,128)(2,1)}, u32[]{:S(2)}, u32[]{:S(2)}) collective-permute-start(bf16[256,1024]{1,0:T(8,128)(2,1)S(1)} %bitcast.74), channel_id=1, source_target_pairs={{0,6},{2,0},{4,2},{6,4},{1,7},{3,1},{5,3},{7,5},{8,14},{10,8},{12,... | collective-permute-start | bytes 1572872 | tf_op jit(solution)/shard_map/ppermute | solution.py:318
  29.6 21.9 %collective-permute-start.9 = (bf16[256,1024]{1,0:T(8,128)(2,1)S(1)}, bf16[256,1024]{1,0:T(8,128)(2,1)}, u32[]{:S(2)}, u32[]{:S(2)}) collective-permute-start(bf16[256,1024]{1,0:T(8,128)(2,1)S(1)} %bitcast.75), channel_id=1, source_target_pairs={{0,4},{2,6},{4,0},{6,2},{1,5},{3,7},{5,1},{7,3},{8,12},{10,14},{12... | collective-permute-start | bytes 1572872 | tf_op jit(solution)/shard_map/ppermute | solution.py:318
  31.4 23.0 %collective-permute-start.10 = (bf16[256,1024]{1,0:T(8,128)(2,1)S(1)}, bf16[256,1024]{1,0:T(8,128)(2,1)}, u32[]{:S(2)}, u32[]{:S(2)}) collective-permute-start(bf16[256,1024]{1,0:T(8,128)(2,1)S(1)} %bitcast.76), channel_id=1, source_target_pairs={{0,1},{1,0},{2,3},{3,2},{4,5},{5,4},{6,7},{7,6},{8,9},{9,8},{10,11... | collective-permute-start | bytes 1572872 | tf_op jit(solution)/shard_map/ppermute | solution.py:326
  31.4 26.5 %copy-start.7 = (bf16[256,1024]{1,0:T(8,128)(2,1)}, bf16[256,1024]{1,0:T(8,128)(2,1)S(1)}, u32[]{:S(2)}) copy-start(bf16[256,1024]{1,0:T(8,128)(2,1)S(1)} %collective-permute-done.7.refs_1_) | copy-start | bytes 1572868
  31.4 24.3 %collective-permute-start.11 = (bf16[256,1024]{1,0:T(8,128)(2,1)S(1)}, bf16[256,1024]{1,0:T(8,128)(2,1)}, u32[]{:S(2)}, u32[]{:S(2)}) collective-permute-start(bf16[256,1024]{1,0:T(8,128)(2,1)S(1)} %collective-permute-done.7.refs_1_), channel_id=1, source_target_pairs={{0,1},{1,0},{2,3},{3,2},{4,5},{5,4},{6,7},{7,6},{8,9},{9,8},{10,11... | collective-permute-start | bytes 1572872 | tf_op jit(solution)/shard_map/ppermute | solution.py:326
  51.5 6.4 %collective-permute-start.12 = (bf16[256,1024]{1,0:T(8,128)(2,1)}, bf16[256,1024]{1,0:T(8,128)(2,1)}, u32[]{:S(2)}, u32[]{:S(2)}) collective-permute-start(bf16[256,1024]{1,0:T(8,128)(2,1)} %collective-permute-done.8.refs_2_), channel_id=1, source_target_pairs={{0,1},{1,0},{2,3},{3,2},{4,5},{5,4},{6,7},{7,6},{8,9},{9,8},{10,11... | collective-permute-start | bytes 1572872 | tf_op jit(solution)/shard_map/ppermute | solution.py:326
  51.5 6.4 %collective-permute-start.13 = (bf16[256,1024]{1,0:T(8,128)(2,1)}, bf16[256,1024]{1,0:T(8,128)(2,1)}, u32[]{:S(2)}, u32[]{:S(2)}) collective-permute-start(bf16[256,1024]{1,0:T(8,128)(2,1)} %collective-permute-done.9.refs_3_), channel_id=1, source_target_pairs={{0,1},{1,0},{2,3},{3,2},{4,5},{5,4},{6,7},{7,6},{8,9},{9,8},{10,11... | collective-permute-start | bytes 1572872 | tf_op jit(solution)/shard_map/ppermute | solution.py:326
  52.0 17.6 %collective-permute-start = (bf16[256,1024]{1,0:T(8,128)(2,1)S(1)}, bf16[256,1024]{1,0:T(8,128)(2,1)}, u32[]{:S(2)}, u32[]{:S(2)}) collective-permute-start(bf16[256,1024]{1,0:T(8,128)(2,1)S(1)} %bitcast.79), channel_id=1, source_target_pairs={{0,2},{2,4},{4,6},{6,0},{1,3},{3,5},{5,7},{7,1},{8,10},{10,12},{12... | collective-permute-start | bytes 1572872 | tf_op jit(solution)/shard_map/ppermute | solution.py:318
  54.4 15.7 %collective-permute-start.1 = (bf16[256,1024]{1,0:T(8,128)(2,1)S(1)}, bf16[256,1024]{1,0:T(8,128)(2,1)}, u32[]{:S(2)}, u32[]{:S(2)}) collective-permute-start(bf16[256,1024]{1,0:T(8,128)(2,1)S(1)} %bitcast.80), channel_id=1, source_target_pairs={{0,6},{2,0},{4,2},{6,4},{1,7},{3,1},{5,3},{7,5},{8,14},{10,8},{12,... | collective-permute-start | bytes 1572872 | tf_op jit(solution)/shard_map/ppermute | solution.py:318
  55.8 24.6 %collective-permute-start.2 = (bf16[256,1024]{1,0:T(8,128)(2,1)S(1)}, bf16[256,1024]{1,0:T(8,128)(2,1)}, u32[]{:S(2)}, u32[]{:S(2)}) collective-permute-start(bf16[256,1024]{1,0:T(8,128)(2,1)S(1)} %bitcast.81), channel_id=1, source_target_pairs={{0,4},{2,6},{4,0},{6,2},{1,5},{3,7},{5,1},{7,3},{8,12},{10,14},{12... | collective-permute-start | bytes 1572872 | tf_op jit(solution)/shard_map/ppermute | solution.py:318
  62.6 30.5 %all-to-all-start.2 = ((bf16[16,192,128]{2,1,0:T(8,128)(2,1)}), bf16[16,192,128]{2,1,0:T(8,128)(2,1)S(1)}, u32[]{:S(2)}, u32[]{:S(2)}) async-start(bf16[16,192,128]{2,1,0:T(8,128)(2,1)} %project.3), calls=%async_computation.2 | async-start | bytes 1572864 | tf_op jit(solution)/shard_map/all_to_all | solution.py:379
  69.5 10.9 %collective-permute-start.3 = (bf16[256,1024]{1,0:T(8,128)(2,1)S(1)}, bf16[256,1024]{1,0:T(8,128)(2,1)S(1)}, u32[]{:S(2)}, u32[]{:S(2)}) collective-permute-start(bf16[256,1024]{1,0:T(8,128)(2,1)S(1)} %bitcast.82), channel_id=1, source_target_pairs={{0,1},{1,0},{2,3},{3,2},{4,5},{5,4},{6,7},{7,6},{8,9},{9,8},{10,11... | collective-permute-start | bytes 1572872 | tf_op jit(solution)/shard_map/ppermute | solution.py:326
  69.6 10.8 %collective-permute-start.4 = (bf16[256,1024]{1,0:T(8,128)(2,1)}, bf16[256,1024]{1,0:T(8,128)(2,1)}, u32[]{:S(2)}, u32[]{:S(2)}) collective-permute-start(bf16[256,1024]{1,0:T(8,128)(2,1)} %collective-permute-done.refs_1_.refs_9_), channel_id=1, source_target_pairs={{0,1},{1,0},{2,3},{3,2},{4,5},{5,4},{6,7},{7,6},{8,9},{9,8},{10,11... | collective-permute-start | bytes 1572872 | tf_op jit(solution)/shard_map/ppermute | solution.py:326
  70.1 10.3 %collective-permute-start.5 = (bf16[256,1024]{1,0:T(8,128)(2,1)}, bf16[256,1024]{1,0:T(8,128)(2,1)}, u32[]{:S(2)}, u32[]{:S(2)}) collective-permute-start(bf16[256,1024]{1,0:T(8,128)(2,1)} %collective-permute-done.1.refs_2_.refs_10_), channel_id=1, source_target_pairs={{0,1},{1,0},{2,3},{3,2},{4,5},{5,4},{6,7},{7,6},{8,9},{9,8},{10,11... | collective-permute-start | bytes 1572872 | tf_op jit(solution)/shard_map/ppermute | solution.py:326
  80.4 2.3 collective-permute-start.6
  80.4 2.2 copy-start.8
  93.1 0.9 copy-start
  93.9 33.7 %all-to-all-start = ((bf16[16,192,256]{2,1,0:T(8,128)(2,1)}), bf16[16,192,256]{2,1,0:T(8,128)(2,1)S(1)}, u32[]{:S(2)}, u32[]{:S(2)}) async-start(bf16[16,192,256]{2,1,0:T(8,128)(2,1)} %project.2), calls=%async_computation | async-start | bytes 3145728 | tf_op jit(solution)/shard_map/all_to_all | solution.py:381
  98.6 1.1 copy-start.1
  127.6 56.4 %all-to-all-start.3 = ((bf16[16,192,256]{2,1,0:T(8,128)(2,1)}), bf16[16,192,256]{2,1,0:T(8,128)(2,1)}, u32[]{:S(2)}, u32[]{:S(2)}) async-start(bf16[16,192,256]{2,1,0:T(8,128)(2,1)} %bitcast.14), calls=%async_computation.3 | async-start | bytes 3145728 | tf_op jit(solution)/shard_map/all_to_all | solution.py:386
  136.5 67.6 %collective-permute-start.14 = (bf16[256,1024]{1,0:T(8,128)(2,1)}, bf16[256,1024]{1,0:T(8,128)(2,1)}, u32[]{:S(2)}, u32[]{:S(2)}) collective-permute-start(bf16[256,1024]{1,0:T(8,128)(2,1)} %constant_dynamic-slice_fusion), channel_id=1, source_target_pairs={{0,0},{1,16},{2,32},{3,48},{4,64},{5,80},{6,96},{7,112},{8,1},{9,1... | collective-permute-start | bytes 1572872 | tf_op jit(solution)/shard_map/ppermute | solution.py:369
  184.0 45.4 %all-to-all-start.4 = ((bf16[16,192,256]{2,1,0:T(8,128)(2,1)}), bf16[16,192,256]{2,1,0:T(8,128)(2,1)S(1)}, u32[]{:S(2)}, u32[]{:S(2)}) async-start(bf16[16,192,256]{2,1,0:T(8,128)(2,1)} %bitcast.15), calls=%async_computation.4 | async-start | bytes 3145728 | tf_op jit(solution)/shard_map/all_to_all | solution.py:389
  197.1 4.8 %copy-start.2 = (bf16[3072,1024]{1,0:T(8,128)(2,1)S(1)}, bf16[3072,1024]{1,0:T(8,128)(2,1)}, u32[]{:S(2)}) copy-start(bf16[3072,1024]{1,0:T(8,128)(2,1)} %all-gather.2.cloned.1.call-done) | copy-start | bytes 18874372
  204.1 1.2 copy-start.11
  205.5 1.6 collective-permute-start.15
  205.6 1.5 collective-permute-start.16
  207.2 8.2 %collective-permute-start.20 = (f32[8,128]{1,0:T(8,128)S(1)}, f32[8,128]{1,0:T(8,128)S(1)}, u32[]{:S(2)}, u32[]{:S(2)}) collective-permute-start(f32[8,128]{1,0:T(8,128)S(1)} %add.133), channel_id=1, source_target_pairs={{0,4},{2,6},{4,0},{6,2},{1,5},{3,7},{5,1},{7,3},{8,12},{10,14},{12... | collective-permute-start | bytes 12296 | tf_op jit(solution)/shard_map/ppermute | solution.py:318
  210.6 6.6 %collective-permute-start.21 = (f32[8,128]{1,0:T(8,128)S(1)}, f32[8,128]{1,0:T(8,128)S(1)}, u32[]{:S(2)}, u32[]{:S(2)}) collective-permute-start(f32[8,128]{1,0:T(8,128)S(1)} %add.133), channel_id=1, source_target_pairs={{0,2},{2,4},{4,6},{6,0},{1,3},{3,5},{5,7},{7,1},{8,10},{10,12},{12... | collective-permute-start | bytes 12296 | tf_op jit(solution)/shard_map/ppermute | solution.py:318
  210.6 6.6 %collective-permute-start.22 = (f32[8,128]{1,0:T(8,128)S(1)}, f32[8,128]{1,0:T(8,128)S(1)}, u32[]{:S(2)}, u32[]{:S(2)}) collective-permute-start(f32[8,128]{1,0:T(8,128)S(1)} %add.133), channel_id=1, source_target_pairs={{0,6},{2,0},{4,2},{6,4},{1,7},{3,1},{5,3},{7,5},{8,14},{10,8},{12,... | collective-permute-start | bytes 12296 | tf_op jit(solution)/shard_map/ppermute | solution.py:318
  213.9 6.2 %collective-permute-start.17 = (bf16[32,1024]{1,0:T(8,128)(2,1)S(1)}, bf16[32,1024]{1,0:T(8,128)(2,1)S(1)}, u32[]{:S(2)}, u32[]{:S(2)}) collective-permute-start(bf16[32,1024]{1,0:T(8,128)(2,1)S(1)} %get-tuple-element.62), channel_id=1, source_target_pairs={{0,2},{2,4},{4,6},{6,0},{1,3},{3,5},{5,7},{7,1},{8,10},{10,12},{12... | collective-permute-start | bytes 196616 | tf_op jit(solution)/shard_map/ppermute | solution.py:318
  214.0 6.2 %collective-permute-start.18 = (bf16[32,1024]{1,0:T(8,128)(2,1)S(1)}, bf16[32,1024]{1,0:T(8,128)(2,1)S(1)}, u32[]{:S(2)}, u32[]{:S(2)}) collective-permute-start(bf16[32,1024]{1,0:T(8,128)(2,1)S(1)} %get-tuple-element.64), channel_id=1, source_target_pairs={{0,4},{2,6},{4,0},{6,2},{1,5},{3,7},{5,1},{7,3},{8,12},{10,14},{12... | collective-permute-start | bytes 196616 | tf_op jit(solution)/shard_map/ppermute | solution.py:318
  215.4 5.6 %collective-permute-start.19 = (bf16[32,1024]{1,0:T(8,128)(2,1)S(1)}, bf16[32,1024]{1,0:T(8,128)(2,1)S(1)}, u32[]{:S(2)}, u32[]{:S(2)}) collective-permute-start(bf16[32,1024]{1,0:T(8,128)(2,1)S(1)} %get-tuple-element.63), channel_id=1, source_target_pairs={{0,6},{2,0},{4,2},{6,4},{1,7},{3,1},{5,3},{7,5},{8,14},{10,8},{12,... | collective-permute-start | bytes 196616 | tf_op jit(solution)/shard_map/ppermute | solution.py:318
  221.0 7.4 %collective-permute-start.24 = (f32[8,128]{1,0:T(8,128)S(1)}, f32[8,128]{1,0:T(8,128)S(1)}, u32[]{:S(2)}, u32[]{:S(2)}) collective-permute-start(f32[8,128]{1,0:T(8,128)S(1)} %add_add_fusion.1), channel_id=1, source_target_pairs={{0,16},{8,24},{16,0},{24,8},{1,17},{9,25},{17,1},{25,9},{2,18},{10... | collective-permute-start | bytes 12296 | tf_op jit(solution)/shard_map/ppermute | solution.py:318
  224.5 4.8 %collective-permute-start.25 = (f32[8,128]{1,0:T(8,128)S(1)}, f32[8,128]{1,0:T(8,128)S(1)}, u32[]{:S(2)}, u32[]{:S(2)}) collective-permute-start(f32[8,128]{1,0:T(8,128)S(1)} %add_add_fusion.1), channel_id=1, source_target_pairs={{0,8},{8,16},{16,24},{24,0},{1,9},{9,17},{17,25},{25,1},{2,10},{10... | collective-permute-start | bytes 12296 | tf_op jit(solution)/shard_map/ppermute | solution.py:318
  225.1 4.3 %collective-permute-start.26 = (f32[8,128]{1,0:T(8,128)S(1)}, f32[8,128]{1,0:T(8,128)S(1)}, u32[]{:S(2)}, u32[]{:S(2)}) collective-permute-start(f32[8,128]{1,0:T(8,128)S(1)} %add_add_fusion.1), channel_id=1, source_target_pairs={{0,24},{8,0},{16,8},{24,16},{1,25},{9,1},{17,9},{25,17},{2,26},{10... | collective-permute-start | bytes 12296 | tf_op jit(solution)/shard_map/ppermute | solution.py:318
  227.7 1.6 collective-permute-start.23
  229.4 1.5 copy-start.4
  230.9 30.5 %all-to-all-start.5 = ((bf16[16,32,1024]{2,1,0:T(8,128)(2,1)}), bf16[16,32,1024]{2,1,0:T(8,128)(2,1)S(1)}, u32[]{:S(2)}, u32[]{:S(2)}) async-start(bf16[16,32,1024]{2,1,0:T(8,128)(2,1)} %broadcast_in_dim.27), calls=%async_computation.5 | async-start | bytes 2097152 | tf_op jit(solution)/shard_map/all_to_all | solution.py:314
  244.6 16.1 %collective-permute-start.27 = (f32[8,128]{1,0:T(8,128)S(1)}, f32[8,128]{1,0:T(8,128)S(1)}, u32[]{:S(2)}, u32[]{:S(2)}) collective-permute-start(f32[8,128]{1,0:T(8,128)S(1)} %add_add_fusion), channel_id=1, source_target_pairs={{0,64},{32,96},{64,0},{96,32},{1,65},{33,97},{65,1},{97,33},{2,66}... | collective-permute-start | bytes 12296 | tf_op jit(solution)/shard_map/ppermute | solution.py:318
  248.1 12.7 %collective-permute-start.28 = (f32[8,128]{1,0:T(8,128)S(1)}, f32[8,128]{1,0:T(8,128)S(1)}, u32[]{:S(2)}, u32[]{:S(2)}) collective-permute-start(f32[8,128]{1,0:T(8,128)S(1)} %add_add_fusion), channel_id=1, source_target_pairs={{0,32},{32,64},{64,96},{96,0},{1,33},{33,65},{65,97},{97,1},{2,34}... | collective-permute-start | bytes 12296 | tf_op jit(solution)/shard_map/ppermute | solution.py:318
  248.7 12.1 %collective-permute-start.29 = (f32[8,128]{1,0:T(8,128)S(1)}, f32[8,128]{1,0:T(8,128)S(1)}, u32[]{:S(2)}, u32[]{:S(2)}) collective-permute-start(f32[8,128]{1,0:T(8,128)S(1)} %add_add_fusion), channel_id=1, source_target_pairs={{0,96},{32,0},{64,32},{96,64},{1,97},{33,1},{65,33},{97,65},{2,98}... | collective-permute-start | bytes 12296 | tf_op jit(solution)/shard_map/ppermute | solution.py:318
Sparse Core Ops, SparseCore 0:
  10.7 87.3 all-gather.1

commit v5 on v4

--- a/solution.py
+++ b/solution.py
@@ -32,10 +32,8 @@
 bf16 = jnp.bfloat16
 
 
-def angles(positions):
-    inverse = 1.0 / rope_base ** (jnp.arange(0, ROPE, 2, dtype=f32) / ROPE)
-    turned = positions.astype(f32)[:, None] * inverse[None, :]
-    return jnp.cos(turned), jnp.sin(turned)
+def inverse_of(index):
+    return 1.0 / rope_base ** ((2 * (index % HALF)).astype(f32) / ROPE)
 
 
 def lanes_of(shape):
@@ -219,15 +217,20 @@
 def project_body(order_ref, nlat_ref, *refs):
     weights, rest = refs[:NDP], refs[NDP:]
     nlat = nlat_ref[...]
-    if len(rest) == 2:
+    if len(rest) == 3:
         rest[1][:, :, 0:128] = rest[0][...]
-    out_ref = rest[-1]
+    out_ref, own_ref = rest[-2:]
     base = out_ref.shape[2] - 128
     for step in range(NDP):
         made = lax.dot_general(nlat, weights[step][...], (((1,), (1,)), ((), ())), preferred_element_type=f32)
         slot = 2 * order_ref[step]
         out_ref[slot, :, base : base + 128] = made[:, 0:128].astype(bf16)
         out_ref[slot + 1, :, base : base + 128] = made[:, 128:256].astype(bf16)
+        for half in range(2):
+
+            @pl.when(slot + half == order_ref[NDP])
+            def _():
+                own_ref[...] = weights[step][128 * half : 128 * half + 128, :]
 
 
 def project(order, nlat, weights, extra):
@@ -236,8 +239,11 @@
     return pl.pallas_call(
         project_body,
         in_specs=[pl.BlockSpec(memory_space=pltpu.SMEM)] + [memory] * (1 + NDP + len(extras)),
-        out_specs=memory,
-        out_shape=jax.ShapeDtypeStruct((NSP, TOKENS, 128 * (1 + len(extras))), bf16),
+        out_specs=[memory, memory],
+        out_shape=[
+            jax.ShapeDtypeStruct((NSP, TOKENS, 128 * (1 + len(extras))), bf16),
+            jax.ShapeDtypeStruct((128, LATENT), bf16),
+        ],
         cost_estimate=pl.CostEstimate(flops=2_000_000_000, bytes_accessed=6_000_000, transcendentals=0),
         name="project",
     )(order, nlat, *weights, *extras)
@@ -326,9 +332,9 @@
     return near + [lax.ppermute(piece, "dp_1", SWAP) for piece in near]
 
 
-def sum_of_four(value, axis):
-    others = [shifted(value, axis, k) for k in (1, 2, 3)]
-    return (value + others[1]) + (others[0] + others[2])
+def as_rows(value):
+    top = lax.reduce_precision(value, 8, 7)
+    return jnp.stack([top, lax.reduce_precision(value - top, 8, 7)] + [jnp.zeros_like(value)] * 14).astype(bf16)
 
 
 def reduce_over_rows(pieces, small):
@@ -336,18 +342,20 @@
     pairs = pieces.reshape(4, 2, *pieces.shape[1:])
     kept = lax.dynamic_index_in_dim(pairs, core, 1, keepdims=False)
     given = lax.dynamic_index_in_dim(pairs, 1 - core, 1, keepdims=False)
-    given, small = lax.optimization_barrier((given, small))
-    given = lax.ppermute(given, "dp_1", SWAP)
-    small = small + lax.ppermute(small, "dp_1", SWAP)
-    kept = kept.astype(f32) + given.astype(f32)
+    extra = jnp.pad(as_rows(small)[None], ((0, 0), (0, 16), (0, 0)))
+    got = lax.ppermute(jnp.concatenate([given, extra]), "dp_1", SWAP).astype(f32)
+    small = small + (got[4, 0] + got[4, 1])
+    kept = kept.astype(f32) + got[:4]
+    extra = as_rows(small)
+    arrived = []
+    for k in (1, 2, 3):
+        sent = lax.dynamic_index_in_dim(kept, (across + k) & 3, 0, keepdims=False).astype(bf16)
+        arrived.append(shifted(jnp.concatenate([sent, extra]), "dp_0", k).astype(f32))
     total = lax.dynamic_index_in_dim(kept, across, 0, keepdims=False)
-    kept = kept.astype(bf16)
-    kept, small = lax.optimization_barrier((kept, small))
-    for k in (1, 2, 3):
-        sent = lax.dynamic_index_in_dim(kept, (across + k) & 3, 0, keepdims=False)
-        total = total + shifted(sent, "dp_0", k).astype(f32)
-    small = sum_of_four(small, "dp_0")
-    return lax.optimization_barrier((total.astype(bf16), small))
+    total = (total + arrived[1][:32]) + (arrived[0][:32] + arrived[2][:32])
+    others = [got[32] + got[33] for got in arrived]
+    small = (small + others[1]) + (others[0] + others[2])
+    return total.astype(bf16), small
 
 
 def program(query, latent, rope_key, gain, key_up, value_up, out_grad):
@@ -360,27 +368,25 @@
     rows = rows.reshape(512, LATENT)
     across, core = lax.axis_index("dp_0"), lax.axis_index("dp_1")
     shards = ((across + jnp.array([0, -1, 1, 2], jnp.int32)) & 3) * 2
-    order = jnp.concatenate([shards + core, shards + 1 - core])
+    order = jnp.concatenate([shards + core, shards + 1 - core, place[None]])
     by_head = rows.reshape(2, 2, 128, LATENT)
     evens = all_shards(by_head[:, 0].reshape(256, LATENT))
     odds = all_shards(by_head[:, 1].reshape(256, LATENT))
-    nlat_all = lax.all_gather(nlat, SP, axis=0, tiled=True)
-    mine = lax.dynamic_slice_in_dim(rows, (place // 8) * 256, 256, axis=0)
-    own = lax.ppermute(mine, ALL, to_heads())
-
-    positions = place * TOKENS + jnp.arange(TOKENS)
-    cosine, sine = angles(positions)
-    cos_lanes = jnp.tile(cosine, (1, 8))
-    sin_lanes = jnp.tile(jnp.concatenate([-sine, sine], axis=1), (1, 4))
+    lane = jnp.arange(128)
+    turned = (place * TOKENS + jnp.arange(TOKENS)).astype(f32)[:, None] * inverse_of(lane)[None, :]
+    cos_lanes = jnp.cos(turned)
+    sin_lanes = jnp.sin(turned) * jnp.where(lane % ROPE < HALF, -1.0, 1.0)[None, :]
     key = jnp.pad(rope_key[0].astype(f32), ((0, 0), (0, 96)))
     first, second = pack(query[0], out_grad[0], key, cos_lanes, sin_lanes)
     first = lax.all_to_all(first, SP, 0, 0, tiled=True).reshape(LENGTH, 256)
-    kv0 = project(order, nlat, evens, None)
+    kv0, own0 = project(order, nlat, evens, None)
+    late, second = lax.optimization_barrier((nlat, second))
+    nlat_all = lax.all_gather(late, SP, axis=0, tiled=True)
     kv0 = lax.all_to_all(kv0, SP, 0, 0, tiled=True).reshape(LENGTH, 128)
-    second = project(order, nlat, odds, second)
+    second, own1 = project(order, nlat, odds, second)
     second = lax.all_to_all(second, SP, 0, 0, tiled=True).reshape(LENGTH, 256)
-    cos_all, sin_all = angles(jnp.arange(LENGTH))
-    cos_all, sin_all = cos_all.T, sin_all.T
+    turned = jnp.arange(LENGTH).astype(f32)[None, :] * inverse_of(jnp.arange(HALF))[:, None]
+    cos_all, sin_all = jnp.cos(turned), jnp.sin(turned)
     g0 = attend(0, first, first, kv0, cos_all, sin_all)
     second, g0 = lax.optimization_barrier((second, g0))
     r0 = lax.all_to_all(g0.reshape(NSP, TOKENS, 256), SP, 0, 0, tiled=True)
@@ -394,14 +400,15 @@
     ]
     part = jnp.concatenate(parts, axis=0)
     pieces = part.astype(bf16).reshape(2, 2, 4, 16, LATENT).transpose(0, 2, 1, 3, 4).reshape(NDP, 32, LATENT)
-    gain_part = (jnp.sum(part * own.astype(f32), axis=0) / gain).reshape(8, 128)
+    own = jnp.concatenate([own0, own1], axis=0)
+    gain_part = jnp.sum(part * own.astype(f32), axis=0) / gain
     piece, gain_part = reduce_over_rows(pieces, gain_part)
     piece = lax.ppermute(piece, ALL, to_rows())
-    gain_part = sum_of_four(gain_part, "sp_1")
-    piece, gain_part = lax.optimization_barrier((piece, gain_part))
-    gain_grad = sum_of_four(gain_part, "sp_0").reshape(LATENT)
     r1, piece = lax.optimization_barrier((r1, piece))
-    grads = everyone(piece, SP, NSP).reshape(NSP, 2, 16, LATENT)
+    piece = jnp.concatenate([piece, as_rows(gain_part)])
+    got = everyone(piece, SP, NSP)
+    grads = got[:, :32].reshape(NSP, 2, 16, LATENT)
+    gain_grad = got[:, 32:34].astype(f32).sum(axis=(0, 1))
     key_grad = grads[:, 0].reshape(256, LATENT).astype(f32)
     value_grad = grads[:, 1].reshape(256, LATENT).astype(f32)
 

time: 271 us -> 249 us (0.919)
  starting transfers between devices: 95.1 us -> 54.9 us
  waiting for transfers between devices: 56.9 us -> 71.4 us
  Pallas kernels: 78.6 us -> 83.1 us
    ppermute x18 -> x9, starting transfers between devices: 33.9 us -> 14.9 us  [shifted(): return lax.ppermute(value, axis, [(i, (i + k) % 4) for i in range(4)])]
    all_to_all x1, waiting for transfers between devices: 0.01 us -> 15.4 us  [everyone(): lax.all_to_all(jnp.broadcast_to(value[None], (size, *value.shape)), axes,...]
    all_to_all x1, waiting for transfers between devices: 0.01 us -> 15 us  [program(): r1 = lax.all_to_all(g1.reshape(NSP, TOKENS, 256), SP, 0, 0, tiled=True)]
    all_to_all x1, waiting for transfers between devices: 14 us -> 0.01 us  [program(): r0 = lax.all_to_all(g0.reshape(NSP, TOKENS, 256), SP, 0, 0, tiled=True)]
    all_to_all x1, starting transfers between devices: 13.8 us -> 4.97 us  [everyone(): lax.all_to_all(jnp.broadcast_to(value[None], (size, *value.shape)), axes,...]
    all_to_all x1, starting transfers between devices: 13.1 us -> 7.18 us  [program(): r1 = lax.all_to_all(g1.reshape(NSP, TOKENS, 256), SP, 0, 0, tiled=True)]
    ppermute x3 -> x1, starting transfers between devices: 5.93 us -> 0.09 us  [reduce_over_rows(): lax.ppermute(jnp.concatenate([given, extra]), 'dp_1', SWAP).astype(f32)]
    pallas_call x2, Pallas kernels: 10.1 us -> 14.4 us  [project(): pl.pallas_call(project_body, in_specs=[pl.BlockSpec(memory_space=pltpu.SM...]
  transfers between devices with their start and end apart: 37 -> 26, of which waited for: 9 -> 9; matrix products, arithmetic and copies ran while one was open for 6% -> 1% of each run, Pallas kernels for 29% -> 32%
where the time goes in v5:
time: 249 us; the launch traced here: 248 us
  Pallas kernels  83.1 us (33%)
  waiting for transfers between devices  71.4 us (29%)
  starting transfers between devices  54.9 us (22%)
  between operations  14.6 us (6%)
  other arithmetic  9.76 us (4%)
  local copies, waits for them, and re-layouts  8.21 us (3%)
  matrix products  6.35 us (3%)
    pallas_call x2, Pallas kernels, attend(): pl.pallas_call(functools.partial(attend_body, head), grid=(1,), in_specs=...  56 us
    ppermute x9, waiting for transfers between devices, shifted(): return lax.ppermute(value, axis, [(i, (i + k) % 4) for i in range(4)])  33.8 us
    all_to_all x1, waiting for transfers between devices, everyone(): lax.all_to_all(jnp.broadcast_to(value[None], (size, *value.shape)), axes,...  15.4 us
    all_to_all x1, waiting for transfers between devices, program(): r1 = lax.all_to_all(g1.reshape(NSP, TOKENS, 256), SP, 0, 0, tiled=True)  15 us
    ppermute x9, starting transfers between devices, shifted(): return lax.ppermute(value, axis, [(i, (i + k) % 4) for i in range(4)])  14.9 us
    pallas_call x2, Pallas kernels, project(): pl.pallas_call(project_body, in_specs=[pl.BlockSpec(memory_space=pltpu.SM...  14.4 us
    all_to_all x1, starting transfers between devices, program(): first = lax.all_to_all(first, SP, 0, 0, tiled=True).reshape(LENGTH, 256)  8.18 us
    pallas_call x1, Pallas kernels, finish(): pl.pallas_call(finish_body, in_specs=[pl.BlockSpec(memory_space=pltpu.SME...  7.89 us
  transfers between devices with their start and end apart: 26, of which 9 were waited for; matrix products, arithmetic and copies ran while one was open for 1% of the time, Pallas kernels for 32%

profile of v5, /device:TPU:0, one launch (start us, length us, event | category | flops | bytes accessed | tf_op | source)
XLA Modules:
  0.0 248.3 jit_solution(17633035745425738869)
XLA Ops:
  7.2 1.2 fusion.1
  8.4 0.8 copy.16
  9.2 0.7 pad_convert_fusion.kr_ref
  9.9 1.9 fusion.3.nlat_ref
  11.8 1.1 fusion.12
  12.9 4.8 %pack.1 = (bf16[16,192,256]{2,1,0:T(8,128)(2,1)}, bf16[16,192,128]{2,1,0:T(8,128)(2,1)}) custom-call(bf16[192,3072]{1,0:T(8,128)(2,1)} %bitcast.82, bf16[192,2048]{1,0:T(8,128)(2,1)} %bitcast.84, f32[192,128]{1,0:T(8,128)} %pad_convert_fusion.kr_ref, f32[192,128]{1,0:T(8,128)} %get-tuple-element.68.cos_ref, f32[192,128]{1,0:T(8,128)} %get-tuple-element.67.sin_ref), custom_call_target="tpu_custom_call" | custom-call | flops 2000000000 | bytes 5000000 | tf_op jit(solution)/shard_map/pack/pallas_call | solution.py:77
  17.8 0.1 pad_maximum_fusion
  17.9 0.1 fusion.34
  18.0 1.7 collective-permute-start.7
  19.7 8.2 %all-to-all-start.1 = ((bf16[16,192,256]{2,1,0:T(8,128)(2,1)}), bf16[16,192,256]{2,1,0:T(8,128)(2,1)S(1)}, u32[]{:S(2)}, u32[]{:S(2)}) async-start(bf16[16,192,256]{2,1,0:T(8,128)(2,1)} %get-tuple-element.26), calls=%async_computation.1 | async-start | bytes 3145728 | tf_op jit(solution)/shard_map/all_to_all | solution.py:381
  27.9 1.8 collective-permute-start.8
  29.7 1.8 collective-permute-start.9
  31.5 1.4 collective-permute-done.7.refs_1_
  32.9 18.7 %collective-permute-done.8.refs_2_ = bf16[256,1024]{1,0:T(8,128)(2,1)} collective-permute-done((bf16[256,1024]{1,0:T(8,128)(2,1)S(1)}, bf16[256,1024]{1,0:T(8,128)(2,1)}, u32[]{:S(2)}, u32[]{:S(2)}) %collective-permute-start.8) | collective-permute-done | bytes 524320 | tf_op jit(solution)/shard_map/ppermute | solution.py:324
  51.6 0.5 collective-permute-start.13
  52.1 2.4 collective-permute-start
  54.5 1.3 collective-permute-start.1
  55.9 1.5 collective-permute-start.2
  57.4 0.6 pad_add_fusion.order_ref
  58.0 6.8 %project.3 = (bf16[16,192,128]{2,1,0:T(8,128)(2,1)}, bf16[128,1024]{1,0:T(8,128)(2,1)}) custom-call(s32[9]{0:T(128)} %pad_add_fusion.order_ref, bf16[192,1024]{1,0:T(8,128)(2,1)} %fusion.3.nlat_ref, bf16[256,1024]{1,0:T(8,128)(2,1)} %bitcast.66, bf16[256,1024]{1,0:T(8,128)(2,1)} %copy-done.6, bf16[256,1024]{1,0:T(8,128)(2,1)} %collective-permute-done.8.refs_2_, ...), custom_call_target="tpu_custom_call" | custom-call | flops 2000000000 | bytes 6000000 | tf_op jit(solution)/shard_map/project/pallas_call | solution.py:239
  64.9 6.9 %all-to-all-start.2 = ((bf16[16,192,128]{2,1,0:T(8,128)(2,1)}), bf16[16,192,128]{2,1,0:T(8,128)(2,1)S(1)}, u32[]{:S(2)}, u32[]{:S(2)}) async-start(bf16[16,192,128]{2,1,0:T(8,128)(2,1)} %get-tuple-element.27), calls=%async_computation.2 | async-start | bytes 1572864 | tf_op jit(solution)/shard_map/all_to_all | solution.py:385
  71.7 0.1 collective-permute-start.3
  71.8 0.5 collective-permute-start.4
  72.3 0.1 collective-permute-start.5
  72.4 8.0 %collective-permute-done.2.refs_3_.refs_11_ = bf16[256,1024]{1,0:T(8,128)(2,1)} collective-permute-done((bf16[256,1024]{1,0:T(8,128)(2,1)S(1)}, bf16[256,1024]{1,0:T(8,128)(2,1)}, u32[]{:S(2)}, u32[]{:S(2)}) %collective-permute-start.2) | collective-permute-done | bytes 524320 | tf_op jit(solution)/shard_map/ppermute | solution.py:324
  80.5 2.2 collective-permute-done.6.refs_7_.refs_15_
  82.7 7.6 %project.2 = (bf16[16,192,256]{2,1,0:T(8,128)(2,1)}, bf16[128,1024]{1,0:T(8,128)(2,1)}) custom-call(s32[9]{0:T(128)} %pad_add_fusion.order_ref, bf16[192,1024]{1,0:T(8,128)(2,1)} %fusion.3.nlat_ref, bf16[256,1024]{1,0:T(8,128)(2,1)} %bitcast.72, bf16[256,1024]{1,0:T(8,128)(2,1)} %collective-permute-done.refs_1_.refs_9_, ...), custom_call_target="tpu_custom_call" | custom-call | flops 2000000000 | bytes 6000000 | tf_op jit(solution)/shard_map/project/pallas_call | solution.py:239
  90.3 5.0 %all-to-all-done.2 = bf16[16,192,128]{2,1,0:T(8,128)(2,1)S(1)} async-done(((bf16[16,192,128]{2,1,0:T(8,128)(2,1)}), bf16[16,192,128]{2,1,0:T(8,128)(2,1)S(1)}, u32[]{:S(2)}, u32[]{:S(2)}) %all-to-all-start.2) | async-done | bytes 786464 | tf_op jit(solution)/shard_map/all_to_all | solution.py:385
  95.3 0.9 copy-done
  96.2 3.9 %all-to-all-start = ((bf16[16,192,256]{2,1,0:T(8,128)(2,1)}), bf16[16,192,256]{2,1,0:T(8,128)(2,1)S(1)}, u32[]{:S(2)}, u32[]{:S(2)}) async-start(bf16[16,192,256]{2,1,0:T(8,128)(2,1)} %get-tuple-element.25), calls=%async_computation | async-start | bytes 3145728 | tf_op jit(solution)/shard_map/all_to_all | solution.py:387
  100.1 0.8 multiply_sine_fusion
  100.9 1.1 copy-done.1
  102.0 27.8 %shard_map.127 = bf16[3072,256]{1,0:T(8,128)(2,1)} custom-call(bf16[3072,256]{1,0:T(8,128)(2,1)S(1)} %bitcast.50, bf16[3072,256]{1,0:T(8,128)(2,1)S(1)} %bitcast.51, bf16[3072,128]{1,0:T(8,128)(2,1)S(1)} %bitcast.55, f32[16,3072]{1,0:T(8,128)S(1)} %get-tuple-element.64.cos_ref, f32[16,3072]{1,0:T(8,128)S(1)} %get-tuple-element.63.sin_ref), custom_call_target="tpu_custom_call" | custom-call | flops 12000000000 | bytes 6000000 | tf_op jit(solution)/shard_map/pallas_call | solution.py:190
  129.8 7.0 %all-to-all-start.3 = ((bf16[16,192,256]{2,1,0:T(8,128)(2,1)}), bf16[16,192,256]{2,1,0:T(8,128)(2,1)}, u32[]{:S(2)}, u32[]{:S(2)}) async-start(bf16[16,192,256]{2,1,0:T(8,128)(2,1)} %bitcast.13), calls=%async_computation.3 | async-start | bytes 3145728 | tf_op jit(solution)/shard_map/all_to_all | solution.py:392
  136.8 28.2 %shard_map.128 = bf16[3072,256]{1,0:T(8,128)(2,1)} custom-call(bf16[3072,256]{1,0:T(8,128)(2,1)S(1)} %bitcast.53, bf16[3072,256]{1,0:T(8,128)(2,1)S(1)} %bitcast.52, bf16[3072,256]{1,0:T(8,128)(2,1)S(1)} %bitcast.54, f32[16,3072]{1,0:T(8,128)S(1)} %get-tuple-element.64.cos_ref, f32[16,3072]{1,0:T(8,128)S(1)} %get-tuple-element.63.sin_ref), custom_call_target="tpu_custom_call" | custom-call | flops 12000000000 | bytes 6000000 | tf_op jit(solution)/shard_map/pallas_call | solution.py:190
  165.0 4.2 %fusion.6 = f32[128,1024]{1,0:T(8,128)S(1)} fusion(bf16[3072,1024]{1,0:T(8,128)(2,1)} %all-gather.2.cloned.1.call-done, bf16[3072,256]{1,0:T(8,128)(2,1)} %shard_map.127), kind=kOutput, calls=%fused_computation.11 | convolution fusion | flops 805306368 | bytes 7602176 | tf_op jit(solution)/shard_map/dot_general | solution.py:398
  169.2 0.6 copy-done.2
  169.8 2.2 fusion.4
  172.0 0.1 fusion
  172.1 0.8 copy-done.10
  172.9 0.1 copy-done.11
  173.0 0.2 multiply_reduce_fusion
  173.4 0.1 collective-permute-start.14
  173.5 7.2 %all-to-all-start.4 = ((bf16[16,192,256]{2,1,0:T(8,128)(2,1)}), bf16[16,192,256]{2,1,0:T(8,128)(2,1)S(1)}, u32[]{:S(2)}, u32[]{:S(2)}) async-start(bf16[16,192,256]{2,1,0:T(8,128)(2,1)} %bitcast.14), calls=%async_computation.4 | async-start | bytes 3145728 | tf_op jit(solution)/shard_map/all_to_all | solution.py:395
  180.7 0.1 convert_element_type.140
  180.9 0.1 slice_add_fusion
  181.1 2.0 collective-permute-start.17
  183.1 0.2 collective-permute-start.16
  183.3 2.1 collective-permute-start.15
  185.4 0.6 collective-permute-done.17
  186.1 5.0 %collective-permute-done.16 = bf16[48,1024]{1,0:T(8,128)(2,1)S(1)} collective-permute-done((bf16[48,1024]{1,0:T(8,128)(2,1)S(1)}, bf16[48,1024]{1,0:T(8,128)(2,1)S(1)}, u32[]{:S(2)}, u32[]{:S(2)}) %collective-permute-start.16) | collective-permute-done | bytes 98336 | tf_op jit(solution)/shard_map/ppermute | solution.py:324
  191.2 0.7 collective-permute-start.18
  191.9 15.0 %all-to-all-done.4.r1_ref = bf16[16,192,256]{2,1,0:T(8,128)(2,1)S(1)} async-done(((bf16[16,192,256]{2,1,0:T(8,128)(2,1)}), bf16[16,192,256]{2,1,0:T(8,128)(2,1)S(1)}, u32[]{:S(2)}, u32[]{:S(2)}) %all-to-all-start.4) | async-done | bytes 1572896 | tf_op jit(solution)/shard_map/all_to_all | solution.py:395
  207.0 1.5 broadcast_in_dim.40
  208.5 0.1 copy-done.3
  208.5 5.0 %all-to-all-start.5 = ((bf16[16,48,1024]{2,1,0:T(8,128)(2,1)}), bf16[16,48,1024]{2,1,0:T(8,128)(2,1)S(1)}, u32[]{:S(2)}, u32[]{:S(2)}) async-start(bf16[16,48,1024]{2,1,0:T(8,128)(2,1)} %broadcast_in_dim.40), calls=%async_computation.5 | async-start | bytes 3145728 | tf_op jit(solution)/shard_map/all_to_all | solution.py:320
  213.5 7.9 %finish.1 = (bf16[192,3072]{1,0:T(8,128)(2,1)}, f32[192,1024]{1,0:T(8,128)}, f32[192,32]{1,0:T(8,128)}) custom-call(s32[9]{0:T(128)} %pad_add_fusion.order_ref, bf16[16,192,256]{2,1,0:T(8,128)(2,1)} %all-to-all-done.3.r0_ref, bf16[16,192,256]{2,1,0:T(8,128)(2,1)} %copy-done.3, bf16[192,1024]{1,0:T(8,128)(2,1)} %bitcast.58, f32[1,1024]{1,0:T(1,128)} %bitcast.78, ...), custom_call_target="tpu_custom_call" | custom-call | flops 2000000000 | bytes 14000000 | tf_op jit(solution)/shard_map/finish/pallas_call | solution.py:296
  221.4 1.6 copy.18
  223.0 15.4 %all-to-all-done.5 = bf16[16,48,1024]{2,1,0:T(8,128)(2,1)S(1)} async-done(((bf16[16,48,1024]{2,1,0:T(8,128)(2,1)}), bf16[16,48,1024]{2,1,0:T(8,128)(2,1)S(1)}, u32[]{:S(2)}, u32[]{:S(2)}) %all-to-all-start.5) | async-done | bytes 1572896 | tf_op jit(solution)/shard_map/all_to_all | solution.py:320
  238.4 0.1 slice.94
  238.4 0.1 fusion.33
  238.6 1.1 bitcast_convert_fusion.1
  239.7 1.1 bitcast_convert_fusion
  240.8 0.7 convert_reduce_fusion
  (84 shorter events, 0.7 us)
Async XLA Ops:
  7.2 157.8 %all-gather.2.cloned.1.call-start = ((), (), s32[]{:S(2)}) async-start(), calls=%async_computation.6 | async-start | bytes 6684672 | tf_op jit(solution)/shard_map/all_gather | solution.py:384
  12.9 4.9 %copy-start.8 = (bf16[256,1024]{1,0:T(8,128)(2,1)S(1)}, bf16[256,1024]{1,0:T(8,128)(2,1)}, u32[]{:S(2)}) copy-start(bf16[256,1024]{1,0:T(8,128)(2,1)} %param.13) | copy-start | bytes 1572868
  12.9 4.9 %copy-start.9 = (bf16[256,1024]{1,0:T(8,128)(2,1)S(1)}, bf16[256,1024]{1,0:T(8,128)(2,1)}, u32[]{:S(2)}) copy-start(bf16[256,1024]{1,0:T(8,128)(2,1)} %param.12) | copy-start | bytes 1572868
  18.0 13.5 %copy-start.4 = (bf16[2,1,128,1024]{3,2,1,0:T(8,128)(2,1)}, bf16[2,1,128,1024]{3,2,1,0:T(8,128)(2,1)S(1)}, u32[]{:S(2)}) copy-start(bf16[2,1,128,1024]{3,2,1,0:T(8,128)(2,1)S(1)} %get-tuple-element.58) | copy-start | bytes 1572868
  18.0 53.7 %copy-start.5 = (bf16[2,1,128,1024]{3,2,1,0:T(8,128)(2,1)}, bf16[2,1,128,1024]{3,2,1,0:T(8,128)(2,1)S(1)}, u32[]{:S(2)}) copy-start(bf16[2,1,128,1024]{3,2,1,0:T(8,128)(2,1)S(1)} %get-tuple-element.59) | copy-start | bytes 1572868
  18.0 14.9 %collective-permute-start.7 = (bf16[256,1024]{1,0:T(8,128)(2,1)S(1)}, bf16[256,1024]{1,0:T(8,128)(2,1)S(1)}, u32[]{:S(2)}, u32[]{:S(2)}) collective-permute-start(bf16[256,1024]{1,0:T(8,128)(2,1)S(1)} %bitcast.62), channel_id=1, source_target_pairs={{0,2},{2,4},{4,6},{6,0},{1,3},{3,5},{5,7},{7,1},{8,10},{10,12},{12... | collective-permute-start | bytes 1572872 | tf_op jit(solution)/shard_map/ppermute | solution.py:324
  19.7 37.7 %copy-start.13 = (s32[4]{0:T(128)S(1)}, s32[4]{0:T(128)}, u32[]{:S(2)}) copy-start(s32[4]{0:T(128)} %constant.116.clone) | copy-start | bytes 52
  19.7 45.2 %all-to-all-start.1 = ((bf16[16,192,256]{2,1,0:T(8,128)(2,1)}), bf16[16,192,256]{2,1,0:T(8,128)(2,1)S(1)}, u32[]{:S(2)}, u32[]{:S(2)}) async-start(bf16[16,192,256]{2,1,0:T(8,128)(2,1)} %get-tuple-element.26), calls=%async_computation.1 | async-start | bytes 3145728 | tf_op jit(solution)/shard_map/all_to_all | solution.py:381
  27.9 23.7 %collective-permute-start.8 = (bf16[256,1024]{1,0:T(8,128)(2,1)S(1)}, bf16[256,1024]{1,0:T(8,128)(2,1)}, u32[]{:S(2)}, u32[]{:S(2)}) collective-permute-start(bf16[256,1024]{1,0:T(8,128)(2,1)S(1)} %bitcast.63), channel_id=1, source_target_pairs={{0,6},{2,0},{4,2},{6,4},{1,7},{3,1},{5,3},{7,5},{8,14},{10,8},{12,... | collective-permute-start | bytes 1572872 | tf_op jit(solution)/shard_map/ppermute | solution.py:324
  29.7 21.9 %collective-permute-start.9 = (bf16[256,1024]{1,0:T(8,128)(2,1)S(1)}, bf16[256,1024]{1,0:T(8,128)(2,1)}, u32[]{:S(2)}, u32[]{:S(2)}) collective-permute-start(bf16[256,1024]{1,0:T(8,128)(2,1)S(1)} %bitcast.64), channel_id=1, source_target_pairs={{0,4},{2,6},{4,0},{6,2},{1,5},{3,7},{5,1},{7,3},{8,12},{10,14},{12... | collective-permute-start | bytes 1572872 | tf_op jit(solution)/shard_map/ppermute | solution.py:324
  31.5 23.0 %collective-permute-start.10 = (bf16[256,1024]{1,0:T(8,128)(2,1)S(1)}, bf16[256,1024]{1,0:T(8,128)(2,1)}, u32[]{:S(2)}, u32[]{:S(2)}) collective-permute-start(bf16[256,1024]{1,0:T(8,128)(2,1)S(1)} %bitcast.65), channel_id=1, source_target_pairs={{0,1},{1,0},{2,3},{3,2},{4,5},{5,4},{6,7},{7,6},{8,9},{9,8},{10,11... | collective-permute-start | bytes 1572872 | tf_op jit(solution)/shard_map/ppermute | solution.py:332
  32.9 25.1 %copy-start.6 = (bf16[256,1024]{1,0:T(8,128)(2,1)}, bf16[256,1024]{1,0:T(8,128)(2,1)S(1)}, u32[]{:S(2)}) copy-start(bf16[256,1024]{1,0:T(8,128)(2,1)S(1)} %collective-permute-done.7.refs_1_) | copy-start | bytes 1572868
  32.9 23.0 %collective-permute-start.11 = (bf16[256,1024]{1,0:T(8,128)(2,1)S(1)}, bf16[256,1024]{1,0:T(8,128)(2,1)}, u32[]{:S(2)}, u32[]{:S(2)}) collective-permute-start(bf16[256,1024]{1,0:T(8,128)(2,1)S(1)} %collective-permute-done.7.refs_1_), channel_id=1, source_target_pairs={{0,1},{1,0},{2,3},{3,2},{4,5},{5,4},{6,7},{7,6},{8,9},{9,8},{10,11... | collective-permute-start | bytes 1572872 | tf_op jit(solution)/shard_map/ppermute | solution.py:332
  51.6 6.4 %collective-permute-start.12 = (bf16[256,1024]{1,0:T(8,128)(2,1)}, bf16[256,1024]{1,0:T(8,128)(2,1)}, u32[]{:S(2)}, u32[]{:S(2)}) collective-permute-start(bf16[256,1024]{1,0:T(8,128)(2,1)} %collective-permute-done.8.refs_2_), channel_id=1, source_target_pairs={{0,1},{1,0},{2,3},{3,2},{4,5},{5,4},{6,7},{7,6},{8,9},{9,8},{10,11... | collective-permute-start | bytes 1572872 | tf_op jit(solution)/shard_map/ppermute | solution.py:332
  51.6 6.4 %collective-permute-start.13 = (bf16[256,1024]{1,0:T(8,128)(2,1)}, bf16[256,1024]{1,0:T(8,128)(2,1)}, u32[]{:S(2)}, u32[]{:S(2)}) collective-permute-start(bf16[256,1024]{1,0:T(8,128)(2,1)} %collective-permute-done.9.refs_3_), channel_id=1, source_target_pairs={{0,1},{1,0},{2,3},{3,2},{4,5},{5,4},{6,7},{7,6},{8,9},{9,8},{10,11... | collective-permute-start | bytes 1572872 | tf_op jit(solution)/shard_map/ppermute | solution.py:332
  52.1 19.7 %collective-permute-start = (bf16[256,1024]{1,0:T(8,128)(2,1)S(1)}, bf16[256,1024]{1,0:T(8,128)(2,1)}, u32[]{:S(2)}, u32[]{:S(2)}) collective-permute-start(bf16[256,1024]{1,0:T(8,128)(2,1)S(1)} %bitcast.68), channel_id=1, source_target_pairs={{0,2},{2,4},{4,6},{6,0},{1,3},{3,5},{5,7},{7,1},{8,10},{10,12},{12... | collective-permute-start | bytes 1572872 | tf_op jit(solution)/shard_map/ppermute | solution.py:324
  54.5 17.8 %collective-permute-start.1 = (bf16[256,1024]{1,0:T(8,128)(2,1)S(1)}, bf16[256,1024]{1,0:T(8,128)(2,1)}, u32[]{:S(2)}, u32[]{:S(2)}) collective-permute-start(bf16[256,1024]{1,0:T(8,128)(2,1)S(1)} %bitcast.69), channel_id=1, source_target_pairs={{0,6},{2,0},{4,2},{6,4},{1,7},{3,1},{5,3},{7,5},{8,14},{10,8},{12,... | collective-permute-start | bytes 1572872 | tf_op jit(solution)/shard_map/ppermute | solution.py:324
  55.9 24.6 %collective-permute-start.2 = (bf16[256,1024]{1,0:T(8,128)(2,1)S(1)}, bf16[256,1024]{1,0:T(8,128)(2,1)}, u32[]{:S(2)}, u32[]{:S(2)}) collective-permute-start(bf16[256,1024]{1,0:T(8,128)(2,1)S(1)} %bitcast.70), channel_id=1, source_target_pairs={{0,4},{2,6},{4,0},{6,2},{1,5},{3,7},{5,1},{7,3},{8,12},{10,14},{12... | collective-permute-start | bytes 1572872 | tf_op jit(solution)/shard_map/ppermute | solution.py:324
  64.9 30.5 %all-to-all-start.2 = ((bf16[16,192,128]{2,1,0:T(8,128)(2,1)}), bf16[16,192,128]{2,1,0:T(8,128)(2,1)S(1)}, u32[]{:S(2)}, u32[]{:S(2)}) async-start(bf16[16,192,128]{2,1,0:T(8,128)(2,1)} %get-tuple-element.27), calls=%async_computation.2 | async-start | bytes 1572864 | tf_op jit(solution)/shard_map/all_to_all | solution.py:385
  71.7 8.8 %collective-permute-start.3 = (bf16[256,1024]{1,0:T(8,128)(2,1)S(1)}, bf16[256,1024]{1,0:T(8,128)(2,1)S(1)}, u32[]{:S(2)}, u32[]{:S(2)}) collective-permute-start(bf16[256,1024]{1,0:T(8,128)(2,1)S(1)} %bitcast.71), channel_id=1, source_target_pairs={{0,1},{1,0},{2,3},{3,2},{4,5},{5,4},{6,7},{7,6},{8,9},{9,8},{10,11... | collective-permute-start | bytes 1572872 | tf_op jit(solution)/shard_map/ppermute | solution.py:332
  71.8 8.7 %collective-permute-start.4 = (bf16[256,1024]{1,0:T(8,128)(2,1)}, bf16[256,1024]{1,0:T(8,128)(2,1)}, u32[]{:S(2)}, u32[]{:S(2)}) collective-permute-start(bf16[256,1024]{1,0:T(8,128)(2,1)} %collective-permute-done.refs_1_.refs_9_), channel_id=1, source_target_pairs={{0,1},{1,0},{2,3},{3,2},{4,5},{5,4},{6,7},{7,6},{8,9},{9,8},{10,11... | collective-permute-start | bytes 1572872 | tf_op jit(solution)/shard_map/ppermute | solution.py:332
  72.3 8.2 %collective-permute-start.5 = (bf16[256,1024]{1,0:T(8,128)(2,1)}, bf16[256,1024]{1,0:T(8,128)(2,1)}, u32[]{:S(2)}, u32[]{:S(2)}) collective-permute-start(bf16[256,1024]{1,0:T(8,128)(2,1)} %collective-permute-done.1.refs_2_.refs_10_), channel_id=1, source_target_pairs={{0,1},{1,0},{2,3},{3,2},{4,5},{5,4},{6,7},{7,6},{8,9},{9,8},{10,11... | collective-permute-start | bytes 1572872 | tf_op jit(solution)/shard_map/ppermute | solution.py:332
  80.5 2.3 collective-permute-start.6
  80.5 2.2 copy-start.7
  95.3 0.9 copy-start
  96.2 33.6 %all-to-all-start = ((bf16[16,192,256]{2,1,0:T(8,128)(2,1)}), bf16[16,192,256]{2,1,0:T(8,128)(2,1)S(1)}, u32[]{:S(2)}, u32[]{:S(2)}) async-start(bf16[16,192,256]{2,1,0:T(8,128)(2,1)} %get-tuple-element.25), calls=%async_computation | async-start | bytes 3145728 | tf_op jit(solution)/shard_map/all_to_all | solution.py:387
  100.8 1.1 copy-start.1
  129.8 35.2 %all-to-all-start.3 = ((bf16[16,192,256]{2,1,0:T(8,128)(2,1)}), bf16[16,192,256]{2,1,0:T(8,128)(2,1)}, u32[]{:S(2)}, u32[]{:S(2)}) async-start(bf16[16,192,256]{2,1,0:T(8,128)(2,1)} %bitcast.13), calls=%async_computation.3 | async-start | bytes 3145728 | tf_op jit(solution)/shard_map/all_to_all | solution.py:392
  165.0 4.8 %copy-start.2 = (bf16[3072,1024]{1,0:T(8,128)(2,1)S(1)}, bf16[3072,1024]{1,0:T(8,128)(2,1)}, u32[]{:S(2)}) copy-start(bf16[3072,1024]{1,0:T(8,128)(2,1)} %all-gather.2.cloned.1.call-done) | copy-start | bytes 18874372
  172.0 1.0 copy-start.10
  172.0 1.0 copy-start.11
  172.0 1.2 copy-start.12
  173.4 7.3 %collective-permute-start.14 = (bf16[5,32,1024]{2,1,0:T(8,128)(2,1)S(1)}, bf16[5,32,1024]{2,1,0:T(8,128)(2,1)S(1)}, u32[]{:S(2)}, u32[]{:S(2)}) collective-permute-start(bf16[5,32,1024]{2,1,0:T(8,128)(2,1)S(1)} %fusion.9), channel_id=1, source_target_pairs={{0,1},{1,0},{2,3},{3,2},{4,5},{5,4},{6,7},{7,6},{8,9},{9,8},{10,11... | collective-permute-start | bytes 983048 | tf_op jit(solution)/shard_map/ppermute | solution.py:346
  173.5 33.4 %all-to-all-start.4 = ((bf16[16,192,256]{2,1,0:T(8,128)(2,1)}), bf16[16,192,256]{2,1,0:T(8,128)(2,1)S(1)}, u32[]{:S(2)}, u32[]{:S(2)}) async-start(bf16[16,192,256]{2,1,0:T(8,128)(2,1)} %bitcast.14), calls=%async_computation.4 | async-start | bytes 3145728 | tf_op jit(solution)/shard_map/all_to_all | solution.py:395
  181.1 5.0 %collective-permute-start.17 = (bf16[48,1024]{1,0:T(8,128)(2,1)S(1)}, bf16[48,1024]{1,0:T(8,128)(2,1)S(1)}, u32[]{:S(2)}, u32[]{:S(2)}) collective-permute-start(bf16[48,1024]{1,0:T(8,128)(2,1)S(1)} %concatenate.42), channel_id=1, source_target_pairs={{0,6},{2,0},{4,2},{6,4},{1,7},{3,1},{5,3},{7,5},{8,14},{10,8},{12,... | collective-permute-start | bytes 294920 | tf_op jit(solution)/shard_map/ppermute | solution.py:324
  183.1 8.0 %collective-permute-start.16 = (bf16[48,1024]{1,0:T(8,128)(2,1)S(1)}, bf16[48,1024]{1,0:T(8,128)(2,1)S(1)}, u32[]{:S(2)}, u32[]{:S(2)}) collective-permute-start(bf16[48,1024]{1,0:T(8,128)(2,1)S(1)} %concatenate.41), channel_id=1, source_target_pairs={{0,2},{2,4},{4,6},{6,0},{1,3},{3,5},{5,7},{7,1},{8,10},{10,12},{12... | collective-permute-start | bytes 294920 | tf_op jit(solution)/shard_map/ppermute | solution.py:324
  183.3 7.8 %collective-permute-start.15 = (bf16[48,1024]{1,0:T(8,128)(2,1)S(1)}, bf16[48,1024]{1,0:T(8,128)(2,1)S(1)}, u32[]{:S(2)}, u32[]{:S(2)}) collective-permute-start(bf16[48,1024]{1,0:T(8,128)(2,1)S(1)} %concatenate.40), channel_id=1, source_target_pairs={{0,4},{2,6},{4,0},{6,2},{1,5},{3,7},{5,1},{7,3},{8,12},{10,14},{12... | collective-permute-start | bytes 294920 | tf_op jit(solution)/shard_map/ppermute | solution.py:324
  191.2 15.7 %collective-permute-start.18 = (bf16[32,1024]{1,0:T(8,128)(2,1)S(1)}, bf16[32,1024]{1,0:T(8,128)(2,1)S(1)}, u32[]{:S(2)}, u32[]{:S(2)}) collective-permute-start(bf16[32,1024]{1,0:T(8,128)(2,1)S(1)} %fusion.11), channel_id=1, source_target_pairs={{0,0},{16,1},{32,2},{48,3},{64,4},{80,5},{96,6},{112,7},{1,8},{17,... | collective-permute-start | bytes 196616 | tf_op jit(solution)/shard_map/ppermute | solution.py:406
  206.9 1.6 copy-start.3
  208.5 29.8 %all-to-all-start.5 = ((bf16[16,48,1024]{2,1,0:T(8,128)(2,1)}), bf16[16,48,1024]{2,1,0:T(8,128)(2,1)S(1)}, u32[]{:S(2)}, u32[]{:S(2)}) async-start(bf16[16,48,1024]{2,1,0:T(8,128)(2,1)} %broadcast_in_dim.40), calls=%async_computation.5 | async-start | bytes 3145728 | tf_op jit(solution)/shard_map/all_to_all | solution.py:320
Sparse Core Ops, SparseCore 0:
  17.9 83.4 all-gather.1

commit v6 on v5

--- a/solution.py
+++ b/solution.py
@@ -22,7 +22,7 @@
 NSP = 16
 NDP = 8
 TOKENS = LENGTH // NSP
-BLOCK = 512
+BLOCK = 768
 SCALE = WIDTH**-0.5
 LOG2E = 1.4426950408889634
 
@@ -100,9 +100,6 @@
         return carry
 
     lax.fori_loop(0, blocks, prepare, 0)
-    key_seg = lax.broadcasted_iota(jnp.int32, (BLOCK, BLOCK), 0) // SPAN
-    query_seg = lax.broadcasted_iota(jnp.int32, (BLOCK, BLOCK), 1) // SPAN
-    allowed = key_seg <= query_seg
 
     def one_block(i, carry):
         rows = pl.ds(pl.multiple_of(i * BLOCK, BLOCK), BLOCK)
@@ -120,23 +117,24 @@
         ).astype(bf16)
         right_d = jnp.where(lane < PLAIN, 0.0, qd).astype(bf16)
 
-        def gather_stats(j, stats, masked):
+        def gather_stats(keys, j, stats, masked, columns):
             top, total, inner = stats
-            keys = pl.ds(pl.multiple_of(j * BLOCK, BLOCK), BLOCK)
             kv = kv_ref[keys, :]
             both = jnp.concatenate([kv, rt_ref[keys, :]], axis=1)
-            scores = jnp.dot(both, left, preferred_element_type=f32) * factor
+            scores = jnp.dot(both, left[:, columns], preferred_element_type=f32) * factor
             if masked:
-                scores = jnp.where(allowed, scores, -jnp.inf)
-            d_probs = jnp.dot(kv, left_d, preferred_element_type=f32)
+                key_seg = lax.broadcasted_iota(jnp.int32, scores.shape, 0) // SPAN
+                query_seg = lax.broadcasted_iota(jnp.int32, scores.shape, 1) // SPAN
+                scores = jnp.where(key_seg <= query_seg, scores, -jnp.inf)
+            d_probs = jnp.dot(kv, left_d[:, columns], preferred_element_type=f32)
             new_top = jnp.maximum(top, jnp.max(scores, axis=0, keepdims=True))
             probs = jnp.exp2(scores - new_top)
             shrink = jnp.exp2(top - new_top)
             total = total * shrink + jnp.sum(probs, axis=0, keepdims=True)
             inner = inner * shrink + jnp.sum(probs * d_probs, axis=0, keepdims=True)
-            p_buf[keys, :] = probs
-            dp_buf[keys, :] = d_probs
-            m_buf[j] = jnp.broadcast_to(new_top, (8, BLOCK))
+            p_buf[keys, columns] = probs
+            dp_buf[keys, columns] = d_probs
+            m_buf[j, :, columns] = jnp.broadcast_to(new_top, (8, new_top.shape[1]))
             return new_top, total, inner
 
         start = (
@@ -144,24 +142,38 @@
             jnp.zeros((1, BLOCK), f32),
             jnp.zeros((1, BLOCK), f32),
         )
-        stats = lax.fori_loop(0, i, functools.partial(gather_stats, masked=False), start)
-        top, total, inner = gather_stats(i, stats, True)
+        half = BLOCK // 2
+        whole, after = slice(0, BLOCK), slice(half, BLOCK)
+
+        def plain_stats(j, stats):
+            return gather_stats(pl.ds(pl.multiple_of(j * BLOCK, BLOCK), BLOCK), j, stats, False, whole)
+
+        upper = pl.ds(pl.multiple_of(i * BLOCK, half), half)
+        lower = pl.ds(pl.multiple_of(i * BLOCK + half, half), half)
+        stats = lax.fori_loop(0, i, plain_stats, start)
+        stats = gather_stats(upper, i, stats, True, whole)
+        later = gather_stats(lower, blocks, [x[:, half:] for x in stats], True, after)
+        top, total, inner = [jnp.concatenate([x[:, :half], y], axis=1) for x, y in zip(stats, later)]
         inverse = 1.0 / total
         inner = inner * inverse
         dq_acc[...] = jnp.zeros((WIDTH, BLOCK), f32)
 
-        def gradients(j, carry):
-            keys = pl.ds(pl.multiple_of(j * BLOCK, BLOCK), BLOCK)
-            grow = jnp.exp2(m_buf[j][0:1] - top) * inverse
-            probs = p_buf[keys, :] * grow
-            ds = (probs * (dp_buf[keys, :] - inner)).astype(bf16)
+        def gradients(keys, j, columns):
+            grow = jnp.exp2(m_buf[j, 0:1, columns] - top[:, columns]) * inverse[:, columns]
+            probs = p_buf[keys, columns] * grow
+            ds = (probs * (dp_buf[keys, columns] - inner[:, columns])).astype(bf16)
             pb = probs.astype(bf16)
-            dq_acc[...] += jnp.dot(kt_buf[:, keys], ds, preferred_element_type=f32)
-            acc[keys, :] += jnp.dot(ds, right, preferred_element_type=f32)
-            acc[keys, 0:128] += jnp.dot(pb, right_d, preferred_element_type=f32)
+            dq_acc[:, columns] += jnp.dot(kt_buf[:, keys], ds, preferred_element_type=f32)
+            acc[keys, :] += jnp.dot(ds, right[columns], preferred_element_type=f32)
+            acc[keys, 0:128] += jnp.dot(pb, right_d[columns], preferred_element_type=f32)
+
+        def plain_gradients(j, carry):
+            gradients(pl.ds(pl.multiple_of(j * BLOCK, BLOCK), BLOCK), j, whole)
             return carry
 
-        lax.fori_loop(0, i + 1, gradients, 0)
+        lax.fori_loop(0, i, plain_gradients, 0)
+        gradients(upper, i, whole)
+        gradients(lower, blocks, after)
         dq = dq_acc[...] * SCALE
         cosine = cos_ref[:, rows]
         sine = sin_ref[:, rows]
@@ -202,12 +214,12 @@
         scratch_shapes=[
             pltpu.VMEM((LENGTH, BLOCK), f32),
             pltpu.VMEM((LENGTH, BLOCK), f32),
-            pltpu.VMEM((LENGTH // BLOCK, 8, BLOCK), f32),
+            pltpu.VMEM((LENGTH // BLOCK + 1, 8, BLOCK), f32),
             pltpu.VMEM((WIDTH, LENGTH), bf16),
             pltpu.VMEM((LENGTH, 256), f32),
             pltpu.VMEM((WIDTH, BLOCK), f32),
         ],
-        compiler_params=pltpu.CompilerParams(vmem_limit_bytes=48 * 1024 * 1024),
+        compiler_params=pltpu.CompilerParams(vmem_limit_bytes=60 * 1024 * 1024),
         cost_estimate=pl.CostEstimate(
             flops=12_000_000_000, bytes_accessed=6_000_000, transcendentals=5_000_000
         ),
@@ -334,7 +346,7 @@
 
 def as_rows(value):
     top = lax.reduce_precision(value, 8, 7)
-    return jnp.stack([top, lax.reduce_precision(value - top, 8, 7)] + [jnp.zeros_like(value)] * 14).astype(bf16)
+    return jnp.stack([top, lax.reduce_precision(value - top, 8, 7)] + [jnp.zeros_like(value)] * 6).astype(bf16)
 
 
 def reduce_over_rows(pieces, small):
@@ -342,7 +354,7 @@
     pairs = pieces.reshape(4, 2, *pieces.shape[1:])
     kept = lax.dynamic_index_in_dim(pairs, core, 1, keepdims=False)
     given = lax.dynamic_index_in_dim(pairs, 1 - core, 1, keepdims=False)
-    extra = jnp.pad(as_rows(small)[None], ((0, 0), (0, 16), (0, 0)))
+    extra = jnp.pad(as_rows(small)[None], ((0, 0), (0, 24), (0, 0)))
     got = lax.ppermute(jnp.concatenate([given, extra]), "dp_1", SWAP).astype(f32)
     small = small + (got[4, 0] + got[4, 1])
     kept = kept.astype(f32) + got[:4]

time: 249 us -> 239 us (0.960)
  Pallas kernels: 83.1 us -> 75.6 us
  waiting for transfers between devices: 71.4 us -> 67.8 us
    pallas_call x2, Pallas kernels: 56 us -> 48.5 us  [attend(): pl.pallas_call(functools.partial(attend_body, head), grid=(1,), in_specs=...]
    all_to_all x1, waiting for transfers between devices: 15.4 us -> 12 us  [everyone(): lax.all_to_all(jnp.broadcast_to(value[None], (size, *value.shape)), axes,...]
    unnamed x30 -> x36, local copies, waits for them, and re-layouts: 6.1 us -> 6.39 us
  transfers between devices with their start and end apart: 26 -> 26, of which waited for: 9 -> 9; matrix products, arithmetic and copies ran while one was open for 1% -> 2% of each run, Pallas kernels for 32% -> 30%
where the time goes in v6:
time: 239 us
  Pallas kernels  75.6 us (32%)
  waiting for transfers between devices  67.8 us (28%)
  starting transfers between devices  55 us (23%)
  between operations  14.6 us (6%)
  other arithmetic  10.6 us (4%)
  local copies, waits for them, and re-layouts  8.49 us (4%)
  matrix products  6.55 us (3%)
    pallas_call x2, Pallas kernels, attend(): pl.pallas_call(functools.partial(attend_body, head), grid=(1,), in_specs=...  48.5 us
    ppermute x9, waiting for transfers between devices, shifted(): return lax.ppermute(value, axis, [(i, (i + k) % 4) for i in range(4)])  33 us
    all_to_all x1, waiting for transfers between devices, program(): r1 = lax.all_to_all(g1.reshape(NSP, TOKENS, 256), SP, 0, 0, tiled=True)  15.5 us
    ppermute x9, starting transfers between devices, shifted(): return lax.ppermute(value, axis, [(i, (i + k) % 4) for i in range(4)])  15.1 us
    pallas_call x2, Pallas kernels, project(): pl.pallas_call(project_body, in_specs=[pl.BlockSpec(memory_space=pltpu.SM...  14.4 us
    all_to_all x1, waiting for transfers between devices, everyone(): lax.all_to_all(jnp.broadcast_to(value[None], (size, *value.shape)), axes,...  12 us
    all_to_all x1, starting transfers between devices, program(): first = lax.all_to_all(first, SP, 0, 0, tiled=True).reshape(LENGTH, 256)  8.18 us
    pallas_call x1, Pallas kernels, finish(): pl.pallas_call(finish_body, in_specs=[pl.BlockSpec(memory_space=pltpu.SME...  7.85 us
  transfers between devices with their start and end apart: 26, of which 9 were waited for; matrix products, arithmetic and copies ran while one was open for 2% of the time, Pallas kernels for 30%

profile of v6, /device:TPU:0, one launch (start us, length us, event | category | flops | bytes accessed | tf_op | source)
XLA Modules:
  0.0 238.6 jit_solution(14760303085105338765)
XLA Ops:
  7.2 1.2 fusion.1
  8.4 0.8 copy.16
  9.2 0.7 pad_convert_fusion.kr_ref
  9.9 1.9 fusion.3.nlat_ref
  11.8 1.1 fusion.12
  12.9 4.8 %pack.1 = (bf16[16,192,256]{2,1,0:T(8,128)(2,1)}, bf16[16,192,128]{2,1,0:T(8,128)(2,1)}) custom-call(bf16[192,3072]{1,0:T(8,128)(2,1)} %bitcast.83, bf16[192,2048]{1,0:T(8,128)(2,1)} %bitcast.85, f32[192,128]{1,0:T(8,128)} %pad_convert_fusion.kr_ref, f32[192,128]{1,0:T(8,128)} %get-tuple-element.68.cos_ref, f32[192,128]{1,0:T(8,128)} %get-tuple-element.67.sin_ref), custom_call_target="tpu_custom_call" | custom-call | flops 2000000000 | bytes 5000000 | tf_op jit(solution)/shard_map/pack/pallas_call | solution.py:77
  17.8 0.1 pad_maximum_fusion
  17.9 0.1 fusion.34
  18.0 1.7 collective-permute-start.7
  19.7 8.2 %all-to-all-start.1 = ((bf16[16,192,256]{2,1,0:T(8,128)(2,1)}), bf16[16,192,256]{2,1,0:T(8,128)(2,1)S(1)}, u32[]{:S(2)}, u32[]{:S(2)}) async-start(bf16[16,192,256]{2,1,0:T(8,128)(2,1)} %get-tuple-element.26), calls=%async_computation.1 | async-start | bytes 3145728 | tf_op jit(solution)/shard_map/all_to_all | solution.py:393
  27.9 1.8 collective-permute-start.8
  29.7 1.8 collective-permute-start.9
  31.5 1.4 collective-permute-done.7.refs_1_
  32.9 18.7 %collective-permute-done.8.refs_2_ = bf16[256,1024]{1,0:T(8,128)(2,1)} collective-permute-done((bf16[256,1024]{1,0:T(8,128)(2,1)S(1)}, bf16[256,1024]{1,0:T(8,128)(2,1)}, u32[]{:S(2)}, u32[]{:S(2)}) %collective-permute-start.8) | collective-permute-done | bytes 524320 | tf_op jit(solution)/shard_map/ppermute | solution.py:336
  51.6 0.5 collective-permute-start.13
  52.1 2.4 %collective-permute-start = (bf16[256,1024]{1,0:T(8,128)(2,1)S(1)}, bf16[256,1024]{1,0:T(8,128)(2,1)}, u32[]{:S(2)}, u32[]{:S(2)}) collective-permute-start(bf16[256,1024]{1,0:T(8,128)(2,1)S(1)} %bitcast.63), channel_id=1, source_target_pairs={{0,2},{2,4},{4,6},{6,0},{1,3},{3,5},{5,7},{7,1},{8,10},{10,12},{12... | collective-permute-start | bytes 1572872 | tf_op jit(solution)/shard_map/ppermute | solution.py:336
  54.5 1.3 collective-permute-start.1
  55.9 1.5 collective-permute-start.2
  57.5 0.6 pad_add_fusion.order_ref
  58.1 6.8 %project.3 = (bf16[16,192,128]{2,1,0:T(8,128)(2,1)}, bf16[128,1024]{1,0:T(8,128)(2,1)}) custom-call(s32[9]{0:T(128)} %pad_add_fusion.order_ref, bf16[192,1024]{1,0:T(8,128)(2,1)} %fusion.3.nlat_ref, bf16[256,1024]{1,0:T(8,128)(2,1)} %bitcast.61, bf16[256,1024]{1,0:T(8,128)(2,1)} %copy-done.9, bf16[256,1024]{1,0:T(8,128)(2,1)} %collective-permute-done.8.refs_2_, ...), custom_call_target="tpu_custom_call" | custom-call | flops 2000000000 | bytes 6000000 | tf_op jit(solution)/shard_map/project/pallas_call | solution.py:251
  64.9 6.9 %all-to-all-start.2 = ((bf16[16,192,128]{2,1,0:T(8,128)(2,1)}), bf16[16,192,128]{2,1,0:T(8,128)(2,1)S(1)}, u32[]{:S(2)}, u32[]{:S(2)}) async-start(bf16[16,192,128]{2,1,0:T(8,128)(2,1)} %get-tuple-element.27), calls=%async_computation.2 | async-start | bytes 1572864 | tf_op jit(solution)/shard_map/all_to_all | solution.py:397
  71.8 0.1 collective-permute-start.3
  71.9 0.5 collective-permute-start.4
  72.4 0.1 collective-permute-start.5
  72.5 8.0 %collective-permute-done.2.refs_3_.refs_11_ = bf16[256,1024]{1,0:T(8,128)(2,1)} collective-permute-done((bf16[256,1024]{1,0:T(8,128)(2,1)S(1)}, bf16[256,1024]{1,0:T(8,128)(2,1)}, u32[]{:S(2)}, u32[]{:S(2)}) %collective-permute-start.2) | collective-permute-done | bytes 524320 | tf_op jit(solution)/shard_map/ppermute | solution.py:336
  80.6 2.2 collective-permute-done.6.refs_7_.refs_15_
  82.8 7.6 %project.2 = (bf16[16,192,256]{2,1,0:T(8,128)(2,1)}, bf16[128,1024]{1,0:T(8,128)(2,1)}) custom-call(s32[9]{0:T(128)} %pad_add_fusion.order_ref, bf16[192,1024]{1,0:T(8,128)(2,1)} %fusion.3.nlat_ref, bf16[256,1024]{1,0:T(8,128)(2,1)} %bitcast.67, bf16[256,1024]{1,0:T(8,128)(2,1)} %collective-permute-done.refs_1_.refs_9_, ...), custom_call_target="tpu_custom_call" | custom-call | flops 2000000000 | bytes 6000000 | tf_op jit(solution)/shard_map/project/pallas_call | solution.py:251
  90.3 5.1 %all-to-all-done.2 = bf16[16,192,128]{2,1,0:T(8,128)(2,1)S(1)} async-done(((bf16[16,192,128]{2,1,0:T(8,128)(2,1)}), bf16[16,192,128]{2,1,0:T(8,128)(2,1)S(1)}, u32[]{:S(2)}, u32[]{:S(2)}) %all-to-all-start.2) | async-done | bytes 786464 | tf_op jit(solution)/shard_map/all_to_all | solution.py:397
  95.4 0.9 copy-done.8
  96.3 3.9 %all-to-all-start = ((bf16[16,192,256]{2,1,0:T(8,128)(2,1)}), bf16[16,192,256]{2,1,0:T(8,128)(2,1)S(1)}, u32[]{:S(2)}, u32[]{:S(2)}) async-start(bf16[16,192,256]{2,1,0:T(8,128)(2,1)} %get-tuple-element.25), calls=%async_computation | async-start | bytes 3145728 | tf_op jit(solution)/shard_map/all_to_all | solution.py:399
  100.2 1.5 multiply_sine_fusion
  101.7 24.2 %shard_map.127 = bf16[3072,256]{1,0:T(8,128)(2,1)} custom-call(bf16[3072,256]{1,0:T(8,128)(2,1)} %bitcast.69, bf16[3072,256]{1,0:T(8,128)(2,1)} %bitcast.70, bf16[3072,128]{1,0:T(8,128)(2,1)} %bitcast.74, f32[16,3072]{1,0:T(8,128)} %get-tuple-element.64.cos_ref, f32[16,3072]{1,0:T(8,128)} %get-tuple-element.63.sin_ref), custom_call_target="tpu_custom_call" | custom-call | flops 12000000000 | bytes 6000000 | tf_op jit(solution)/shard_map/pallas_call | solution.py:202
  125.8 1.2 copy-done.7
  127.1 7.0 %all-to-all-start.3 = ((bf16[16,192,256]{2,1,0:T(8,128)(2,1)}), bf16[16,192,256]{2,1,0:T(8,128)(2,1)S(1)}, u32[]{:S(2)}, u32[]{:S(2)}) async-start(bf16[16,192,256]{2,1,0:T(8,128)(2,1)} %bitcast.53), calls=%async_computation.3 | async-start | bytes 3145728 | tf_op jit(solution)/shard_map/all_to_all | solution.py:404
  134.1 0.1 pad.18.clone
  134.2 0.1 pad.17.clone
  134.2 24.3 %shard_map.128 = bf16[3072,256]{1,0:T(8,128)(2,1)} custom-call(bf16[3072,256]{1,0:T(8,128)(2,1)} %bitcast.72, bf16[3072,256]{1,0:T(8,128)(2,1)} %bitcast.71, bf16[3072,256]{1,0:T(8,128)(2,1)} %bitcast.73, f32[16,3072]{1,0:T(8,128)} %get-tuple-element.64.cos_ref, f32[16,3072]{1,0:T(8,128)} %get-tuple-element.63.sin_ref), custom_call_target="tpu_custom_call" | custom-call | flops 12000000000 | bytes 6000000 | tf_op jit(solution)/shard_map/pallas_call | solution.py:202
  158.6 4.4 %fusion.6 = f32[128,1024]{1,0:T(8,128)S(1)} fusion(bf16[3072,1024]{1,0:T(8,128)(2,1)} %all-gather.2.cloned.1.call-done, bf16[3072,256]{1,0:T(8,128)(2,1)S(1)} %copy-done.3), kind=kOutput, calls=%fused_computation.11 | convolution fusion | flops 805306368 | bytes 7602176 | tf_op jit(solution)/shard_map/dot_general | solution.py:410
  163.0 0.7 copy-done
  163.8 2.2 fusion.4
  166.0 0.8 copy-done.13
  166.9 0.1 copy-done.14
  167.0 0.2 multiply_reduce_fusion
  167.3 0.1 maximum_maximum_fusion
  167.4 0.1 collective-permute-start.14
  167.5 7.2 %all-to-all-start.4 = ((bf16[16,192,256]{2,1,0:T(8,128)(2,1)}), bf16[16,192,256]{2,1,0:T(8,128)(2,1)S(1)}, u32[]{:S(2)}, u32[]{:S(2)}) async-start(bf16[16,192,256]{2,1,0:T(8,128)(2,1)} %bitcast.14), calls=%async_computation.4 | async-start | bytes 3145728 | tf_op jit(solution)/shard_map/all_to_all | solution.py:407
  175.0 2.2 collective-permute-start.17
  177.3 0.2 collective-permute-start.16
  177.5 2.1 collective-permute-start.15
  179.6 0.3 collective-permute-done.17
  179.9 4.7 %collective-permute-done.16 = bf16[40,1024]{1,0:T(8,128)(2,1)S(1)} collective-permute-done((bf16[40,1024]{1,0:T(8,128)(2,1)S(1)}, bf16[40,1024]{1,0:T(8,128)(2,1)S(1)}, u32[]{:S(2)}, u32[]{:S(2)}) %collective-permute-start.16) | collective-permute-done | bytes 81952 | tf_op jit(solution)/shard_map/ppermute | solution.py:336
  184.7 0.7 collective-permute-start.18
  185.4 15.5 %all-to-all-done.4.r1_ref = bf16[16,192,256]{2,1,0:T(8,128)(2,1)S(1)} async-done(((bf16[16,192,256]{2,1,0:T(8,128)(2,1)}), bf16[16,192,256]{2,1,0:T(8,128)(2,1)S(1)}, u32[]{:S(2)}, u32[]{:S(2)}) %all-to-all-start.4) | async-done | bytes 1572896 | tf_op jit(solution)/shard_map/all_to_all | solution.py:407
  201.0 1.4 broadcast_in_dim.40
  202.3 0.1 copy-done.2
  202.5 4.8 %all-to-all-start.5 = ((bf16[16,40,1024]{2,1,0:T(8,128)(2,1)}), bf16[16,40,1024]{2,1,0:T(8,128)(2,1)S(1)}, u32[]{:S(2)}, u32[]{:S(2)}) async-start(bf16[16,40,1024]{2,1,0:T(8,128)(2,1)} %broadcast_in_dim.40), calls=%async_computation.5 | async-start | bytes 2621440 | tf_op jit(solution)/shard_map/all_to_all | solution.py:332
  207.3 7.8 %finish.1 = (bf16[192,3072]{1,0:T(8,128)(2,1)}, f32[192,1024]{1,0:T(8,128)}, f32[192,32]{1,0:T(8,128)}) custom-call(s32[9]{0:T(128)} %pad_add_fusion.order_ref, bf16[16,192,256]{2,1,0:T(8,128)(2,1)} %copy-done.1, bf16[16,192,256]{2,1,0:T(8,128)(2,1)} %copy-done.2, bf16[192,1024]{1,0:T(8,128)(2,1)} %bitcast.52, f32[1,1024]{1,0:T(1,128)} %bitcast.79, ...), custom_call_target="tpu_custom_call" | custom-call | flops 2000000000 | bytes 14000000 | tf_op jit(solution)/shard_map/finish/pallas_call | solution.py:308
  215.1 1.6 copy.18
  216.7 12.0 %all-to-all-done.5 = bf16[16,40,1024]{2,1,0:T(8,128)(2,1)S(1)} async-done(((bf16[16,40,1024]{2,1,0:T(8,128)(2,1)}), bf16[16,40,1024]{2,1,0:T(8,128)(2,1)S(1)}, u32[]{:S(2)}, u32[]{:S(2)}) %all-to-all-start.5) | async-done | bytes 1310752 | tf_op jit(solution)/shard_map/all_to_all | solution.py:332
  228.7 0.1 slice.94
  228.8 0.1 fusion.33
  228.9 1.1 bitcast_convert_fusion.1
  230.0 1.1 bitcast_convert_fusion
  231.1 0.7 convert_reduce_fusion
  (90 shorter events, 0.9 us)
Async XLA Ops:
  7.2 151.4 %all-gather.2.cloned.1.call-start = ((), (), s32[]{:S(2)}) async-start(), calls=%async_computation.6 | async-start | bytes 6684672 | tf_op jit(solution)/shard_map/all_gather | solution.py:396
  12.9 4.9 %copy-start.11 = (bf16[256,1024]{1,0:T(8,128)(2,1)S(1)}, bf16[256,1024]{1,0:T(8,128)(2,1)}, u32[]{:S(2)}) copy-start(bf16[256,1024]{1,0:T(8,128)(2,1)} %param.13) | copy-start | bytes 1572868
  12.9 4.9 %copy-start.12 = (bf16[256,1024]{1,0:T(8,128)(2,1)S(1)}, bf16[256,1024]{1,0:T(8,128)(2,1)}, u32[]{:S(2)}) copy-start(bf16[256,1024]{1,0:T(8,128)(2,1)} %param.12) | copy-start | bytes 1572868
  18.0 13.5 %copy-start.4 = (bf16[2,1,128,1024]{3,2,1,0:T(8,128)(2,1)}, bf16[2,1,128,1024]{3,2,1,0:T(8,128)(2,1)S(1)}, u32[]{:S(2)}) copy-start(bf16[2,1,128,1024]{3,2,1,0:T(8,128)(2,1)S(1)} %get-tuple-element.58) | copy-start | bytes 1572868
  18.0 53.8 %copy-start.5 = (bf16[2,1,128,1024]{3,2,1,0:T(8,128)(2,1)}, bf16[2,1,128,1024]{3,2,1,0:T(8,128)(2,1)S(1)}, u32[]{:S(2)}) copy-start(bf16[2,1,128,1024]{3,2,1,0:T(8,128)(2,1)S(1)} %get-tuple-element.59) | copy-start | bytes 1572868
  18.0 14.9 %collective-permute-start.7 = (bf16[256,1024]{1,0:T(8,128)(2,1)S(1)}, bf16[256,1024]{1,0:T(8,128)(2,1)S(1)}, u32[]{:S(2)}, u32[]{:S(2)}) collective-permute-start(bf16[256,1024]{1,0:T(8,128)(2,1)S(1)} %bitcast.57), channel_id=1, source_target_pairs={{0,2},{2,4},{4,6},{6,0},{1,3},{3,5},{5,7},{7,1},{8,10},{10,12},{12... | collective-permute-start | bytes 1572872 | tf_op jit(solution)/shard_map/ppermute | solution.py:336
  19.7 37.7 %copy-start.16 = (s32[4]{0:T(128)S(1)}, s32[4]{0:T(128)}, u32[]{:S(2)}) copy-start(s32[4]{0:T(128)} %constant.115.clone) | copy-start | bytes 52
  19.7 45.2 %all-to-all-start.1 = ((bf16[16,192,256]{2,1,0:T(8,128)(2,1)}), bf16[16,192,256]{2,1,0:T(8,128)(2,1)S(1)}, u32[]{:S(2)}, u32[]{:S(2)}) async-start(bf16[16,192,256]{2,1,0:T(8,128)(2,1)} %get-tuple-element.26), calls=%async_computation.1 | async-start | bytes 3145728 | tf_op jit(solution)/shard_map/all_to_all | solution.py:393
  27.9 23.7 %collective-permute-start.8 = (bf16[256,1024]{1,0:T(8,128)(2,1)S(1)}, bf16[256,1024]{1,0:T(8,128)(2,1)}, u32[]{:S(2)}, u32[]{:S(2)}) collective-permute-start(bf16[256,1024]{1,0:T(8,128)(2,1)S(1)} %bitcast.58), channel_id=1, source_target_pairs={{0,6},{2,0},{4,2},{6,4},{1,7},{3,1},{5,3},{7,5},{8,14},{10,8},{12,... | collective-permute-start | bytes 1572872 | tf_op jit(solution)/shard_map/ppermute | solution.py:336
  29.7 21.9 %collective-permute-start.9 = (bf16[256,1024]{1,0:T(8,128)(2,1)S(1)}, bf16[256,1024]{1,0:T(8,128)(2,1)}, u32[]{:S(2)}, u32[]{:S(2)}) collective-permute-start(bf16[256,1024]{1,0:T(8,128)(2,1)S(1)} %bitcast.59), channel_id=1, source_target_pairs={{0,4},{2,6},{4,0},{6,2},{1,5},{3,7},{5,1},{7,3},{8,12},{10,14},{12... | collective-permute-start | bytes 1572872 | tf_op jit(solution)/shard_map/ppermute | solution.py:336
  31.5 23.0 %collective-permute-start.10 = (bf16[256,1024]{1,0:T(8,128)(2,1)S(1)}, bf16[256,1024]{1,0:T(8,128)(2,1)}, u32[]{:S(2)}, u32[]{:S(2)}) collective-permute-start(bf16[256,1024]{1,0:T(8,128)(2,1)S(1)} %bitcast.60), channel_id=1, source_target_pairs={{0,1},{1,0},{2,3},{3,2},{4,5},{5,4},{6,7},{7,6},{8,9},{9,8},{10,11... | collective-permute-start | bytes 1572872 | tf_op jit(solution)/shard_map/ppermute | solution.py:344
  32.9 25.1 %copy-start.9 = (bf16[256,1024]{1,0:T(8,128)(2,1)}, bf16[256,1024]{1,0:T(8,128)(2,1)S(1)}, u32[]{:S(2)}) copy-start(bf16[256,1024]{1,0:T(8,128)(2,1)S(1)} %collective-permute-done.7.refs_1_) | copy-start | bytes 1572868
  32.9 23.0 %collective-permute-start.11 = (bf16[256,1024]{1,0:T(8,128)(2,1)S(1)}, bf16[256,1024]{1,0:T(8,128)(2,1)}, u32[]{:S(2)}, u32[]{:S(2)}) collective-permute-start(bf16[256,1024]{1,0:T(8,128)(2,1)S(1)} %collective-permute-done.7.refs_1_), channel_id=1, source_target_pairs={{0,1},{1,0},{2,3},{3,2},{4,5},{5,4},{6,7},{7,6},{8,9},{9,8},{10,11... | collective-permute-start | bytes 1572872 | tf_op jit(solution)/shard_map/ppermute | solution.py:344
  51.6 6.4 %collective-permute-start.12 = (bf16[256,1024]{1,0:T(8,128)(2,1)}, bf16[256,1024]{1,0:T(8,128)(2,1)}, u32[]{:S(2)}, u32[]{:S(2)}) collective-permute-start(bf16[256,1024]{1,0:T(8,128)(2,1)} %collective-permute-done.8.refs_2_), channel_id=1, source_target_pairs={{0,1},{1,0},{2,3},{3,2},{4,5},{5,4},{6,7},{7,6},{8,9},{9,8},{10,11... | collective-permute-start | bytes 1572872 | tf_op jit(solution)/shard_map/ppermute | solution.py:344
  51.6 6.4 %collective-permute-start.13 = (bf16[256,1024]{1,0:T(8,128)(2,1)}, bf16[256,1024]{1,0:T(8,128)(2,1)}, u32[]{:S(2)}, u32[]{:S(2)}) collective-permute-start(bf16[256,1024]{1,0:T(8,128)(2,1)} %collective-permute-done.9.refs_3_), channel_id=1, source_target_pairs={{0,1},{1,0},{2,3},{3,2},{4,5},{5,4},{6,7},{7,6},{8,9},{9,8},{10,11... | collective-permute-start | bytes 1572872 | tf_op jit(solution)/shard_map/ppermute | solution.py:344
  52.1 19.8 %collective-permute-start = (bf16[256,1024]{1,0:T(8,128)(2,1)S(1)}, bf16[256,1024]{1,0:T(8,128)(2,1)}, u32[]{:S(2)}, u32[]{:S(2)}) collective-permute-start(bf16[256,1024]{1,0:T(8,128)(2,1)S(1)} %bitcast.63), channel_id=1, source_target_pairs={{0,2},{2,4},{4,6},{6,0},{1,3},{3,5},{5,7},{7,1},{8,10},{10,12},{12... | collective-permute-start | bytes 1572872 | tf_op jit(solution)/shard_map/ppermute | solution.py:336
  54.5 17.8 %collective-permute-start.1 = (bf16[256,1024]{1,0:T(8,128)(2,1)S(1)}, bf16[256,1024]{1,0:T(8,128)(2,1)}, u32[]{:S(2)}, u32[]{:S(2)}) collective-permute-start(bf16[256,1024]{1,0:T(8,128)(2,1)S(1)} %bitcast.64), channel_id=1, source_target_pairs={{0,6},{2,0},{4,2},{6,4},{1,7},{3,1},{5,3},{7,5},{8,14},{10,8},{12,... | collective-permute-start | bytes 1572872 | tf_op jit(solution)/shard_map/ppermute | solution.py:336
  55.9 24.6 %collective-permute-start.2 = (bf16[256,1024]{1,0:T(8,128)(2,1)S(1)}, bf16[256,1024]{1,0:T(8,128)(2,1)}, u32[]{:S(2)}, u32[]{:S(2)}) collective-permute-start(bf16[256,1024]{1,0:T(8,128)(2,1)S(1)} %bitcast.65), channel_id=1, source_target_pairs={{0,4},{2,6},{4,0},{6,2},{1,5},{3,7},{5,1},{7,3},{8,12},{10,14},{12... | collective-permute-start | bytes 1572872 | tf_op jit(solution)/shard_map/ppermute | solution.py:336
  64.9 25.4 %copy-start.6 = (bf16[16,192,256]{2,1,0:T(8,128)(2,1)}, bf16[16,192,256]{2,1,0:T(8,128)(2,1)S(1)}, u32[]{:S(2)}) copy-start(bf16[16,192,256]{2,1,0:T(8,128)(2,1)S(1)} %all-to-all-done.1) | copy-start | bytes 4718596
  64.9 30.5 %all-to-all-start.2 = ((bf16[16,192,128]{2,1,0:T(8,128)(2,1)}), bf16[16,192,128]{2,1,0:T(8,128)(2,1)S(1)}, u32[]{:S(2)}, u32[]{:S(2)}) async-start(bf16[16,192,128]{2,1,0:T(8,128)(2,1)} %get-tuple-element.27), calls=%async_computation.2 | async-start | bytes 1572864 | tf_op jit(solution)/shard_map/all_to_all | solution.py:397
  71.8 8.7 %collective-permute-start.3 = (bf16[256,1024]{1,0:T(8,128)(2,1)S(1)}, bf16[256,1024]{1,0:T(8,128)(2,1)S(1)}, u32[]{:S(2)}, u32[]{:S(2)}) collective-permute-start(bf16[256,1024]{1,0:T(8,128)(2,1)S(1)} %bitcast.66), channel_id=1, source_target_pairs={{0,1},{1,0},{2,3},{3,2},{4,5},{5,4},{6,7},{7,6},{8,9},{9,8},{10,11... | collective-permute-start | bytes 1572872 | tf_op jit(solution)/shard_map/ppermute | solution.py:344
  71.9 8.6 %collective-permute-start.4 = (bf16[256,1024]{1,0:T(8,128)(2,1)}, bf16[256,1024]{1,0:T(8,128)(2,1)}, u32[]{:S(2)}, u32[]{:S(2)}) collective-permute-start(bf16[256,1024]{1,0:T(8,128)(2,1)} %collective-permute-done.refs_1_.refs_9_), channel_id=1, source_target_pairs={{0,1},{1,0},{2,3},{3,2},{4,5},{5,4},{6,7},{7,6},{8,9},{9,8},{10,11... | collective-permute-start | bytes 1572872 | tf_op jit(solution)/shard_map/ppermute | solution.py:344
  72.4 8.2 %collective-permute-start.5 = (bf16[256,1024]{1,0:T(8,128)(2,1)}, bf16[256,1024]{1,0:T(8,128)(2,1)}, u32[]{:S(2)}, u32[]{:S(2)}) collective-permute-start(bf16[256,1024]{1,0:T(8,128)(2,1)} %collective-permute-done.1.refs_2_.refs_10_), channel_id=1, source_target_pairs={{0,1},{1,0},{2,3},{3,2},{4,5},{5,4},{6,7},{7,6},{8,9},{9,8},{10,11... | collective-permute-start | bytes 1572872 | tf_op jit(solution)/shard_map/ppermute | solution.py:344
  80.5 2.3 collective-permute-start.6
  80.5 2.2 copy-start.10
  95.4 0.9 copy-start.8
  96.3 29.6 %all-to-all-start = ((bf16[16,192,256]{2,1,0:T(8,128)(2,1)}), bf16[16,192,256]{2,1,0:T(8,128)(2,1)S(1)}, u32[]{:S(2)}, u32[]{:S(2)}) async-start(bf16[16,192,256]{2,1,0:T(8,128)(2,1)} %get-tuple-element.25), calls=%async_computation | async-start | bytes 3145728 | tf_op jit(solution)/shard_map/all_to_all | solution.py:399
  125.8 1.2 copy-start.7
  127.1 31.5 %all-to-all-start.3 = ((bf16[16,192,256]{2,1,0:T(8,128)(2,1)}), bf16[16,192,256]{2,1,0:T(8,128)(2,1)S(1)}, u32[]{:S(2)}, u32[]{:S(2)}) async-start(bf16[16,192,256]{2,1,0:T(8,128)(2,1)} %bitcast.53), calls=%async_computation.3 | async-start | bytes 3145728 | tf_op jit(solution)/shard_map/all_to_all | solution.py:404
  134.2 24.4 %copy-start.3 = (bf16[3072,256]{1,0:T(8,128)(2,1)S(1)}, bf16[3072,256]{1,0:T(8,128)(2,1)}, u32[]{:S(2)}) copy-start(bf16[3072,256]{1,0:T(8,128)(2,1)} %shard_map.127) | copy-start | bytes 4718596
  158.6 4.4 %copy-start.1 = (bf16[16,192,256]{2,1,0:T(8,128)(2,1)}, bf16[16,192,256]{2,1,0:T(8,128)(2,1)S(1)}, u32[]{:S(2)}) copy-start(bf16[16,192,256]{2,1,0:T(8,128)(2,1)S(1)} %all-to-all-done.3.r0_ref) | copy-start | bytes 4718596
  158.6 5.2 %copy-start = (bf16[3072,1024]{1,0:T(8,128)(2,1)S(1)}, bf16[3072,1024]{1,0:T(8,128)(2,1)}, u32[]{:S(2)}) copy-start(bf16[3072,1024]{1,0:T(8,128)(2,1)} %all-gather.2.cloned.1.call-done) | copy-start | bytes 18874372
  165.9 1.0 copy-start.13
  165.9 1.0 copy-start.14
  165.9 1.2 copy-start.15
  167.4 7.3 %collective-permute-start.14 = (bf16[5,32,1024]{2,1,0:T(8,128)(2,1)S(1)}, bf16[5,32,1024]{2,1,0:T(8,128)(2,1)S(1)}, u32[]{:S(2)}, u32[]{:S(2)}) collective-permute-start(bf16[5,32,1024]{2,1,0:T(8,128)(2,1)S(1)} %fusion.9), channel_id=1, source_target_pairs={{0,1},{1,0},{2,3},{3,2},{4,5},{5,4},{6,7},{7,6},{8,9},{9,8},{10,11... | collective-permute-start | bytes 983048 | tf_op jit(solution)/shard_map/ppermute | solution.py:358
  167.5 33.4 %all-to-all-start.4 = ((bf16[16,192,256]{2,1,0:T(8,128)(2,1)}), bf16[16,192,256]{2,1,0:T(8,128)(2,1)S(1)}, u32[]{:S(2)}, u32[]{:S(2)}) async-start(bf16[16,192,256]{2,1,0:T(8,128)(2,1)} %bitcast.14), calls=%async_computation.4 | async-start | bytes 3145728 | tf_op jit(solution)/shard_map/all_to_all | solution.py:407
  175.0 4.8 %collective-permute-start.17 = (bf16[40,1024]{1,0:T(8,128)(2,1)S(1)}, bf16[40,1024]{1,0:T(8,128)(2,1)S(1)}, u32[]{:S(2)}, u32[]{:S(2)}) collective-permute-start(bf16[40,1024]{1,0:T(8,128)(2,1)S(1)} %concatenate.42), channel_id=1, source_target_pairs={{0,6},{2,0},{4,2},{6,4},{1,7},{3,1},{5,3},{7,5},{8,14},{10,8},{12,... | collective-permute-start | bytes 245768 | tf_op jit(solution)/shard_map/ppermute | solution.py:336
  177.3 7.3 %collective-permute-start.16 = (bf16[40,1024]{1,0:T(8,128)(2,1)S(1)}, bf16[40,1024]{1,0:T(8,128)(2,1)S(1)}, u32[]{:S(2)}, u32[]{:S(2)}) collective-permute-start(bf16[40,1024]{1,0:T(8,128)(2,1)S(1)} %concatenate.41), channel_id=1, source_target_pairs={{0,2},{2,4},{4,6},{6,0},{1,3},{3,5},{5,7},{7,1},{8,10},{10,12},{12... | collective-permute-start | bytes 245768 | tf_op jit(solution)/shard_map/ppermute | solution.py:336
  177.5 7.1 %collective-permute-start.15 = (bf16[40,1024]{1,0:T(8,128)(2,1)S(1)}, bf16[40,1024]{1,0:T(8,128)(2,1)S(1)}, u32[]{:S(2)}, u32[]{:S(2)}) collective-permute-start(bf16[40,1024]{1,0:T(8,128)(2,1)S(1)} %concatenate.40), channel_id=1, source_target_pairs={{0,4},{2,6},{4,0},{6,2},{1,5},{3,7},{5,1},{7,3},{8,12},{10,14},{12... | collective-permute-start | bytes 245768 | tf_op jit(solution)/shard_map/ppermute | solution.py:336
  184.7 16.3 %collective-permute-start.18 = (bf16[32,1024]{1,0:T(8,128)(2,1)S(1)}, bf16[32,1024]{1,0:T(8,128)(2,1)S(1)}, u32[]{:S(2)}, u32[]{:S(2)}) collective-permute-start(bf16[32,1024]{1,0:T(8,128)(2,1)S(1)} %fusion.11), channel_id=1, source_target_pairs={{0,0},{16,1},{32,2},{48,3},{64,4},{80,5},{96,6},{112,7},{1,8},{17,... | collective-permute-start | bytes 196616 | tf_op jit(solution)/shard_map/ppermute | solution.py:418
  200.9 1.6 copy-start.2
  202.5 26.2 %all-to-all-start.5 = ((bf16[16,40,1024]{2,1,0:T(8,128)(2,1)}), bf16[16,40,1024]{2,1,0:T(8,128)(2,1)S(1)}, u32[]{:S(2)}, u32[]{:S(2)}) async-start(bf16[16,40,1024]{2,1,0:T(8,128)(2,1)} %broadcast_in_dim.40), calls=%async_computation.5 | async-start | bytes 2621440 | tf_op jit(solution)/shard_map/all_to_all | solution.py:332
Sparse Core Ops, SparseCore 0:
  17.9 83.4 all-gather.1

commit v7 on v6

--- a/solution.py
+++ b/solution.py
@@ -62,15 +62,17 @@
         out_ref[slot, :, 128:256] = third.astype(bf16)
         other_ref[slot] = second.astype(bf16)
 
-    for pair in range(NSP // 2):
+    def one_pair(pair, carry):
         a0, a1, a2 = [
-            q_ref[:, 384 * pair + 128 * k : 384 * pair + 128 * (k + 1)].astype(f32) for k in range(3)
+            q_ref[:, pl.ds(pl.multiple_of(384 * pair + 128 * k, 128), 128)].astype(f32) for k in range(3)
         ]
-        g0 = g_ref[:, 256 * pair : 256 * pair + 128].astype(f32)
-        g1 = g_ref[:, 256 * pair + 128 : 256 * pair + 256].astype(f32)
+        g0, g1 = [g_ref[:, pl.ds(pl.multiple_of(256 * pair + 128 * k, 128), 128)].astype(f32) for k in range(2)]
         qn1 = jnp.where(lane < ROPE, pltpu.roll(a0, ROPE, 1), pltpu.roll(a1, ROPE, 1))
         emit(2 * pair, a0, pltpu.roll(a0, 64, 1), qn1, pltpu.roll(a1, 64, 1), g0)
         emit(2 * pair + 1, pltpu.roll(a1, 64, 1), a2, pltpu.roll(a2, 96, 1), a2, g1)
+        return carry
+
+    lax.fori_loop(0, NSP // 2, one_pair, 0)
 
 
 def pack(query, grads, key, cosine, sine):
@@ -219,7 +221,7 @@
             pltpu.VMEM((LENGTH, 256), f32),
             pltpu.VMEM((WIDTH, BLOCK), f32),
         ],
-        compiler_params=pltpu.CompilerParams(vmem_limit_bytes=60 * 1024 * 1024),
+        compiler_params=pltpu.CompilerParams(vmem_limit_bytes=36 * 1024 * 1024),
         cost_estimate=pl.CostEstimate(
             flops=12_000_000_000, bytes_accessed=6_000_000, transcendentals=5_000_000
         ),

time: 239 us -> 236 us (0.987)
  Pallas kernels: 75.6 us -> 73.2 us
    pallas_call x2, Pallas kernels: 48.5 us -> 45.5 us  [attend(): pl.pallas_call(functools.partial(attend_body, head), grid=(1,), in_specs=...]
    unnamed x36 -> x30, local copies, waits for them, and re-layouts: 6.39 us -> 6.13 us
  transfers between devices with their start and end apart: 26 -> 26, of which waited for: 9 -> 9; matrix products, arithmetic and copies ran while one was open for 2% -> 2% of each run, Pallas kernels for 30% -> 29%
where the time goes in v7:
time: 236 us; the launch traced here: 235 us
  Pallas kernels  73.2 us (31%)
  waiting for transfers between devices  67.9 us (29%)
  starting transfers between devices  55 us (23%)
  between operations  14.6 us (6%)
  other arithmetic  9.83 us (4%)
  local copies, waits for them, and re-layouts  8.24 us (3%)
  matrix products  6.35 us (3%)
    pallas_call x2, Pallas kernels, attend(): pl.pallas_call(functools.partial(attend_body, head), grid=(1,), in_specs=...  45.5 us
    ppermute x9, waiting for transfers between devices, shifted(): return lax.ppermute(value, axis, [(i, (i + k) % 4) for i in range(4)])  33.1 us
    all_to_all x1, waiting for transfers between devices, program(): r1 = lax.all_to_all(g1.reshape(NSP, TOKENS, 256), SP, 0, 0, tiled=True)  15.7 us
    ppermute x9, starting transfers between devices, shifted(): return lax.ppermute(value, axis, [(i, (i + k) % 4) for i in range(4)])  14.9 us
    pallas_call x2, Pallas kernels, project(): pl.pallas_call(project_body, in_specs=[pl.BlockSpec(memory_space=pltpu.SM...  14.4 us
    all_to_all x1, waiting for transfers between devices, everyone(): lax.all_to_all(jnp.broadcast_to(value[None], (size, *value.shape)), axes,...  11.9 us
    all_to_all x1, starting transfers between devices, program(): first = lax.all_to_all(first, SP, 0, 0, tiled=True).reshape(LENGTH, 256)  8.18 us
    pallas_call x1, Pallas kernels, finish(): pl.pallas_call(finish_body, in_specs=[pl.BlockSpec(memory_space=pltpu.SME...  7.9 us
  transfers between devices with their start and end apart: 26, of which 9 were waited for; matrix products, arithmetic and copies ran while one was open for 2% of the time, Pallas kernels for 29%

profile of v7, /device:TPU:0, one launch (start us, length us, event | category | flops | bytes accessed | tf_op | source)
XLA Modules:
  0.0 235.1 jit_solution(6464603118381164676)
XLA Ops:
  7.2 1.2 fusion.1
  8.4 0.8 copy.16
  9.2 0.7 pad_convert_fusion.kr_ref
  9.9 1.9 fusion.3.nlat_ref
  11.8 1.1 fusion.12
  12.9 5.5 %pack.1 = (bf16[16,192,256]{2,1,0:T(8,128)(2,1)}, bf16[16,192,128]{2,1,0:T(8,128)(2,1)}) custom-call(bf16[192,3072]{1,0:T(8,128)(2,1)} %bitcast.82, bf16[192,2048]{1,0:T(8,128)(2,1)} %bitcast.84, f32[192,128]{1,0:T(8,128)} %pad_convert_fusion.kr_ref, f32[192,128]{1,0:T(8,128)} %get-tuple-element.68.cos_ref, f32[192,128]{1,0:T(8,128)} %get-tuple-element.67.sin_ref), custom_call_target="tpu_custom_call" | custom-call | flops 2000000000 | bytes 5000000 | tf_op jit(solution)/shard_map/pack/pallas_call | solution.py:79
  18.4 0.1 pad_maximum_fusion
  18.5 0.1 fusion.34
  18.6 1.7 collective-permute-start.7
  20.3 8.2 %all-to-all-start.1 = ((bf16[16,192,256]{2,1,0:T(8,128)(2,1)}), bf16[16,192,256]{2,1,0:T(8,128)(2,1)S(1)}, u32[]{:S(2)}, u32[]{:S(2)}) async-start(bf16[16,192,256]{2,1,0:T(8,128)(2,1)} %get-tuple-element.26), calls=%async_computation.1 | async-start | bytes 3145728 | tf_op jit(solution)/shard_map/all_to_all | solution.py:395
  28.5 1.8 collective-permute-start.8
  30.3 1.8 collective-permute-start.9
  32.1 1.4 collective-permute-done.7.refs_1_
  33.5 18.7 %collective-permute-done.8.refs_2_ = bf16[256,1024]{1,0:T(8,128)(2,1)} collective-permute-done((bf16[256,1024]{1,0:T(8,128)(2,1)S(1)}, bf16[256,1024]{1,0:T(8,128)(2,1)}, u32[]{:S(2)}, u32[]{:S(2)}) %collective-permute-start.8) | collective-permute-done | bytes 524320 | tf_op jit(solution)/shard_map/ppermute | solution.py:338
  52.2 0.5 collective-permute-start.13
  52.7 2.4 %collective-permute-start = (bf16[256,1024]{1,0:T(8,128)(2,1)S(1)}, bf16[256,1024]{1,0:T(8,128)(2,1)}, u32[]{:S(2)}, u32[]{:S(2)}) collective-permute-start(bf16[256,1024]{1,0:T(8,128)(2,1)S(1)} %bitcast.68), channel_id=1, source_target_pairs={{0,2},{2,4},{4,6},{6,0},{1,3},{3,5},{5,7},{7,1},{8,10},{10,12},{12... | collective-permute-start | bytes 1572872 | tf_op jit(solution)/shard_map/ppermute | solution.py:338
  55.1 1.3 collective-permute-start.1
  56.5 1.5 collective-permute-start.2
  58.0 0.6 pad_add_fusion.order_ref
  58.6 6.8 %project.3 = (bf16[16,192,128]{2,1,0:T(8,128)(2,1)}, bf16[128,1024]{1,0:T(8,128)(2,1)}) custom-call(s32[9]{0:T(128)} %pad_add_fusion.order_ref, bf16[192,1024]{1,0:T(8,128)(2,1)} %fusion.3.nlat_ref, bf16[256,1024]{1,0:T(8,128)(2,1)} %bitcast.66, bf16[256,1024]{1,0:T(8,128)(2,1)} %copy-done.6, bf16[256,1024]{1,0:T(8,128)(2,1)} %collective-permute-done.8.refs_2_, ...), custom_call_target="tpu_custom_call" | custom-call | flops 2000000000 | bytes 6000000 | tf_op jit(solution)/shard_map/project/pallas_call | solution.py:253
  65.5 6.9 %all-to-all-start.2 = ((bf16[16,192,128]{2,1,0:T(8,128)(2,1)}), bf16[16,192,128]{2,1,0:T(8,128)(2,1)S(1)}, u32[]{:S(2)}, u32[]{:S(2)}) async-start(bf16[16,192,128]{2,1,0:T(8,128)(2,1)} %get-tuple-element.27), calls=%async_computation.2 | async-start | bytes 1572864 | tf_op jit(solution)/shard_map/all_to_all | solution.py:399
  72.3 0.1 collective-permute-start.3
  72.5 0.5 collective-permute-start.4
  72.9 0.1 collective-permute-start.5
  73.0 8.0 %collective-permute-done.2.refs_3_.refs_11_ = bf16[256,1024]{1,0:T(8,128)(2,1)} collective-permute-done((bf16[256,1024]{1,0:T(8,128)(2,1)S(1)}, bf16[256,1024]{1,0:T(8,128)(2,1)}, u32[]{:S(2)}, u32[]{:S(2)}) %collective-permute-start.2) | collective-permute-done | bytes 524320 | tf_op jit(solution)/shard_map/ppermute | solution.py:338
  81.1 2.2 collective-permute-done.6.refs_7_.refs_15_
  83.3 7.6 %project.2 = (bf16[16,192,256]{2,1,0:T(8,128)(2,1)}, bf16[128,1024]{1,0:T(8,128)(2,1)}) custom-call(s32[9]{0:T(128)} %pad_add_fusion.order_ref, bf16[192,1024]{1,0:T(8,128)(2,1)} %fusion.3.nlat_ref, bf16[256,1024]{1,0:T(8,128)(2,1)} %bitcast.72, bf16[256,1024]{1,0:T(8,128)(2,1)} %collective-permute-done.refs_1_.refs_9_, ...), custom_call_target="tpu_custom_call" | custom-call | flops 2000000000 | bytes 6000000 | tf_op jit(solution)/shard_map/project/pallas_call | solution.py:253
  90.9 5.0 %all-to-all-done.2 = bf16[16,192,128]{2,1,0:T(8,128)(2,1)S(1)} async-done(((bf16[16,192,128]{2,1,0:T(8,128)(2,1)}), bf16[16,192,128]{2,1,0:T(8,128)(2,1)S(1)}, u32[]{:S(2)}, u32[]{:S(2)}) %all-to-all-start.2) | async-done | bytes 786464 | tf_op jit(solution)/shard_map/all_to_all | solution.py:399
  95.9 0.9 copy-done
  96.8 3.9 %all-to-all-start = ((bf16[16,192,256]{2,1,0:T(8,128)(2,1)}), bf16[16,192,256]{2,1,0:T(8,128)(2,1)S(1)}, u32[]{:S(2)}, u32[]{:S(2)}) async-start(bf16[16,192,256]{2,1,0:T(8,128)(2,1)} %get-tuple-element.25), calls=%async_computation | async-start | bytes 3145728 | tf_op jit(solution)/shard_map/all_to_all | solution.py:401
  100.7 0.8 multiply_sine_fusion
  101.5 1.1 copy-done.1
  102.6 22.5 %shard_map.127 = bf16[3072,256]{1,0:T(8,128)(2,1)} custom-call(bf16[3072,256]{1,0:T(8,128)(2,1)S(1)} %bitcast.50, bf16[3072,256]{1,0:T(8,128)(2,1)S(1)} %bitcast.51, bf16[3072,128]{1,0:T(8,128)(2,1)S(1)} %bitcast.55, f32[16,3072]{1,0:T(8,128)S(1)} %get-tuple-element.64.cos_ref, f32[16,3072]{1,0:T(8,128)S(1)} %get-tuple-element.63.sin_ref), custom_call_target="tpu_custom_call" | custom-call | flops 12000000000 | bytes 6000000 | tf_op jit(solution)/shard_map/pallas_call | solution.py:204
  125.1 7.0 %all-to-all-start.3 = ((bf16[16,192,256]{2,1,0:T(8,128)(2,1)}), bf16[16,192,256]{2,1,0:T(8,128)(2,1)}, u32[]{:S(2)}, u32[]{:S(2)}) async-start(bf16[16,192,256]{2,1,0:T(8,128)(2,1)} %bitcast.13), calls=%async_computation.3 | async-start | bytes 3145728 | tf_op jit(solution)/shard_map/all_to_all | solution.py:406
  132.1 0.1 pad.18.clone
  132.2 0.1 pad.17.clone
  132.3 22.9 %shard_map.128 = bf16[3072,256]{1,0:T(8,128)(2,1)} custom-call(bf16[3072,256]{1,0:T(8,128)(2,1)S(1)} %bitcast.53, bf16[3072,256]{1,0:T(8,128)(2,1)S(1)} %bitcast.52, bf16[3072,256]{1,0:T(8,128)(2,1)S(1)} %bitcast.54, f32[16,3072]{1,0:T(8,128)S(1)} %get-tuple-element.64.cos_ref, f32[16,3072]{1,0:T(8,128)S(1)} %get-tuple-element.63.sin_ref), custom_call_target="tpu_custom_call" | custom-call | flops 12000000000 | bytes 6000000 | tf_op jit(solution)/shard_map/pallas_call | solution.py:204
  155.3 4.2 %fusion.6 = f32[128,1024]{1,0:T(8,128)S(1)} fusion(bf16[3072,1024]{1,0:T(8,128)(2,1)} %all-gather.2.cloned.1.call-done, bf16[3072,256]{1,0:T(8,128)(2,1)} %shard_map.127), kind=kOutput, calls=%fused_computation.11 | convolution fusion | flops 805306368 | bytes 7602176 | tf_op jit(solution)/shard_map/dot_general | solution.py:412
  159.4 0.6 copy-done.2
  160.1 2.2 fusion.4
  162.4 0.8 copy-done.10
  163.2 0.1 copy-done.11
  163.3 0.2 multiply_reduce_fusion
  163.6 0.1 maximum_maximum_fusion
  163.7 0.1 collective-permute-start.14
  163.8 7.4 %all-to-all-start.4 = ((bf16[16,192,256]{2,1,0:T(8,128)(2,1)}), bf16[16,192,256]{2,1,0:T(8,128)(2,1)S(1)}, u32[]{:S(2)}, u32[]{:S(2)}) async-start(bf16[16,192,256]{2,1,0:T(8,128)(2,1)} %bitcast.14), calls=%async_computation.4 | async-start | bytes 3145728 | tf_op jit(solution)/shard_map/all_to_all | solution.py:409
  171.5 2.0 collective-permute-start.17
  173.6 0.2 collective-permute-start.16
  173.8 2.1 collective-permute-start.15
  175.9 0.3 collective-permute-done.17
  176.2 4.7 %collective-permute-done.16 = bf16[40,1024]{1,0:T(8,128)(2,1)S(1)} collective-permute-done((bf16[40,1024]{1,0:T(8,128)(2,1)S(1)}, bf16[40,1024]{1,0:T(8,128)(2,1)S(1)}, u32[]{:S(2)}, u32[]{:S(2)}) %collective-permute-start.16) | collective-permute-done | bytes 81952 | tf_op jit(solution)/shard_map/ppermute | solution.py:338
  181.0 0.7 collective-permute-start.18
  181.7 15.7 %all-to-all-done.4.r1_ref = bf16[16,192,256]{2,1,0:T(8,128)(2,1)S(1)} async-done(((bf16[16,192,256]{2,1,0:T(8,128)(2,1)}), bf16[16,192,256]{2,1,0:T(8,128)(2,1)S(1)}, u32[]{:S(2)}, u32[]{:S(2)}) %all-to-all-start.4) | async-done | bytes 1572896 | tf_op jit(solution)/shard_map/all_to_all | solution.py:409
  197.5 1.4 broadcast_in_dim.40
  198.9 0.1 copy-done.3
  199.0 4.8 %all-to-all-start.5 = ((bf16[16,40,1024]{2,1,0:T(8,128)(2,1)}), bf16[16,40,1024]{2,1,0:T(8,128)(2,1)S(1)}, u32[]{:S(2)}, u32[]{:S(2)}) async-start(bf16[16,40,1024]{2,1,0:T(8,128)(2,1)} %broadcast_in_dim.40), calls=%async_computation.5 | async-start | bytes 2621440 | tf_op jit(solution)/shard_map/all_to_all | solution.py:334
  203.8 7.9 %finish.1 = (bf16[192,3072]{1,0:T(8,128)(2,1)}, f32[192,1024]{1,0:T(8,128)}, f32[192,32]{1,0:T(8,128)}) custom-call(s32[9]{0:T(128)} %pad_add_fusion.order_ref, bf16[16,192,256]{2,1,0:T(8,128)(2,1)} %all-to-all-done.3.r0_ref, bf16[16,192,256]{2,1,0:T(8,128)(2,1)} %copy-done.3, bf16[192,1024]{1,0:T(8,128)(2,1)} %bitcast.58, f32[1,1024]{1,0:T(1,128)} %bitcast.78, ...), custom_call_target="tpu_custom_call" | custom-call | flops 2000000000 | bytes 14000000 | tf_op jit(solution)/shard_map/finish/pallas_call | solution.py:310
  211.7 1.6 copy.18
  213.3 11.9 %all-to-all-done.5 = bf16[16,40,1024]{2,1,0:T(8,128)(2,1)S(1)} async-done(((bf16[16,40,1024]{2,1,0:T(8,128)(2,1)}), bf16[16,40,1024]{2,1,0:T(8,128)(2,1)S(1)}, u32[]{:S(2)}, u32[]{:S(2)}) %all-to-all-start.5) | async-done | bytes 1310752 | tf_op jit(solution)/shard_map/all_to_all | solution.py:334
  225.2 0.1 slice.94
  225.3 0.1 fusion.33
  225.4 1.1 bitcast_convert_fusion.1
  226.5 1.1 bitcast_convert_fusion
  227.6 0.7 convert_reduce_fusion
  (84 shorter events, 0.9 us)
Async XLA Ops:
  7.2 148.1 %all-gather.2.cloned.1.call-start = ((), (), s32[]{:S(2)}) async-start(), calls=%async_computation.6 | async-start | bytes 6684672 | tf_op jit(solution)/shard_map/all_gather | solution.py:398
  12.9 5.5 %copy-start.8 = (bf16[256,1024]{1,0:T(8,128)(2,1)S(1)}, bf16[256,1024]{1,0:T(8,128)(2,1)}, u32[]{:S(2)}) copy-start(bf16[256,1024]{1,0:T(8,128)(2,1)} %param.13) | copy-start | bytes 1572868
  12.9 5.5 %copy-start.9 = (bf16[256,1024]{1,0:T(8,128)(2,1)S(1)}, bf16[256,1024]{1,0:T(8,128)(2,1)}, u32[]{:S(2)}) copy-start(bf16[256,1024]{1,0:T(8,128)(2,1)} %param.12) | copy-start | bytes 1572868
  18.6 13.5 %copy-start.4 = (bf16[2,1,128,1024]{3,2,1,0:T(8,128)(2,1)}, bf16[2,1,128,1024]{3,2,1,0:T(8,128)(2,1)S(1)}, u32[]{:S(2)}) copy-start(bf16[2,1,128,1024]{3,2,1,0:T(8,128)(2,1)S(1)} %get-tuple-element.58) | copy-start | bytes 1572868
  18.6 53.7 %copy-start.5 = (bf16[2,1,128,1024]{3,2,1,0:T(8,128)(2,1)}, bf16[2,1,128,1024]{3,2,1,0:T(8,128)(2,1)S(1)}, u32[]{:S(2)}) copy-start(bf16[2,1,128,1024]{3,2,1,0:T(8,128)(2,1)S(1)} %get-tuple-element.59) | copy-start | bytes 1572868
  18.6 14.9 %collective-permute-start.7 = (bf16[256,1024]{1,0:T(8,128)(2,1)S(1)}, bf16[256,1024]{1,0:T(8,128)(2,1)S(1)}, u32[]{:S(2)}, u32[]{:S(2)}) collective-permute-start(bf16[256,1024]{1,0:T(8,128)(2,1)S(1)} %bitcast.62), channel_id=1, source_target_pairs={{0,2},{2,4},{4,6},{6,0},{1,3},{3,5},{5,7},{7,1},{8,10},{10,12},{12... | collective-permute-start | bytes 1572872 | tf_op jit(solution)/shard_map/ppermute | solution.py:338
  20.3 37.7 %copy-start.13 = (s32[4]{0:T(128)S(1)}, s32[4]{0:T(128)}, u32[]{:S(2)}) copy-start(s32[4]{0:T(128)} %constant.115.clone) | copy-start | bytes 52
  20.3 45.2 %all-to-all-start.1 = ((bf16[16,192,256]{2,1,0:T(8,128)(2,1)}), bf16[16,192,256]{2,1,0:T(8,128)(2,1)S(1)}, u32[]{:S(2)}, u32[]{:S(2)}) async-start(bf16[16,192,256]{2,1,0:T(8,128)(2,1)} %get-tuple-element.26), calls=%async_computation.1 | async-start | bytes 3145728 | tf_op jit(solution)/shard_map/all_to_all | solution.py:395
  28.5 23.7 %collective-permute-start.8 = (bf16[256,1024]{1,0:T(8,128)(2,1)S(1)}, bf16[256,1024]{1,0:T(8,128)(2,1)}, u32[]{:S(2)}, u32[]{:S(2)}) collective-permute-start(bf16[256,1024]{1,0:T(8,128)(2,1)S(1)} %bitcast.63), channel_id=1, source_target_pairs={{0,6},{2,0},{4,2},{6,4},{1,7},{3,1},{5,3},{7,5},{8,14},{10,8},{12,... | collective-permute-start | bytes 1572872 | tf_op jit(solution)/shard_map/ppermute | solution.py:338
  30.3 21.9 %collective-permute-start.9 = (bf16[256,1024]{1,0:T(8,128)(2,1)S(1)}, bf16[256,1024]{1,0:T(8,128)(2,1)}, u32[]{:S(2)}, u32[]{:S(2)}) collective-permute-start(bf16[256,1024]{1,0:T(8,128)(2,1)S(1)} %bitcast.64), channel_id=1, source_target_pairs={{0,4},{2,6},{4,0},{6,2},{1,5},{3,7},{5,1},{7,3},{8,12},{10,14},{12... | collective-permute-start | bytes 1572872 | tf_op jit(solution)/shard_map/ppermute | solution.py:338
  32.1 23.0 %collective-permute-start.10 = (bf16[256,1024]{1,0:T(8,128)(2,1)S(1)}, bf16[256,1024]{1,0:T(8,128)(2,1)}, u32[]{:S(2)}, u32[]{:S(2)}) collective-permute-start(bf16[256,1024]{1,0:T(8,128)(2,1)S(1)} %bitcast.65), channel_id=1, source_target_pairs={{0,1},{1,0},{2,3},{3,2},{4,5},{5,4},{6,7},{7,6},{8,9},{9,8},{10,11... | collective-permute-start | bytes 1572872 | tf_op jit(solution)/shard_map/ppermute | solution.py:346
  33.5 25.1 %copy-start.6 = (bf16[256,1024]{1,0:T(8,128)(2,1)}, bf16[256,1024]{1,0:T(8,128)(2,1)S(1)}, u32[]{:S(2)}) copy-start(bf16[256,1024]{1,0:T(8,128)(2,1)S(1)} %collective-permute-done.7.refs_1_) | copy-start | bytes 1572868
  33.5 23.0 %collective-permute-start.11 = (bf16[256,1024]{1,0:T(8,128)(2,1)S(1)}, bf16[256,1024]{1,0:T(8,128)(2,1)}, u32[]{:S(2)}, u32[]{:S(2)}) collective-permute-start(bf16[256,1024]{1,0:T(8,128)(2,1)S(1)} %collective-permute-done.7.refs_1_), channel_id=1, source_target_pairs={{0,1},{1,0},{2,3},{3,2},{4,5},{5,4},{6,7},{7,6},{8,9},{9,8},{10,11... | collective-permute-start | bytes 1572872 | tf_op jit(solution)/shard_map/ppermute | solution.py:346
  52.2 6.4 %collective-permute-start.12 = (bf16[256,1024]{1,0:T(8,128)(2,1)}, bf16[256,1024]{1,0:T(8,128)(2,1)}, u32[]{:S(2)}, u32[]{:S(2)}) collective-permute-start(bf16[256,1024]{1,0:T(8,128)(2,1)} %collective-permute-done.8.refs_2_), channel_id=1, source_target_pairs={{0,1},{1,0},{2,3},{3,2},{4,5},{5,4},{6,7},{7,6},{8,9},{9,8},{10,11... | collective-permute-start | bytes 1572872 | tf_op jit(solution)/shard_map/ppermute | solution.py:346
  52.2 6.4 %collective-permute-start.13 = (bf16[256,1024]{1,0:T(8,128)(2,1)}, bf16[256,1024]{1,0:T(8,128)(2,1)}, u32[]{:S(2)}, u32[]{:S(2)}) collective-permute-start(bf16[256,1024]{1,0:T(8,128)(2,1)} %collective-permute-done.9.refs_3_), channel_id=1, source_target_pairs={{0,1},{1,0},{2,3},{3,2},{4,5},{5,4},{6,7},{7,6},{8,9},{9,8},{10,11... | collective-permute-start | bytes 1572872 | tf_op jit(solution)/shard_map/ppermute | solution.py:346
  52.7 19.7 %collective-permute-start = (bf16[256,1024]{1,0:T(8,128)(2,1)S(1)}, bf16[256,1024]{1,0:T(8,128)(2,1)}, u32[]{:S(2)}, u32[]{:S(2)}) collective-permute-start(bf16[256,1024]{1,0:T(8,128)(2,1)S(1)} %bitcast.68), channel_id=1, source_target_pairs={{0,2},{2,4},{4,6},{6,0},{1,3},{3,5},{5,7},{7,1},{8,10},{10,12},{12... | collective-permute-start | bytes 1572872 | tf_op jit(solution)/shard_map/ppermute | solution.py:338
  55.1 17.8 %collective-permute-start.1 = (bf16[256,1024]{1,0:T(8,128)(2,1)S(1)}, bf16[256,1024]{1,0:T(8,128)(2,1)}, u32[]{:S(2)}, u32[]{:S(2)}) collective-permute-start(bf16[256,1024]{1,0:T(8,128)(2,1)S(1)} %bitcast.69), channel_id=1, source_target_pairs={{0,6},{2,0},{4,2},{6,4},{1,7},{3,1},{5,3},{7,5},{8,14},{10,8},{12,... | collective-permute-start | bytes 1572872 | tf_op jit(solution)/shard_map/ppermute | solution.py:338
  56.5 24.6 %collective-permute-start.2 = (bf16[256,1024]{1,0:T(8,128)(2,1)S(1)}, bf16[256,1024]{1,0:T(8,128)(2,1)}, u32[]{:S(2)}, u32[]{:S(2)}) collective-permute-start(bf16[256,1024]{1,0:T(8,128)(2,1)S(1)} %bitcast.70), channel_id=1, source_target_pairs={{0,4},{2,6},{4,0},{6,2},{1,5},{3,7},{5,1},{7,3},{8,12},{10,14},{12... | collective-permute-start | bytes 1572872 | tf_op jit(solution)/shard_map/ppermute | solution.py:338
  65.5 30.5 %all-to-all-start.2 = ((bf16[16,192,128]{2,1,0:T(8,128)(2,1)}), bf16[16,192,128]{2,1,0:T(8,128)(2,1)S(1)}, u32[]{:S(2)}, u32[]{:S(2)}) async-start(bf16[16,192,128]{2,1,0:T(8,128)(2,1)} %get-tuple-element.27), calls=%async_computation.2 | async-start | bytes 1572864 | tf_op jit(solution)/shard_map/all_to_all | solution.py:399
  72.3 8.8 %collective-permute-start.3 = (bf16[256,1024]{1,0:T(8,128)(2,1)S(1)}, bf16[256,1024]{1,0:T(8,128)(2,1)S(1)}, u32[]{:S(2)}, u32[]{:S(2)}) collective-permute-start(bf16[256,1024]{1,0:T(8,128)(2,1)S(1)} %bitcast.71), channel_id=1, source_target_pairs={{0,1},{1,0},{2,3},{3,2},{4,5},{5,4},{6,7},{7,6},{8,9},{9,8},{10,11... | collective-permute-start | bytes 1572872 | tf_op jit(solution)/shard_map/ppermute | solution.py:346
  72.5 8.7 %collective-permute-start.4 = (bf16[256,1024]{1,0:T(8,128)(2,1)}, bf16[256,1024]{1,0:T(8,128)(2,1)}, u32[]{:S(2)}, u32[]{:S(2)}) collective-permute-start(bf16[256,1024]{1,0:T(8,128)(2,1)} %collective-permute-done.refs_1_.refs_9_), channel_id=1, source_target_pairs={{0,1},{1,0},{2,3},{3,2},{4,5},{5,4},{6,7},{7,6},{8,9},{9,8},{10,11... | collective-permute-start | bytes 1572872 | tf_op jit(solution)/shard_map/ppermute | solution.py:346
  72.9 8.2 %collective-permute-start.5 = (bf16[256,1024]{1,0:T(8,128)(2,1)}, bf16[256,1024]{1,0:T(8,128)(2,1)}, u32[]{:S(2)}, u32[]{:S(2)}) collective-permute-start(bf16[256,1024]{1,0:T(8,128)(2,1)} %collective-permute-done.1.refs_2_.refs_10_), channel_id=1, source_target_pairs={{0,1},{1,0},{2,3},{3,2},{4,5},{5,4},{6,7},{7,6},{8,9},{9,8},{10,11... | collective-permute-start | bytes 1572872 | tf_op jit(solution)/shard_map/ppermute | solution.py:346
  81.1 2.3 collective-permute-start.6
  81.1 2.2 copy-start.7
  95.9 0.9 copy-start
  96.8 28.3 %all-to-all-start = ((bf16[16,192,256]{2,1,0:T(8,128)(2,1)}), bf16[16,192,256]{2,1,0:T(8,128)(2,1)S(1)}, u32[]{:S(2)}, u32[]{:S(2)}) async-start(bf16[16,192,256]{2,1,0:T(8,128)(2,1)} %get-tuple-element.25), calls=%async_computation | async-start | bytes 3145728 | tf_op jit(solution)/shard_map/all_to_all | solution.py:401
  101.5 1.1 copy-start.1
  125.1 30.1 %all-to-all-start.3 = ((bf16[16,192,256]{2,1,0:T(8,128)(2,1)}), bf16[16,192,256]{2,1,0:T(8,128)(2,1)}, u32[]{:S(2)}, u32[]{:S(2)}) async-start(bf16[16,192,256]{2,1,0:T(8,128)(2,1)} %bitcast.13), calls=%async_computation.3 | async-start | bytes 3145728 | tf_op jit(solution)/shard_map/all_to_all | solution.py:406
  155.2 4.8 %copy-start.2 = (bf16[3072,1024]{1,0:T(8,128)(2,1)S(1)}, bf16[3072,1024]{1,0:T(8,128)(2,1)}, u32[]{:S(2)}) copy-start(bf16[3072,1024]{1,0:T(8,128)(2,1)} %all-gather.2.cloned.1.call-done) | copy-start | bytes 18874372
  162.2 1.0 copy-start.10
  162.3 1.0 copy-start.11
  162.3 1.2 copy-start.12
  163.7 7.5 %collective-permute-start.14 = (bf16[5,32,1024]{2,1,0:T(8,128)(2,1)S(1)}, bf16[5,32,1024]{2,1,0:T(8,128)(2,1)S(1)}, u32[]{:S(2)}, u32[]{:S(2)}) collective-permute-start(bf16[5,32,1024]{2,1,0:T(8,128)(2,1)S(1)} %fusion.9), channel_id=1, source_target_pairs={{0,1},{1,0},{2,3},{3,2},{4,5},{5,4},{6,7},{7,6},{8,9},{9,8},{10,11... | collective-permute-start | bytes 983048 | tf_op jit(solution)/shard_map/ppermute | solution.py:360
  163.8 33.6 %all-to-all-start.4 = ((bf16[16,192,256]{2,1,0:T(8,128)(2,1)}), bf16[16,192,256]{2,1,0:T(8,128)(2,1)S(1)}, u32[]{:S(2)}, u32[]{:S(2)}) async-start(bf16[16,192,256]{2,1,0:T(8,128)(2,1)} %bitcast.14), calls=%async_computation.4 | async-start | bytes 3145728 | tf_op jit(solution)/shard_map/all_to_all | solution.py:409
  171.5 4.6 %collective-permute-start.17 = (bf16[40,1024]{1,0:T(8,128)(2,1)S(1)}, bf16[40,1024]{1,0:T(8,128)(2,1)S(1)}, u32[]{:S(2)}, u32[]{:S(2)}) collective-permute-start(bf16[40,1024]{1,0:T(8,128)(2,1)S(1)} %concatenate.42), channel_id=1, source_target_pairs={{0,6},{2,0},{4,2},{6,4},{1,7},{3,1},{5,3},{7,5},{8,14},{10,8},{12,... | collective-permute-start | bytes 245768 | tf_op jit(solution)/shard_map/ppermute | solution.py:338
  173.6 7.3 %collective-permute-start.16 = (bf16[40,1024]{1,0:T(8,128)(2,1)S(1)}, bf16[40,1024]{1,0:T(8,128)(2,1)S(1)}, u32[]{:S(2)}, u32[]{:S(2)}) collective-permute-start(bf16[40,1024]{1,0:T(8,128)(2,1)S(1)} %concatenate.41), channel_id=1, source_target_pairs={{0,2},{2,4},{4,6},{6,0},{1,3},{3,5},{5,7},{7,1},{8,10},{10,12},{12... | collective-permute-start | bytes 245768 | tf_op jit(solution)/shard_map/ppermute | solution.py:338
  173.8 7.1 %collective-permute-start.15 = (bf16[40,1024]{1,0:T(8,128)(2,1)S(1)}, bf16[40,1024]{1,0:T(8,128)(2,1)S(1)}, u32[]{:S(2)}, u32[]{:S(2)}) collective-permute-start(bf16[40,1024]{1,0:T(8,128)(2,1)S(1)} %concatenate.40), channel_id=1, source_target_pairs={{0,4},{2,6},{4,0},{6,2},{1,5},{3,7},{5,1},{7,3},{8,12},{10,14},{12... | collective-permute-start | bytes 245768 | tf_op jit(solution)/shard_map/ppermute | solution.py:338
  181.0 16.5 %collective-permute-start.18 = (bf16[32,1024]{1,0:T(8,128)(2,1)S(1)}, bf16[32,1024]{1,0:T(8,128)(2,1)S(1)}, u32[]{:S(2)}, u32[]{:S(2)}) collective-permute-start(bf16[32,1024]{1,0:T(8,128)(2,1)S(1)} %fusion.11), channel_id=1, source_target_pairs={{0,0},{16,1},{32,2},{48,3},{64,4},{80,5},{96,6},{112,7},{1,8},{17,... | collective-permute-start | bytes 196616 | tf_op jit(solution)/shard_map/ppermute | solution.py:420
  197.4 1.6 copy-start.3
  199.0 26.2 %all-to-all-start.5 = ((bf16[16,40,1024]{2,1,0:T(8,128)(2,1)}), bf16[16,40,1024]{2,1,0:T(8,128)(2,1)S(1)}, u32[]{:S(2)}, u32[]{:S(2)}) async-start(bf16[16,40,1024]{2,1,0:T(8,128)(2,1)} %broadcast_in_dim.40), calls=%async_computation.5 | async-start | bytes 2621440 | tf_op jit(solution)/shard_map/all_to_all | solution.py:334
Sparse Core Ops, SparseCore 0:
  18.5 83.4 all-gather.1

commit v8 on v7

--- a/solution.py
+++ b/solution.py
@@ -320,6 +320,55 @@
         cost_estimate=pl.CostEstimate(flops=2_000_000_000, bytes_accessed=14_000_000, transcendentals=0),
         name="finish",
     )(order, r0, r1, latent, gain, cosine, sine, *evens, *odds)
+
+
+def weigh_body(g0_ref, g1_ref, nlat_ref, own0_ref, own1_ref, gain_ref, out_ref, small_ref, acc):
+    step = pl.program_id(0)
+    both = jnp.concatenate([g0_ref[...], g1_ref[...]], axis=1)
+    added = lax.dot_general(both, nlat_ref[...], (((0,), (0,)), ((), ())), preferred_element_type=f32)
+
+    @pl.when(step == 0)
+    def _():
+        acc[...] = added
+
+    @pl.when(step > 0)
+    def _():
+        acc[...] += added
+
+    @pl.when(step == pl.num_programs(0) - 1)
+    def _():
+        small = jnp.zeros((1, LATENT), f32)
+        for head, own_ref in enumerate((own0_ref, own1_ref)):
+            rows = slice(128 * head, 128 * head + 128)
+            small = small + jnp.sum(acc[rows, :] * own_ref[...].astype(f32), axis=0, keepdims=True)
+            for piece in range(4):
+                for kind in range(2):
+                    start = 128 * head + 64 * kind + 16 * piece
+                    out_ref[4 * head + piece, 16 * kind : 16 * kind + 16] = acc[start : start + 16, :].astype(bf16)
+        small_ref[...] = small / gain_ref[...]
+
+
+def weigh(g0, g1, nlat_all, own0, own1, gain):
+    return pl.pallas_call(
+        weigh_body,
+        grid=(LENGTH // BLOCK,),
+        in_specs=[
+            pl.BlockSpec((BLOCK, 128), lambda g: (g, 0)),
+            pl.BlockSpec((BLOCK, 128), lambda g: (g, 0)),
+            pl.BlockSpec((BLOCK, LATENT), lambda g: (g, 0)),
+            pl.BlockSpec((128, LATENT), lambda g: (0, 0)),
+            pl.BlockSpec((128, LATENT), lambda g: (0, 0)),
+            pl.BlockSpec((1, LATENT), lambda g: (0, 0)),
+        ],
+        out_specs=[
+            pl.BlockSpec((NDP, 32, LATENT), lambda g: (0, 0, 0)),
+            pl.BlockSpec((1, LATENT), lambda g: (0, 0)),
+        ],
+        out_shape=[jax.ShapeDtypeStruct((NDP, 32, LATENT), bf16), jax.ShapeDtypeStruct((1, LATENT), f32)],
+        scratch_shapes=[pltpu.VMEM((256, LATENT), f32)],
+        cost_estimate=pl.CostEstimate(flops=2_000_000_000, bytes_accessed=9_000_000, transcendentals=0),
+        name="weigh",
+    )(g0, g1, nlat_all, own0, own1, gain)
 
 
 def to_heads():
@@ -408,15 +457,8 @@
     r0, g1 = lax.optimization_barrier((r0, g1))
     r1 = lax.all_to_all(g1.reshape(NSP, TOKENS, 256), SP, 0, 0, tiled=True)
 
-    parts = [
-        lax.dot_general(g[:, 0:128], nlat_all, (((0,), (0,)), ((), ())), preferred_element_type=f32)
-        for g in (g0, g1)
-    ]
-    part = jnp.concatenate(parts, axis=0)
-    pieces = part.astype(bf16).reshape(2, 2, 4, 16, LATENT).transpose(0, 2, 1, 3, 4).reshape(NDP, 32, LATENT)
-    own = jnp.concatenate([own0, own1], axis=0)
-    gain_part = jnp.sum(part * own.astype(f32), axis=0) / gain
-    piece, gain_part = reduce_over_rows(pieces, gain_part)
+    pieces, gain_part = weigh(g0, g1, nlat_all, own0, own1, gain_row)
+    piece, gain_part = reduce_over_rows(pieces, gain_part[0])
     piece = lax.ppermute(piece, ALL, to_rows())
     r1, piece = lax.optimization_barrier((r1, piece))
     piece = jnp.concatenate([piece, as_rows(gain_part)])

time: 236 us -> 236 us (level)
  Pallas kernels: 73.2 us -> 79.7 us
  matrix products: 6.35 us -> 0 us
    pallas_call x0 -> x1, Pallas kernels: none -> 6.57 us  [weigh(): pl.pallas_call(weigh_body, grid=(LENGTH // BLOCK,), in_specs=[pl.BlockSpe...]
    dot_general x2 -> x0, matrix products: 6.35 us -> none  [program(): lax.dot_general(g[:, 0:128], nlat_all, (((0,), (0,)), ((), ())), preferre...]
    ppermute x9, waiting for transfers between devices: 33.1 us -> 30.2 us  [shifted(): return lax.ppermute(value, axis, [(i, (i + k) % 4) for i in range(4)])]
    unnamed x30 -> x26, local copies, waits for them, and re-layouts: 6.13 us -> 5.07 us
where the time goes in v8:
time: 236 us; the launch traced here: 235 us
  Pallas kernels  79.7 us (34%)
  waiting for transfers between devices  66.1 us (28%)
  starting transfers between devices  56.3 us (24%)
  between operations  14.4 us (6%)
  other arithmetic  10.3 us (4%)
  local copies, waits for them, and re-layouts  8.04 us (3%)
    pallas_call x2, Pallas kernels, attend(): pl.pallas_call(functools.partial(attend_body, head), grid=(1,), in_specs=...  45.5 us
    ppermute x9, waiting for transfers between devices, shifted(): return lax.ppermute(value, axis, [(i, (i + k) % 4) for i in range(4)])  30.2 us
    all_to_all x1, waiting for transfers between devices, program(): r1 = lax.all_to_all(g1.reshape(NSP, TOKENS, 256), SP, 0, 0, tiled=True)  16.6 us
    ppermute x9, starting transfers between devices, shifted(): return lax.ppermute(value, axis, [(i, (i + k) % 4) for i in range(4)])  16.3 us
    pallas_call x2, Pallas kernels, project(): pl.pallas_call(project_body, in_specs=[pl.BlockSpec(memory_space=pltpu.SM...  14.4 us
    all_to_all x1, waiting for transfers between devices, everyone(): lax.all_to_all(jnp.broadcast_to(value[None], (size, *value.shape)), axes,...  12 us
    all_to_all x1, starting transfers between devices, program(): first = lax.all_to_all(first, SP, 0, 0, tiled=True).reshape(LENGTH, 256)  8.18 us
    pallas_call x1, Pallas kernels, finish(): pl.pallas_call(finish_body, in_specs=[pl.BlockSpec(memory_space=pltpu.SME...  7.85 us
  transfers between devices with their start and end apart: 26, of which 9 were waited for; matrix products, arithmetic and copies ran while one was open for 2% of the time, Pallas kernels for 29%

profile of v8, /device:TPU:0, one launch (start us, length us, event | category | flops | bytes accessed | tf_op | source)
XLA Modules:
  0.0 234.9 jit_solution(17973185491712680460)
XLA Ops:
  7.2 1.2 fusion
  8.4 0.8 copy.16
  9.2 0.7 pad_convert_fusion.kr_ref
  9.9 1.9 fusion.2.nlat_ref
  11.8 1.1 fusion.7
  12.9 5.5 %pack.1 = (bf16[16,192,256]{2,1,0:T(8,128)(2,1)}, bf16[16,192,128]{2,1,0:T(8,128)(2,1)}) custom-call(bf16[192,3072]{1,0:T(8,128)(2,1)} %bitcast.82, bf16[192,2048]{1,0:T(8,128)(2,1)} %bitcast.84, f32[192,128]{1,0:T(8,128)} %pad_convert_fusion.kr_ref, f32[192,128]{1,0:T(8,128)} %get-tuple-element.72.cos_ref, f32[192,128]{1,0:T(8,128)} %get-tuple-element.71.sin_ref), custom_call_target="tpu_custom_call" | custom-call | flops 2000000000 | bytes 5000000 | tf_op jit(solution)/shard_map/pack/pallas_call | solution.py:79
  18.4 0.1 pad_maximum_fusion
  18.6 0.1 fusion.37
  18.7 1.7 collective-permute-start.7
  20.3 8.2 %all-to-all-start.1 = ((bf16[16,192,256]{2,1,0:T(8,128)(2,1)}), bf16[16,192,256]{2,1,0:T(8,128)(2,1)S(1)}, u32[]{:S(2)}, u32[]{:S(2)}) async-start(bf16[16,192,256]{2,1,0:T(8,128)(2,1)} %get-tuple-element.28), calls=%async_computation.1 | async-start | bytes 3145728 | tf_op jit(solution)/shard_map/all_to_all | solution.py:444
  28.5 1.8 collective-permute-start.8
  30.3 1.8 collective-permute-start.9
  32.1 1.4 collective-permute-done.7.refs_1_
  33.5 18.7 %collective-permute-done.8.refs_2_ = bf16[256,1024]{1,0:T(8,128)(2,1)} collective-permute-done((bf16[256,1024]{1,0:T(8,128)(2,1)S(1)}, bf16[256,1024]{1,0:T(8,128)(2,1)}, u32[]{:S(2)}, u32[]{:S(2)}) %collective-permute-start.8) | collective-permute-done | bytes 524320 | tf_op jit(solution)/shard_map/ppermute | solution.py:387
  52.2 0.5 collective-permute-start.13
  52.7 2.4 %collective-permute-start = (bf16[256,1024]{1,0:T(8,128)(2,1)S(1)}, bf16[256,1024]{1,0:T(8,128)(2,1)}, u32[]{:S(2)}, u32[]{:S(2)}) collective-permute-start(bf16[256,1024]{1,0:T(8,128)(2,1)S(1)} %bitcast.68), channel_id=1, source_target_pairs={{0,2},{2,4},{4,6},{6,0},{1,3},{3,5},{5,7},{7,1},{8,10},{10,12},{12... | collective-permute-start | bytes 1572872 | tf_op jit(solution)/shard_map/ppermute | solution.py:387
  55.2 1.3 collective-permute-start.1
  56.5 1.5 collective-permute-start.2
  58.1 0.6 pad_add_fusion.order_ref
  58.7 6.8 %project.3 = (bf16[16,192,128]{2,1,0:T(8,128)(2,1)}, bf16[128,1024]{1,0:T(8,128)(2,1)}) custom-call(s32[9]{0:T(128)} %pad_add_fusion.order_ref, bf16[192,1024]{1,0:T(8,128)(2,1)} %fusion.2.nlat_ref, bf16[256,1024]{1,0:T(8,128)(2,1)} %bitcast.66, bf16[256,1024]{1,0:T(8,128)(2,1)} %copy-done.5, bf16[256,1024]{1,0:T(8,128)(2,1)} %collective-permute-done.8.refs_2_, ...), custom_call_target="tpu_custom_call" | custom-call | flops 2000000000 | bytes 6000000 | tf_op jit(solution)/shard_map/project/pallas_call | solution.py:253
  65.5 6.9 %all-to-all-start.2 = ((bf16[16,192,128]{2,1,0:T(8,128)(2,1)}), bf16[16,192,128]{2,1,0:T(8,128)(2,1)S(1)}, u32[]{:S(2)}, u32[]{:S(2)}) async-start(bf16[16,192,128]{2,1,0:T(8,128)(2,1)} %get-tuple-element.29), calls=%async_computation.2 | async-start | bytes 1572864 | tf_op jit(solution)/shard_map/all_to_all | solution.py:448
  72.4 0.1 collective-permute-start.3
  72.5 0.5 collective-permute-start.4
  73.0 0.1 collective-permute-start.5
  73.1 8.0 %collective-permute-done.2.refs_3_.refs_11_ = bf16[256,1024]{1,0:T(8,128)(2,1)} collective-permute-done((bf16[256,1024]{1,0:T(8,128)(2,1)S(1)}, bf16[256,1024]{1,0:T(8,128)(2,1)}, u32[]{:S(2)}, u32[]{:S(2)}) %collective-permute-start.2) | collective-permute-done | bytes 524320 | tf_op jit(solution)/shard_map/ppermute | solution.py:387
  81.2 2.2 collective-permute-done.6.refs_7_.refs_15_
  83.4 7.6 %project.2 = (bf16[16,192,256]{2,1,0:T(8,128)(2,1)}, bf16[128,1024]{1,0:T(8,128)(2,1)}) custom-call(s32[9]{0:T(128)} %pad_add_fusion.order_ref, bf16[192,1024]{1,0:T(8,128)(2,1)} %fusion.2.nlat_ref, bf16[256,1024]{1,0:T(8,128)(2,1)} %bitcast.72, bf16[256,1024]{1,0:T(8,128)(2,1)} %collective-permute-done.refs_1_.refs_9_, ...), custom_call_target="tpu_custom_call" | custom-call | flops 2000000000 | bytes 6000000 | tf_op jit(solution)/shard_map/project/pallas_call | solution.py:253
  90.9 5.0 %all-to-all-done.2 = bf16[16,192,128]{2,1,0:T(8,128)(2,1)S(1)} async-done(((bf16[16,192,128]{2,1,0:T(8,128)(2,1)}), bf16[16,192,128]{2,1,0:T(8,128)(2,1)S(1)}, u32[]{:S(2)}, u32[]{:S(2)}) %all-to-all-start.2) | async-done | bytes 786464 | tf_op jit(solution)/shard_map/all_to_all | solution.py:448
  96.0 0.9 copy-done
  96.8 3.9 %all-to-all-start = ((bf16[16,192,256]{2,1,0:T(8,128)(2,1)}), bf16[16,192,256]{2,1,0:T(8,128)(2,1)S(1)}, u32[]{:S(2)}, u32[]{:S(2)}) async-start(bf16[16,192,256]{2,1,0:T(8,128)(2,1)} %get-tuple-element.27), calls=%async_computation | async-start | bytes 3145728 | tf_op jit(solution)/shard_map/all_to_all | solution.py:450
  100.7 0.8 multiply_sine_fusion
  101.5 1.1 copy-done.1
  102.6 22.6 %shard_map.127.g0_ref = bf16[3072,256]{1,0:T(8,128)(2,1)} custom-call(bf16[3072,256]{1,0:T(8,128)(2,1)S(1)} %bitcast.53, bf16[3072,256]{1,0:T(8,128)(2,1)S(1)} %bitcast.54, bf16[3072,128]{1,0:T(8,128)(2,1)S(1)} %bitcast.58, f32[16,3072]{1,0:T(8,128)S(1)} %get-tuple-element.68.cos_ref, f32[16,3072]{1,0:T(8,128)S(1)} %get-tuple-element.67.sin_ref), custom_call_target="tpu_custom_call" | custom-call | flops 12000000000 | bytes 6000000 | tf_op jit(solution)/shard_map/pallas_call | solution.py:204
  125.2 7.0 %all-to-all-start.3 = ((bf16[16,192,256]{2,1,0:T(8,128)(2,1)}), bf16[16,192,256]{2,1,0:T(8,128)(2,1)}, u32[]{:S(2)}, u32[]{:S(2)}) async-start(bf16[16,192,256]{2,1,0:T(8,128)(2,1)} %bitcast.13), calls=%async_computation.3 | async-start | bytes 3145728 | tf_op jit(solution)/shard_map/all_to_all | solution.py:455
  132.3 0.1 pad.17.clone
  132.3 0.1 pad.18.clone
  132.4 22.9 %shard_map.128.g1_ref = bf16[3072,256]{1,0:T(8,128)(2,1)} custom-call(bf16[3072,256]{1,0:T(8,128)(2,1)S(1)} %bitcast.56, bf16[3072,256]{1,0:T(8,128)(2,1)S(1)} %bitcast.55, bf16[3072,256]{1,0:T(8,128)(2,1)S(1)} %bitcast.57, f32[16,3072]{1,0:T(8,128)S(1)} %get-tuple-element.68.cos_ref, f32[16,3072]{1,0:T(8,128)S(1)} %get-tuple-element.67.sin_ref), custom_call_target="tpu_custom_call" | custom-call | flops 12000000000 | bytes 6000000 | tf_op jit(solution)/shard_map/pallas_call | solution.py:204
  155.3 6.6 %weigh.1 = (bf16[8,32,1024]{2,1,0:T(8,128)(2,1)}, f32[1,1024]{1,0:T(1,128)}) custom-call(bf16[3072,256]{1,0:T(8,128)(2,1)} %shard_map.127.g0_ref, bf16[3072,256]{1,0:T(8,128)(2,1)} %shard_map.128.g1_ref, bf16[3072,1024]{1,0:T(8,128)(2,1)} %all-gather.2.cloned.1.call-done.nlat_ref, bf16[128,1024]{1,0:T(8,128)(2,1)} %get-tuple-element.35.own0_ref, ...), custom_call_target="tpu_custom_call" | custom-call | flops 2000000000 | bytes 9000000 | tf_op jit(solution)/shard_map/weigh/pallas_call | solution.py:352
  161.9 0.7 fusion.11
  162.6 1.0 dynamic-slice_bitcast_fusion
  163.5 0.1 maximum_maximum_fusion
  163.6 0.1 collective-permute-start.14
  163.8 7.3 %all-to-all-start.4 = ((bf16[16,192,256]{2,1,0:T(8,128)(2,1)}), bf16[16,192,256]{2,1,0:T(8,128)(2,1)S(1)}, u32[]{:S(2)}, u32[]{:S(2)}) async-start(bf16[16,192,256]{2,1,0:T(8,128)(2,1)} %bitcast.14), calls=%async_computation.4 | async-start | bytes 3145728 | tf_op jit(solution)/shard_map/all_to_all | solution.py:458
  171.1 0.1 convert_element_type.127
  171.2 0.1 slice_add_fusion
  171.3 0.5 copy-done.10
  171.9 2.1 collective-permute-start.15
  174.0 0.8 collective-permute-start.16
  174.8 2.8 %collective-permute-start.17 = (bf16[40,1024]{1,0:T(8,128)(2,1)S(1)}, bf16[40,1024]{1,0:T(8,128)(2,1)S(1)}, u32[]{:S(2)}, u32[]{:S(2)}) collective-permute-start(bf16[40,1024]{1,0:T(8,128)(2,1)S(1)} %concatenate.34), channel_id=1, source_target_pairs={{0,6},{2,0},{4,2},{6,4},{1,7},{3,1},{5,3},{7,5},{8,14},{10,8},{12,... | collective-permute-start | bytes 245768 | tf_op jit(solution)/shard_map/ppermute | solution.py:387
  177.6 0.4 collective-permute-done.15
  178.1 1.7 collective-permute-done.16
  179.8 0.7 collective-permute-start.18
  180.6 16.6 %all-to-all-done.4.r1_ref = bf16[16,192,256]{2,1,0:T(8,128)(2,1)S(1)} async-done(((bf16[16,192,256]{2,1,0:T(8,128)(2,1)}), bf16[16,192,256]{2,1,0:T(8,128)(2,1)S(1)}, u32[]{:S(2)}, u32[]{:S(2)}) %all-to-all-start.4) | async-done | bytes 1572896 | tf_op jit(solution)/shard_map/all_to_all | solution.py:458
  197.2 1.4 broadcast_in_dim.40
  198.6 0.1 copy-done.2
  198.7 4.8 %all-to-all-start.5 = ((bf16[16,40,1024]{2,1,0:T(8,128)(2,1)}), bf16[16,40,1024]{2,1,0:T(8,128)(2,1)S(1)}, u32[]{:S(2)}, u32[]{:S(2)}) async-start(bf16[16,40,1024]{2,1,0:T(8,128)(2,1)} %broadcast_in_dim.40), calls=%async_computation.5 | async-start | bytes 2621440 | tf_op jit(solution)/shard_map/all_to_all | solution.py:383
  203.5 7.8 %finish.1 = (bf16[192,3072]{1,0:T(8,128)(2,1)}, f32[192,1024]{1,0:T(8,128)}, f32[192,32]{1,0:T(8,128)}) custom-call(s32[9]{0:T(128)} %pad_add_fusion.order_ref, bf16[16,192,256]{2,1,0:T(8,128)(2,1)} %all-to-all-done.3.r0_ref, bf16[16,192,256]{2,1,0:T(8,128)(2,1)} %copy-done.2, bf16[192,1024]{1,0:T(8,128)(2,1)} %bitcast.61, f32[1,1024]{1,0:T(1,128)} %bitcast.81, ...), custom_call_target="tpu_custom_call" | custom-call | flops 2000000000 | bytes 14000000 | tf_op jit(solution)/shard_map/finish/pallas_call | solution.py:310
  211.4 1.6 copy.18
  213.0 12.0 %all-to-all-done.5 = bf16[16,40,1024]{2,1,0:T(8,128)(2,1)S(1)} async-done(((bf16[16,40,1024]{2,1,0:T(8,128)(2,1)}), bf16[16,40,1024]{2,1,0:T(8,128)(2,1)S(1)}, u32[]{:S(2)}, u32[]{:S(2)}) %all-to-all-start.5) | async-done | bytes 1310752 | tf_op jit(solution)/shard_map/all_to_all | solution.py:383
  224.9 0.1 slice.86
  225.0 0.1 fusion.36
  225.1 1.1 bitcast_convert_fusion
  226.2 1.1 bitcast_convert_fusion.1
  227.4 0.7 convert_reduce_fusion
  (67 shorter events, 0.6 us)
Async XLA Ops:
  7.2 148.1 %all-gather.2.cloned.1.call-start = ((), (), s32[]{:S(2)}) async-start(), calls=%async_computation.6 | async-start | bytes 6684672 | tf_op jit(solution)/shard_map/all_gather | solution.py:447
  12.9 5.5 %copy-start.8 = (bf16[256,1024]{1,0:T(8,128)(2,1)S(1)}, bf16[256,1024]{1,0:T(8,128)(2,1)}, u32[]{:S(2)}) copy-start(bf16[256,1024]{1,0:T(8,128)(2,1)} %param.13) | copy-start | bytes 1572868
  12.9 5.5 %copy-start.9 = (bf16[256,1024]{1,0:T(8,128)(2,1)S(1)}, bf16[256,1024]{1,0:T(8,128)(2,1)}, u32[]{:S(2)}) copy-start(bf16[256,1024]{1,0:T(8,128)(2,1)} %param.12) | copy-start | bytes 1572868
  18.6 13.5 %copy-start.3 = (bf16[2,1,128,1024]{3,2,1,0:T(8,128)(2,1)}, bf16[2,1,128,1024]{3,2,1,0:T(8,128)(2,1)S(1)}, u32[]{:S(2)}) copy-start(bf16[2,1,128,1024]{3,2,1,0:T(8,128)(2,1)S(1)} %get-tuple-element.62) | copy-start | bytes 1572868
  18.6 53.7 %copy-start.4 = (bf16[2,1,128,1024]{3,2,1,0:T(8,128)(2,1)}, bf16[2,1,128,1024]{3,2,1,0:T(8,128)(2,1)S(1)}, u32[]{:S(2)}) copy-start(bf16[2,1,128,1024]{3,2,1,0:T(8,128)(2,1)S(1)} %get-tuple-element.63) | copy-start | bytes 1572868
  18.7 14.9 %collective-permute-start.7 = (bf16[256,1024]{1,0:T(8,128)(2,1)S(1)}, bf16[256,1024]{1,0:T(8,128)(2,1)S(1)}, u32[]{:S(2)}, u32[]{:S(2)}) collective-permute-start(bf16[256,1024]{1,0:T(8,128)(2,1)S(1)} %bitcast.62), channel_id=1, source_target_pairs={{0,2},{2,4},{4,6},{6,0},{1,3},{3,5},{5,7},{7,1},{8,10},{10,12},{12... | collective-permute-start | bytes 1572872 | tf_op jit(solution)/shard_map/ppermute | solution.py:387
  20.3 37.7 %copy-start.11 = (s32[4]{0:T(128)S(1)}, s32[4]{0:T(128)}, u32[]{:S(2)}) copy-start(s32[4]{0:T(128)} %constant.115.clone) | copy-start | bytes 52
  20.3 45.2 %all-to-all-start.1 = ((bf16[16,192,256]{2,1,0:T(8,128)(2,1)}), bf16[16,192,256]{2,1,0:T(8,128)(2,1)S(1)}, u32[]{:S(2)}, u32[]{:S(2)}) async-start(bf16[16,192,256]{2,1,0:T(8,128)(2,1)} %get-tuple-element.28), calls=%async_computation.1 | async-start | bytes 3145728 | tf_op jit(solution)/shard_map/all_to_all | solution.py:444
  28.5 23.7 %collective-permute-start.8 = (bf16[256,1024]{1,0:T(8,128)(2,1)S(1)}, bf16[256,1024]{1,0:T(8,128)(2,1)}, u32[]{:S(2)}, u32[]{:S(2)}) collective-permute-start(bf16[256,1024]{1,0:T(8,128)(2,1)S(1)} %bitcast.63), channel_id=1, source_target_pairs={{0,6},{2,0},{4,2},{6,4},{1,7},{3,1},{5,3},{7,5},{8,14},{10,8},{12,... | collective-permute-start | bytes 1572872 | tf_op jit(solution)/shard_map/ppermute | solution.py:387
  30.3 21.9 %collective-permute-start.9 = (bf16[256,1024]{1,0:T(8,128)(2,1)S(1)}, bf16[256,1024]{1,0:T(8,128)(2,1)}, u32[]{:S(2)}, u32[]{:S(2)}) collective-permute-start(bf16[256,1024]{1,0:T(8,128)(2,1)S(1)} %bitcast.64), channel_id=1, source_target_pairs={{0,4},{2,6},{4,0},{6,2},{1,5},{3,7},{5,1},{7,3},{8,12},{10,14},{12... | collective-permute-start | bytes 1572872 | tf_op jit(solution)/shard_map/ppermute | solution.py:387
  32.1 23.0 %collective-permute-start.10 = (bf16[256,1024]{1,0:T(8,128)(2,1)S(1)}, bf16[256,1024]{1,0:T(8,128)(2,1)}, u32[]{:S(2)}, u32[]{:S(2)}) collective-permute-start(bf16[256,1024]{1,0:T(8,128)(2,1)S(1)} %bitcast.65), channel_id=1, source_target_pairs={{0,1},{1,0},{2,3},{3,2},{4,5},{5,4},{6,7},{7,6},{8,9},{9,8},{10,11... | collective-permute-start | bytes 1572872 | tf_op jit(solution)/shard_map/ppermute | solution.py:395
  33.5 25.1 %copy-start.5 = (bf16[256,1024]{1,0:T(8,128)(2,1)}, bf16[256,1024]{1,0:T(8,128)(2,1)S(1)}, u32[]{:S(2)}) copy-start(bf16[256,1024]{1,0:T(8,128)(2,1)S(1)} %collective-permute-done.7.refs_1_) | copy-start | bytes 1572868
  33.5 23.0 %collective-permute-start.11 = (bf16[256,1024]{1,0:T(8,128)(2,1)S(1)}, bf16[256,1024]{1,0:T(8,128)(2,1)}, u32[]{:S(2)}, u32[]{:S(2)}) collective-permute-start(bf16[256,1024]{1,0:T(8,128)(2,1)S(1)} %collective-permute-done.7.refs_1_), channel_id=1, source_target_pairs={{0,1},{1,0},{2,3},{3,2},{4,5},{5,4},{6,7},{7,6},{8,9},{9,8},{10,11... | collective-permute-start | bytes 1572872 | tf_op jit(solution)/shard_map/ppermute | solution.py:395
  52.2 6.4 %collective-permute-start.12 = (bf16[256,1024]{1,0:T(8,128)(2,1)}, bf16[256,1024]{1,0:T(8,128)(2,1)}, u32[]{:S(2)}, u32[]{:S(2)}) collective-permute-start(bf16[256,1024]{1,0:T(8,128)(2,1)} %collective-permute-done.8.refs_2_), channel_id=1, source_target_pairs={{0,1},{1,0},{2,3},{3,2},{4,5},{5,4},{6,7},{7,6},{8,9},{9,8},{10,11... | collective-permute-start | bytes 1572872 | tf_op jit(solution)/shard_map/ppermute | solution.py:395
  52.2 6.4 %collective-permute-start.13 = (bf16[256,1024]{1,0:T(8,128)(2,1)}, bf16[256,1024]{1,0:T(8,128)(2,1)}, u32[]{:S(2)}, u32[]{:S(2)}) collective-permute-start(bf16[256,1024]{1,0:T(8,128)(2,1)} %collective-permute-done.9.refs_3_), channel_id=1, source_target_pairs={{0,1},{1,0},{2,3},{3,2},{4,5},{5,4},{6,7},{7,6},{8,9},{9,8},{10,11... | collective-permute-start | bytes 1572872 | tf_op jit(solution)/shard_map/ppermute | solution.py:395
  52.7 19.7 %collective-permute-start = (bf16[256,1024]{1,0:T(8,128)(2,1)S(1)}, bf16[256,1024]{1,0:T(8,128)(2,1)}, u32[]{:S(2)}, u32[]{:S(2)}) collective-permute-start(bf16[256,1024]{1,0:T(8,128)(2,1)S(1)} %bitcast.68), channel_id=1, source_target_pairs={{0,2},{2,4},{4,6},{6,0},{1,3},{3,5},{5,7},{7,1},{8,10},{10,12},{12... | collective-permute-start | bytes 1572872 | tf_op jit(solution)/shard_map/ppermute | solution.py:387
  55.2 17.8 %collective-permute-start.1 = (bf16[256,1024]{1,0:T(8,128)(2,1)S(1)}, bf16[256,1024]{1,0:T(8,128)(2,1)}, u32[]{:S(2)}, u32[]{:S(2)}) collective-permute-start(bf16[256,1024]{1,0:T(8,128)(2,1)S(1)} %bitcast.69), channel_id=1, source_target_pairs={{0,6},{2,0},{4,2},{6,4},{1,7},{3,1},{5,3},{7,5},{8,14},{10,8},{12,... | collective-permute-start | bytes 1572872 | tf_op jit(solution)/shard_map/ppermute | solution.py:387
  56.5 24.6 %collective-permute-start.2 = (bf16[256,1024]{1,0:T(8,128)(2,1)S(1)}, bf16[256,1024]{1,0:T(8,128)(2,1)}, u32[]{:S(2)}, u32[]{:S(2)}) collective-permute-start(bf16[256,1024]{1,0:T(8,128)(2,1)S(1)} %bitcast.70), channel_id=1, source_target_pairs={{0,4},{2,6},{4,0},{6,2},{1,5},{3,7},{5,1},{7,3},{8,12},{10,14},{12... | collective-permute-start | bytes 1572872 | tf_op jit(solution)/shard_map/ppermute | solution.py:387
  65.5 30.5 %all-to-all-start.2 = ((bf16[16,192,128]{2,1,0:T(8,128)(2,1)}), bf16[16,192,128]{2,1,0:T(8,128)(2,1)S(1)}, u32[]{:S(2)}, u32[]{:S(2)}) async-start(bf16[16,192,128]{2,1,0:T(8,128)(2,1)} %get-tuple-element.29), calls=%async_computation.2 | async-start | bytes 1572864 | tf_op jit(solution)/shard_map/all_to_all | solution.py:448
  72.4 8.8 %collective-permute-start.3 = (bf16[256,1024]{1,0:T(8,128)(2,1)S(1)}, bf16[256,1024]{1,0:T(8,128)(2,1)S(1)}, u32[]{:S(2)}, u32[]{:S(2)}) collective-permute-start(bf16[256,1024]{1,0:T(8,128)(2,1)S(1)} %bitcast.71), channel_id=1, source_target_pairs={{0,1},{1,0},{2,3},{3,2},{4,5},{5,4},{6,7},{7,6},{8,9},{9,8},{10,11... | collective-permute-start | bytes 1572872 | tf_op jit(solution)/shard_map/ppermute | solution.py:395
  72.5 8.7 %collective-permute-start.4 = (bf16[256,1024]{1,0:T(8,128)(2,1)}, bf16[256,1024]{1,0:T(8,128)(2,1)}, u32[]{:S(2)}, u32[]{:S(2)}) collective-permute-start(bf16[256,1024]{1,0:T(8,128)(2,1)} %collective-permute-done.refs_1_.refs_9_), channel_id=1, source_target_pairs={{0,1},{1,0},{2,3},{3,2},{4,5},{5,4},{6,7},{7,6},{8,9},{9,8},{10,11... | collective-permute-start | bytes 1572872 | tf_op jit(solution)/shard_map/ppermute | solution.py:395
  73.0 8.2 %collective-permute-start.5 = (bf16[256,1024]{1,0:T(8,128)(2,1)}, bf16[256,1024]{1,0:T(8,128)(2,1)}, u32[]{:S(2)}, u32[]{:S(2)}) collective-permute-start(bf16[256,1024]{1,0:T(8,128)(2,1)} %collective-permute-done.1.refs_2_.refs_10_), channel_id=1, source_target_pairs={{0,1},{1,0},{2,3},{3,2},{4,5},{5,4},{6,7},{7,6},{8,9},{9,8},{10,11... | collective-permute-start | bytes 1572872 | tf_op jit(solution)/shard_map/ppermute | solution.py:395
  81.1 2.3 collective-permute-start.6
  81.1 2.2 copy-start.6
  96.0 0.9 copy-start
  96.8 28.4 %all-to-all-start = ((bf16[16,192,256]{2,1,0:T(8,128)(2,1)}), bf16[16,192,256]{2,1,0:T(8,128)(2,1)S(1)}, u32[]{:S(2)}, u32[]{:S(2)}) async-start(bf16[16,192,256]{2,1,0:T(8,128)(2,1)} %get-tuple-element.27), calls=%async_computation | async-start | bytes 3145728 | tf_op jit(solution)/shard_map/all_to_all | solution.py:450
  101.5 1.1 copy-start.1
  125.2 30.1 %all-to-all-start.3 = ((bf16[16,192,256]{2,1,0:T(8,128)(2,1)}), bf16[16,192,256]{2,1,0:T(8,128)(2,1)}, u32[]{:S(2)}, u32[]{:S(2)}) async-start(bf16[16,192,256]{2,1,0:T(8,128)(2,1)} %bitcast.13), calls=%async_computation.3 | async-start | bytes 3145728 | tf_op jit(solution)/shard_map/all_to_all | solution.py:455
  163.6 7.5 %collective-permute-start.14 = (bf16[5,32,1024]{2,1,0:T(8,128)(2,1)S(1)}, bf16[5,32,1024]{2,1,0:T(8,128)(2,1)S(1)}, u32[]{:S(2)}, u32[]{:S(2)}) collective-permute-start(bf16[5,32,1024]{2,1,0:T(8,128)(2,1)S(1)} %fusion.4), channel_id=1, source_target_pairs={{0,1},{1,0},{2,3},{3,2},{4,5},{5,4},{6,7},{7,6},{8,9},{9,8},{10,11... | collective-permute-start | bytes 983048 | tf_op jit(solution)/shard_map/ppermute | solution.py:409
  163.7 7.4 %copy-start.7 = (bf16[8,32,1024]{2,1,0:T(8,128)(2,1)S(1)}, bf16[8,32,1024]{2,1,0:T(8,128)(2,1)}, u32[]{:S(2)}) copy-start(bf16[8,32,1024]{2,1,0:T(8,128)(2,1)} %get-tuple-element.37) | copy-start | bytes 1572868
  163.8 33.4 %all-to-all-start.4 = ((bf16[16,192,256]{2,1,0:T(8,128)(2,1)}), bf16[16,192,256]{2,1,0:T(8,128)(2,1)S(1)}, u32[]{:S(2)}, u32[]{:S(2)}) async-start(bf16[16,192,256]{2,1,0:T(8,128)(2,1)} %bitcast.14), calls=%async_computation.4 | async-start | bytes 3145728 | tf_op jit(solution)/shard_map/all_to_all | solution.py:458
  171.1 0.7 copy-start.10
  171.9 6.2 %collective-permute-start.15 = (bf16[40,1024]{1,0:T(8,128)(2,1)S(1)}, bf16[40,1024]{1,0:T(8,128)(2,1)S(1)}, u32[]{:S(2)}, u32[]{:S(2)}) collective-permute-start(bf16[40,1024]{1,0:T(8,128)(2,1)S(1)} %concatenate.32), channel_id=1, source_target_pairs={{0,4},{2,6},{4,0},{6,2},{1,5},{3,7},{5,1},{7,3},{8,12},{10,14},{12... | collective-permute-start | bytes 245768 | tf_op jit(solution)/shard_map/ppermute | solution.py:387
  174.0 5.8 %collective-permute-start.16 = (bf16[40,1024]{1,0:T(8,128)(2,1)S(1)}, bf16[40,1024]{1,0:T(8,128)(2,1)S(1)}, u32[]{:S(2)}, u32[]{:S(2)}) collective-permute-start(bf16[40,1024]{1,0:T(8,128)(2,1)S(1)} %concatenate.33), channel_id=1, source_target_pairs={{0,2},{2,4},{4,6},{6,0},{1,3},{3,5},{5,7},{7,1},{8,10},{10,12},{12... | collective-permute-start | bytes 245768 | tf_op jit(solution)/shard_map/ppermute | solution.py:387
  174.8 4.9 %collective-permute-start.17 = (bf16[40,1024]{1,0:T(8,128)(2,1)S(1)}, bf16[40,1024]{1,0:T(8,128)(2,1)S(1)}, u32[]{:S(2)}, u32[]{:S(2)}) collective-permute-start(bf16[40,1024]{1,0:T(8,128)(2,1)S(1)} %concatenate.34), channel_id=1, source_target_pairs={{0,6},{2,0},{4,2},{6,4},{1,7},{3,1},{5,3},{7,5},{8,14},{10,8},{12,... | collective-permute-start | bytes 245768 | tf_op jit(solution)/shard_map/ppermute | solution.py:387
  179.8 17.4 %collective-permute-start.18 = (bf16[32,1024]{1,0:T(8,128)(2,1)S(1)}, bf16[32,1024]{1,0:T(8,128)(2,1)S(1)}, u32[]{:S(2)}, u32[]{:S(2)}) collective-permute-start(bf16[32,1024]{1,0:T(8,128)(2,1)S(1)} %fusion.6), channel_id=1, source_target_pairs={{0,0},{16,1},{32,2},{48,3},{64,4},{80,5},{96,6},{112,7},{1,8},{17,... | collective-permute-start | bytes 196616 | tf_op jit(solution)/shard_map/ppermute | solution.py:462
  197.2 1.6 copy-start.2
  198.7 26.2 %all-to-all-start.5 = ((bf16[16,40,1024]{2,1,0:T(8,128)(2,1)}), bf16[16,40,1024]{2,1,0:T(8,128)(2,1)S(1)}, u32[]{:S(2)}, u32[]{:S(2)}) async-start(bf16[16,40,1024]{2,1,0:T(8,128)(2,1)} %broadcast_in_dim.40), calls=%async_computation.5 | async-start | bytes 2621440 | tf_op jit(solution)/shard_map/all_to_all | solution.py:383
Sparse Core Ops, SparseCore 0:
  18.5 83.4 all-gather.1

commit v9 on v8

--- a/solution.py
+++ b/solution.py
@@ -23,6 +23,7 @@
 NDP = 8
 TOKENS = LENGTH // NSP
 BLOCK = 768
+BLOCKS = (768, 1024)
 SCALE = WIDTH**-0.5
 LOG2E = 1.4426950408889634
 
@@ -88,28 +89,29 @@
 
 
 def attend_body(head, qd_ref, rt_ref, kv_ref, cos_ref, sin_ref, out_ref, p_buf, dp_buf, m_buf, kt_buf, acc, dq_acc):
-    blocks = LENGTH // BLOCK
-    lane = lanes_of((BLOCK, 128))
+    block = BLOCKS[head]
+    blocks = LENGTH // block
+    lane = lanes_of((block, 128))
     factor = SCALE * LOG2E
     low = 0 if head == 0 else 96
 
     def prepare(j, carry):
-        rows = pl.ds(pl.multiple_of(j * BLOCK, BLOCK), BLOCK)
+        rows = pl.ds(pl.multiple_of(j * block, block), block)
         kt = kv_ref[rows, :].astype(f32).T
         rt = rt_ref[rows, :].astype(f32).T
         kt_buf[:, rows] = jnp.concatenate([kt[0:PLAIN], rt[ROPE : 2 * ROPE]], axis=0).astype(bf16)
-        acc[rows, :] = jnp.zeros((BLOCK, 256), f32)
+        acc[rows, :] = jnp.zeros((block, 256), f32)
         return carry
 
     lax.fori_loop(0, blocks, prepare, 0)
 
     def one_block(i, carry):
-        rows = pl.ds(pl.multiple_of(i * BLOCK, BLOCK), BLOCK)
+        rows = pl.ds(pl.multiple_of(i * block, block), block)
         qd = qd_ref[rows, :].astype(f32)
         rt = rt_ref[rows, :].astype(f32)
         qdt = qd.T
         rtt = rt.T
-        none = jnp.zeros((32, BLOCK), f32)
+        none = jnp.zeros((32, block), f32)
         left = jnp.concatenate(
             [qdt[0:PLAIN], none, none, none, rtt[low : low + ROPE], none, none], axis=0
         ).astype(bf16)
@@ -140,25 +142,25 @@
             return new_top, total, inner
 
         start = (
-            jnp.full((1, BLOCK), jnp.finfo(f32).min, f32),
-            jnp.zeros((1, BLOCK), f32),
-            jnp.zeros((1, BLOCK), f32),
+            jnp.full((1, block), jnp.finfo(f32).min, f32),
+            jnp.zeros((1, block), f32),
+            jnp.zeros((1, block), f32),
         )
-        half = BLOCK // 2
-        whole, after = slice(0, BLOCK), slice(half, BLOCK)
+        half = block // 2
+        whole, after = slice(0, block), slice(half, block)
 
         def plain_stats(j, stats):
-            return gather_stats(pl.ds(pl.multiple_of(j * BLOCK, BLOCK), BLOCK), j, stats, False, whole)
-
-        upper = pl.ds(pl.multiple_of(i * BLOCK, half), half)
-        lower = pl.ds(pl.multiple_of(i * BLOCK + half, half), half)
+            return gather_stats(pl.ds(pl.multiple_of(j * block, block), block), j, stats, False, whole)
+
+        upper = pl.ds(pl.multiple_of(i * block, half), half)
+        lower = pl.ds(pl.multiple_of(i * block + half, half), half)
         stats = lax.fori_loop(0, i, plain_stats, start)
         stats = gather_stats(upper, i, stats, True, whole)
         later = gather_stats(lower, blocks, [x[:, half:] for x in stats], True, after)
         top, total, inner = [jnp.concatenate([x[:, :half], y], axis=1) for x, y in zip(stats, later)]
         inverse = 1.0 / total
         inner = inner * inverse
-        dq_acc[...] = jnp.zeros((WIDTH, BLOCK), f32)
+        dq_acc[...] = jnp.zeros((WIDTH, block), f32)
 
         def gradients(keys, j, columns):
             grow = jnp.exp2(m_buf[j, 0:1, columns] - top[:, columns]) * inverse[:, columns]
@@ -170,7 +172,7 @@
             acc[keys, 0:128] += jnp.dot(pb, right_d[columns], preferred_element_type=f32)
 
         def plain_gradients(j, carry):
-            gradients(pl.ds(pl.multiple_of(j * BLOCK, BLOCK), BLOCK), j, whole)
+            gradients(pl.ds(pl.multiple_of(j * block, block), block), j, whole)
             return carry
 
         lax.fori_loop(0, i, plain_gradients, 0)
@@ -188,7 +190,7 @@
     lax.fori_loop(0, blocks, one_block, 0)
 
     def finish(j, carry):
-        rows = pl.ds(pl.multiple_of(j * BLOCK, BLOCK), BLOCK)
+        rows = pl.ds(pl.multiple_of(j * block, block), block)
         plain = acc[rows, 0:128]
         out_ref[rows, 0:128] = jnp.where(lane < PLAIN, plain * SCALE, plain).astype(bf16)
         turned = acc[rows, 128:256] * SCALE
@@ -201,6 +203,7 @@
 
 
 def attend(head, arrived, turned, kv, cosine, sine):
+    block = BLOCKS[head]
     return pl.pallas_call(
         functools.partial(attend_body, head),
         grid=(1,),
@@ -214,14 +217,14 @@
         out_specs=pl.BlockSpec((LENGTH, 256), lambda g: (0, 0)),
         out_shape=jax.ShapeDtypeStruct((LENGTH, 256), bf16),
         scratch_shapes=[
-            pltpu.VMEM((LENGTH, BLOCK), f32),
-            pltpu.VMEM((LENGTH, BLOCK), f32),
-            pltpu.VMEM((LENGTH // BLOCK + 1, 8, BLOCK), f32),
+            pltpu.VMEM((LENGTH, block), f32),
+            pltpu.VMEM((LENGTH, block), f32),
+            pltpu.VMEM((LENGTH // block + 1, 8, block), f32),
             pltpu.VMEM((WIDTH, LENGTH), bf16),
             pltpu.VMEM((LENGTH, 256), f32),
-            pltpu.VMEM((WIDTH, BLOCK), f32),
-        ],
-        compiler_params=pltpu.CompilerParams(vmem_limit_bytes=36 * 1024 * 1024),
+            pltpu.VMEM((WIDTH, block), f32),
+        ],
+        compiler_params=pltpu.CompilerParams(vmem_limit_bytes=(36, 46)[head] * 1024 * 1024),
         cost_estimate=pl.CostEstimate(
             flops=12_000_000_000, bytes_accessed=6_000_000, transcendentals=5_000_000
         ),

time: 236 us -> 235 us (level)
  no operation moved by 1% of the time
where the time goes in v9:
time: 235 us; the launch traced here: 234 us
  Pallas kernels  78.9 us (34%)
  waiting for transfers between devices  66.3 us (28%)
  starting transfers between devices  56.1 us (24%)
  between operations  14.4 us (6%)
  other arithmetic  10.3 us (4%)
  local copies, waits for them, and re-layouts  8.04 us (3%)
    pallas_call x2, Pallas kernels, attend(): pl.pallas_call(functools.partial(attend_body, head), grid=(1,), in_specs=...  44.6 us
    ppermute x9, waiting for transfers between devices, shifted(): return lax.ppermute(value, axis, [(i, (i + k) % 4) for i in range(4)])  30.4 us
    all_to_all x1, waiting for transfers between devices, program(): r1 = lax.all_to_all(g1.reshape(NSP, TOKENS, 256), SP, 0, 0, tiled=True)  16.6 us
    ppermute x9, starting transfers between devices, shifted(): return lax.ppermute(value, axis, [(i, (i + k) % 4) for i in range(4)])  16.1 us
    pallas_call x2, Pallas kernels, project(): pl.pallas_call(project_body, in_specs=[pl.BlockSpec(memory_space=pltpu.SM...  14.4 us
    all_to_all x1, waiting for transfers between devices, everyone(): lax.all_to_all(jnp.broadcast_to(value[None], (size, *value.shape)), axes,...  12 us
    all_to_all x1, starting transfers between devices, program(): first = lax.all_to_all(first, SP, 0, 0, tiled=True).reshape(LENGTH, 256)  8.18 us
    pallas_call x1, Pallas kernels, finish(): pl.pallas_call(finish_body, in_specs=[pl.BlockSpec(memory_space=pltpu.SME...  7.86 us
  transfers between devices with their start and end apart: 26, of which 9 were waited for; matrix products, arithmetic and copies ran while one was open for 2% of the time, Pallas kernels for 29%

profile of v9, /device:TPU:0, one launch (start us, length us, event | category | flops | bytes accessed | tf_op | source)
XLA Modules:
  0.0 234.0 jit_solution(15343265178282174399)
XLA Ops:
  7.2 1.2 fusion
  8.4 0.8 copy.16
  9.2 0.7 pad_convert_fusion.kr_ref
  9.9 1.9 fusion.2.nlat_ref
  11.8 1.1 fusion.7
  12.9 5.5 %pack.1 = (bf16[16,192,256]{2,1,0:T(8,128)(2,1)}, bf16[16,192,128]{2,1,0:T(8,128)(2,1)}) custom-call(bf16[192,3072]{1,0:T(8,128)(2,1)} %bitcast.82, bf16[192,2048]{1,0:T(8,128)(2,1)} %bitcast.84, f32[192,128]{1,0:T(8,128)} %pad_convert_fusion.kr_ref, f32[192,128]{1,0:T(8,128)} %get-tuple-element.72.cos_ref, f32[192,128]{1,0:T(8,128)} %get-tuple-element.71.sin_ref), custom_call_target="tpu_custom_call" | custom-call | flops 2000000000 | bytes 5000000 | tf_op jit(solution)/shard_map/pack/pallas_call | solution.py:80
  18.4 0.1 pad_maximum_fusion
  18.6 0.1 fusion.37
  18.7 1.7 collective-permute-start.7
  20.3 8.2 %all-to-all-start.1 = ((bf16[16,192,256]{2,1,0:T(8,128)(2,1)}), bf16[16,192,256]{2,1,0:T(8,128)(2,1)S(1)}, u32[]{:S(2)}, u32[]{:S(2)}) async-start(bf16[16,192,256]{2,1,0:T(8,128)(2,1)} %get-tuple-element.28), calls=%async_computation.1 | async-start | bytes 3145728 | tf_op jit(solution)/shard_map/all_to_all | solution.py:447
  28.5 1.8 collective-permute-start.8
  30.3 1.8 collective-permute-start.9
  32.1 1.4 collective-permute-done.7.refs_1_
  33.5 18.7 %collective-permute-done.8.refs_2_ = bf16[256,1024]{1,0:T(8,128)(2,1)} collective-permute-done((bf16[256,1024]{1,0:T(8,128)(2,1)S(1)}, bf16[256,1024]{1,0:T(8,128)(2,1)}, u32[]{:S(2)}, u32[]{:S(2)}) %collective-permute-start.8) | collective-permute-done | bytes 524320 | tf_op jit(solution)/shard_map/ppermute | solution.py:390
  52.2 0.5 collective-permute-start.13
  52.7 2.4 %collective-permute-start = (bf16[256,1024]{1,0:T(8,128)(2,1)S(1)}, bf16[256,1024]{1,0:T(8,128)(2,1)}, u32[]{:S(2)}, u32[]{:S(2)}) collective-permute-start(bf16[256,1024]{1,0:T(8,128)(2,1)S(1)} %bitcast.68), channel_id=1, source_target_pairs={{0,2},{2,4},{4,6},{6,0},{1,3},{3,5},{5,7},{7,1},{8,10},{10,12},{12... | collective-permute-start | bytes 1572872 | tf_op jit(solution)/shard_map/ppermute | solution.py:390
  55.2 1.3 collective-permute-start.1
  56.5 1.5 collective-permute-start.2
  58.1 0.6 pad_add_fusion.order_ref
  58.7 6.8 %project.3 = (bf16[16,192,128]{2,1,0:T(8,128)(2,1)}, bf16[128,1024]{1,0:T(8,128)(2,1)}) custom-call(s32[9]{0:T(128)} %pad_add_fusion.order_ref, bf16[192,1024]{1,0:T(8,128)(2,1)} %fusion.2.nlat_ref, bf16[256,1024]{1,0:T(8,128)(2,1)} %bitcast.66, bf16[256,1024]{1,0:T(8,128)(2,1)} %copy-done.5, bf16[256,1024]{1,0:T(8,128)(2,1)} %collective-permute-done.8.refs_2_, ...), custom_call_target="tpu_custom_call" | custom-call | flops 2000000000 | bytes 6000000 | tf_op jit(solution)/shard_map/project/pallas_call | solution.py:256
  65.5 6.9 %all-to-all-start.2 = ((bf16[16,192,128]{2,1,0:T(8,128)(2,1)}), bf16[16,192,128]{2,1,0:T(8,128)(2,1)S(1)}, u32[]{:S(2)}, u32[]{:S(2)}) async-start(bf16[16,192,128]{2,1,0:T(8,128)(2,1)} %get-tuple-element.29), calls=%async_computation.2 | async-start | bytes 1572864 | tf_op jit(solution)/shard_map/all_to_all | solution.py:451
  72.4 0.1 collective-permute-start.3
  72.5 0.5 collective-permute-start.4
  73.0 0.1 collective-permute-start.5
  73.1 8.0 %collective-permute-done.2.refs_3_.refs_11_ = bf16[256,1024]{1,0:T(8,128)(2,1)} collective-permute-done((bf16[256,1024]{1,0:T(8,128)(2,1)S(1)}, bf16[256,1024]{1,0:T(8,128)(2,1)}, u32[]{:S(2)}, u32[]{:S(2)}) %collective-permute-start.2) | collective-permute-done | bytes 524320 | tf_op jit(solution)/shard_map/ppermute | solution.py:390
  81.2 2.2 collective-permute-done.6.refs_7_.refs_15_
  83.4 7.6 %project.2 = (bf16[16,192,256]{2,1,0:T(8,128)(2,1)}, bf16[128,1024]{1,0:T(8,128)(2,1)}) custom-call(s32[9]{0:T(128)} %pad_add_fusion.order_ref, bf16[192,1024]{1,0:T(8,128)(2,1)} %fusion.2.nlat_ref, bf16[256,1024]{1,0:T(8,128)(2,1)} %bitcast.72, bf16[256,1024]{1,0:T(8,128)(2,1)} %collective-permute-done.refs_1_.refs_9_, ...), custom_call_target="tpu_custom_call" | custom-call | flops 2000000000 | bytes 6000000 | tf_op jit(solution)/shard_map/project/pallas_call | solution.py:256
  90.9 5.0 %all-to-all-done.2 = bf16[16,192,128]{2,1,0:T(8,128)(2,1)S(1)} async-done(((bf16[16,192,128]{2,1,0:T(8,128)(2,1)}), bf16[16,192,128]{2,1,0:T(8,128)(2,1)S(1)}, u32[]{:S(2)}, u32[]{:S(2)}) %all-to-all-start.2) | async-done | bytes 786464 | tf_op jit(solution)/shard_map/all_to_all | solution.py:451
  96.0 0.9 copy-done
  96.8 3.9 %all-to-all-start = ((bf16[16,192,256]{2,1,0:T(8,128)(2,1)}), bf16[16,192,256]{2,1,0:T(8,128)(2,1)S(1)}, u32[]{:S(2)}, u32[]{:S(2)}) async-start(bf16[16,192,256]{2,1,0:T(8,128)(2,1)} %get-tuple-element.27), calls=%async_computation | async-start | bytes 3145728 | tf_op jit(solution)/shard_map/all_to_all | solution.py:453
  100.7 0.8 multiply_sine_fusion
  101.5 1.1 copy-done.1
  102.6 22.6 %shard_map.127.g0_ref = bf16[3072,256]{1,0:T(8,128)(2,1)} custom-call(bf16[3072,256]{1,0:T(8,128)(2,1)S(1)} %bitcast.53, bf16[3072,256]{1,0:T(8,128)(2,1)S(1)} %bitcast.54, bf16[3072,128]{1,0:T(8,128)(2,1)S(1)} %bitcast.58, f32[16,3072]{1,0:T(8,128)S(1)} %get-tuple-element.68.cos_ref, f32[16,3072]{1,0:T(8,128)S(1)} %get-tuple-element.67.sin_ref), custom_call_target="tpu_custom_call" | custom-call | flops 12000000000 | bytes 6000000 | tf_op jit(solution)/shard_map/pallas_call | solution.py:207
  125.2 7.0 %all-to-all-start.3 = ((bf16[16,192,256]{2,1,0:T(8,128)(2,1)}), bf16[16,192,256]{2,1,0:T(8,128)(2,1)}, u32[]{:S(2)}, u32[]{:S(2)}) async-start(bf16[16,192,256]{2,1,0:T(8,128)(2,1)} %bitcast.13), calls=%async_computation.3 | async-start | bytes 3145728 | tf_op jit(solution)/shard_map/all_to_all | solution.py:458
  132.3 0.1 pad.17.clone
  132.3 0.1 pad.18.clone
  132.4 22.1 %shard_map.128.g1_ref = bf16[3072,256]{1,0:T(8,128)(2,1)} custom-call(bf16[3072,256]{1,0:T(8,128)(2,1)S(1)} %bitcast.56, bf16[3072,256]{1,0:T(8,128)(2,1)S(1)} %bitcast.55, bf16[3072,256]{1,0:T(8,128)(2,1)S(1)} %bitcast.57, f32[16,3072]{1,0:T(8,128)S(1)} %get-tuple-element.68.cos_ref, f32[16,3072]{1,0:T(8,128)S(1)} %get-tuple-element.67.sin_ref), custom_call_target="tpu_custom_call" | custom-call | flops 12000000000 | bytes 6000000 | tf_op jit(solution)/shard_map/pallas_call | solution.py:207
  154.5 6.6 %weigh.1 = (bf16[8,32,1024]{2,1,0:T(8,128)(2,1)}, f32[1,1024]{1,0:T(1,128)}) custom-call(bf16[3072,256]{1,0:T(8,128)(2,1)} %shard_map.127.g0_ref, bf16[3072,256]{1,0:T(8,128)(2,1)} %shard_map.128.g1_ref, bf16[3072,1024]{1,0:T(8,128)(2,1)} %all-gather.2.cloned.1.call-done.nlat_ref, bf16[128,1024]{1,0:T(8,128)(2,1)} %get-tuple-element.35.own0_ref, ...), custom_call_target="tpu_custom_call" | custom-call | flops 2000000000 | bytes 9000000 | tf_op jit(solution)/shard_map/weigh/pallas_call | solution.py:355
  161.1 0.7 fusion.11
  161.7 1.0 dynamic-slice_bitcast_fusion
  162.7 0.1 maximum_maximum_fusion
  162.8 0.1 collective-permute-start.14
  162.9 7.3 %all-to-all-start.4 = ((bf16[16,192,256]{2,1,0:T(8,128)(2,1)}), bf16[16,192,256]{2,1,0:T(8,128)(2,1)S(1)}, u32[]{:S(2)}, u32[]{:S(2)}) async-start(bf16[16,192,256]{2,1,0:T(8,128)(2,1)} %bitcast.14), calls=%async_computation.4 | async-start | bytes 3145728 | tf_op jit(solution)/shard_map/all_to_all | solution.py:461
  170.3 0.1 convert_element_type.127
  170.4 0.1 slice_add_fusion
  170.5 0.5 copy-done.10
  171.0 2.1 collective-permute-start.15
  173.2 0.8 collective-permute-start.16
  174.0 2.6 %collective-permute-start.17 = (bf16[40,1024]{1,0:T(8,128)(2,1)S(1)}, bf16[40,1024]{1,0:T(8,128)(2,1)S(1)}, u32[]{:S(2)}, u32[]{:S(2)}) collective-permute-start(bf16[40,1024]{1,0:T(8,128)(2,1)S(1)} %concatenate.34), channel_id=1, source_target_pairs={{0,6},{2,0},{4,2},{6,4},{1,7},{3,1},{5,3},{7,5},{8,14},{10,8},{12,... | collective-permute-start | bytes 245768 | tf_op jit(solution)/shard_map/ppermute | solution.py:390
  176.6 0.7 collective-permute-done.15
  177.3 1.7 collective-permute-done.16
  179.0 0.7 collective-permute-start.18
  179.7 16.6 %all-to-all-done.4.r1_ref = bf16[16,192,256]{2,1,0:T(8,128)(2,1)S(1)} async-done(((bf16[16,192,256]{2,1,0:T(8,128)(2,1)}), bf16[16,192,256]{2,1,0:T(8,128)(2,1)S(1)}, u32[]{:S(2)}, u32[]{:S(2)}) %all-to-all-start.4) | async-done | bytes 1572896 | tf_op jit(solution)/shard_map/all_to_all | solution.py:461
  196.4 1.4 broadcast_in_dim.40
  197.8 0.1 copy-done.2
  197.9 4.8 %all-to-all-start.5 = ((bf16[16,40,1024]{2,1,0:T(8,128)(2,1)}), bf16[16,40,1024]{2,1,0:T(8,128)(2,1)S(1)}, u32[]{:S(2)}, u32[]{:S(2)}) async-start(bf16[16,40,1024]{2,1,0:T(8,128)(2,1)} %broadcast_in_dim.40), calls=%async_computation.5 | async-start | bytes 2621440 | tf_op jit(solution)/shard_map/all_to_all | solution.py:386
  202.7 7.9 %finish.1 = (bf16[192,3072]{1,0:T(8,128)(2,1)}, f32[192,1024]{1,0:T(8,128)}, f32[192,32]{1,0:T(8,128)}) custom-call(s32[9]{0:T(128)} %pad_add_fusion.order_ref, bf16[16,192,256]{2,1,0:T(8,128)(2,1)} %all-to-all-done.3.r0_ref, bf16[16,192,256]{2,1,0:T(8,128)(2,1)} %copy-done.2, bf16[192,1024]{1,0:T(8,128)(2,1)} %bitcast.61, f32[1,1024]{1,0:T(1,128)} %bitcast.81, ...), custom_call_target="tpu_custom_call" | custom-call | flops 2000000000 | bytes 14000000 | tf_op jit(solution)/shard_map/finish/pallas_call | solution.py:313
  210.6 1.6 copy.18
  212.1 12.0 %all-to-all-done.5 = bf16[16,40,1024]{2,1,0:T(8,128)(2,1)S(1)} async-done(((bf16[16,40,1024]{2,1,0:T(8,128)(2,1)}), bf16[16,40,1024]{2,1,0:T(8,128)(2,1)S(1)}, u32[]{:S(2)}, u32[]{:S(2)}) %all-to-all-start.5) | async-done | bytes 1310752 | tf_op jit(solution)/shard_map/all_to_all | solution.py:386
  224.1 0.1 slice.86
  224.2 0.1 fusion.36
  224.3 1.1 bitcast_convert_fusion
  225.4 1.1 bitcast_convert_fusion.1
  226.5 0.7 convert_reduce_fusion
  (67 shorter events, 0.6 us)
Async XLA Ops:
  7.2 147.3 %all-gather.2.cloned.1.call-start = ((), (), s32[]{:S(2)}) async-start(), calls=%async_computation.6 | async-start | bytes 6684672 | tf_op jit(solution)/shard_map/all_gather | solution.py:450
  12.9 5.5 %copy-start.8 = (bf16[256,1024]{1,0:T(8,128)(2,1)S(1)}, bf16[256,1024]{1,0:T(8,128)(2,1)}, u32[]{:S(2)}) copy-start(bf16[256,1024]{1,0:T(8,128)(2,1)} %param.13) | copy-start | bytes 1572868
  12.9 5.5 %copy-start.9 = (bf16[256,1024]{1,0:T(8,128)(2,1)S(1)}, bf16[256,1024]{1,0:T(8,128)(2,1)}, u32[]{:S(2)}) copy-start(bf16[256,1024]{1,0:T(8,128)(2,1)} %param.12) | copy-start | bytes 1572868
  18.6 13.5 %copy-start.3 = (bf16[2,1,128,1024]{3,2,1,0:T(8,128)(2,1)}, bf16[2,1,128,1024]{3,2,1,0:T(8,128)(2,1)S(1)}, u32[]{:S(2)}) copy-start(bf16[2,1,128,1024]{3,2,1,0:T(8,128)(2,1)S(1)} %get-tuple-element.62) | copy-start | bytes 1572868
  18.6 53.7 %copy-start.4 = (bf16[2,1,128,1024]{3,2,1,0:T(8,128)(2,1)}, bf16[2,1,128,1024]{3,2,1,0:T(8,128)(2,1)S(1)}, u32[]{:S(2)}) copy-start(bf16[2,1,128,1024]{3,2,1,0:T(8,128)(2,1)S(1)} %get-tuple-element.63) | copy-start | bytes 1572868
  18.7 14.9 %collective-permute-start.7 = (bf16[256,1024]{1,0:T(8,128)(2,1)S(1)}, bf16[256,1024]{1,0:T(8,128)(2,1)S(1)}, u32[]{:S(2)}, u32[]{:S(2)}) collective-permute-start(bf16[256,1024]{1,0:T(8,128)(2,1)S(1)} %bitcast.62), channel_id=1, source_target_pairs={{0,2},{2,4},{4,6},{6,0},{1,3},{3,5},{5,7},{7,1},{8,10},{10,12},{12... | collective-permute-start | bytes 1572872 | tf_op jit(solution)/shard_map/ppermute | solution.py:390
  20.3 37.7 %copy-start.11 = (s32[4]{0:T(128)S(1)}, s32[4]{0:T(128)}, u32[]{:S(2)}) copy-start(s32[4]{0:T(128)} %constant.115.clone) | copy-start | bytes 52
  20.3 45.2 %all-to-all-start.1 = ((bf16[16,192,256]{2,1,0:T(8,128)(2,1)}), bf16[16,192,256]{2,1,0:T(8,128)(2,1)S(1)}, u32[]{:S(2)}, u32[]{:S(2)}) async-start(bf16[16,192,256]{2,1,0:T(8,128)(2,1)} %get-tuple-element.28), calls=%async_computation.1 | async-start | bytes 3145728 | tf_op jit(solution)/shard_map/all_to_all | solution.py:447
  28.5 23.7 %collective-permute-start.8 = (bf16[256,1024]{1,0:T(8,128)(2,1)S(1)}, bf16[256,1024]{1,0:T(8,128)(2,1)}, u32[]{:S(2)}, u32[]{:S(2)}) collective-permute-start(bf16[256,1024]{1,0:T(8,128)(2,1)S(1)} %bitcast.63), channel_id=1, source_target_pairs={{0,6},{2,0},{4,2},{6,4},{1,7},{3,1},{5,3},{7,5},{8,14},{10,8},{12,... | collective-permute-start | bytes 1572872 | tf_op jit(solution)/shard_map/ppermute | solution.py:390
  30.3 21.9 %collective-permute-start.9 = (bf16[256,1024]{1,0:T(8,128)(2,1)S(1)}, bf16[256,1024]{1,0:T(8,128)(2,1)}, u32[]{:S(2)}, u32[]{:S(2)}) collective-permute-start(bf16[256,1024]{1,0:T(8,128)(2,1)S(1)} %bitcast.64), channel_id=1, source_target_pairs={{0,4},{2,6},{4,0},{6,2},{1,5},{3,7},{5,1},{7,3},{8,12},{10,14},{12... | collective-permute-start | bytes 1572872 | tf_op jit(solution)/shard_map/ppermute | solution.py:390
  32.1 23.0 %collective-permute-start.10 = (bf16[256,1024]{1,0:T(8,128)(2,1)S(1)}, bf16[256,1024]{1,0:T(8,128)(2,1)}, u32[]{:S(2)}, u32[]{:S(2)}) collective-permute-start(bf16[256,1024]{1,0:T(8,128)(2,1)S(1)} %bitcast.65), channel_id=1, source_target_pairs={{0,1},{1,0},{2,3},{3,2},{4,5},{5,4},{6,7},{7,6},{8,9},{9,8},{10,11... | collective-permute-start | bytes 1572872 | tf_op jit(solution)/shard_map/ppermute | solution.py:398
  33.5 25.1 %copy-start.5 = (bf16[256,1024]{1,0:T(8,128)(2,1)}, bf16[256,1024]{1,0:T(8,128)(2,1)S(1)}, u32[]{:S(2)}) copy-start(bf16[256,1024]{1,0:T(8,128)(2,1)S(1)} %collective-permute-done.7.refs_1_) | copy-start | bytes 1572868
  33.5 23.0 %collective-permute-start.11 = (bf16[256,1024]{1,0:T(8,128)(2,1)S(1)}, bf16[256,1024]{1,0:T(8,128)(2,1)}, u32[]{:S(2)}, u32[]{:S(2)}) collective-permute-start(bf16[256,1024]{1,0:T(8,128)(2,1)S(1)} %collective-permute-done.7.refs_1_), channel_id=1, source_target_pairs={{0,1},{1,0},{2,3},{3,2},{4,5},{5,4},{6,7},{7,6},{8,9},{9,8},{10,11... | collective-permute-start | bytes 1572872 | tf_op jit(solution)/shard_map/ppermute | solution.py:398
  52.2 6.4 %collective-permute-start.12 = (bf16[256,1024]{1,0:T(8,128)(2,1)}, bf16[256,1024]{1,0:T(8,128)(2,1)}, u32[]{:S(2)}, u32[]{:S(2)}) collective-permute-start(bf16[256,1024]{1,0:T(8,128)(2,1)} %collective-permute-done.8.refs_2_), channel_id=1, source_target_pairs={{0,1},{1,0},{2,3},{3,2},{4,5},{5,4},{6,7},{7,6},{8,9},{9,8},{10,11... | collective-permute-start | bytes 1572872 | tf_op jit(solution)/shard_map/ppermute | solution.py:398
  52.2 6.4 %collective-permute-start.13 = (bf16[256,1024]{1,0:T(8,128)(2,1)}, bf16[256,1024]{1,0:T(8,128)(2,1)}, u32[]{:S(2)}, u32[]{:S(2)}) collective-permute-start(bf16[256,1024]{1,0:T(8,128)(2,1)} %collective-permute-done.9.refs_3_), channel_id=1, source_target_pairs={{0,1},{1,0},{2,3},{3,2},{4,5},{5,4},{6,7},{7,6},{8,9},{9,8},{10,11... | collective-permute-start | bytes 1572872 | tf_op jit(solution)/shard_map/ppermute | solution.py:398
  52.7 19.7 %collective-permute-start = (bf16[256,1024]{1,0:T(8,128)(2,1)S(1)}, bf16[256,1024]{1,0:T(8,128)(2,1)}, u32[]{:S(2)}, u32[]{:S(2)}) collective-permute-start(bf16[256,1024]{1,0:T(8,128)(2,1)S(1)} %bitcast.68), channel_id=1, source_target_pairs={{0,2},{2,4},{4,6},{6,0},{1,3},{3,5},{5,7},{7,1},{8,10},{10,12},{12... | collective-permute-start | bytes 1572872 | tf_op jit(solution)/shard_map/ppermute | solution.py:390
  55.2 17.8 %collective-permute-start.1 = (bf16[256,1024]{1,0:T(8,128)(2,1)S(1)}, bf16[256,1024]{1,0:T(8,128)(2,1)}, u32[]{:S(2)}, u32[]{:S(2)}) collective-permute-start(bf16[256,1024]{1,0:T(8,128)(2,1)S(1)} %bitcast.69), channel_id=1, source_target_pairs={{0,6},{2,0},{4,2},{6,4},{1,7},{3,1},{5,3},{7,5},{8,14},{10,8},{12,... | collective-permute-start | bytes 1572872 | tf_op jit(solution)/shard_map/ppermute | solution.py:390
  56.5 24.6 %collective-permute-start.2 = (bf16[256,1024]{1,0:T(8,128)(2,1)S(1)}, bf16[256,1024]{1,0:T(8,128)(2,1)}, u32[]{:S(2)}, u32[]{:S(2)}) collective-permute-start(bf16[256,1024]{1,0:T(8,128)(2,1)S(1)} %bitcast.70), channel_id=1, source_target_pairs={{0,4},{2,6},{4,0},{6,2},{1,5},{3,7},{5,1},{7,3},{8,12},{10,14},{12... | collective-permute-start | bytes 1572872 | tf_op jit(solution)/shard_map/ppermute | solution.py:390
  65.5 30.5 %all-to-all-start.2 = ((bf16[16,192,128]{2,1,0:T(8,128)(2,1)}), bf16[16,192,128]{2,1,0:T(8,128)(2,1)S(1)}, u32[]{:S(2)}, u32[]{:S(2)}) async-start(bf16[16,192,128]{2,1,0:T(8,128)(2,1)} %get-tuple-element.29), calls=%async_computation.2 | async-start | bytes 1572864 | tf_op jit(solution)/shard_map/all_to_all | solution.py:451
  72.4 8.8 %collective-permute-start.3 = (bf16[256,1024]{1,0:T(8,128)(2,1)S(1)}, bf16[256,1024]{1,0:T(8,128)(2,1)S(1)}, u32[]{:S(2)}, u32[]{:S(2)}) collective-permute-start(bf16[256,1024]{1,0:T(8,128)(2,1)S(1)} %bitcast.71), channel_id=1, source_target_pairs={{0,1},{1,0},{2,3},{3,2},{4,5},{5,4},{6,7},{7,6},{8,9},{9,8},{10,11... | collective-permute-start | bytes 1572872 | tf_op jit(solution)/shard_map/ppermute | solution.py:398
  72.5 8.7 %collective-permute-start.4 = (bf16[256,1024]{1,0:T(8,128)(2,1)}, bf16[256,1024]{1,0:T(8,128)(2,1)}, u32[]{:S(2)}, u32[]{:S(2)}) collective-permute-start(bf16[256,1024]{1,0:T(8,128)(2,1)} %collective-permute-done.refs_1_.refs_9_), channel_id=1, source_target_pairs={{0,1},{1,0},{2,3},{3,2},{4,5},{5,4},{6,7},{7,6},{8,9},{9,8},{10,11... | collective-permute-start | bytes 1572872 | tf_op jit(solution)/shard_map/ppermute | solution.py:398
  73.0 8.2 %collective-permute-start.5 = (bf16[256,1024]{1,0:T(8,128)(2,1)}, bf16[256,1024]{1,0:T(8,128)(2,1)}, u32[]{:S(2)}, u32[]{:S(2)}) collective-permute-start(bf16[256,1024]{1,0:T(8,128)(2,1)} %collective-permute-done.1.refs_2_.refs_10_), channel_id=1, source_target_pairs={{0,1},{1,0},{2,3},{3,2},{4,5},{5,4},{6,7},{7,6},{8,9},{9,8},{10,11... | collective-permute-start | bytes 1572872 | tf_op jit(solution)/shard_map/ppermute | solution.py:398
  81.1 2.3 collective-permute-start.6
  81.1 2.2 copy-start.6
  96.0 0.9 copy-start
  96.8 28.4 %all-to-all-start = ((bf16[16,192,256]{2,1,0:T(8,128)(2,1)}), bf16[16,192,256]{2,1,0:T(8,128)(2,1)S(1)}, u32[]{:S(2)}, u32[]{:S(2)}) async-start(bf16[16,192,256]{2,1,0:T(8,128)(2,1)} %get-tuple-element.27), calls=%async_computation | async-start | bytes 3145728 | tf_op jit(solution)/shard_map/all_to_all | solution.py:453
  101.5 1.1 copy-start.1
  125.2 29.3 %all-to-all-start.3 = ((bf16[16,192,256]{2,1,0:T(8,128)(2,1)}), bf16[16,192,256]{2,1,0:T(8,128)(2,1)}, u32[]{:S(2)}, u32[]{:S(2)}) async-start(bf16[16,192,256]{2,1,0:T(8,128)(2,1)} %bitcast.13), calls=%async_computation.3 | async-start | bytes 3145728 | tf_op jit(solution)/shard_map/all_to_all | solution.py:458
  162.8 7.4 %collective-permute-start.14 = (bf16[5,32,1024]{2,1,0:T(8,128)(2,1)S(1)}, bf16[5,32,1024]{2,1,0:T(8,128)(2,1)S(1)}, u32[]{:S(2)}, u32[]{:S(2)}) collective-permute-start(bf16[5,32,1024]{2,1,0:T(8,128)(2,1)S(1)} %fusion.4), channel_id=1, source_target_pairs={{0,1},{1,0},{2,3},{3,2},{4,5},{5,4},{6,7},{7,6},{8,9},{9,8},{10,11... | collective-permute-start | bytes 983048 | tf_op jit(solution)/shard_map/ppermute | solution.py:412
  162.9 7.4 %copy-start.7 = (bf16[8,32,1024]{2,1,0:T(8,128)(2,1)S(1)}, bf16[8,32,1024]{2,1,0:T(8,128)(2,1)}, u32[]{:S(2)}) copy-start(bf16[8,32,1024]{2,1,0:T(8,128)(2,1)} %get-tuple-element.37) | copy-start | bytes 1572868
  162.9 33.4 %all-to-all-start.4 = ((bf16[16,192,256]{2,1,0:T(8,128)(2,1)}), bf16[16,192,256]{2,1,0:T(8,128)(2,1)S(1)}, u32[]{:S(2)}, u32[]{:S(2)}) async-start(bf16[16,192,256]{2,1,0:T(8,128)(2,1)} %bitcast.14), calls=%async_computation.4 | async-start | bytes 3145728 | tf_op jit(solution)/shard_map/all_to_all | solution.py:461
  170.3 0.7 copy-start.10
  171.0 6.2 %collective-permute-start.15 = (bf16[40,1024]{1,0:T(8,128)(2,1)S(1)}, bf16[40,1024]{1,0:T(8,128)(2,1)S(1)}, u32[]{:S(2)}, u32[]{:S(2)}) collective-permute-start(bf16[40,1024]{1,0:T(8,128)(2,1)S(1)} %concatenate.32), channel_id=1, source_target_pairs={{0,4},{2,6},{4,0},{6,2},{1,5},{3,7},{5,1},{7,3},{8,12},{10,14},{12... | collective-permute-start | bytes 245768 | tf_op jit(solution)/shard_map/ppermute | solution.py:390
  173.2 5.8 %collective-permute-start.16 = (bf16[40,1024]{1,0:T(8,128)(2,1)S(1)}, bf16[40,1024]{1,0:T(8,128)(2,1)S(1)}, u32[]{:S(2)}, u32[]{:S(2)}) collective-permute-start(bf16[40,1024]{1,0:T(8,128)(2,1)S(1)} %concatenate.33), channel_id=1, source_target_pairs={{0,2},{2,4},{4,6},{6,0},{1,3},{3,5},{5,7},{7,1},{8,10},{10,12},{12... | collective-permute-start | bytes 245768 | tf_op jit(solution)/shard_map/ppermute | solution.py:390
  174.0 4.9 %collective-permute-start.17 = (bf16[40,1024]{1,0:T(8,128)(2,1)S(1)}, bf16[40,1024]{1,0:T(8,128)(2,1)S(1)}, u32[]{:S(2)}, u32[]{:S(2)}) collective-permute-start(bf16[40,1024]{1,0:T(8,128)(2,1)S(1)} %concatenate.34), channel_id=1, source_target_pairs={{0,6},{2,0},{4,2},{6,4},{1,7},{3,1},{5,3},{7,5},{8,14},{10,8},{12,... | collective-permute-start | bytes 245768 | tf_op jit(solution)/shard_map/ppermute | solution.py:390
  179.0 17.4 %collective-permute-start.18 = (bf16[32,1024]{1,0:T(8,128)(2,1)S(1)}, bf16[32,1024]{1,0:T(8,128)(2,1)S(1)}, u32[]{:S(2)}, u32[]{:S(2)}) collective-permute-start(bf16[32,1024]{1,0:T(8,128)(2,1)S(1)} %fusion.6), channel_id=1, source_target_pairs={{0,0},{16,1},{32,2},{48,3},{64,4},{80,5},{96,6},{112,7},{1,8},{17,... | collective-permute-start | bytes 196616 | tf_op jit(solution)/shard_map/ppermute | solution.py:465
  196.4 1.6 copy-start.2
  197.9 26.2 %all-to-all-start.5 = ((bf16[16,40,1024]{2,1,0:T(8,128)(2,1)}), bf16[16,40,1024]{2,1,0:T(8,128)(2,1)S(1)}, u32[]{:S(2)}, u32[]{:S(2)}) async-start(bf16[16,40,1024]{2,1,0:T(8,128)(2,1)} %broadcast_in_dim.40), calls=%async_computation.5 | async-start | bytes 2621440 | tf_op jit(solution)/shard_map/all_to_all | solution.py:386
Sparse Core Ops, SparseCore 0:
  18.5 83.4 all-gather.1
